TPU v7x, 32 devices: a whole 2x2x4 slice. The times are simulated.
32 devices in a mesh: sp: 4 (over z), fs: 4 (over y, x), tp: 2 (over core).
Axes of the slice: x: 2, y: 2, z: 4, core: 2. Of those that a mesh axis runs over, the one named last changes fastest.
Arguments:
- activations: bfloat16 [2048, 4096], P(('fs', 'sp'), 'tp'), parts along dimension 0, may hold values from -6 to 6
- input_norm_gain: float32 [4096], replicated, may hold values from 0.1 to 1.9
- window_query_weight: bfloat16 [4096, 2048], P('sp', 'tp'), may hold values from -0.09375 to 0.09375
- window_key_weight: bfloat16 [4096, 512], P('sp', 'tp'), may hold values from -0.09375 to 0.09375
- window_value_weight: bfloat16 [4096, 512], P('sp', 'tp'), may hold values from -0.09375 to 0.09375
- linear_query_weight: bfloat16 [4096, 1024], P('sp', 'tp'), may hold values from -0.09375 to 0.09375
- linear_key_weight: bfloat16 [4096, 1024], P('sp', 'tp'), may hold values from -0.09375 to 0.09375
- linear_value_weight: bfloat16 [4096, 2048], P('sp', 'tp'), may hold values from -0.09375 to 0.09375
- decay_down_factor: bfloat16 [4096, 16], replicated, may hold values from -0.09375 to 0.09375
- decay_up_factor: bfloat16 [16, 1024], P(None, 'tp'), may hold values from -1.5 to 1.5
- decay_offset_bias: float32 [1024], P('tp'), may hold values from -0.5 to 9
- extra_fading_exponent: float32 [2048, 8], P(('fs', 'sp'), 'tp'), parts along dimension 0, may hold values from -1.5 to 0
- starting_state: float32 [8, 128, 256], P('tp'), may hold values from -12 to 12
- head_sink_logit: float32 [32], P('tp'), may hold values from 1 to 5
- linear_head_gain: float32 [256], replicated, may hold values from 0.1 to 1.9
- window_output_weight: bfloat16 [2048, 4096], P('tp', 'sp'), may hold values from -0.09375 to 0.09375
- linear_output_weight: bfloat16 [2048, 4096], P('tp', 'sp'), may hold values from -0.09375 to 0.09375
Outputs:
- mixer_output: bfloat16 [2048, 4096], P(('fs', 'sp', 'tp')), parts along dimension 0
There are 4 independent parts, one for each index of `fs`. A program takes and returns all parts, laid end to end along the dimension named above; an argument that names none is the same for every part. Nothing has to cross between parts.
All inputs are finite; a program needn't handle non-finite values.
Results may differ from a plain program's by a relative error of at most 0.019.
Values may be sent and summed in bfloat16 or wider, within the bound.
No kernel may reach another device: no remote copies, remote signals or barrier semaphores. Data moves between devices by JAX's collectives and lax.ppermute only.
A program may use at most 128 MiB of HBM per device.

v0:
```python
import jax
import jax.numpy as jnp
from jax import lax
from jax.sharding import PartitionSpec as P

QH = 32
HD = 64
WINDOW = 128
LOOKUP_FEATURES = 128
DV = 256
SPAN = 64


EPS = 1e-05
FADING_SOFTNESS = 16.0
HIGH_PRECISION = lax.Precision.HIGHEST


def passed_along(value, axis, steps):
    count = lax.axis_size(axis)
    leading, last = (max(0, -steps), min(count, count - steps))
    return lax.ppermute(value, axis, [(source, source + steps) for source in range(leading, last)])


def prefix(x, axis, combine, identity):
    peers, place = (lax.axis_size(axis), lax.axis_index(axis))
    everything = jax.tree.map(
        lambda part, kind: lax.all_gather(part.astype(kind), axis), x, (jnp.bfloat16, jnp.bfloat16)
    )
    start = jax.tree.map(
        lambda part, zero: jnp.broadcast_to(jnp.asarray(zero, part.dtype), part.shape), x, identity
    )

    def hop(k, before):
        reached = k < place
        new = combine(
            before, jax.tree.map(lambda part, own: part[k].astype(own.dtype), everything, x)
        )
        return jax.tree.map(lambda a, b: jnp.where(reached, a, b), new, before)

    return lax.fori_loop(0, peers, hop, start)


def window_attention(near_query, near_keys, near_values, head_sink_logit):
    stream_extent = near_query.shape[0]
    key_heads = near_keys.shape[1] // HD
    heads_here = near_query.shape[1] // HD
    groups = heads_here // key_heads
    blocks = stream_extent // WINDOW
    tail_rows = jnp.stack([near_keys, near_values])
    before = passed_along(tail_rows, "sp", 1)

    def banded(previous, current):
        extended = jnp.concatenate([previous, current], axis=0)
        earlier = extended[:stream_extent].reshape(blocks, WINDOW, key_heads, HD)
        present = extended[WINDOW:].reshape(blocks, WINDOW, key_heads, HD)
        return jnp.concatenate([earlier, present], axis=1)

    key_band = banded(before[0], near_keys)
    value_band = banded(before[1], near_values)
    queries = near_query.reshape(blocks, WINDOW, key_heads, groups, HD)
    scores = jnp.einsum(
        "nqhgd,nkhd->hgnqk", queries, key_band, preferred_element_type=jnp.float32
    ) * HD ** (-0.5)
    head_ids = lax.axis_index("tp") * heads_here + jnp.arange(heads_here, dtype=jnp.int32)
    slopes = jnp.exp2(-8.0 * (head_ids + 1).astype(jnp.float32) / QH).reshape(key_heads, groups)
    query_pos = jnp.arange(WINDOW, dtype=jnp.int32)
    key_pos = jnp.arange(2 * WINDOW, dtype=jnp.int32)
    distance = query_pos[:, None] - key_pos[None, :] + WINDOW
    start_pos = (
        lax.axis_index("sp") * stream_extent + (jnp.arange(blocks, dtype=jnp.int32) - 1) * WINDOW
    )
    absolute = start_pos[:, None] + key_pos[None, :]
    allowed = ((distance >= 0) & (distance < WINDOW))[None] & (absolute >= 0)[:, None, :]
    biased = scores - slopes[:, :, None, None, None] * distance.astype(jnp.float32)
    weights = jnp.where(allowed, jnp.exp(biased), 0.0)
    denominator = (
        jnp.sum(weights, axis=-1, keepdims=True)
        + jnp.exp(head_sink_logit.reshape(key_heads, groups))[:, :, None, None, None]
    )
    attention = (weights / denominator).astype(jnp.bfloat16)
    attended = jnp.einsum(
        "hgnqk,nkhd->nqhgd", attention, value_band, preferred_element_type=jnp.float32
    )
    return attended.reshape(stream_extent, heads_here * HD).astype(jnp.bfloat16)


def linear_attention(
    gated_query, gated_keys, gated_values, fading_exponent, linear_head_gain, starting_state
):
    stream_extent = gated_query.shape[0]
    head_total = gated_query.shape[1] // LOOKUP_FEATURES
    span_count = stream_extent // SPAN
    scaled_query = gated_query.astype(jnp.float32).reshape(
        span_count, SPAN, head_total, LOOKUP_FEATURES
    ) * LOOKUP_FEATURES ** (-0.5)
    keys_wide = gated_keys.astype(jnp.float32).reshape(
        span_count, SPAN, head_total, LOOKUP_FEATURES
    )
    values_wide = gated_values.astype(jnp.float32).reshape(span_count, SPAN, head_total, DV)
    running = jnp.cumsum(
        fading_exponent.reshape(span_count, SPAN, head_total, LOOKUP_FEATURES), axis=1
    )
    span_end = running[:, -1]
    query_with_decay = scaled_query * jnp.exp(running)
    inverse_keys = keys_wide * jnp.exp(-running)
    ending_keys = keys_wide * jnp.exp(span_end[:, None] - running)
    inner = jnp.einsum("nchk,nshk->nhcs", query_with_decay, inverse_keys, precision=HIGH_PRECISION)
    lower = jnp.tril(jnp.ones((SPAN, SPAN), dtype=bool))
    inner = jnp.where(lower, inner, 0.0)
    within = jnp.einsum("nhcs,nshv->nchv", inner, values_wide, precision=HIGH_PRECISION)

    def advance(running_state, inputs):
        query_portion, key_portion, value_portion, scale_factor = inputs
        layer_output = jnp.einsum(
            "fmy,mys->fms", query_portion, running_state, precision=HIGH_PRECISION
        )
        running_state = running_state * scale_factor[..., None] + jnp.einsum(
            "gxp,gxz->xpz", key_portion, value_portion, precision=HIGH_PRECISION
        )
        return (running_state, layer_output)

    start_state = jnp.zeros((head_total, LOOKUP_FEATURES, DV), jnp.float32)
    state_end, carried = lax.scan(
        advance, start_state, (query_with_decay, ending_keys, values_wide, jnp.exp(span_end))
    )
    device_decay = jnp.exp(jnp.sum(span_end, axis=0))
    prefix_sums = jnp.cumsum(span_end, axis=0) - span_end

    def combine(earlier, later):
        return (earlier[0] * later[0], later[0][..., None] * earlier[1] + later[1])

    decay_before, state_before = prefix(
        (device_decay, state_end),
        "sp",
        combine,
        (jnp.ones_like(device_decay), jnp.zeros_like(state_end)),
    )
    incoming_rows = state_before + decay_before[..., None] * starting_state
    crossing = jnp.einsum(
        "qwso,soz->qwsz",
        query_with_decay * jnp.exp(prefix_sums)[:, None],
        incoming_rows,
        precision=HIGH_PRECISION,
    )
    flat = (within + carried + crossing).reshape(stream_extent, head_total, DV)
    normal = (
        flat * lax.rsqrt(jnp.mean(flat * flat, axis=-1, keepdims=True) + EPS) * linear_head_gain
    )
    return normal.reshape(stream_extent, head_total * DV).astype(jnp.bfloat16)


def local(
    activations,
    input_norm_gain,
    window_query_weight,
    window_key_weight,
    window_value_weight,
    linear_query_weight,
    linear_key_weight,
    linear_value_weight,
    decay_down_factor,
    decay_up_factor,
    decay_offset_bias,
    extra_fading_exponent,
    starting_state,
    head_sink_logit,
    linear_head_gain,
    window_output_weight,
    linear_output_weight,
):
    gathered = lax.all_gather(activations, "tp", axis=1, tiled=True)
    widened = gathered.astype(jnp.float32)
    normed = (
        widened
        * lax.rsqrt(jnp.mean(widened * widened, axis=1, keepdims=True) + EPS)
        * input_norm_gain
    ).astype(jnp.bfloat16)
    row_total = normed.shape[0]
    matrices = (
        window_query_weight,
        window_key_weight,
        window_value_weight,
        linear_query_weight,
        linear_key_weight,
        linear_value_weight,
    )
    segments = (
        lax.all_gather(matrices[0], "sp", axis=0, tiled=True),
        lax.all_gather(matrices[1], "sp", axis=0, tiled=True),
        lax.all_gather(matrices[2], "sp", axis=0, tiled=True),
        lax.all_gather(matrices[3], "sp", axis=0, tiled=True),
        lax.all_gather(matrices[4], "sp", axis=0, tiled=True),
        lax.all_gather(matrices[5], "sp", axis=0, tiled=True),
    )
    projected = tuple(
        (jnp.dot(normed, segment, preferred_element_type=jnp.float32) for segment in segments)
    )
    near_query, near_keys, near_values, gated_query, gated_keys, gated_values = [
        product.astype(jnp.bfloat16) for product in projected
    ]
    low_rank = jnp.dot(normed, decay_down_factor, preferred_element_type=jnp.float32).astype(
        jnp.bfloat16
    )
    attention_energies = (
        jnp.dot(low_rank, decay_up_factor, preferred_element_type=jnp.float32) + decay_offset_bias
    )
    head_total = extra_fading_exponent.shape[1]
    fading_exponent = (jax.nn.log_sigmoid(attention_energies) / FADING_SOFTNESS).reshape(
        row_total, head_total, LOOKUP_FEATURES
    ) + extra_fading_exponent[:, :, None]
    near_out = window_attention(near_query, near_keys, near_values, head_sink_logit)
    gated_out = linear_attention(
        gated_query, gated_keys, gated_values, fading_exponent, linear_head_gain, starting_state
    )
    window_full, linear_full = (
        lax.all_gather(window_output_weight, "sp", axis=1, tiled=True),
        lax.all_gather(linear_output_weight, "sp", axis=1, tiled=True),
    )
    return lax.psum_scatter(
        (
            jnp.dot(near_out, window_full, preferred_element_type=jnp.float32)
            + jnp.dot(gated_out, linear_full, preferred_element_type=jnp.float32)
        ).astype(jnp.bfloat16),
        "tp",
        scatter_dimension=0,
        tiled=True,
    )


def solution(mesh):
    placed = (
        P(("fs", "sp"), "tp"),
        P(),
        P("sp", "tp"),
        P("sp", "tp"),
        P("sp", "tp"),
        P("sp", "tp"),
        P("sp", "tp"),
        P("sp", "tp"),
        P(),
        P(None, "tp"),
        P("tp"),
        P(("fs", "sp"), "tp"),
        P("tp", None, None),
        P("tp"),
        P(),
        P("tp", "sp"),
        P("tp", "sp"),
    )
    return jax.shard_map(
        local, mesh=mesh, in_specs=placed, out_specs=P(("fs", "sp", "tp"), None), check_vma=False
    )
```

profile of v0, /device:TPU:0, one launch (start us, length us, event | category | flops | bytes accessed | tf_op | source)
XLA Modules:
  0.0 922.4 jit_solution(5273713908400685786)
XLA Ops:
  6.5 0.7 all-gather.14.cloned.1.call-update
  7.3 0.7 all-gather.26.cloned.1.call-update
  8.1 0.7 all-gather.28.cloned.1.call-update
  8.8 0.5 all-gather.24.cloned.1.call-update
  9.4 0.5 all-gather.16.cloned.1.call-update
  10.0 0.5 all-gather.18.cloned.1.call-update
  10.5 0.7 all-gather.20.cloned.1.call-update
  11.3 0.7 all-gather.22.cloned.1.call-update
  12.1 0.1 copy.80
  12.2 8.4 all-gather.14.cloned.1.call-done
  20.7 1.5 fusion.13
  22.2 2.1 fusion.31
  24.4 0.1 reshape.212
  24.5 0.2 fusion.36
  24.7 79.4 %all-gather.26.cloned.1.call-done = bf16[4096,512]{1,0:T(8,128)(2,1)} async-done(((bf16[1024,512]{1,0:T(8,128)(2,1)}), bf16[4096,512]{1,0:T(8,128)(2,1)}) %all-gather.26.cloned.1.call-update) | async-done | bytes 4194320 | tf_op jit(solution)/shard_map/all_gather | solution.py:192
  104.2 3.0 fusion.23
  107.2 77.8 %all-gather.28.cloned.1.call-done = bf16[4096,512]{1,0:T(8,128)(2,1)} async-done(((bf16[1024,512]{1,0:T(8,128)(2,1)}), bf16[4096,512]{1,0:T(8,128)(2,1)}) %all-gather.28.cloned.1.call-update) | async-done | bytes 4194320 | tf_op jit(solution)/shard_map/all_gather | solution.py:193
  185.0 2.9 fusion.21
  188.1 0.9 exponential_multiply_fusion.1
  189.1 145.5 %all-gather.24.cloned.1.call-done = bf16[4096,1024]{1,0:T(8,128)(2,1)} async-done(((bf16[1024,1024]{1,0:T(8,128)(2,1)}), bf16[4096,1024]{1,0:T(8,128)(2,1)}) %all-gather.24.cloned.1.call-update) | async-done | bytes 8388624 | tf_op jit(solution)/shard_map/all_gather | solution.py:194
  334.6 4.7 convolution_convert_fusion
  339.3 0.2 reshape.211
  339.5 3.8 while.29
  339.5 1.1 fusion.87
  340.7 0.7 convolution_add_fusion.4
  341.4 1.1 fusion.87
  342.6 0.7 convolution_add_fusion.4
  343.4 0.8 convert_element_type.128
  344.2 0.5 all-gather.30.cloned.1.call-update
  345.0 0.1 fusion.48
  345.1 34.8 %all-gather.16.cloned.1.call-done = bf16[4096,256]{1,0:T(8,128)(2,1)} async-done(((bf16[1024,256]{1,0:T(8,128)(2,1)}), bf16[4096,256]{1,0:T(8,128)(2,1)}) %all-gather.16.cloned.1.call-update) | async-done | bytes 2097168 | tf_op jit(solution)/shard_map/all_gather | solution.py:190
  379.9 2.1 convolution_convert_fusion.6
  382.0 43.8 %all-gather.18.cloned.1.call-done = bf16[4096,256]{1,0:T(8,128)(2,1)} async-done(((bf16[1024,256]{1,0:T(8,128)(2,1)}), bf16[4096,256]{1,0:T(8,128)(2,1)}) %all-gather.18.cloned.1.call-update) | async-done | bytes 2097168 | tf_op jit(solution)/shard_map/all_gather | solution.py:191
  425.8 2.1 convolution_convert_fusion.5
  427.9 2.1 collective-permute-start
  430.0 9.4 %all-gather.2 = bf16[4,4,128]{2,1,0:T(4,128)(2,1)S(1)} all-gather(bf16[1,4,128]{2,1,0:T(4,128)(2,1)S(1)} %fusion.50), channel_id=2, replica_groups=mesh['sp'=4,'fs'=4,'tp'=2] {'sp'}, dimensions={0}, use_global_device_ids=true | all-gather | bytes 5120 | tf_op jit(solution)/shard_map/all_gather | solution.py:28
  439.4 0.1 copy.63
  439.5 0.1 copy.61
  439.7 0.1 copy.62
  439.8 0.1 copy.60
  439.9 1.3 convolution_select_fusion
  441.2 134.7 %all-gather.20.cloned.1.call-done = bf16[4096,1024]{1,0:T(8,128)(2,1)} async-done(((bf16[1024,1024]{1,0:T(8,128)(2,1)}), bf16[4096,1024]{1,0:T(8,128)(2,1)}) %all-gather.20.cloned.1.call-update) | async-done | bytes 8388624 | tf_op jit(solution)/shard_map/all_gather | solution.py:189
  575.8 4.7 convolution_convert_fusion.2
  580.5 0.2 copy.64
  580.7 0.8 fusion.64
  581.6 0.3 convolution_convert_fusion.1
  581.9 143.3 %all-gather.22.cloned.1.call-done = bf16[1024,4096]{1,0:T(8,128)(2,1)} async-done(((bf16[1024,1024]{1,0:T(8,128)(2,1)}), bf16[1024,4096]{1,0:T(8,128)(2,1)}) %all-gather.22.cloned.1.call-update) | async-done | bytes 8388624 | tf_op jit(solution)/shard_map/all_gather | solution.py:217
  725.2 4.7 fusion.65
  729.9 23.1 %all-gather.32.cloned.1.call-done = bf16[16,128,256]{2,1,0:T(8,128)(2,1)} async-done(((bf16[4,128,256]{2,1,0:T(8,128)(2,1)}), bf16[16,128,256]{2,1,0:T(8,128)(2,1)}) %all-gather.32.cloned.1.call-update) | async-done | bytes 1048592 | tf_op jit(solution)/shard_map/all_gather | solution.py:28
  753.0 4.8 while.30
  753.0 1.2 fusion.88
  754.3 1.1 fusion.88
  755.5 1.1 fusion.88
  756.7 1.1 fusion.88
  757.9 1.8 convolution_bitcast_fusion.1
  759.7 1.4 multiply_reduce_fusion
  761.2 0.1 copy.81
  761.3 0.2 mul.189
  761.5 0.1 copy.85
  761.6 0.3 copy.74
  761.9 0.1 copy.84
  762.0 141.4 %all-gather.30.cloned.1.call-done = bf16[1024,4096]{1,0:T(8,128)(2,1)} async-done(((bf16[1024,1024]{1,0:T(8,128)(2,1)}), bf16[1024,4096]{1,0:T(8,128)(2,1)}) %all-gather.30.cloned.1.call-update) | async-done | bytes 8388624 | tf_op jit(solution)/shard_map/all_gather | solution.py:218
  903.4 5.7 fusion.12
  909.1 6.7 reduce-scatter.2.cloned.1.call-done
  (75 shorter events, 1.2 us)
Async XLA Ops:
  6.5 15.7 %copy-start = (bf16[4096,16]{0,1:T(8,128)(2,1)S(1)}, bf16[4096,16]{0,1:T(8,128)(2,1)}, u32[]{:S(2)}) copy-start(bf16[4096,16]{0,1:T(8,128)(2,1)} %param.29) | copy-start | bytes 393220
  6.5 14.1 %all-gather.14.cloned.1.call-start = ((), (), s32[]{:S(2)}) async-start(), calls=%async_computation.1 | async-start | bytes 1572864 | tf_op jit(solution)/shard_map/all_gather | solution.py:172
  7.3 96.9 %all-gather.26.cloned.1.call-start = ((), (), s32[]{:S(2)}) async-start(), calls=%async_computation.7 | async-start | bytes 5242880 | tf_op jit(solution)/shard_map/all_gather | solution.py:192
  8.0 177.0 %all-gather.28.cloned.1.call-start = ((), (), s32[]{:S(2)}) async-start(), calls=%async_computation.8 | async-start | bytes 5242880 | tf_op jit(solution)/shard_map/all_gather | solution.py:193
  8.7 325.9 %all-gather.24.cloned.1.call-start = ((), (), s32[]{:S(2)}) async-start(), calls=%async_computation.6 | async-start | bytes 10485760 | tf_op jit(solution)/shard_map/all_gather | solution.py:194
  9.3 370.6 %all-gather.16.cloned.1.call-start = ((), (), s32[]{:S(2)}) async-start(), calls=%async_computation.2 | async-start | bytes 2621440 | tf_op jit(solution)/shard_map/all_gather | solution.py:190
  9.9 415.9 %all-gather.18.cloned.1.call-start = ((), (), s32[]{:S(2)}) async-start(), calls=%async_computation.3 | async-start | bytes 2621440 | tf_op jit(solution)/shard_map/all_gather | solution.py:191
  10.5 1.6 copy-start.5
  10.5 565.3 %all-gather.20.cloned.1.call-start = ((), (), s32[]{:S(2)}) async-start(), calls=%async_computation.4 | async-start | bytes 10485760 | tf_op jit(solution)/shard_map/all_gather | solution.py:189
  11.2 11.0 %copy-start.7 = (bf16[16,512]{1,0:T(8,128)(2,1)S(1)}, bf16[16,512]{1,0:T(8,128)(2,1)}, u32[]{:S(2)}) copy-start(bf16[16,512]{1,0:T(8,128)(2,1)} %param.30) | copy-start | bytes 49156
  11.3 11.0 %copy-start.8 = (f32[4096]{0:T(1024)S(1)}, f32[4096]{0:T(1024)}, u32[]{:S(2)}) copy-start(f32[4096]{0:T(1024)} %param.22) | copy-start | bytes 49156
  11.3 11.0 %copy-start.10 = (f32[512]{0:T(512)S(1)}, f32[512]{0:T(512)}, u32[]{:S(2)}) copy-start(f32[512]{0:T(512)} %param.31) | copy-start | bytes 6148
  11.3 714.0 %all-gather.22.cloned.1.call-start = ((), (), s32[]{:S(2)}) async-start(), calls=%async_computation.5 | async-start | bytes 10485760 | tf_op jit(solution)/shard_map/all_gather | solution.py:217
  12.0 741.0 %all-gather.32.cloned.1.call-start = ((), (), s32[]{:S(2)}) async-start(), calls=%async_computation.11 | async-start | bytes 1310720 | tf_op jit(solution)/shard_map/all_gather | solution.py:28
  22.2 82.0 %copy-start.2 = (bf16[128,4096]{1,0:T(8,128)(2,1)S(1)}, bf16[128,4096]{1,0:T(8,128)(2,1)}, u32[]{:S(2)}) copy-start(bf16[128,4096]{1,0:T(8,128)(2,1)} %all-gather.14.cloned.1.call-done) | copy-start | bytes 3145732
  343.3 1.5 copy-start.11
  343.4 1.6 copy-start.6
  343.4 36.5 %copy-start.9 = (f32[4096]{0:T(1024)S(1)}, f32[4096]{0:T(1024)}, u32[]{:S(2)}) copy-start(f32[4096]{0:T(1024)} %param.22) | copy-start | bytes 49156
  344.2 559.3 %all-gather.30.cloned.1.call-start = ((), (), s32[]{:S(2)}) async-start(), calls=%async_computation.9 | async-start | bytes 10485760 | tf_op jit(solution)/shard_map/all_gather | solution.py:218
  344.8 571.1 %reduce-scatter.2.cloned.1.call-start = ((), (), s32[]{:S(2)}) async-start(), calls=%async_computation.10 | async-start | bytes 1572864 | tf_op jit(solution)/shard_map/reduce_scatter | solution.py:220
  427.9 11.7 %collective-permute-start = (bf16[2,128,256]{2,1,0:T(8,128)(2,1)S(1)}, bf16[2,128,256]{2,1,0:T(8,128)(2,1)S(1)}, u32[]{:S(2)}, u32[]{:S(2)}) collective-permute-start(bf16[2,128,256]{2,1,0:T(8,128)(2,1)S(1)} %pad_maximum_fusion), channel_id=1, source_target_pairs={{0,8},{8,16},{16,24},{1,9},{9,17},{17,25},{2,10},{10,18},{18,26},{... | collective-permute-start | bytes 393224 | tf_op jit(solution)/shard_map/ppermute | solution.py:22
  753.0 4.9 copy-start.3
  757.9 1.8 copy-start.4
  903.4 12.4 %copy-start.1 = (bf16[4096,16]{0,1:T(8,128)(2,1)S(1)}, bf16[4096,16]{0,1:T(8,128)(2,1)}, u32[]{:S(2)}) copy-start(bf16[4096,16]{0,1:T(8,128)(2,1)} %param.29) | copy-start | bytes 393220
Sparse Core Ops, SparseCore 0:
  8.9 11.7 all-gather.13
  22.2 81.9 all-gather.25
  105.7 79.2 all-gather.27
  186.5 148.0 all-gather.23
  336.0 43.8 all-gather.15
  381.3 44.4 all-gather.17
  427.4 148.3 all-gather.19
  577.4 147.7 all-gather.21
  726.8 26.1 all-gather.31
  754.4 148.9 all-gather.29
  909.3 6.5 reduce-scatter.1
where the time goes:
time: 923 us; the launch traced here: 922 us
  waiting for transfers between devices  845 us (92%)
  matrix products  41.2 us (4%)
  between operations  13.7 us (1%)
  blocking collectives  9.38 us (1%)
    all_gather x1, waiting for transfers between devices, local(): lax.all_gather(matrices[5], 'sp', axis=0, tiled=True)  146 us
    all_gather x1, waiting for transfers between devices, local(): lax.all_gather(window_output_weight, 'sp', axis=1, tiled=True)  143 us
    all_gather x1, waiting for transfers between devices, local(): lax.all_gather(linear_output_weight, 'sp', axis=1, tiled=True)  141 us
    all_gather x1, waiting for transfers between devices, local(): lax.all_gather(matrices[0], 'sp', axis=0, tiled=True)  135 us
    all_gather x1, waiting for transfers between devices, local(): lax.all_gather(matrices[3], 'sp', axis=0, tiled=True)  79.4 us
    all_gather x1, waiting for transfers between devices, local(): lax.all_gather(matrices[4], 'sp', axis=0, tiled=True)  77.8 us
    all_gather x1, waiting for transfers between devices, local(): lax.all_gather(matrices[2], 'sp', axis=0, tiled=True)  43.8 us
    all_gather x1, waiting for transfers between devices, local(): lax.all_gather(matrices[1], 'sp', axis=0, tiled=True)  34.8 us
  transfers between devices with their start and end apart: 12, of which 11 were waited for; matrix products, arithmetic and copies ran while one was open for 5% of the time, Pallas kernels for 0%

commit v1 on v0

--- a/solution.py
+++ b/solution.py
@@ -1,6 +1,10 @@
+import functools
+
 import jax
 import jax.numpy as jnp
 from jax import lax
+from jax.experimental import pallas as pl
+from jax.experimental.pallas import tpu as pltpu
 from jax.sharding import PartitionSpec as P
 
 QH = 32
@@ -228,6 +232,582 @@
     )
 
 
+def _pairs(peers, depths, core):
+    out = []
+    for d in depths:
+        out.append((d * 2 + core, (d + 1) * 2 + core))
+        out.append(((peers - 1 - d) * 2 + 1 - core, (peers - 2 - d) * 2 + 1 - core))
+    return out
+
+
+SWAP = [(0, 1), (1, 0)]
+VMEM = pl.BlockSpec(memory_space=pltpu.VMEM)
+SMEM = pl.BlockSpec(memory_space=pltpu.SMEM)
+ANY = pl.BlockSpec(memory_space=pl.ANY)
+BY_COLUMNS = (((1,), (1,)), ((), ()))
+BY_ROWS = (((0,), (0,)), ((), ()))
+
+
+def _call(kernel, name, out_shape, flops, moved, **kw):
+    return pl.pallas_call(
+        kernel,
+        out_shape=out_shape,
+        compiler_params=pltpu.CompilerParams(vmem_limit_bytes=48 * 1024 * 1024),
+        cost_estimate=pl.CostEstimate(flops=flops, bytes_accessed=moved, transcendentals=0),
+        name=name,
+        **kw,
+    )
+
+
+def _prefetch(scalars, grid, in_specs, out_specs, scratch=()):
+    return pltpu.PrefetchScalarGridSpec(
+        num_scalar_prefetch=scalars, grid=grid, in_specs=in_specs, out_specs=out_specs, scratch_shapes=scratch
+    )
+
+
+def norm_kernel(place_ref, x_ref, fade_ref, mate_ref, gain_ref, down_ref, out_ref):
+    me = place_ref[0]
+    pieces, rows, wide = out_ref.shape
+    half_model = x_ref.shape[1]
+    cut = 2 * half_model // pieces
+    fades = fade_ref.shape[1]
+    own = x_ref[pl.ds(pl.multiple_of(me * rows, rows), rows), :].astype(jnp.float32)
+    mate = mate_ref[:, :half_model].astype(jnp.float32)
+    square = jnp.sum(own * own, axis=1, keepdims=True) + jnp.sum(mate * mate, axis=1, keepdims=True)
+    scale = lax.rsqrt(square / (2 * half_model) + EPS)
+    low_rank = None
+    for side, value in ((me, own), (1 - me, mate)):
+        start = pl.multiple_of(side * half_model, half_model)
+        normed = (value * scale * gain_ref[:, pl.ds(start, half_model)]).astype(jnp.bfloat16)
+        part = jnp.dot(normed, down_ref[pl.ds(start, half_model), :], preferred_element_type=jnp.float32)
+        low_rank = part if low_rank is None else low_rank + part
+        for k in range(pieces // 2):
+            out_ref[side * (pieces // 2) + k, :, :cut] = normed[:, k * cut : (k + 1) * cut]
+    mine = fade_ref[pl.ds(pl.multiple_of(me * rows, rows), rows), :]
+    theirs = mate_ref[:, half_model : half_model + fades]
+    tail = jnp.concatenate(
+        [
+            low_rank.astype(jnp.bfloat16).astype(jnp.float32),
+            jnp.where(me == 0, mine, theirs).astype(jnp.float32),
+            jnp.where(me == 0, theirs, mine).astype(jnp.float32),
+            jnp.zeros((rows, wide - cut - low_rank.shape[1] - 2 * fades), jnp.float32),
+        ],
+        axis=1,
+    ).astype(jnp.bfloat16)
+    for k in range(pieces):
+        out_ref[k, :, cut:] = tail
+
+
+def pack_kernel(key_heads, side_ref, wq, wk, wv, lq, lk, lv, out_ref):
+    step = pl.program_id(0)
+    half = out_ref.shape[2] // 2
+    keys_and_values = step == 0
+    queries = (step > 0) & (step <= key_heads)
+    head_items = (step > key_heads) & ((step - key_heads) % 2 == 1)
+    head_values = (step > key_heads) & ((step - key_heads) % 2 == 0)
+
+    @pl.when(keys_and_values)
+    def _():
+        out_ref[0, :, :half] = wk[...]
+        out_ref[0, :, half:] = wv[...]
+
+    @pl.when(queries)
+    def _():
+        out_ref[0] = wq[...]
+
+    @pl.when(head_items)
+    def _():
+        out_ref[0, :, :half] = lq[...]
+        out_ref[0, :, half:] = lk[...]
+
+    @pl.when(head_values)
+    def _():
+        out_ref[0] = lv[...]
+
+
+def pack_items(side, lin, key_heads, matrices):
+    depth = matrices[0].shape[0]
+    width = 2 * LOOKUP_FEATURES
+    count = 1 + key_heads + 2 * lin
+    fixed = pl.BlockSpec((depth, width // 2), lambda i, side: (0, side[0]))
+    query = pl.BlockSpec(
+        (depth, width), lambda i, side: (0, side[0] * key_heads + jnp.clip(i - 1, 0, key_heads - 1))
+    )
+    head = lambda i, side: (0, side[0] * lin + jnp.clip((i - 1 - key_heads) // 2, 0, lin - 1))
+    narrow, full = pl.BlockSpec((depth, width // 2), head), pl.BlockSpec((depth, width), head)
+    return _call(
+        functools.partial(pack_kernel, key_heads),
+        "pack_items",
+        jax.ShapeDtypeStruct((count, depth, width), jnp.bfloat16),
+        10**9,
+        4 * count * depth * width,
+        grid_spec=_prefetch(
+            1,
+            (count,),
+            [query, fixed, fixed, narrow, narrow, full],
+            pl.BlockSpec((1, depth, width), lambda i, side: (i, 0, 0)),
+        ),
+    )(side, *matrices)
+
+
+def partial_kernel(index_ref, mine_ref, theirs_ref, own_ref, other_ref, *rest):
+    out_ref = rest[-1]
+    width = own_ref.shape[-1]
+    rows = mine_ref.shape[0]
+    for top, x_ref in enumerate((mine_ref, theirs_ref)):
+        for half, weight in enumerate((own_ref, other_ref)):
+            at = slice(top * rows, (top + 1) * rows)
+            span = slice(half * width, (half + 1) * width)
+            total = jnp.dot(x_ref[...], weight[0], preferred_element_type=jnp.float32)
+            if len(rest) == 2:
+                total = total + rest[0][at, span].astype(jnp.float32)
+            out_ref[at, span] = total.astype(out_ref.dtype)
+
+
+def partial_sum(index, mine, theirs, own, other, arrived):
+    rows = mine.shape[0]
+    _, depth, width = own.shape
+    operands = [mine, theirs, own, other] + ([] if arrived is None else [arrived])
+    whole = pl.BlockSpec((2 * rows, 2 * width), lambda i, index: (0, 0))
+    tokens = pl.BlockSpec((rows, depth), lambda i, index: (0, 0))
+    block = pl.BlockSpec((1, depth, width), lambda i, index: (index[0], 0, 0))
+    return _call(
+        partial_kernel,
+        "partial_sum",
+        jax.ShapeDtypeStruct((2 * rows, 2 * width), jnp.bfloat16),
+        8 * rows * depth * width,
+        4 * depth * (rows + width),
+        grid_spec=_prefetch(
+            1, (1,), [tokens, tokens, block, block] + ([] if arrived is None else [whole]), whole
+        ),
+    )(index, *operands)
+
+
+def decay_kernel(lin, rank, place_ref, mine_ref, theirs_ref, own_ref, other_ref, out_ref):
+    me, side = place_ref[0], place_ref[1]
+    rows = mine_ref.shape[0]
+    features = LOOKUP_FEATURES
+    all_heads = 4 * lin
+    lower = (
+        lax.broadcasted_iota(jnp.int32, (SPAN, SPAN), 0) >= lax.broadcasted_iota(jnp.int32, (SPAN, SPAN), 1)
+    ).astype(jnp.bfloat16)
+    for top, tail_ref in enumerate((mine_ref, theirs_ref)):
+        tail = tail_ref[...]
+        low_rank = tail[:, :rank]
+        parts = [
+            tail[:, rank + k * 2 * lin : rank + (k + 1) * 2 * lin].astype(jnp.float32) for k in range(6)
+        ]
+        by_core = [parts[0] + parts[1] + parts[2], parts[3] + parts[4] + parts[5]]
+        fades = [jnp.where(me == 0, by_core[0], by_core[1]), jnp.where(me == 0, by_core[1], by_core[0])]
+        for head in range(lin):
+            for owner, small_ref in enumerate((own_ref, other_ref)):
+                at = pl.ds(pl.multiple_of((side * lin + head) * features, features), features)
+                up = small_ref[:rank, at].astype(jnp.bfloat16)
+                energy = jnp.dot(low_rank, up, preferred_element_type=jnp.float32) + small_ref[rank : rank + 1, at]
+                soft = jnp.minimum(energy, 0.0) - jnp.log1p(jnp.exp(-jnp.abs(energy)))
+                both = fades[owner]
+                fade = jnp.where(side == 0, both[:, head : head + 1], both[:, lin + head : lin + head + 1])
+                step = soft * (1.0 / FADING_SOFTNESS) + fade
+                high = step.astype(jnp.bfloat16)
+                rest = step - high.astype(jnp.float32)
+                middle = rest.astype(jnp.bfloat16)
+                low = (rest - middle.astype(jnp.float32)).astype(jnp.bfloat16)
+                column = (2 * head + owner) * features
+                for span in range(rows // SPAN):
+                    cut = slice(span * SPAN, (span + 1) * SPAN)
+                    out_ref[top * rows + span * SPAN : top * rows + (span + 1) * SPAN, column : column + features] = (
+                        jnp.dot(lower, high[cut], preferred_element_type=jnp.float32)
+                        + jnp.dot(lower, middle[cut], preferred_element_type=jnp.float32)
+                        + jnp.dot(lower, low[cut], preferred_element_type=jnp.float32)
+                    )
+
+
+def decay_sums(place, lin, rank, mine, theirs, own, other):
+    rows, wide = mine.shape
+    lanes = LOOKUP_FEATURES
+    tail = pl.BlockSpec((rows, lanes), lambda i, place: (0, wide // lanes - 1))
+    whole = lambda shape: pl.BlockSpec(shape, lambda i, place: (0, 0))
+    out = (2 * rows, 2 * lin * LOOKUP_FEATURES)
+    return _call(
+        functools.partial(decay_kernel, lin, rank),
+        "decay_sums",
+        jax.ShapeDtypeStruct(out, jnp.float32),
+        10**9,
+        2**20,
+        grid_spec=_prefetch(
+            1, (1,), [tail, tail, whole(own.shape), whole(other.shape)], whole(out)
+        ),
+    )(place, mine, theirs, own, other)
+
+
+def linear_kernel(lin, head, half, place_ref, query_key_ref, value_ref, running_ref, own_ref, other_ref, gain_ref, out_ref):
+    me, side = place_ref[0], place_ref[1]
+    rows, width = query_key_ref.shape
+    features = LOOKUP_FEATURES
+    values = width // 2
+    lower = lax.broadcasted_iota(jnp.int32, (SPAN, SPAN), 0) >= lax.broadcasted_iota(
+        jnp.int32, (SPAN, SPAN), 1
+    )
+    states = [state_ref[side * lin + head].T for state_ref in (own_ref, other_ref)]
+    for span in range(rows // SPAN):
+        per = half // SPAN
+        device, inside = span // (2 * per), span % (2 * per)
+        apart = jnp.where(me == inside // per, 0, rows // 2)
+        at = pl.ds(pl.multiple_of(apart + device * half + (inside % per) * SPAN, SPAN), SPAN)
+        for owner in range(2):
+            base = owner * values
+            running = running_ref[at, owner * features : (owner + 1) * features]
+            query = query_key_ref[at, base : base + features].astype(jnp.float32)
+            key = query_key_ref[at, base + features : base + 2 * features].astype(jnp.float32)
+            value = value_ref[at, base : base + values]
+            end = running[SPAN - 1 : SPAN]
+            scaled = (query * features ** (-0.5) * jnp.exp(running)).astype(jnp.bfloat16)
+            inverse = (key * jnp.exp(-running)).astype(jnp.bfloat16)
+            ending = (key * jnp.exp(end - running)).astype(jnp.bfloat16)
+            inner = lax.dot_general(scaled, inverse, BY_COLUMNS, preferred_element_type=jnp.float32)
+            inner = jnp.where(lower, inner, 0.0).astype(jnp.bfloat16)
+            state = states[owner]
+            raw = jnp.dot(inner, value, preferred_element_type=jnp.float32) + lax.dot_general(
+                scaled, state.astype(jnp.bfloat16), BY_COLUMNS, preferred_element_type=jnp.float32
+            )
+            states[owner] = state * jnp.exp(end) + lax.dot_general(
+                value, ending, BY_ROWS, preferred_element_type=jnp.float32
+            )
+            scale = lax.rsqrt(jnp.mean(raw * raw, axis=-1, keepdims=True) + EPS)
+            out_ref[at, base : base + values] = (raw * scale * gain_ref[...]).astype(out_ref.dtype)
+
+
+def linear_heads(place, lin, head, half, query_key, value, running, own, other, gain):
+    rows, width = query_key.shape
+    whole = lambda a: pl.BlockSpec(a.shape, lambda i, place: (0,) * a.ndim)
+    block = pl.BlockSpec((rows, 2 * LOOKUP_FEATURES), lambda i, place: (0, head))
+    return _call(
+        functools.partial(linear_kernel, lin, head, half),
+        "linear_heads",
+        jax.ShapeDtypeStruct((rows, width), jnp.bfloat16),
+        2 * 10**9,
+        2**21,
+        grid_spec=_prefetch(
+            1,
+            (1,),
+            [whole(query_key), whole(value), block, whole(own), whole(other), whole(gain)],
+            pl.BlockSpec((rows, width), lambda i, place: (0, 0)),
+        ),
+    )(place, query_key, value, running, own, other, gain)
+
+
+def window_kernel(group, half, place_ref, slope_ref, sink_ref, key_value_ref, query_ref, out_ref):
+    me = place_ref[0]
+    rows = query_ref.shape[0]
+    owners, groups = slope_ref.shape
+    pair = key_value_ref.shape[1] // (2 * owners)
+    from_query = lax.broadcasted_iota(jnp.int32, (WINDOW, WINDOW), 0)
+    from_key = lax.broadcasted_iota(jnp.int32, (WINDOW, WINDOW), 1)
+    present = from_key <= from_query
+    distance = jnp.where(present, from_query - from_key, from_query - from_key + WINDOW).astype(jnp.float32)
+    unit = min(half, WINDOW)
+
+    def places(block):
+        out = []
+        for piece in range(WINDOW // unit):
+            start = block * WINDOW + piece * unit
+            device, inside = start // (2 * half), start % (2 * half)
+            apart = jnp.where(me == inside // half, 0, rows // 2)
+            out.append(pl.ds(pl.multiple_of(apart + device * half + inside % half, unit), unit))
+        return out
+
+    for owner in range(owners):
+        key_at = owner * 2 * pair + group * HD
+        value_at = key_at + pair
+        base = owner * groups * HD
+        biases = [slope_ref[owner, head] * distance for head in range(groups)]
+        past_keys, past_values = None, None
+        for block in range(rows // WINDOW):
+            first = block == 0
+            at = places(block)
+            keys = jnp.concatenate([key_value_ref[a, key_at : key_at + HD] for a in at], axis=0)
+            values = jnp.concatenate([key_value_ref[a, value_at : value_at + HD] for a in at], axis=0)
+            band_keys = keys if first else jnp.concatenate([past_keys, keys], axis=0)
+            band_values = values if first else jnp.concatenate([past_values, values], axis=0)
+            past_keys, past_values = keys, values
+            queries = jnp.concatenate(
+                [query_ref[a, base + head * HD : base + (head + 1) * HD] for head in range(groups) for a in at],
+                axis=0,
+            )
+            scores = lax.dot_general(queries, band_keys, BY_COLUMNS, preferred_element_type=jnp.float32)
+            probs = []
+            for head in range(groups):
+                mine = scores[head * WINDOW : (head + 1) * WINDOW]
+                if first:
+                    weight = jnp.where(present, jnp.exp(mine * HD ** (-0.5) - biases[head]), 0.0)
+                else:
+                    score = jnp.where(present, mine[:, WINDOW:], mine[:, :WINDOW])
+                    weight = jnp.exp(score * HD ** (-0.5) - biases[head])
+                total = jnp.sum(weight, axis=-1, keepdims=True) + sink_ref[owner, head]
+                share = weight / total
+                if first:
+                    probs.append(share.astype(jnp.bfloat16))
+                else:
+                    probs.append(
+                        jnp.concatenate(
+                            [
+                                jnp.where(present, 0.0, share).astype(jnp.bfloat16),
+                                jnp.where(present, share, 0.0).astype(jnp.bfloat16),
+                            ],
+                            axis=1,
+                        )
+                    )
+            outs = jnp.dot(jnp.concatenate(probs, axis=0), band_values, preferred_element_type=jnp.float32)
+            joined = jnp.concatenate(
+                [outs[head * WINDOW : (head + 1) * WINDOW] for head in range(groups)], axis=1
+            ).astype(out_ref.dtype)
+            for piece, a in enumerate(at):
+                out_ref[a, base : base + groups * HD] = joined[piece * unit : (piece + 1) * unit]
+
+
+def window_heads(place, group, half, slopes, sinks, key_value, query):
+    return _call(
+        functools.partial(window_kernel, group, half),
+        "window_heads",
+        jax.ShapeDtypeStruct(query.shape, jnp.bfloat16),
+        2 * 10**9,
+        2**21,
+        in_specs=[SMEM, SMEM, SMEM, VMEM, VMEM],
+        out_specs=VMEM,
+    )(place, slopes, sinks, key_value, query)
+
+
+def output_kernel(pieces, hops, place_ref, *refs):
+    passed = refs[: pieces + hops]
+    own_ref, other_ref = refs[pieces + hops : pieces + hops + 2]
+    before = refs[pieces + hops + 2 : -3]
+    out_ref, held, arrival = refs[-3:]
+    depth = place_ref[2]
+    for at in range(hops + 1):
+
+        @pl.when(depth == at)
+        def _():
+            for piece in range(pieces):
+                pltpu.make_async_copy(passed[piece + at], held.at[piece], arrival.at[piece]).start()
+
+    for piece in range(pieces):
+        pltpu.make_async_copy(passed[piece], held.at[piece], arrival.at[piece]).wait()
+    width = held.shape[2] // 2
+    rows = held.shape[1]
+    columns = out_ref.shape[1]
+    block = columns // 4
+    for part in range(4):
+        span = slice(part * block, (part + 1) * block)
+        total = before[0][:, span] if before else jnp.zeros((rows, block), jnp.float32)
+        for piece in range(pieces):
+            lines = slice(piece * width, (piece + 1) * width)
+            total = total + jnp.dot(held[piece, :, :width], own_ref[lines, span], preferred_element_type=jnp.float32)
+            total = total + jnp.dot(held[piece, :, width:], other_ref[lines, span], preferred_element_type=jnp.float32)
+        out_ref[:, span] = total.astype(out_ref.dtype)
+
+
+def output_sum(place, passed, hops, own, other, before, kind):
+    rows, width = passed[0].shape
+    pieces = len(passed) - hops
+    lines, columns = other.shape
+    whole = pl.BlockSpec((rows, columns), lambda i, place: (0, 0))
+    return _call(
+        functools.partial(output_kernel, pieces, hops),
+        "output_sum",
+        jax.ShapeDtypeStruct((rows, columns), kind),
+        4 * rows * columns * lines,
+        8 * rows * columns,
+        grid_spec=_prefetch(
+            1,
+            (1,),
+            [ANY] * len(passed)
+            + [
+                pl.BlockSpec((lines, columns), lambda i, place: (place[1], 0)),
+                pl.BlockSpec((lines, columns), lambda i, place: (0, 0)),
+            ]
+            + ([] if before is None else [whole]),
+            whole,
+            [pltpu.VMEM((pieces, rows, width), jnp.bfloat16), pltpu.SemaphoreType.DMA((pieces,))],
+        ),
+    )(place, *passed, own, other, *([] if before is None else [before]))
+
+
+def resident(
+    activations,
+    input_norm_gain,
+    window_query_weight,
+    window_key_weight,
+    window_value_weight,
+    linear_query_weight,
+    linear_key_weight,
+    linear_value_weight,
+    decay_down_factor,
+    decay_up_factor,
+    decay_offset_bias,
+    extra_fading_exponent,
+    starting_state,
+    head_sink_logit,
+    linear_head_gain,
+    window_output_weight,
+    linear_output_weight,
+):
+    peers = lax.axis_size("sp")
+    hops = peers - 1
+    line, me = lax.axis_index("sp"), lax.axis_index("tp")
+    depth = jnp.where(me == 0, line, hops - line)
+    far, near = 1 - me, me
+    place = jnp.stack([me, far, hops - depth]).astype(jnp.int32)
+    rows, half_model = activations.shape
+    half = rows // 2
+    bf16, f32 = jnp.bfloat16, jnp.float32
+    lin = extra_fading_exponent.shape[1] // 2
+    key_heads = window_key_weight.shape[1] // HD // 2
+    query_heads = window_query_weight.shape[1] // HD // 2
+    groups = query_heads // key_heads
+    rank = decay_down_factor.shape[1]
+    swap = lambda value: lax.ppermute(value, "tp", SWAP)
+
+    high = lax.reduce_precision(extra_fading_exponent, 8, 7)
+    rest = extra_fading_exponent - high
+    middle = lax.reduce_precision(rest, 8, 7)
+    fade = jnp.concatenate([high, middle, rest - middle], axis=1).astype(bf16)
+    message = jnp.concatenate([activations, fade], axis=1)
+    message = jnp.pad(message, ((0, 0), (0, LOOKUP_FEATURES - fade.shape[1])))
+    mate = swap(lax.dynamic_slice_in_dim(message, far * half, half, axis=0))
+    wide = 2 * half_model // peers + LOOKUP_FEATURES
+    outgoing = _call(
+        norm_kernel,
+        "norm",
+        jax.ShapeDtypeStruct((peers, half, wide), bf16),
+        10**9,
+        2**21,
+        in_specs=[SMEM] + [VMEM] * 5,
+        out_specs=VMEM,
+    )(place, activations, fade, mate, input_norm_gain.reshape(1, -1), decay_down_factor)
+
+    (
+        outgoing,
+        matrices,
+        window_output_weight,
+        linear_output_weight,
+        starting_state,
+        decay_up_factor,
+        decay_offset_bias,
+        head_sink_logit,
+    ) = lax.optimization_barrier(
+        (
+            outgoing,
+            (
+                window_query_weight,
+                window_key_weight,
+                window_value_weight,
+                linear_query_weight,
+                linear_key_weight,
+                linear_value_weight,
+            ),
+            window_output_weight,
+            linear_output_weight,
+            starting_state,
+            decay_up_factor,
+            decay_offset_bias,
+            head_sink_logit,
+        )
+    )
+    incoming = lax.all_to_all(outgoing, "sp", 0, 0, tiled=True)
+    other_in = swap(pack_items(near.reshape(1), lin, key_heads, matrices))
+    own_in = pack_items(far.reshape(1), lin, key_heads, matrices)
+    features = decay_up_factor.shape[1]
+    own_small = jnp.concatenate(
+        [
+            decay_up_factor.astype(f32),
+            decay_offset_bias.reshape(1, features),
+            jnp.pad(head_sink_logit, (0, features - head_sink_logit.shape[0])).reshape(1, features),
+            jnp.zeros((6, features), f32),
+        ],
+        axis=0,
+    )
+    other_small = swap(own_small)
+    other_state = swap(starting_state)
+    lines = linear_output_weight.shape[0] // 2
+    other_linear = swap(lax.dynamic_slice_in_dim(linear_output_weight, near * lines, lines, axis=0))
+    lines = window_output_weight.shape[0] // 2
+    other_window = swap(lax.dynamic_slice_in_dim(window_output_weight, near * lines, lines, axis=0))
+
+    mine = incoming.reshape(peers * half, wide)
+    theirs = swap(incoming).reshape(peers * half, wide)
+
+    count = 1 + key_heads + 2 * lin
+    arrived, finals = {}, []
+    for step in range(count + 2 * hops):
+        index = jnp.clip(step - 2 * depth, 0, count - 1).astype(jnp.int32).reshape(1)
+        value = partial_sum(index, mine, theirs, own_in, other_in, arrived.get(step - 2))
+        depths = [d for d in range(hops) if 0 <= step - 2 * d < count]
+        if depths:
+            arrived[step] = lax.ppermute(value, ("sp", "tp"), _pairs(peers, depths, 0))
+        if step >= 2 * hops:
+            finals.append(value)
+
+    running = decay_sums(place, lin, rank, mine, theirs, own_small, other_small)
+    sinks = jnp.stack(
+        [
+            lax.dynamic_slice_in_dim(small[rank + 1], far * query_heads, query_heads).reshape(key_heads, groups)
+            for small in (own_small, other_small)
+        ]
+    )
+    sinks = jnp.exp(sinks)
+    attended = []
+    for group in range(key_heads):
+        number = jnp.stack([me, 1 - me])[:, None] * (2 * query_heads) + (
+            far * query_heads + group * groups + jnp.arange(groups, dtype=jnp.int32)
+        )
+        slopes = jnp.exp2(-8.0 * (number + 1).astype(f32) / QH)
+        attended.append(
+            window_heads(place, group, half, slopes, sinks[:, group], finals[0], finals[1 + group])
+        )
+    for head in range(lin):
+        first = 1 + key_heads + 2 * head
+        attended.append(
+            linear_heads(
+                place,
+                lin,
+                head,
+                half,
+                finals[first],
+                finals[first + 1],
+                running,
+                starting_state,
+                other_state,
+                linear_head_gain.reshape(1, DV),
+            )
+        )
+
+    pieces = len(attended)
+    passed = []
+    for step in range(pieces + hops):
+        if step == 0:
+            now = attended[0]
+        elif step < pieces:
+            now = jnp.where(depth == hops, attended[step], back)
+        else:
+            now = back
+        passed.append(now)
+        depths = [d for d in range(hops) if 0 <= step - d < pieces]
+        if depths:
+            back = lax.ppermute(now, ("sp", "tp"), _pairs(peers, depths, 1))
+    terms = output_sum(
+        place, passed[: key_heads + hops], hops, window_output_weight, other_window, None, f32
+    )
+    terms = output_sum(place, passed[key_heads:], hops, linear_output_weight, other_linear, terms, bf16)
+
+    kept, given = terms[: peers * half], swap(terms[peers * half :])
+    result = (kept.astype(f32) + given.astype(f32)).astype(bf16)
+    return lax.all_to_all(result, "sp", 0, 1, tiled=True)
+
+
+def fits(mesh):
+    return mesh.shape["tp"] == 2 and mesh.shape["sp"] > 1
+
+
 def solution(mesh):
     placed = (
         P(("fs", "sp"), "tp"),
@@ -249,5 +829,6 @@
         P("tp", "sp"),
     )
     return jax.shard_map(
-        local, mesh=mesh, in_specs=placed, out_specs=P(("fs", "sp", "tp"), None), check_vma=False
-    )
+        resident if fits(mesh) else local,
+        mesh=mesh, in_specs=placed, out_specs=P(("fs", "sp", "tp"), None), check_vma=False
+    )

time: 923 us -> 213 us (0.23)
  waiting for transfers between devices: 845 us -> 32.7 us
  Pallas kernels: 0 us -> 63.1 us
  matrix products: 41.2 us -> 0 us
  starting transfers between devices: 2.46 us -> 39.6 us
  blocking collectives: 9.38 us -> 39.7 us
  local copies, waits for them, and re-layouts: 2.26 us -> 30.6 us
  between operations: 13.7 us -> 0.61 us
    all_gather x10 -> x0, waiting for transfers between devices: 832 us -> none  [the longest x1 146 us: local(): lax.all_gather(matrices[5], 'sp', axis=0, tiled=True)]
    pallas_call x0 -> x23, Pallas kernels: none -> 63.1 us  [the longest x13 27 us: partial_sum(): _call(partial_kernel, 'partial_sum', jax.ShapeDtypeStruct((2 * rows, 2 *...]
    dot_general x18 -> x0, matrix products: 41.2 us -> none  [the longest x6 19.4 us: local(): jnp.dot(normed, segment, preferred_element_type=jnp.float32)]
    all_to_all x0 -> x2, blocking collectives: none -> 39.7 us  [the longest x1 22.2 us: resident(): incoming = lax.all_to_all(outgoing, 'sp', 0, 0, tiled=True)]
    ppermute x1 -> x25, starting transfers between devices: 2.08 us -> 39.6 us  [the longest x11 26.6 us: resident(): arrived[step] = lax.ppermute(value, ('sp', 'tp'), _pairs(peers, depths, 0))]
    ppermute x1 -> x25, waiting for transfers between devices: 0.01 us -> 32.7 us  [the longest x6 25.1 us: resident(): back = lax.ppermute(now, ('sp', 'tp'), _pairs(peers, depths, 1))]
    unnamed x28 -> x60, local copies, waits for them, and re-layouts: 0.26 us -> 25.8 us
    all_gather x1 -> x0, blocking collectives: 9.38 us -> none  [prefix(): lax.all_gather(part.astype(kind), axis)]
  transfers between devices with their start and end apart: 12 -> 25, of which waited for: 11 -> 9; matrix products, arithmetic and copies ran while one was open for 5% -> 3% of each run, Pallas kernels for 0% -> 24%
where the time goes in v1:
time: 213 us; the launch traced here: 211 us
  Pallas kernels  63.1 us (30%)
  blocking collectives  39.7 us (19%)
  starting transfers between devices  39.6 us (19%)
  waiting for transfers between devices  32.7 us (15%)
  local copies, waits for them, and re-layouts  30.6 us (14%)
  other arithmetic  4.68 us (2%)
    pallas_call x13, Pallas kernels, partial_sum(): _call(partial_kernel, 'partial_sum', jax.ShapeDtypeStruct((2 * rows, 2 *...  27 us
    ppermute x11, starting transfers between devices, resident(): arrived[step] = lax.ppermute(value, ('sp', 'tp'), _pairs(peers, depths, 0))  26.6 us
    unnamed x60, local copies, waits for them, and re-layouts  25.8 us
    ppermute x6, waiting for transfers between devices, resident(): back = lax.ppermute(now, ('sp', 'tp'), _pairs(peers, depths, 1))  25.1 us
    all_to_all x1, blocking collectives, resident(): incoming = lax.all_to_all(outgoing, 'sp', 0, 0, tiled=True)  22.2 us
    all_to_all x1, blocking collectives, resident(): return lax.all_to_all(result, 'sp', 0, 1, tiled=True)  17.5 us
    pallas_call x2, Pallas kernels, pack_items(): _call(functools.partial(pack_kernel, key_heads), 'pack_items', jax.ShapeD...  10.7 us
    ppermute x6, starting transfers between devices, resident(): back = lax.ppermute(now, ('sp', 'tp'), _pairs(peers, depths, 1))  8.13 us
  transfers between devices with their start and end apart: 25, of which 9 were waited for; matrix products, arithmetic and copies ran while one was open for 3% of the time, Pallas kernels for 24%

profile of v1, /device:TPU:0, one launch (start us, length us, event | category | flops | bytes accessed | tf_op | source)
XLA Modules:
  0.0 211.0 jit_solution(13788057717627646160)
XLA Ops:
  1.6 1.2 concatenate.16
  4.1 1.3 copy.37.down_ref
  5.6 1.4 copy-done.18
  8.0 1.5 norm.1
  10.6 5.4 %pack_items.3 = bf16[7,1024,256]{2,1,0:T(8,128)(2,1)} custom-call(s32[1]{0:T(128)} %bitcast.side_ref, bf16[1024,1024]{1,0:T(8,128)(2,1)S(1)} %copy-done.9, bf16[1024,256]{1,0:T(8,128)(2,1)S(1)} %copy-done.14, bf16[1024,256]{1,0:T(8,128)(2,1)S(1)} %copy-done.16, bf16[1024,512]{1,0:T(8,128)(2,1)S(1)} %copy-done.10, bf16[1024,512]{1,0:T(8,128)(2,1)S(1)} %copy-done.12, ...), custom_call_target="tpu_custom_call" | custom-call | flops 1000000000 | bytes 7340032 | tf_op jit(solution)/shard_map/pack_items/pallas_call | solution.py:338
  16.5 22.2 %all_to_all.24 = bf16[4,64,1152]{2,1,0:T(8,128)(2,1)S(1)} all-to-all(bf16[4,64,1152]{2,1,0:T(8,128)(2,1)S(1)} %norm.1), channel_id=1, replica_groups=mesh['sp'=4,'fs'=4,'tp'=2] {'sp'}, dimensions={0} | all-to-all | bytes 1179648 | tf_op jit(solution)/shard_map/all_to_all | solution.py:716
  38.7 1.2 copy-done.11
  39.9 1.2 copy-done.13
  43.2 5.3 %pack_items.2.own_ref = bf16[7,1024,256]{2,1,0:T(8,128)(2,1)} custom-call(s32[1]{0:T(128)} %bitcast.1.side_ref, bf16[1024,1024]{1,0:T(8,128)(2,1)S(1)} %copy-done.9, bf16[1024,256]{1,0:T(8,128)(2,1)S(1)} %copy-done.15, bf16[1024,256]{1,0:T(8,128)(2,1)S(1)} %copy-done.17, bf16[1024,512]{1,0:T(8,128)(2,1)S(1)} %copy-done.11, bf16[1024,512]{1,0:T(8,128)(2,1)S(1)} %copy-done.13, ...), custom_call_target="tpu_custom_call" | custom-call | flops 1000000000 | bytes 7340032 | tf_op jit(solution)/shard_map/pack_items/pallas_call | solution.py:338
  48.6 2.0 copy-done
  50.6 1.8 partial_sum.18
  52.4 2.3 %collective-permute-start.7 = (bf16[512,512]{1,0:T(8,128)(2,1)S(1)}, bf16[512,512]{1,0:T(8,128)(2,1)S(1)}, u32[]{:S(2)}, u32[]{:S(2)}) collective-permute-start(bf16[512,512]{1,0:T(8,128)(2,1)S(1)} %partial_sum.18), channel_id=1, source_target_pairs={{0,8},{25,17},{2,10},{27,19},{4,12},{29,21},{6,14},{31,23}} | collective-permute-start | bytes 1572872 | tf_op jit(solution)/shard_map/ppermute | solution.py:746
  54.8 2.0 copy-done.1
  56.8 1.8 partial_sum.13
  58.6 1.3 collective-permute-start.3
  60.0 1.5 collective-permute-done.7.rest_0_
  61.4 2.0 copy-done.2
  63.5 1.8 partial_sum.19
  65.3 4.4 %collective-permute-start.8 = (bf16[512,512]{1,0:T(8,128)(2,1)S(1)}, bf16[512,512]{1,0:T(8,128)(2,1)S(1)}, u32[]{:S(2)}, u32[]{:S(2)}) collective-permute-start(bf16[512,512]{1,0:T(8,128)(2,1)S(1)} %partial_sum.19), channel_id=1, source_target_pairs={{0,8},{25,17},{8,16},{17,9},{2,10},{27,19},{10,18},{19,11},{4,12},... | collective-permute-start | bytes 1572872 | tf_op jit(solution)/shard_map/ppermute | solution.py:746
  69.7 1.8 partial_sum.14
  71.5 1.9 collective-permute-start.4
  73.7 2.6 %collective-permute-done.8.rest_0_ = bf16[512,512]{1,0:T(8,128)(2,1)S(1)} collective-permute-done((bf16[512,512]{1,0:T(8,128)(2,1)S(1)}, bf16[512,512]{1,0:T(8,128)(2,1)S(1)}, u32[]{:S(2)}, u32[]{:S(2)}) %collective-permute-start.8) | collective-permute-done | bytes 524320 | tf_op jit(solution)/shard_map/ppermute | solution.py:746
  76.3 2.0 copy-done.3
  78.4 1.8 partial_sum.20
  80.2 4.4 %collective-permute-start.9 = (bf16[512,512]{1,0:T(8,128)(2,1)S(1)}, bf16[512,512]{1,0:T(8,128)(2,1)S(1)}, u32[]{:S(2)}, u32[]{:S(2)}) collective-permute-start(bf16[512,512]{1,0:T(8,128)(2,1)S(1)} %partial_sum.20), channel_id=1, source_target_pairs={{0,8},{25,17},{8,16},{17,9},{16,24},{9,1},{2,10},{27,19},{10,18},{... | collective-permute-start | bytes 1572872 | tf_op jit(solution)/shard_map/ppermute | solution.py:746
  84.6 2.6 %partial_sum.15 = bf16[512,512]{1,0:T(8,128)(2,1)} custom-call(s32[1]{0:T(128)} %bitcast.8.index_ref, bf16[256,1152]{1,0:T(8,128)(2,1)S(1)} %bitcast.33, bf16[256,1152]{1,0:T(8,128)(2,1)S(1)} %bitcast.47, bf16[7,1024,256]{2,1,0:T(8,128)(2,1)S(1)} %copy-done.3, bf16[7,1024,256]{2,1,0:T(8,128)(2,1)} %collective-permute-done.2.other_ref, ...), custom_call_target="tpu_custom_call" | custom-call | flops 536870912 | bytes 2097152 | tf_op jit(solution)/shard_map/partial_sum/pallas_call | solution.py:374
  87.3 1.9 collective-permute-start.5
  91.3 2.0 copy-done.4
  93.3 1.8 partial_sum.21.key_value_ref
  95.1 5.2 %collective-permute-start.10 = (bf16[512,512]{1,0:T(8,128)(2,1)S(1)}, bf16[512,512]{1,0:T(8,128)(2,1)}, u32[]{:S(2)}, u32[]{:S(2)}) collective-permute-start(bf16[512,512]{1,0:T(8,128)(2,1)S(1)} %partial_sum.21.key_value_ref), channel_id=1, source_target_pairs={{0,8},{25,17},{8,16},{17,9},{16,24},{9,1},{2,10},{27,19},{10,18},{... | collective-permute-start | bytes 1572872 | tf_op jit(solution)/shard_map/ppermute | solution.py:746
  100.3 1.8 partial_sum.16.query_ref
  102.2 2.9 %window_heads.3.refs_0_ = bf16[512,512]{1,0:T(8,128)(2,1)S(1)} custom-call(s32[3]{0:T(128)S(1)} %pad_add_fusion.place_ref, f32[2,4]{1,0:T(2,128)S(1)} %get-tuple-element.36.slope_ref, f32[2,4]{1,0:T(2,128)S(1)} %bitcast.57, bf16[512,512]{1,0:T(8,128)(2,1)S(1)} %partial_sum.21.key_value_ref, bf16[512,512]{1,0:T(8,128)(2,1)S(1)} %partial_sum.16.query_ref), custom_call_target="tpu_custom_call" | custom-call | flops 2000000000 | bytes 2097152 | tf_op jit(solution)/shard_map/window_heads/pallas_call | solution.py:569
  105.1 1.5 collective-permute-start.14
  106.6 1.5 collective-permute-start.6
  108.1 2.0 copy-done.5
  110.1 2.0 partial_sum.22.query_ref
  112.1 1.5 collective-permute-start.11
  113.6 3.9 %window_heads.2 = bf16[512,512]{1,0:T(8,128)(2,1)S(1)} custom-call(s32[3]{0:T(128)S(1)} %pad_add_fusion.place_ref, f32[2,4]{1,0:T(2,128)S(1)} %get-tuple-element.37.slope_ref, f32[2,4]{1,0:T(2,128)S(1)} %bitcast.56, bf16[512,512]{1,0:T(8,128)(2,1)S(1)} %partial_sum.21.key_value_ref, bf16[512,512]{1,0:T(8,128)(2,1)S(1)} %partial_sum.22.query_ref), custom_call_target="tpu_custom_call" | custom-call | flops 2000000000 | bytes 2097152 | tf_op jit(solution)/shard_map/window_heads/pallas_call | solution.py:569
  118.6 1.5 collective-permute-start.15
  120.1 2.9 %decay_sums.1.running_ref = f32[512,512]{1,0:T(8,128)S(1)} custom-call(s32[3]{0:T(128)S(1)} %pad_add_fusion.place_ref, bf16[256,1152]{1,0:T(8,128)(2,1)S(1)} %bitcast.37, bf16[256,1152]{1,0:T(8,128)(2,1)S(1)} %bitcast.51, f32[24,512]{1,0:T(8,128)S(1)} %maximum_maximum_fusion.own_ref, f32[24,512]{1,0:T(8,128)S(1)} %collective-permute-done.12.other_ref), custom_call_target="tpu_custom_call" | custom-call | flops 1000000000 | bytes 1048576 | tf_op jit(solution)/shard_map/decay_sums/pallas_call | solution.py:431
  123.0 3.1 %partial_sum.17.query_key_ref = bf16[512,512]{1,0:T(8,128)(2,1)} custom-call(s32[1]{0:T(128)} %bitcast.3.index_ref, bf16[256,1152]{1,0:T(8,128)(2,1)S(1)} %bitcast.38, bf16[256,1152]{1,0:T(8,128)(2,1)S(1)} %bitcast.52, bf16[7,1024,256]{2,1,0:T(8,128)(2,1)S(1)} %copy-done.6, bf16[7,1024,256]{2,1,0:T(8,128)(2,1)} %collective-permute-done.2.other_ref, ...), custom_call_target="tpu_custom_call" | custom-call | flops 536870912 | bytes 2097152 | tf_op jit(solution)/shard_map/partial_sum/pallas_call | solution.py:374
  126.1 1.5 collective-permute-start.16
  127.6 2.8 %partial_sum.23.value_ref = bf16[512,512]{1,0:T(8,128)(2,1)} custom-call(s32[1]{0:T(128)} %bitcast.11.index_ref, bf16[256,1152]{1,0:T(8,128)(2,1)S(1)} %bitcast.39, bf16[256,1152]{1,0:T(8,128)(2,1)S(1)} %bitcast.53, bf16[7,1024,256]{2,1,0:T(8,128)(2,1)S(1)} %copy-done.6, bf16[7,1024,256]{2,1,0:T(8,128)(2,1)} %collective-permute-done.2.other_ref, ...), custom_call_target="tpu_custom_call" | custom-call | flops 536870912 | bytes 2097152 | tf_op jit(solution)/shard_map/partial_sum/pallas_call | solution.py:374
  131.1 3.8 %linear_heads.2 = bf16[512,512]{1,0:T(8,128)(2,1)S(1)} custom-call(s32[3]{0:T(128)S(1)} %pad_add_fusion.place_ref, bf16[512,512]{1,0:T(8,128)(2,1)} %partial_sum.17.query_key_ref, bf16[512,512]{1,0:T(8,128)(2,1)} %partial_sum.23.value_ref, f32[512,512]{1,0:T(8,128)S(1)} %decay_sums.1.running_ref, f32[4,128,256]{2,1,0:T(8,128)} %own_ref.1, ...), custom_call_target="tpu_custom_call" | custom-call | flops 2000000000 | bytes 2097152 | tf_op jit(solution)/shard_map/linear_heads/pallas_call | solution.py:484
  134.9 1.1 broadcast_select_fusion.1.refs_2_.refs_0_
  136.0 1.3 collective-permute-start.18
  137.4 2.0 copy-done.7
  139.4 2.0 partial_sum.24.query_key_ref
  141.4 1.9 partial_sum.25.value_ref
  143.3 3.5 %linear_heads.3 = bf16[512,512]{1,0:T(8,128)(2,1)S(1)} custom-call(s32[3]{0:T(128)S(1)} %pad_add_fusion.place_ref, bf16[512,512]{1,0:T(8,128)(2,1)S(1)} %partial_sum.24.query_key_ref, bf16[512,512]{1,0:T(8,128)(2,1)S(1)} %partial_sum.25.value_ref, f32[512,512]{1,0:T(8,128)S(1)} %copy-done.23, f32[4,128,256]{2,1,0:T(8,128)} %own_ref.1, ...), custom_call_target="tpu_custom_call" | custom-call | flops 2000000000 | bytes 2097152 | tf_op jit(solution)/shard_map/linear_heads/pallas_call | solution.py:484
  146.8 5.3 %collective-permute-done.18 = bf16[512,512]{1,0:T(8,128)(2,1)} collective-permute-done((bf16[512,512]{1,0:T(8,128)(2,1)S(1)}, bf16[512,512]{1,0:T(8,128)(2,1)}, u32[]{:S(2)}, u32[]{:S(2)}) %collective-permute-start.18) | collective-permute-done | bytes 524320 | tf_op jit(solution)/shard_map/ppermute | solution.py:796
  153.1 1.3 collective-permute-start.19
  154.5 1.4 constant_dynamic-slice_fusion
  155.9 3.7 %collective-permute-start.23 = (bf16[512,1024]{1,0:T(8,128)(2,1)S(1)}, bf16[512,1024]{1,0:T(8,128)(2,1)S(1)}, u32[]{:S(2)}, u32[]{:S(2)}) collective-permute-start(bf16[512,1024]{1,0:T(8,128)(2,1)S(1)} %constant_dynamic-slice_fusion), channel_id=1, source_target_pairs={{0,1},{1,0},{2,3},{3,2},{4,5},{5,4},{6,7},{7,6},{8,9},{9,8},{10,11... | collective-permute-start | bytes 3145736 | tf_op jit(solution)/shard_map/ppermute | solution.py:668
  159.7 4.6 %collective-permute-done.19.refs_4_.refs_2_ = bf16[512,512]{1,0:T(8,128)(2,1)S(1)} collective-permute-done((bf16[512,512]{1,0:T(8,128)(2,1)S(1)}, bf16[512,512]{1,0:T(8,128)(2,1)S(1)}, u32[]{:S(2)}, u32[]{:S(2)}) %collective-permute-start.19) | collective-permute-done | bytes 524320 | tf_op jit(solution)/shard_map/ppermute | solution.py:796
  164.2 1.3 collective-permute-start.20
  165.6 10.0 %collective-permute-done.20.refs_3_ = bf16[512,512]{1,0:T(8,128)(2,1)S(1)} collective-permute-done((bf16[512,512]{1,0:T(8,128)(2,1)S(1)}, bf16[512,512]{1,0:T(8,128)(2,1)S(1)}, u32[]{:S(2)}, u32[]{:S(2)}) %collective-permute-start.20) | collective-permute-done | bytes 524320 | tf_op jit(solution)/shard_map/ppermute | solution.py:796
  175.6 1.3 collective-permute-start.21
  176.9 3.1 %output_sum.2.refs_7_ = f32[512,1024]{1,0:T(8,128)S(1)} custom-call(s32[3]{0:T(128)S(1)} %pad_add_fusion.place_ref, bf16[512,512]{1,0:T(8,128)(2,1)S(1)} %window_heads.3.refs_0_, bf16[512,512]{1,0:T(8,128)(2,1)S(1)} %broadcast_select_fusion.2.refs_1_, bf16[512,512]{1,0:T(8,128)(2,1)S(1)} %broadcast_select_fusion.1.refs_2_.refs_0_, ...), custom_call_target="tpu_custom_call" | custom-call | flops 1073741824 | bytes 4194304 | tf_op jit(solution)/shard_map/output_sum/pallas_call | solution.py:614
  180.0 1.3 copy-done.8
  181.4 5.3 %collective-permute-done.21.refs_4_ = bf16[512,512]{1,0:T(8,128)(2,1)S(1)} collective-permute-done((bf16[512,512]{1,0:T(8,128)(2,1)S(1)}, bf16[512,512]{1,0:T(8,128)(2,1)S(1)}, u32[]{:S(2)}, u32[]{:S(2)}) %collective-permute-start.21) | collective-permute-done | bytes 524320 | tf_op jit(solution)/shard_map/ppermute | solution.py:796
  186.7 3.8 %output_sum.3 = bf16[512,1024]{1,0:T(8,128)(2,1)S(1)} custom-call(s32[3]{0:T(128)S(1)} %pad_add_fusion.place_ref, bf16[512,512]{1,0:T(8,128)(2,1)S(1)} %broadcast_select_fusion.1.refs_2_.refs_0_, bf16[512,512]{1,0:T(8,128)(2,1)S(1)} %broadcast_select_fusion.refs_3_.refs_1_, bf16[512,512]{1,0:T(8,128)(2,1)S(1)} %collective-permute-done.19.refs_4_.refs_2_, ...), custom_call_target="tpu_custom_call" | custom-call | flops 1073741824 | bytes 4194304 | tf_op jit(solution)/shard_map/output_sum/pallas_call | solution.py:614
  190.6 1.9 collective-permute-done.24
  192.7 17.5 %all_to_all.25 = bf16[4,64,1024]{2,1,0:T(8,128)(2,1)S(1)} all-to-all(bf16[4,64,1024]{2,1,0:T(8,128)(2,1)S(1)} %bitcast.61), channel_id=1, replica_groups=mesh['sp'=4,'fs'=4,'tp'=2] {'sp'}, dimensions={0} | all-to-all | bytes 1048576 | tf_op jit(solution)/shard_map/all_to_all | solution.py:804
  (102 shorter events, 14.3 us)
Async XLA Ops:
  0.0 4.1 %copy-start.25 = (bf16[4096,16]{0,1:T(8,128)(2,1)S(1)}, bf16[4096,16]{0,1:T(8,128)(2,1)}, u32[]{:S(2)}) copy-start(bf16[4096,16]{0,1:T(8,128)(2,1)} %param.25) | copy-start | bytes 393220
  0.0 5.6 %copy-start.20 = (f32[4096]{0:T(1024)S(1)}, f32[4096]{0:T(1024)}, u32[]{:S(2)}) copy-start(f32[4096]{0:T(1024)} %param.18) | copy-start | bytes 49156
  3.6 2.0 collective-permute-start
  4.1 5.4 %copy-start.12 = (bf16[1024,512]{1,0:T(8,128)(2,1)S(1)}, bf16[1024,512]{1,0:T(8,128)(2,1)}, u32[]{:S(2)}) copy-start(bf16[1024,512]{1,0:T(8,128)(2,1)} %lk.1) | copy-start | bytes 3145732
  5.4 4.1 %copy-start.9 = (bf16[1024,1024]{1,0:T(8,128)(2,1)S(1)}, bf16[1024,1024]{1,0:T(8,128)(2,1)}, u32[]{:S(2)}) copy-start(bf16[1024,1024]{1,0:T(8,128)(2,1)} %wq.1) | copy-start | bytes 6291460
  5.4 4.1 %copy-start.10 = (bf16[1024,512]{1,0:T(8,128)(2,1)S(1)}, bf16[1024,512]{1,0:T(8,128)(2,1)}, u32[]{:S(2)}) copy-start(bf16[1024,512]{1,0:T(8,128)(2,1)} %lq.1) | copy-start | bytes 3145732
  5.4 4.1 %copy-start.14 = (bf16[1024,256]{1,0:T(8,128)(2,1)S(1)}, bf16[1024,256]{1,0:T(8,128)(2,1)}, u32[]{:S(2)}) copy-start(bf16[1024,256]{1,0:T(8,128)(2,1)} %wk.1) | copy-start | bytes 1572868
  5.6 1.4 copy-start.18
  7.0 1.0 copy-start.19
  9.5 1.0 copy-start.16
  16.0 32.6 %collective-permute-start.2 = (bf16[7,1024,256]{2,1,0:T(8,128)(2,1)}, bf16[7,1024,256]{2,1,0:T(8,128)(2,1)}, u32[]{:S(2)}, u32[]{:S(2)}) collective-permute-start(bf16[7,1024,256]{2,1,0:T(8,128)(2,1)} %pack_items.3), channel_id=1, source_target_pairs={{0,1},{1,0},{2,3},{3,2},{4,5},{5,4},{6,7},{7,6},{8,9},{9,8},{10,11... | collective-permute-start | bytes 11010056 | tf_op jit(solution)/shard_map/ppermute | solution.py:668
  38.7 9.9 %collective-permute-start.1 = (bf16[4,64,1152]{2,1,0:T(8,128)(2,1)S(1)}, bf16[4,64,1152]{2,1,0:T(8,128)(2,1)S(1)}, u32[]{:S(2)}, u32[]{:S(2)}) collective-permute-start(bf16[4,64,1152]{2,1,0:T(8,128)(2,1)S(1)} %all_to_all.24), channel_id=1, source_target_pairs={{0,1},{1,0},{2,3},{3,2},{4,5},{5,4},{6,7},{7,6},{8,9},{9,8},{10,11... | collective-permute-start | bytes 1769480 | tf_op jit(solution)/shard_map/ppermute | solution.py:668
  38.7 1.2 copy-start.11
  39.9 1.2 copy-start.13
  41.1 1.0 copy-start.15
  42.2 1.0 copy-start.17
  48.6 2.0 copy-start
  52.4 9.0 %collective-permute-start.7 = (bf16[512,512]{1,0:T(8,128)(2,1)S(1)}, bf16[512,512]{1,0:T(8,128)(2,1)S(1)}, u32[]{:S(2)}, u32[]{:S(2)}) collective-permute-start(bf16[512,512]{1,0:T(8,128)(2,1)S(1)} %partial_sum.18), channel_id=1, source_target_pairs={{0,8},{25,17},{2,10},{27,19},{4,12},{29,21},{6,14},{31,23}} | collective-permute-start | bytes 1572872 | tf_op jit(solution)/shard_map/ppermute | solution.py:746
  54.8 2.0 copy-start.1
  58.6 11.1 %collective-permute-start.3 = (bf16[512,512]{1,0:T(8,128)(2,1)S(1)}, bf16[512,512]{1,0:T(8,128)(2,1)S(1)}, u32[]{:S(2)}, u32[]{:S(2)}) collective-permute-start(bf16[512,512]{1,0:T(8,128)(2,1)S(1)} %partial_sum.13), channel_id=1, source_target_pairs={{0,8},{25,17},{2,10},{27,19},{4,12},{29,21},{6,14},{31,23}} | collective-permute-start | bytes 1572872 | tf_op jit(solution)/shard_map/ppermute | solution.py:746
  61.4 2.0 copy-start.2
  65.3 11.1 %collective-permute-start.8 = (bf16[512,512]{1,0:T(8,128)(2,1)S(1)}, bf16[512,512]{1,0:T(8,128)(2,1)S(1)}, u32[]{:S(2)}, u32[]{:S(2)}) collective-permute-start(bf16[512,512]{1,0:T(8,128)(2,1)S(1)} %partial_sum.19), channel_id=1, source_target_pairs={{0,8},{25,17},{8,16},{17,9},{2,10},{27,19},{10,18},{19,11},{4,12},... | collective-permute-start | bytes 1572872 | tf_op jit(solution)/shard_map/ppermute | solution.py:746
  69.7 4.0 %copy-start.28 = (f32[16]{0:T(128)S(1)}, f32[16]{0:T(128)}, u32[]{:S(2)}) copy-start(f32[16]{0:T(128)} %param.30) | copy-start | bytes 196
  69.7 4.0 %copy-start.26 = (bf16[16,512]{1,0:T(8,128)(2,1)S(1)}, bf16[16,512]{1,0:T(8,128)(2,1)}, u32[]{:S(2)}) copy-start(bf16[16,512]{1,0:T(8,128)(2,1)} %param.26) | copy-start | bytes 49156
  71.5 13.1 %collective-permute-start.4 = (bf16[512,512]{1,0:T(8,128)(2,1)S(1)}, bf16[512,512]{1,0:T(8,128)(2,1)S(1)}, u32[]{:S(2)}, u32[]{:S(2)}) collective-permute-start(bf16[512,512]{1,0:T(8,128)(2,1)S(1)} %partial_sum.14), channel_id=1, source_target_pairs={{0,8},{25,17},{8,16},{17,9},{2,10},{27,19},{10,18},{19,11},{4,12},... | collective-permute-start | bytes 1572872 | tf_op jit(solution)/shard_map/ppermute | solution.py:746
  76.3 2.0 copy-start.3
  80.2 11.1 %collective-permute-start.9 = (bf16[512,512]{1,0:T(8,128)(2,1)S(1)}, bf16[512,512]{1,0:T(8,128)(2,1)S(1)}, u32[]{:S(2)}, u32[]{:S(2)}) collective-permute-start(bf16[512,512]{1,0:T(8,128)(2,1)S(1)} %partial_sum.20), channel_id=1, source_target_pairs={{0,8},{25,17},{8,16},{17,9},{16,24},{9,1},{2,10},{27,19},{10,18},{... | collective-permute-start | bytes 1572872 | tf_op jit(solution)/shard_map/ppermute | solution.py:746
  84.6 4.5 %copy-start.27 = (f32[512]{0:T(512)S(1)}, f32[512]{0:T(512)}, u32[]{:S(2)}) copy-start(f32[512]{0:T(512)} %param.27) | copy-start | bytes 6148
  87.3 13.1 %collective-permute-start.5 = (bf16[512,512]{1,0:T(8,128)(2,1)}, bf16[512,512]{1,0:T(8,128)(2,1)S(1)}, u32[]{:S(2)}, u32[]{:S(2)}) collective-permute-start(bf16[512,512]{1,0:T(8,128)(2,1)} %partial_sum.15), channel_id=1, source_target_pairs={{0,8},{25,17},{8,16},{17,9},{16,24},{9,1},{2,10},{27,19},{10,18},{... | collective-permute-start | bytes 1572872 | tf_op jit(solution)/shard_map/ppermute | solution.py:746
  89.3 1.2 collective-permute-start.12
  91.3 2.0 copy-start.4
  95.1 13.0 %collective-permute-start.10 = (bf16[512,512]{1,0:T(8,128)(2,1)S(1)}, bf16[512,512]{1,0:T(8,128)(2,1)}, u32[]{:S(2)}, u32[]{:S(2)}) collective-permute-start(bf16[512,512]{1,0:T(8,128)(2,1)S(1)} %partial_sum.21.key_value_ref), channel_id=1, source_target_pairs={{0,8},{25,17},{8,16},{17,9},{16,24},{9,1},{2,10},{27,19},{10,18},{... | collective-permute-start | bytes 1572872 | tf_op jit(solution)/shard_map/ppermute | solution.py:746
  105.1 12.4 %collective-permute-start.14 = (bf16[512,512]{1,0:T(8,128)(2,1)S(1)}, bf16[512,512]{1,0:T(8,128)(2,1)}, u32[]{:S(2)}, u32[]{:S(2)}) collective-permute-start(bf16[512,512]{1,0:T(8,128)(2,1)S(1)} %window_heads.3.refs_0_), channel_id=1, source_target_pairs={{1,9},{24,16},{3,11},{26,18},{5,13},{28,20},{7,15},{30,22}} | collective-permute-start | bytes 1572872 | tf_op jit(solution)/shard_map/ppermute | solution.py:796
  106.6 24.5 %collective-permute-start.13 = (f32[4,128,256]{2,1,0:T(8,128)}, f32[4,128,256]{2,1,0:T(8,128)}, u32[]{:S(2)}, u32[]{:S(2)}) collective-permute-start(f32[4,128,256]{2,1,0:T(8,128)} %own_ref.1), channel_id=1, source_target_pairs={{0,1},{1,0},{2,3},{3,2},{4,5},{5,4},{6,7},{7,6},{8,9},{9,8},{10,11... | collective-permute-start | bytes 1572872 | tf_op jit(solution)/shard_map/ppermute | solution.py:668
  106.6 16.4 %collective-permute-start.6 = (bf16[512,512]{1,0:T(8,128)(2,1)S(1)}, bf16[512,512]{1,0:T(8,128)(2,1)}, u32[]{:S(2)}, u32[]{:S(2)}) collective-permute-start(bf16[512,512]{1,0:T(8,128)(2,1)S(1)} %partial_sum.16.query_ref), channel_id=1, source_target_pairs={{8,16},{17,9},{16,24},{9,1},{10,18},{19,11},{18,26},{11,3},{12,20}... | collective-permute-start | bytes 1572872 | tf_op jit(solution)/shard_map/ppermute | solution.py:746
  108.1 2.0 copy-start.5
  112.1 15.5 %collective-permute-start.11 = (bf16[512,512]{1,0:T(8,128)(2,1)S(1)}, bf16[512,512]{1,0:T(8,128)(2,1)}, u32[]{:S(2)}, u32[]{:S(2)}) collective-permute-start(bf16[512,512]{1,0:T(8,128)(2,1)S(1)} %partial_sum.22.query_ref), channel_id=1, source_target_pairs={{8,16},{17,9},{16,24},{9,1},{10,18},{19,11},{18,26},{11,3},{12,20}... | collective-permute-start | bytes 1572872 | tf_op jit(solution)/shard_map/ppermute | solution.py:746
  118.6 16.3 %collective-permute-start.15 = (bf16[512,512]{1,0:T(8,128)(2,1)S(1)}, bf16[512,512]{1,0:T(8,128)(2,1)}, u32[]{:S(2)}, u32[]{:S(2)}) collective-permute-start(bf16[512,512]{1,0:T(8,128)(2,1)S(1)} %broadcast_select_fusion.2.refs_1_), channel_id=1, source_target_pairs={{1,9},{24,16},{9,17},{16,8},{3,11},{26,18},{11,19},{18,10},{5,13},... | collective-permute-start | bytes 1572872 | tf_op jit(solution)/shard_map/ppermute | solution.py:796
  120.1 2.9 %copy-start.6 = (bf16[7,1024,256]{2,1,0:T(8,128)(2,1)S(1)}, bf16[7,1024,256]{2,1,0:T(8,128)(2,1)}, u32[]{:S(2)}) copy-start(bf16[7,1024,256]{2,1,0:T(8,128)(2,1)} %pack_items.2.own_ref) | copy-start | bytes 11010052
  123.0 8.1 %copy-start.22 = (f32[512,512]{1,0:T(8,128)}, f32[512,512]{1,0:T(8,128)S(1)}, u32[]{:S(2)}) copy-start(f32[512,512]{1,0:T(8,128)S(1)} %decay_sums.1.running_ref) | copy-start | bytes 3145732
  126.1 11.2 %collective-permute-start.16 = (bf16[512,512]{1,0:T(8,128)(2,1)}, bf16[512,512]{1,0:T(8,128)(2,1)}, u32[]{:S(2)}, u32[]{:S(2)}) collective-permute-start(bf16[512,512]{1,0:T(8,128)(2,1)} %partial_sum.17.query_key_ref), channel_id=1, source_target_pairs={{16,24},{9,1},{18,26},{11,3},{20,28},{13,5},{22,30},{15,7}} | collective-permute-start | bytes 1572872 | tf_op jit(solution)/shard_map/ppermute | solution.py:746
  127.6 3.5 %copy-start.21 = (f32[256]{0:T(256)S(1)}, f32[256]{0:T(256)}, u32[]{:S(2)}) copy-start(f32[256]{0:T(256)} %param.31) | copy-start | bytes 3076
  130.4 11.0 %collective-permute-start.17 = (bf16[512,512]{1,0:T(8,128)(2,1)}, bf16[512,512]{1,0:T(8,128)(2,1)S(1)}, u32[]{:S(2)}, u32[]{:S(2)}) collective-permute-start(bf16[512,512]{1,0:T(8,128)(2,1)} %partial_sum.23.value_ref), channel_id=1, source_target_pairs={{16,24},{9,1},{18,26},{11,3},{20,28},{13,5},{22,30},{15,7}} | collective-permute-start | bytes 1572872 | tf_op jit(solution)/shard_map/ppermute | solution.py:746
  136.0 16.0 %collective-permute-start.18 = (bf16[512,512]{1,0:T(8,128)(2,1)S(1)}, bf16[512,512]{1,0:T(8,128)(2,1)}, u32[]{:S(2)}, u32[]{:S(2)}) collective-permute-start(bf16[512,512]{1,0:T(8,128)(2,1)S(1)} %broadcast_select_fusion.1.refs_2_.refs_0_), channel_id=1, source_target_pairs={{1,9},{24,16},{9,17},{16,8},{17,25},{8,0},{3,11},{26,18},{11,19},{... | collective-permute-start | bytes 1572872 | tf_op jit(solution)/shard_map/ppermute | solution.py:796
  137.3 2.0 copy-start.7
  141.4 1.9 copy-start.23
  153.1 11.1 %collective-permute-start.19 = (bf16[512,512]{1,0:T(8,128)(2,1)S(1)}, bf16[512,512]{1,0:T(8,128)(2,1)S(1)}, u32[]{:S(2)}, u32[]{:S(2)}) collective-permute-start(bf16[512,512]{1,0:T(8,128)(2,1)S(1)} %broadcast_select_fusion.refs_3_.refs_1_), channel_id=1, source_target_pairs={{1,9},{24,16},{9,17},{16,8},{17,25},{8,0},{3,11},{26,18},{11,19},{... | collective-permute-start | bytes 1572872 | tf_op jit(solution)/shard_map/ppermute | solution.py:796
  154.4 5.1 %copy-start.24 = (bf16[1024,1024]{1,0:T(8,128)(2,1)S(1)}, bf16[1024,1024]{1,0:T(8,128)(2,1)}, u32[]{:S(2)}) copy-start(bf16[1024,1024]{1,0:T(8,128)(2,1)} %refs_5_.1) | copy-start | bytes 6291460
  155.9 21.0 %collective-permute-start.23 = (bf16[512,1024]{1,0:T(8,128)(2,1)S(1)}, bf16[512,1024]{1,0:T(8,128)(2,1)S(1)}, u32[]{:S(2)}, u32[]{:S(2)}) collective-permute-start(bf16[512,1024]{1,0:T(8,128)(2,1)S(1)} %constant_dynamic-slice_fusion), channel_id=1, source_target_pairs={{0,1},{1,0},{2,3},{3,2},{4,5},{5,4},{6,7},{7,6},{8,9},{9,8},{10,11... | collective-permute-start | bytes 3145736 | tf_op jit(solution)/shard_map/ppermute | solution.py:668
  164.2 11.4 %collective-permute-start.20 = (bf16[512,512]{1,0:T(8,128)(2,1)S(1)}, bf16[512,512]{1,0:T(8,128)(2,1)S(1)}, u32[]{:S(2)}, u32[]{:S(2)}) collective-permute-start(bf16[512,512]{1,0:T(8,128)(2,1)S(1)} %collective-permute-done.19.refs_4_.refs_2_), channel_id=1, source_target_pairs={{9,17},{16,8},{17,25},{8,0},{11,19},{18,10},{19,27},{10,2},{13,21}... | collective-permute-start | bytes 1572872 | tf_op jit(solution)/shard_map/ppermute | solution.py:796
  165.5 15.9 %collective-permute-start.22 = (bf16[512,1024]{1,0:T(8,128)(2,1)S(1)}, bf16[512,1024]{1,0:T(8,128)(2,1)S(1)}, u32[]{:S(2)}, u32[]{:S(2)}) collective-permute-start(bf16[512,1024]{1,0:T(8,128)(2,1)S(1)} %constant_dynamic-slice_fusion.1), channel_id=1, source_target_pairs={{0,1},{1,0},{2,3},{3,2},{4,5},{5,4},{6,7},{7,6},{8,9},{9,8},{10,11... | collective-permute-start | bytes 3145736 | tf_op jit(solution)/shard_map/ppermute | solution.py:668
  175.6 11.1 %collective-permute-start.21 = (bf16[512,512]{1,0:T(8,128)(2,1)S(1)}, bf16[512,512]{1,0:T(8,128)(2,1)S(1)}, u32[]{:S(2)}, u32[]{:S(2)}) collective-permute-start(bf16[512,512]{1,0:T(8,128)(2,1)S(1)} %collective-permute-done.20.refs_3_), channel_id=1, source_target_pairs={{17,25},{8,0},{19,27},{10,2},{21,29},{12,4},{23,31},{14,6}} | collective-permute-start | bytes 1572872 | tf_op jit(solution)/shard_map/ppermute | solution.py:796
  180.0 1.3 copy-start.8
  190.5 2.0 collective-permute-start.24

commit v2 on v1

--- a/solution.py
+++ b/solution.py
@@ -6,6 +6,7 @@
 from jax.experimental import pallas as pl
 from jax.experimental.pallas import tpu as pltpu
 from jax.sharding import PartitionSpec as P
+
 
 QH = 32
 HD = 64
@@ -248,13 +249,12 @@
 BY_ROWS = (((0,), (0,)), ((), ()))
 
 
-def _call(kernel, name, out_shape, flops, moved, **kw):
+def _call(kernel, out_shape, flops, moved, **kw):
     return pl.pallas_call(
         kernel,
         out_shape=out_shape,
-        compiler_params=pltpu.CompilerParams(vmem_limit_bytes=48 * 1024 * 1024),
+        compiler_params=pltpu.CompilerParams(vmem_limit_bytes=58 * 1024 * 1024),
         cost_estimate=pl.CostEstimate(flops=flops, bytes_accessed=moved, transcendentals=0),
-        name=name,
         **kw,
     )
 
@@ -265,9 +265,10 @@
     )
 
 
-def norm_kernel(place_ref, x_ref, fade_ref, mate_ref, gain_ref, down_ref, out_ref):
-    me = place_ref[0]
-    pieces, rows, wide = out_ref.shape
+def norm_kernel(place_ref, x_ref, fade_ref, mate_ref, gain_ref, down_ref, *out_refs):
+    me, line = place_ref[0], place_ref[3]
+    pieces = len(out_refs)
+    rows, wide = out_refs[0].shape
     half_model = x_ref.shape[1]
     cut = 2 * half_model // pieces
     fades = fade_ref.shape[1]
@@ -282,7 +283,13 @@
         part = jnp.dot(normed, down_ref[pl.ds(start, half_model), :], preferred_element_type=jnp.float32)
         low_rank = part if low_rank is None else low_rank + part
         for k in range(pieces // 2):
-            out_ref[side * (pieces // 2) + k, :, :cut] = normed[:, k * cut : (k + 1) * cut]
+            away = lax.rem(side * (pieces // 2) + k - line + pieces, pieces)
+            for offset, out_ref in enumerate(out_refs):
+
+                @pl.when(away == offset)
+                def _():
+                    out_ref[:, :cut] = normed[:, k * cut : (k + 1) * cut]
+
     mine = fade_ref[pl.ds(pl.multiple_of(me * rows, rows), rows), :]
     theirs = mate_ref[:, half_model : half_model + fades]
     tail = jnp.concatenate(
@@ -294,8 +301,74 @@
         ],
         axis=1,
     ).astype(jnp.bfloat16)
-    for k in range(pieces):
-        out_ref[k, :, cut:] = tail
+    for out_ref in out_refs:
+        out_ref[:, cut:] = tail
+
+
+def collect_kernel(place_ref, *refs):
+    pieces = len(refs) - 1
+    for offset in range(pieces):
+        refs[-1][lax.rem(place_ref[3] - offset + pieces, pieces)] = refs[offset][...]
+
+
+def collect(place, parts):
+    rows, wide = parts[0].shape
+    return _call(
+        collect_kernel,
+        jax.ShapeDtypeStruct((len(parts), rows, wide), parts[0].dtype),
+        10**8,
+        2**21,
+        in_specs=[SMEM] + [VMEM] * len(parts),
+        out_specs=VMEM,
+    )(place, *parts)
+
+
+def join_kernel(place_ref, kept_ref, given_ref, *out_refs):
+    pieces = len(out_refs)
+    rows = out_refs[0].shape[0]
+    for offset, out_ref in enumerate(out_refs):
+        at = pl.ds(pl.multiple_of(lax.rem(place_ref[3] + offset, pieces) * rows, rows), rows)
+        out_ref[...] = (kept_ref[at].astype(jnp.float32) + given_ref[at].astype(jnp.float32)).astype(out_ref.dtype)
+
+
+def join(place, kept, given, pieces):
+    rows, columns = kept.shape
+    return _call(
+        join_kernel,
+        [jax.ShapeDtypeStruct((rows // pieces, columns), kept.dtype)] * pieces,
+        10**8,
+        2**21,
+        in_specs=[SMEM, VMEM, VMEM],
+        out_specs=[VMEM] * pieces,
+    )(place, kept, given)
+
+
+def spread_kernel(place_ref, *refs):
+    pieces = len(refs) - 1
+    columns = refs[0].shape[1]
+    for offset in range(pieces):
+        start = lax.rem(place_ref[3] - offset + pieces, pieces) * columns
+        refs[-1][:, pl.ds(pl.multiple_of(start, columns), columns)] = refs[offset][...]
+
+
+def spread(place, parts):
+    rows, columns = parts[0].shape
+    return _call(
+        spread_kernel,
+        jax.ShapeDtypeStruct((rows, len(parts) * columns), parts[0].dtype),
+        10**8,
+        2**21,
+        in_specs=[SMEM] + [VMEM] * len(parts),
+        out_specs=VMEM,
+    )(place, *parts)
+
+
+def to_offsets(parts):
+    peers = len(parts)
+    out = [parts[0]]
+    for k in range(1, peers):
+        out.append(lax.ppermute(parts[k], "sp", [(i, (i + k) % peers) for i in range(peers)]))
+    return out
 
 
 def pack_kernel(key_heads, side_ref, wq, wk, wv, lq, lk, lv, out_ref):
@@ -337,7 +410,6 @@
     narrow, full = pl.BlockSpec((depth, width // 2), head), pl.BlockSpec((depth, width), head)
     return _call(
         functools.partial(pack_kernel, key_heads),
-        "pack_items",
         jax.ShapeDtypeStruct((count, depth, width), jnp.bfloat16),
         10**9,
         4 * count * depth * width,
@@ -373,7 +445,6 @@
     block = pl.BlockSpec((1, depth, width), lambda i, index: (index[0], 0, 0))
     return _call(
         partial_kernel,
-        "partial_sum",
         jax.ShapeDtypeStruct((2 * rows, 2 * width), jnp.bfloat16),
         8 * rows * depth * width,
         4 * depth * (rows + width),
@@ -387,7 +458,6 @@
     me, side = place_ref[0], place_ref[1]
     rows = mine_ref.shape[0]
     features = LOOKUP_FEATURES
-    all_heads = 4 * lin
     lower = (
         lax.broadcasted_iota(jnp.int32, (SPAN, SPAN), 0) >= lax.broadcasted_iota(jnp.int32, (SPAN, SPAN), 1)
     ).astype(jnp.bfloat16)
@@ -430,7 +500,6 @@
     out = (2 * rows, 2 * lin * LOOKUP_FEATURES)
     return _call(
         functools.partial(decay_kernel, lin, rank),
-        "decay_sums",
         jax.ShapeDtypeStruct(out, jnp.float32),
         10**9,
         2**20,
@@ -483,7 +552,6 @@
     block = pl.BlockSpec((rows, 2 * LOOKUP_FEATURES), lambda i, place: (0, head))
     return _call(
         functools.partial(linear_kernel, lin, head, half),
-        "linear_heads",
         jax.ShapeDtypeStruct((rows, width), jnp.bfloat16),
         2 * 10**9,
         2**21,
@@ -568,7 +636,6 @@
 def window_heads(place, group, half, slopes, sinks, key_value, query):
     return _call(
         functools.partial(window_kernel, group, half),
-        "window_heads",
         jax.ShapeDtypeStruct(query.shape, jnp.bfloat16),
         2 * 10**9,
         2**21,
@@ -577,44 +644,56 @@
     )(place, slopes, sinks, key_value, query)
 
 
-def output_kernel(pieces, hops, place_ref, *refs):
-    passed = refs[: pieces + hops]
-    own_ref, other_ref = refs[pieces + hops : pieces + hops + 2]
-    before = refs[pieces + hops + 2 : -3]
-    out_ref, held, arrival = refs[-3:]
+def output_kernel(sources, place_ref, *refs):
+    count = 1 + max(max(row) for row in sources)
+    pieces = len(sources)
+    passed = refs[:count]
+    own_ref, other_ref = refs[count : count + 2]
+    held, arrival = refs[-2:]
+    rest = refs[count + 2 : -2]
+    split = rest[-1].shape[0] != held.shape[1]
+    outs = rest[-2:] if split else rest[-1:]
+    before = rest[: len(rest) - len(outs)]
     depth = place_ref[2]
-    for at in range(hops + 1):
+    for at in range(len(sources[0])):
 
         @pl.when(depth == at)
         def _():
             for piece in range(pieces):
-                pltpu.make_async_copy(passed[piece + at], held.at[piece], arrival.at[piece]).start()
+                pltpu.make_async_copy(passed[sources[piece][at]], held.at[piece], arrival.at[piece]).start()
 
     for piece in range(pieces):
-        pltpu.make_async_copy(passed[piece], held.at[piece], arrival.at[piece]).wait()
+        pltpu.make_async_copy(passed[0], held.at[piece], arrival.at[piece]).wait()
     width = held.shape[2] // 2
-    rows = held.shape[1]
-    columns = out_ref.shape[1]
-    block = columns // 4
-    for part in range(4):
-        span = slice(part * block, (part + 1) * block)
-        total = before[0][:, span] if before else jnp.zeros((rows, block), jnp.float32)
-        for piece in range(pieces):
-            lines = slice(piece * width, (piece + 1) * width)
-            total = total + jnp.dot(held[piece, :, :width], own_ref[lines, span], preferred_element_type=jnp.float32)
-            total = total + jnp.dot(held[piece, :, width:], other_ref[lines, span], preferred_element_type=jnp.float32)
-        out_ref[:, span] = total.astype(out_ref.dtype)
-
-
-def output_sum(place, passed, hops, own, other, before, kind):
+    rows = outs[0].shape[0]
+    columns = outs[0].shape[1]
+    block = columns // 2
+    for top, out_ref in enumerate(outs):
+        at = slice(top * rows, (top + 1) * rows)
+        for part in range(2):
+            span = slice(part * block, (part + 1) * block)
+            total = before[0][at, span] if before else jnp.zeros((rows, block), jnp.float32)
+            for piece in range(pieces):
+                lines = slice(piece * width, (piece + 1) * width)
+                total = total + jnp.dot(
+                    held[piece, at, :width], own_ref[lines, span], preferred_element_type=jnp.float32
+                )
+                total = total + jnp.dot(
+                    held[piece, at, width:], other_ref[lines, span], preferred_element_type=jnp.float32
+                )
+            out_ref[:, span] = total.astype(out_ref.dtype)
+
+
+def output_sum(place, passed, sources, own, other, before, split):
     rows, width = passed[0].shape
-    pieces = len(passed) - hops
+    pieces = len(sources)
     lines, columns = other.shape
+    kind, parts = (jnp.bfloat16, 2) if split else (jnp.float32, 1)
     whole = pl.BlockSpec((rows, columns), lambda i, place: (0, 0))
+    out = pl.BlockSpec((rows // parts, columns), lambda i, place: (0, 0))
     return _call(
-        functools.partial(output_kernel, pieces, hops),
-        "output_sum",
-        jax.ShapeDtypeStruct((rows, columns), kind),
+        functools.partial(output_kernel, sources),
+        [jax.ShapeDtypeStruct((rows // parts, columns), kind)] * parts,
         4 * rows * columns * lines,
         8 * rows * columns,
         grid_spec=_prefetch(
@@ -626,7 +705,7 @@
                 pl.BlockSpec((lines, columns), lambda i, place: (0, 0)),
             ]
             + ([] if before is None else [whole]),
-            whole,
+            [out] * parts,
             [pltpu.VMEM((pieces, rows, width), jnp.bfloat16), pltpu.SemaphoreType.DMA((pieces,))],
         ),
     )(place, *passed, own, other, *([] if before is None else [before]))
@@ -656,7 +735,7 @@
     line, me = lax.axis_index("sp"), lax.axis_index("tp")
     depth = jnp.where(me == 0, line, hops - line)
     far, near = 1 - me, me
-    place = jnp.stack([me, far, hops - depth]).astype(jnp.int32)
+    place = jnp.stack([me, far, hops - depth, line]).astype(jnp.int32)
     rows, half_model = activations.shape
     half = rows // 2
     bf16, f32 = jnp.bfloat16, jnp.float32
@@ -677,12 +756,11 @@
     wide = 2 * half_model // peers + LOOKUP_FEATURES
     outgoing = _call(
         norm_kernel,
-        "norm",
-        jax.ShapeDtypeStruct((peers, half, wide), bf16),
+        [jax.ShapeDtypeStruct((half, wide), bf16)] * peers,
         10**9,
         2**21,
         in_specs=[SMEM] + [VMEM] * 5,
-        out_specs=VMEM,
+        out_specs=[VMEM] * peers,
     )(place, activations, fade, mate, input_norm_gain.reshape(1, -1), decay_down_factor)
 
     (
@@ -713,8 +791,9 @@
             head_sink_logit,
         )
     )
-    incoming = lax.all_to_all(outgoing, "sp", 0, 0, tiled=True)
-    other_in = swap(pack_items(near.reshape(1), lin, key_heads, matrices))
+    incoming = to_offsets(outgoing)
+    packed = pack_items(near.reshape(1), lin, key_heads, matrices)
+    other_in = swap(packed)
     own_in = pack_items(far.reshape(1), lin, key_heads, matrices)
     features = decay_up_factor.shape[1]
     own_small = jnp.concatenate(
@@ -733,6 +812,7 @@
     lines = window_output_weight.shape[0] // 2
     other_window = swap(lax.dynamic_slice_in_dim(window_output_weight, near * lines, lines, axis=0))
 
+    incoming = collect(place, incoming)
     mine = incoming.reshape(peers * half, wide)
     theirs = swap(incoming).reshape(peers * half, wide)
 
@@ -782,26 +862,27 @@
         )
 
     pieces = len(attended)
-    passed = []
-    for step in range(pieces + hops):
-        if step == 0:
-            now = attended[0]
-        elif step < pieces:
-            now = jnp.where(depth == hops, attended[step], back)
-        else:
-            now = back
-        passed.append(now)
-        depths = [d for d in range(hops) if 0 <= step - d < pieces]
-        if depths:
-            back = lax.ppermute(now, ("sp", "tp"), _pairs(peers, depths, 1))
-    terms = output_sum(
-        place, passed[: key_heads + hops], hops, window_output_weight, other_window, None, f32
-    )
-    terms = output_sum(place, passed[key_heads:], hops, linear_output_weight, other_linear, terms, bf16)
-
-    kept, given = terms[: peers * half], swap(terms[peers * half :])
-    result = (kept.astype(f32) + given.astype(f32)).astype(bf16)
-    return lax.all_to_all(result, "sp", 0, 1, tiled=True)
+    held = []
+    for piece in range(pieces):
+        seen = [attended[piece]]
+        for hop in range(hops):
+            if piece < pieces - 1:
+                seen.append(lax.ppermute(seen[-1], ("sp", "tp"), _pairs(peers, [hop], 1)))
+            else:
+                last = hops - hop
+                straight = [(hops * 2, (hops - last) * 2), (1, last * 2 + 1)]
+                seen.insert(1, lax.ppermute(seen[0], ("sp", "tp"), straight))
+        held.append(seen)
+    table = lambda count: tuple(tuple(range(k * peers, (k + 1) * peers)) for k in range(count))
+    flat = lambda lists: [value for seen in lists for value in seen]
+    (terms,) = output_sum(
+        place, flat(held[:key_heads]), table(key_heads), window_output_weight, other_window, None, False
+    )
+    kept, given = output_sum(
+        place, flat(held[key_heads:]), table(lin), linear_output_weight, other_linear, terms, True
+    )
+
+    return spread(place, to_offsets(join(place, kept, swap(given), peers)))
 
 
 def fits(mesh):
@@ -828,7 +909,9 @@
         P("tp", "sp"),
         P("tp", "sp"),
     )
-    return jax.shard_map(
-        resident if fits(mesh) else local,
-        mesh=mesh, in_specs=placed, out_specs=P(("fs", "sp", "tp"), None), check_vma=False
-    )
+    if not fits(mesh):
+        return jax.shard_map(
+            local, mesh=mesh, in_specs=placed, out_specs=P(("fs", "sp", "tp"), None), check_vma=False
+        )
+
+    return jax.shard_map(resident, mesh=mesh, in_specs=placed, out_specs=P(("fs", "sp", "tp"), None), check_vma=False)

time: 213 us -> 234 us (1.099)
  blocking collectives: 39.7 us -> 0 us
  Pallas kernels: 63.1 us -> 100 us
  starting transfers between devices: 39.6 us -> 62.6 us
  waiting for transfers between devices: 32.7 us -> 48.6 us
  local copies, waits for them, and re-layouts: 30.6 us -> 18 us
    all_to_all x2 -> x0, blocking collectives: 39.7 us -> none  [the longest x1 22.2 us: resident(): incoming = lax.all_to_all(outgoing, 'sp', 0, 0, tiled=True)]
    pallas_call x23 -> x26, Pallas kernels: 63.1 us -> 100 us  [the longest x13 41.3 us: partial_sum(): _call(partial_kernel, jax.ShapeDtypeStruct((2 * rows, 2 * width), jnp.bfl...]
    ppermute x6 -> x18, starting transfers between devices: 8.13 us -> 26.1 us  [the longest x9 12.6 us: resident(): seen.append(lax.ppermute(seen[-1], ('sp', 'tp'), _pairs(peers, [hop], 1)))]
    ppermute x6 -> x18, waiting for transfers between devices: 25.1 us -> 37.2 us  [the longest x3 19.1 us: resident(): seen.insert(1, lax.ppermute(seen[0], ('sp', 'tp'), straight))]
    unnamed x60 -> x72, local copies, waits for them, and re-layouts: 25.8 us -> 14.5 us
    ppermute x8, starting transfers between devices: 4.81 us -> 8.49 us  [resident(): swap = lambda value: lax.ppermute(value, 'tp', SWAP)]
    ppermute x11, waiting for transfers between devices: 4.63 us -> 8.18 us  [resident(): arrived[step] = lax.ppermute(value, ('sp', 'tp'), _pairs(peers, depths, 0))]
    select_n x3 -> x0, other arithmetic: 3.33 us -> none  [resident(): now = jnp.where(depth == hops, attended[step], back)]
  transfers between devices with their start and end apart: 25 -> 37, of which waited for: 9 -> 11; matrix products, arithmetic and copies ran while one was open for 3% -> 2% of each run, Pallas kernels for 24% -> 33%
where the time goes in v2:
time: 234 us; the launch traced here: 233 us
  Pallas kernels  100 us (43%)
  starting transfers between devices  62.6 us (27%)
  waiting for transfers between devices  48.6 us (21%)
  local copies, waits for them, and re-layouts  18 us (8%)
  other arithmetic  2.8 us (1%)
    pallas_call x13, Pallas kernels, partial_sum(): _call(partial_kernel, jax.ShapeDtypeStruct((2 * rows, 2 * width), jnp.bfl...  41.3 us
    ppermute x11, starting transfers between devices, resident(): arrived[step] = lax.ppermute(value, ('sp', 'tp'), _pairs(peers, depths, 0))  28 us
    ppermute x3, waiting for transfers between devices, resident(): seen.insert(1, lax.ppermute(seen[0], ('sp', 'tp'), straight))  19.1 us
    ppermute x6, waiting for transfers between devices, to_offsets(): lax.ppermute(parts[k], 'sp', [(i, (i + k) % peers) for i in range(peers)])  17.9 us
    unnamed x72, local copies, waits for them, and re-layouts  14.5 us
    pallas_call x2, Pallas kernels, pack_items(): _call(functools.partial(pack_kernel, key_heads), jax.ShapeDtypeStruct((co...  13 us
    ppermute x9, starting transfers between devices, resident(): seen.append(lax.ppermute(seen[-1], ('sp', 'tp'), _pairs(peers, [hop], 1)))  12.6 us
    pallas_call x2, Pallas kernels, output_sum(): _call(functools.partial(output_kernel, sources), [jax.ShapeDtypeStruct((r...  12.2 us
  transfers between devices with their start and end apart: 37, of which 11 were waited for; matrix products, arithmetic and copies ran while one was open for 2% of the time, Pallas kernels for 33%

profile of v2, /device:TPU:0, one launch (start us, length us, event | category | flops | bytes accessed | tf_op | source)
XLA Modules:
  0.0 232.6 jit_solution(11751488435625625633)
XLA Ops:
  1.7 1.2 concatenate.16
  3.4 1.3 copy.34.down_ref
  6.7 3.1 %shard_map.163 = (bf16[64,1152]{1,0:T(8,128)(2,1)}, bf16[64,1152]{1,0:T(8,128)(2,1)}, bf16[64,1152]{1,0:T(8,128)(2,1)}, bf16[64,1152]{1,0:T(8,128)(2,1)}) custom-call(s32[4]{0:T(128)} %pad_add_fusion.place_ref, bf16[128,2048]{1,0:T(8,128)(2,1)} %x_ref.1, bf16[128,12]{1,0:T(8,128)(2,1)} %pad_maximum_fusion.fade_ref, bf16[64,2176]{1,0:T(8,128)(2,1)} %copy-done.31, ...), custom_call_target="tpu_custom_call" | custom-call | flops 1000000000 | bytes 2097152 | tf_op jit(solution)/shard_map/pallas_call | solution.py:757
  9.8 6.5 %shard_map.166 = bf16[7,1024,256]{2,1,0:T(8,128)(2,1)} custom-call(s32[1]{0:T(128)} %bitcast.side_ref, bf16[1024,1024]{1,0:T(8,128)(2,1)} %wq.1, bf16[1024,256]{1,0:T(8,128)(2,1)} %wk.1, bf16[1024,256]{1,0:T(8,128)(2,1)} %wv.1, bf16[1024,512]{1,0:T(8,128)(2,1)} %lq.1, bf16[1024,512]{1,0:T(8,128)(2,1)} %lk.1, bf16[1024,1024]{1,0:T(8,128)(2,1)} %lv.1), custom_call_target="tpu_custom_call" | custom-call | flops 1000000000 | bytes 7340032 | tf_op jit(solution)/shard_map/pallas_call | solution.py:411
  16.4 3.0 %collective-permute-start.1 = (bf16[64,1152]{1,0:T(8,128)(2,1)S(1)}, bf16[64,1152]{1,0:T(8,128)(2,1)S(1)}, u32[]{:S(2)}, u32[]{:S(2)}) collective-permute-start(bf16[64,1152]{1,0:T(8,128)(2,1)S(1)} %copy-done.34), channel_id=1, source_target_pairs={{0,8},{8,16},{16,24},{24,0},{1,9},{9,17},{17,25},{25,1},{2,10},{10... | collective-permute-start | bytes 442376 | tf_op jit(solution)/shard_map/ppermute | solution.py:370
  19.4 2.6 %collective-permute-start.2 = (bf16[64,1152]{1,0:T(8,128)(2,1)S(1)}, bf16[64,1152]{1,0:T(8,128)(2,1)S(1)}, u32[]{:S(2)}, u32[]{:S(2)}) collective-permute-start(bf16[64,1152]{1,0:T(8,128)(2,1)S(1)} %copy-done.33), channel_id=1, source_target_pairs={{0,16},{8,24},{16,0},{24,8},{1,17},{9,25},{17,1},{25,9},{2,18},{10... | collective-permute-start | bytes 442376 | tf_op jit(solution)/shard_map/ppermute | solution.py:370
  22.0 1.3 collective-permute-start.3
  23.4 2.9 %collective-permute-done.1.refs_1_ = bf16[64,1152]{1,0:T(8,128)(2,1)S(1)} collective-permute-done((bf16[64,1152]{1,0:T(8,128)(2,1)S(1)}, bf16[64,1152]{1,0:T(8,128)(2,1)S(1)}, u32[]{:S(2)}, u32[]{:S(2)}) %collective-permute-start.1) | collective-permute-done | bytes 147488 | tf_op jit(solution)/shard_map/ppermute | solution.py:370
  26.2 5.7 %collective-permute-done.2.refs_2_ = bf16[64,1152]{1,0:T(8,128)(2,1)S(1)} collective-permute-done((bf16[64,1152]{1,0:T(8,128)(2,1)S(1)}, bf16[64,1152]{1,0:T(8,128)(2,1)S(1)}, u32[]{:S(2)}, u32[]{:S(2)}) %collective-permute-start.2) | collective-permute-done | bytes 147488 | tf_op jit(solution)/shard_map/ppermute | solution.py:370
  33.3 2.0 shard_map.164
  35.3 6.5 %shard_map.165.own_ref = bf16[7,1024,256]{2,1,0:T(8,128)(2,1)} custom-call(s32[1]{0:T(128)} %bitcast.1.side_ref, bf16[1024,1024]{1,0:T(8,128)(2,1)} %wq.1, bf16[1024,256]{1,0:T(8,128)(2,1)} %wk.1, bf16[1024,256]{1,0:T(8,128)(2,1)} %wv.1, bf16[1024,512]{1,0:T(8,128)(2,1)} %lq.1, bf16[1024,512]{1,0:T(8,128)(2,1)} %lk.1, bf16[1024,1024]{1,0:T(8,128)(2,1)} %lv.1), custom_call_target="tpu_custom_call" | custom-call | flops 1000000000 | bytes 7340032 | tf_op jit(solution)/shard_map/pallas_call | solution.py:411
  42.6 3.0 %shard_map.167 = bf16[512,512]{1,0:T(8,128)(2,1)} custom-call(s32[1]{0:T(128)} %bitcast.11.index_ref, bf16[256,1152]{1,0:T(8,128)(2,1)} %bitcast.25, bf16[256,1152]{1,0:T(8,128)(2,1)} %bitcast.39, bf16[7,1024,256]{2,1,0:T(8,128)(2,1)} %shard_map.165.own_ref, bf16[7,1024,256]{2,1,0:T(8,128)(2,1)} %collective-permute-done.5.other_ref), custom_call_target="tpu_custom_call" | custom-call | flops 536870912 | bytes 2097152 | tf_op jit(solution)/shard_map/pallas_call | solution.py:446
  45.6 4.9 %collective-permute-start.6 = (bf16[512,512]{1,0:T(8,128)(2,1)}, bf16[512,512]{1,0:T(8,128)(2,1)S(1)}, u32[]{:S(2)}, u32[]{:S(2)}) collective-permute-start(bf16[512,512]{1,0:T(8,128)(2,1)} %shard_map.167), channel_id=1, source_target_pairs={{0,8},{25,17},{2,10},{27,19},{4,12},{29,21},{6,14},{31,23}} | collective-permute-start | bytes 1572872 | tf_op jit(solution)/shard_map/ppermute | solution.py:826
  50.5 3.1 %shard_map.172 = bf16[512,512]{1,0:T(8,128)(2,1)} custom-call(s32[1]{0:T(128)} %bitcast.17.index_ref, bf16[256,1152]{1,0:T(8,128)(2,1)} %bitcast.26, bf16[256,1152]{1,0:T(8,128)(2,1)} %bitcast.40, bf16[7,1024,256]{2,1,0:T(8,128)(2,1)} %shard_map.165.own_ref, bf16[7,1024,256]{2,1,0:T(8,128)(2,1)} %collective-permute-done.5.other_ref), custom_call_target="tpu_custom_call" | custom-call | flops 536870912 | bytes 2097152 | tf_op jit(solution)/shard_map/pallas_call | solution.py:446
  53.6 1.3 collective-permute-start.10
  54.9 2.6 %collective-permute-done.6.rest_0_ = bf16[512,512]{1,0:T(8,128)(2,1)S(1)} collective-permute-done((bf16[512,512]{1,0:T(8,128)(2,1)}, bf16[512,512]{1,0:T(8,128)(2,1)S(1)}, u32[]{:S(2)}, u32[]{:S(2)}) %collective-permute-start.6) | collective-permute-done | bytes 524320 | tf_op jit(solution)/shard_map/ppermute | solution.py:826
  58.3 3.2 %shard_map.168 = bf16[512,512]{1,0:T(8,128)(2,1)} custom-call(s32[1]{0:T(128)} %bitcast.10.index_ref, bf16[256,1152]{1,0:T(8,128)(2,1)} %bitcast.27, bf16[256,1152]{1,0:T(8,128)(2,1)} %bitcast.41, bf16[7,1024,256]{2,1,0:T(8,128)(2,1)} %shard_map.165.own_ref, bf16[7,1024,256]{2,1,0:T(8,128)(2,1)} %collective-permute-done.5.other_ref, bf16[512,512]{1,0:T(8,128)(2,1)} %copy-done.17), custom_call_target="tpu_custom_call" | custom-call | flops 536870912 | bytes 2097152 | tf_op jit(solution)/shard_map/pallas_call | solution.py:446
  61.5 4.3 %collective-permute-start.7 = (bf16[512,512]{1,0:T(8,128)(2,1)}, bf16[512,512]{1,0:T(8,128)(2,1)S(1)}, u32[]{:S(2)}, u32[]{:S(2)}) collective-permute-start(bf16[512,512]{1,0:T(8,128)(2,1)} %shard_map.168), channel_id=1, source_target_pairs={{0,8},{25,17},{8,16},{17,9},{2,10},{27,19},{10,18},{19,11},{4,12},... | collective-permute-start | bytes 1572872 | tf_op jit(solution)/shard_map/ppermute | solution.py:826
  66.6 3.2 %shard_map.173 = bf16[512,512]{1,0:T(8,128)(2,1)} custom-call(s32[1]{0:T(128)} %bitcast.16.index_ref, bf16[256,1152]{1,0:T(8,128)(2,1)} %bitcast.28, bf16[256,1152]{1,0:T(8,128)(2,1)} %bitcast.42, bf16[7,1024,256]{2,1,0:T(8,128)(2,1)} %shard_map.165.own_ref, bf16[7,1024,256]{2,1,0:T(8,128)(2,1)} %collective-permute-done.5.other_ref, bf16[512,512]{1,0:T(8,128)(2,1)} %copy-done.16), custom_call_target="tpu_custom_call" | custom-call | flops 536870912 | bytes 2097152 | tf_op jit(solution)/shard_map/pallas_call | solution.py:446
  69.8 1.9 collective-permute-start.11
  73.6 3.2 %shard_map.169 = bf16[512,512]{1,0:T(8,128)(2,1)} custom-call(s32[1]{0:T(128)} %bitcast.9.index_ref, bf16[256,1152]{1,0:T(8,128)(2,1)} %bitcast.29, bf16[256,1152]{1,0:T(8,128)(2,1)} %bitcast.43, bf16[7,1024,256]{2,1,0:T(8,128)(2,1)} %shard_map.165.own_ref, bf16[7,1024,256]{2,1,0:T(8,128)(2,1)} %collective-permute-done.5.other_ref, bf16[512,512]{1,0:T(8,128)(2,1)} %copy-done.5), custom_call_target="tpu_custom_call" | custom-call | flops 536870912 | bytes 2097152 | tf_op jit(solution)/shard_map/pallas_call | solution.py:446
  76.8 4.3 %collective-permute-start.8 = (bf16[512,512]{1,0:T(8,128)(2,1)}, bf16[512,512]{1,0:T(8,128)(2,1)S(1)}, u32[]{:S(2)}, u32[]{:S(2)}) collective-permute-start(bf16[512,512]{1,0:T(8,128)(2,1)} %shard_map.169), channel_id=1, source_target_pairs={{0,8},{25,17},{8,16},{17,9},{16,24},{9,1},{2,10},{27,19},{10,18},{... | collective-permute-start | bytes 1572872 | tf_op jit(solution)/shard_map/ppermute | solution.py:826
  81.9 3.3 %shard_map.174 = bf16[512,512]{1,0:T(8,128)(2,1)} custom-call(s32[1]{0:T(128)} %bitcast.15.index_ref, bf16[256,1152]{1,0:T(8,128)(2,1)} %bitcast.30, bf16[256,1152]{1,0:T(8,128)(2,1)} %bitcast.44, bf16[7,1024,256]{2,1,0:T(8,128)(2,1)} %shard_map.165.own_ref, bf16[7,1024,256]{2,1,0:T(8,128)(2,1)} %collective-permute-done.5.other_ref, bf16[512,512]{1,0:T(8,128)(2,1)} %copy-done.6), custom_call_target="tpu_custom_call" | custom-call | flops 536870912 | bytes 2097152 | tf_op jit(solution)/shard_map/pallas_call | solution.py:446
  85.1 1.9 collective-permute-start.12
  88.1 1.1 collective-permute-done.15.other_ref
  89.3 4.7 %collective-permute-done.12.rest_0_ = bf16[512,512]{1,0:T(8,128)(2,1)S(1)} collective-permute-done((bf16[512,512]{1,0:T(8,128)(2,1)}, bf16[512,512]{1,0:T(8,128)(2,1)S(1)}, u32[]{:S(2)}, u32[]{:S(2)}) %collective-permute-start.12) | collective-permute-done | bytes 524320 | tf_op jit(solution)/shard_map/ppermute | solution.py:826
  94.8 3.2 %shard_map.175.key_value_ref = bf16[512,512]{1,0:T(8,128)(2,1)} custom-call(s32[1]{0:T(128)} %bitcast.14.index_ref, bf16[256,1152]{1,0:T(8,128)(2,1)} %bitcast.31, bf16[256,1152]{1,0:T(8,128)(2,1)} %bitcast.45, bf16[7,1024,256]{2,1,0:T(8,128)(2,1)} %shard_map.165.own_ref, bf16[7,1024,256]{2,1,0:T(8,128)(2,1)} %collective-permute-done.5.other_ref, ...), custom_call_target="tpu_custom_call" | custom-call | flops 536870912 | bytes 2097152 | tf_op jit(solution)/shard_map/pallas_call | solution.py:446
  98.0 4.3 %collective-permute-start.13 = (bf16[512,512]{1,0:T(8,128)(2,1)}, bf16[512,512]{1,0:T(8,128)(2,1)S(1)}, u32[]{:S(2)}, u32[]{:S(2)}) collective-permute-start(bf16[512,512]{1,0:T(8,128)(2,1)} %shard_map.175.key_value_ref), channel_id=1, source_target_pairs={{0,8},{25,17},{8,16},{17,9},{16,24},{9,1},{2,10},{27,19},{10,18},{... | collective-permute-start | bytes 1572872 | tf_op jit(solution)/shard_map/ppermute | solution.py:826
  103.1 3.2 %shard_map.170.query_ref = bf16[512,512]{1,0:T(8,128)(2,1)} custom-call(s32[1]{0:T(128)} %bitcast.8.index_ref, bf16[256,1152]{1,0:T(8,128)(2,1)} %bitcast.32, bf16[256,1152]{1,0:T(8,128)(2,1)} %bitcast.46, bf16[7,1024,256]{2,1,0:T(8,128)(2,1)} %shard_map.165.own_ref, bf16[7,1024,256]{2,1,0:T(8,128)(2,1)} %collective-permute-done.5.other_ref, ...), custom_call_target="tpu_custom_call" | custom-call | flops 536870912 | bytes 2097152 | tf_op jit(solution)/shard_map/pallas_call | solution.py:446
  107.6 4.4 %shard_map.183.refs_0_ = bf16[512,512]{1,0:T(8,128)(2,1)} custom-call(s32[4]{0:T(128)} %pad_add_fusion.place_ref, f32[2,4]{1,0:T(2,128)} %get-tuple-element.63.slope_ref, f32[2,4]{1,0:T(2,128)} %bitcast.56, bf16[512,512]{1,0:T(8,128)(2,1)} %shard_map.175.key_value_ref, bf16[512,512]{1,0:T(8,128)(2,1)} %shard_map.170.query_ref), custom_call_target="tpu_custom_call" | custom-call | flops 2000000000 | bytes 2097152 | tf_op jit(solution)/shard_map/pallas_call | solution.py:637
  112.0 1.4 collective-permute-start.26
  114.2 3.2 %shard_map.176.query_ref = bf16[512,512]{1,0:T(8,128)(2,1)} custom-call(s32[1]{0:T(128)} %bitcast.13.index_ref, bf16[256,1152]{1,0:T(8,128)(2,1)} %bitcast.33, bf16[256,1152]{1,0:T(8,128)(2,1)} %bitcast.47, bf16[7,1024,256]{2,1,0:T(8,128)(2,1)} %shard_map.165.own_ref, bf16[7,1024,256]{2,1,0:T(8,128)(2,1)} %collective-permute-done.5.other_ref, ...), custom_call_target="tpu_custom_call" | custom-call | flops 536870912 | bytes 2097152 | tf_op jit(solution)/shard_map/pallas_call | solution.py:446
  117.4 1.5 collective-permute-start.14
  119.7 3.2 %shard_map.171.query_key_ref = bf16[512,512]{1,0:T(8,128)(2,1)} custom-call(s32[1]{0:T(128)} %bitcast.4.index_ref, bf16[256,1152]{1,0:T(8,128)(2,1)} %bitcast.34, bf16[256,1152]{1,0:T(8,128)(2,1)} %bitcast.48, bf16[7,1024,256]{2,1,0:T(8,128)(2,1)} %shard_map.165.own_ref, bf16[7,1024,256]{2,1,0:T(8,128)(2,1)} %collective-permute-done.5.other_ref, ...), custom_call_target="tpu_custom_call" | custom-call | flops 536870912 | bytes 2097152 | tf_op jit(solution)/shard_map/pallas_call | solution.py:446
  122.9 1.5 collective-permute-start.20
  124.3 5.5 %shard_map.184.refs_4_ = bf16[512,512]{1,0:T(8,128)(2,1)} custom-call(s32[4]{0:T(128)} %pad_add_fusion.place_ref, f32[2,4]{1,0:T(2,128)} %get-tuple-element.62.slope_ref, f32[2,4]{1,0:T(2,128)} %bitcast.55, bf16[512,512]{1,0:T(8,128)(2,1)} %shard_map.175.key_value_ref, bf16[512,512]{1,0:T(8,128)(2,1)} %shard_map.176.query_ref), custom_call_target="tpu_custom_call" | custom-call | flops 2000000000 | bytes 2097152 | tf_op jit(solution)/shard_map/pallas_call | solution.py:637
  129.9 1.4 collective-permute-start.29
  131.4 4.9 %shard_map.178.running_ref = f32[512,512]{1,0:T(8,128)} custom-call(s32[4]{0:T(128)} %pad_add_fusion.place_ref, bf16[256,1152]{1,0:T(8,128)(2,1)} %bitcast.35, bf16[256,1152]{1,0:T(8,128)(2,1)} %bitcast.49, f32[24,512]{1,0:T(8,128)} %copy-done.26, f32[24,512]{1,0:T(8,128)} %copy-done.30), custom_call_target="tpu_custom_call" | custom-call | flops 1000000000 | bytes 1048576 | tf_op jit(solution)/shard_map/pallas_call | solution.py:501
  136.3 4.5 %collective-permute-start.32 = (bf16[512,1024]{1,0:T(8,128)(2,1)S(1)}, bf16[512,1024]{1,0:T(8,128)(2,1)S(1)}, u32[]{:S(2)}, u32[]{:S(2)}) collective-permute-start(bf16[512,1024]{1,0:T(8,128)(2,1)S(1)} %constant_dynamic-slice_fusion), channel_id=1, source_target_pairs={{0,1},{1,0},{2,3},{3,2},{4,5},{5,4},{6,7},{7,6},{8,9},{9,8},{10,11... | collective-permute-start | bytes 3145736 | tf_op jit(solution)/shard_map/ppermute | solution.py:747
  140.7 1.5 collective-permute-start.27
  142.2 3.2 %shard_map.177.value_ref = bf16[512,512]{1,0:T(8,128)(2,1)} custom-call(s32[1]{0:T(128)} %bitcast.12.index_ref, bf16[256,1152]{1,0:T(8,128)(2,1)} %bitcast.36, bf16[256,1152]{1,0:T(8,128)(2,1)} %bitcast.50, bf16[7,1024,256]{2,1,0:T(8,128)(2,1)} %shard_map.165.own_ref, bf16[7,1024,256]{2,1,0:T(8,128)(2,1)} %collective-permute-done.5.other_ref, ...), custom_call_target="tpu_custom_call" | custom-call | flops 536870912 | bytes 2097152 | tf_op jit(solution)/shard_map/pallas_call | solution.py:446
  145.4 5.0 %shard_map.179.refs_0_ = bf16[512,512]{1,0:T(8,128)(2,1)} custom-call(s32[4]{0:T(128)} %pad_add_fusion.place_ref, bf16[512,512]{1,0:T(8,128)(2,1)} %shard_map.171.query_key_ref, bf16[512,512]{1,0:T(8,128)(2,1)} %shard_map.177.value_ref, f32[512,512]{1,0:T(8,128)} %shard_map.178.running_ref, f32[4,128,256]{2,1,0:T(8,128)} %own_ref.1, ...), custom_call_target="tpu_custom_call" | custom-call | flops 2000000000 | bytes 2097152 | tf_op jit(solution)/shard_map/pallas_call | solution.py:553
  150.3 1.5 collective-permute-start.17
  151.8 1.5 collective-permute-start.21
  153.3 1.5 collective-permute-start.30
  154.8 1.1 constant_dynamic-slice_fusion.2
  155.9 3.3 %collective-permute-start.25 = (bf16[512,1024]{1,0:T(8,128)(2,1)}, bf16[512,1024]{1,0:T(8,128)(2,1)S(1)}, u32[]{:S(2)}, u32[]{:S(2)}) collective-permute-start(bf16[512,1024]{1,0:T(8,128)(2,1)} %constant_dynamic-slice_fusion.2), channel_id=1, source_target_pairs={{0,1},{1,0},{2,3},{3,2},{4,5},{5,4},{6,7},{7,6},{8,9},{9,8},{10,11... | collective-permute-start | bytes 3145736 | tf_op jit(solution)/shard_map/ppermute | solution.py:747
  159.2 1.3 collective-permute-start.28
  160.5 1.5 collective-permute-start.18
  162.0 1.3 collective-permute-start.31
  163.3 3.2 %shard_map.180.query_key_ref = bf16[512,512]{1,0:T(8,128)(2,1)} custom-call(s32[1]{0:T(128)} %bitcast.21.index_ref, bf16[256,1152]{1,0:T(8,128)(2,1)} %bitcast.37, bf16[256,1152]{1,0:T(8,128)(2,1)} %bitcast.51, bf16[7,1024,256]{2,1,0:T(8,128)(2,1)} %shard_map.165.own_ref, bf16[7,1024,256]{2,1,0:T(8,128)(2,1)} %collective-permute-done.5.other_ref, ...), custom_call_target="tpu_custom_call" | custom-call | flops 536870912 | bytes 2097152 | tf_op jit(solution)/shard_map/pallas_call | solution.py:446
  166.5 3.2 %shard_map.181.value_ref = bf16[512,512]{1,0:T(8,128)(2,1)} custom-call(s32[1]{0:T(128)} %bitcast.22.index_ref, bf16[256,1152]{1,0:T(8,128)(2,1)} %bitcast.38, bf16[256,1152]{1,0:T(8,128)(2,1)} %bitcast.52, bf16[7,1024,256]{2,1,0:T(8,128)(2,1)} %shard_map.165.own_ref, bf16[7,1024,256]{2,1,0:T(8,128)(2,1)} %collective-permute-done.5.other_ref, ...), custom_call_target="tpu_custom_call" | custom-call | flops 536870912 | bytes 2097152 | tf_op jit(solution)/shard_map/pallas_call | solution.py:446
  169.7 4.8 %shard_map.182.refs_4_ = bf16[512,512]{1,0:T(8,128)(2,1)} custom-call(s32[4]{0:T(128)} %pad_add_fusion.place_ref, bf16[512,512]{1,0:T(8,128)(2,1)} %shard_map.180.query_key_ref, bf16[512,512]{1,0:T(8,128)(2,1)} %shard_map.181.value_ref, f32[512,512]{1,0:T(8,128)} %shard_map.178.running_ref, f32[4,128,256]{2,1,0:T(8,128)} %own_ref.1, ...), custom_call_target="tpu_custom_call" | custom-call | flops 2000000000 | bytes 2097152 | tf_op jit(solution)/shard_map/pallas_call | solution.py:553
  176.0 1.3 collective-permute-start.24
  177.5 1.3 collective-permute-start.19
  178.8 6.0 %shard_map.185.refs_10_ = f32[512,1024]{1,0:T(8,128)} custom-call(s32[4]{0:T(128)} %pad_add_fusion.place_ref, bf16[512,512]{1,0:T(8,128)(2,1)} %shard_map.183.refs_0_, bf16[512,512]{1,0:T(8,128)(2,1)} %collective-permute-done.26.refs_1_, bf16[512,512]{1,0:T(8,128)(2,1)} %collective-permute-done.27.refs_2_, bf16[512,512]{1,0:T(8,128)(2,1)} %collective-permute-done.28.refs_3_, ...), custom_call_target="tpu_custom_call" | custom-call | flops 1073741824 | bytes 4194304 | tf_op jit(solution)/shard_map/pallas_call | solution.py:694
  184.8 19.1 %collective-permute-done.24.refs_7_ = bf16[512,512]{1,0:T(8,128)(2,1)S(1)} collective-permute-done((bf16[512,512]{1,0:T(8,128)(2,1)}, bf16[512,512]{1,0:T(8,128)(2,1)S(1)}, u32[]{:S(2)}, u32[]{:S(2)}) %collective-permute-start.24) | collective-permute-done | bytes 524320 | tf_op jit(solution)/shard_map/ppermute | solution.py:874
  205.5 6.2 %shard_map.186 = (bf16[256,1024]{1,0:T(8,128)(2,1)}, bf16[256,1024]{1,0:T(8,128)(2,1)}) custom-call(s32[4]{0:T(128)} %pad_add_fusion.place_ref, bf16[512,512]{1,0:T(8,128)(2,1)} %shard_map.179.refs_0_, bf16[512,512]{1,0:T(8,128)(2,1)} %collective-permute-done.17.refs_1_, bf16[512,512]{1,0:T(8,128)(2,1)} %collective-permute-done.18.refs_2_, ...), custom_call_target="tpu_custom_call" | custom-call | flops 1073741824 | bytes 4194304 | tf_op jit(solution)/shard_map/pallas_call | solution.py:694
  211.8 2.1 collective-permute-done.33.given_ref
  214.7 2.1 shard_map.187
  217.1 3.5 %collective-permute-start.36 = (bf16[64,1024]{1,0:T(8,128)(2,1)}, bf16[64,1024]{1,0:T(8,128)(2,1)S(1)}, u32[]{:S(2)}, u32[]{:S(2)}) collective-permute-start(bf16[64,1024]{1,0:T(8,128)(2,1)} %get-tuple-element.56), channel_id=1, source_target_pairs={{0,24},{8,0},{16,8},{24,16},{1,25},{9,1},{17,9},{25,17},{2,26},{10... | collective-permute-start | bytes 393224 | tf_op jit(solution)/shard_map/ppermute | solution.py:370
  220.6 4.7 %collective-permute-done.34.refs_1_ = bf16[64,1024]{1,0:T(8,128)(2,1)S(1)} collective-permute-done((bf16[64,1024]{1,0:T(8,128)(2,1)}, bf16[64,1024]{1,0:T(8,128)(2,1)S(1)}, u32[]{:S(2)}, u32[]{:S(2)}) %collective-permute-start.34) | collective-permute-done | bytes 131104 | tf_op jit(solution)/shard_map/ppermute | solution.py:370
  225.3 4.6 %collective-permute-done.35.refs_2_ = bf16[64,1024]{1,0:T(8,128)(2,1)S(1)} collective-permute-done((bf16[64,1024]{1,0:T(8,128)(2,1)}, bf16[64,1024]{1,0:T(8,128)(2,1)S(1)}, u32[]{:S(2)}, u32[]{:S(2)}) %collective-permute-start.35) | collective-permute-done | bytes 131104 | tf_op jit(solution)/shard_map/ppermute | solution.py:370
  230.6 1.9 shard_map.188
  (133 shorter events, 21.4 us)
Async XLA Ops:
  0.0 3.4 %copy-start.22 = (bf16[4096,16]{0,1:T(8,128)(2,1)S(1)}, bf16[4096,16]{0,1:T(8,128)(2,1)}, u32[]{:S(2)}) copy-start(bf16[4096,16]{0,1:T(8,128)(2,1)} %param.25) | copy-start | bytes 393220
  2.9 3.2 %collective-permute-start = (bf16[64,2176]{1,0:T(8,128)(2,1)S(1)}, bf16[64,2176]{1,0:T(8,128)(2,1)S(1)}, u32[]{:S(2)}, u32[]{:S(2)}) collective-permute-start(bf16[64,2176]{1,0:T(8,128)(2,1)S(1)} %pad_dynamic-slice_fusion), channel_id=1, source_target_pairs={{0,1},{1,0},{2,3},{3,2},{4,5},{5,4},{6,7},{7,6},{8,9},{9,8},{10,11... | collective-permute-start | bytes 835592 | tf_op jit(solution)/shard_map/ppermute | solution.py:747
  9.8 6.6 %copy-start.34 = (bf16[64,1152]{1,0:T(8,128)(2,1)S(1)}, bf16[64,1152]{1,0:T(8,128)(2,1)}, u32[]{:S(2)}) copy-start(bf16[64,1152]{1,0:T(8,128)(2,1)} %get-tuple-element.36) | copy-start | bytes 442372
  9.8 9.6 %copy-start.33 = (bf16[64,1152]{1,0:T(8,128)(2,1)S(1)}, bf16[64,1152]{1,0:T(8,128)(2,1)}, u32[]{:S(2)}) copy-start(bf16[64,1152]{1,0:T(8,128)(2,1)} %get-tuple-element.37) | copy-start | bytes 442372
  9.8 12.2 %copy-start.32 = (bf16[64,1152]{1,0:T(8,128)(2,1)S(1)}, bf16[64,1152]{1,0:T(8,128)(2,1)}, u32[]{:S(2)}) copy-start(bf16[64,1152]{1,0:T(8,128)(2,1)} %get-tuple-element.38) | copy-start | bytes 442372
  16.3 25.4 %collective-permute-start.5 = (bf16[7,1024,256]{2,1,0:T(8,128)(2,1)}, bf16[7,1024,256]{2,1,0:T(8,128)(2,1)}, u32[]{:S(2)}, u32[]{:S(2)}) collective-permute-start(bf16[7,1024,256]{2,1,0:T(8,128)(2,1)} %shard_map.166), channel_id=1, source_target_pairs={{0,1},{1,0},{2,3},{3,2},{4,5},{5,4},{6,7},{7,6},{8,9},{9,8},{10,11... | collective-permute-start | bytes 11010056 | tf_op jit(solution)/shard_map/ppermute | solution.py:747
  16.4 9.9 %collective-permute-start.1 = (bf16[64,1152]{1,0:T(8,128)(2,1)S(1)}, bf16[64,1152]{1,0:T(8,128)(2,1)S(1)}, u32[]{:S(2)}, u32[]{:S(2)}) collective-permute-start(bf16[64,1152]{1,0:T(8,128)(2,1)S(1)} %copy-done.34), channel_id=1, source_target_pairs={{0,8},{8,16},{16,24},{24,0},{1,9},{9,17},{17,25},{25,1},{2,10},{10... | collective-permute-start | bytes 442376 | tf_op jit(solution)/shard_map/ppermute | solution.py:370
  19.4 12.5 %collective-permute-start.2 = (bf16[64,1152]{1,0:T(8,128)(2,1)S(1)}, bf16[64,1152]{1,0:T(8,128)(2,1)S(1)}, u32[]{:S(2)}, u32[]{:S(2)}) collective-permute-start(bf16[64,1152]{1,0:T(8,128)(2,1)S(1)} %copy-done.33), channel_id=1, source_target_pairs={{0,16},{8,24},{16,0},{24,8},{1,17},{9,25},{17,1},{25,9},{2,18},{10... | collective-permute-start | bytes 442376 | tf_op jit(solution)/shard_map/ppermute | solution.py:370
  22.0 9.9 %collective-permute-start.3 = (bf16[64,1152]{1,0:T(8,128)(2,1)S(1)}, bf16[64,1152]{1,0:T(8,128)(2,1)S(1)}, u32[]{:S(2)}, u32[]{:S(2)}) collective-permute-start(bf16[64,1152]{1,0:T(8,128)(2,1)S(1)} %copy-done.32), channel_id=1, source_target_pairs={{0,24},{8,0},{16,8},{24,16},{1,25},{9,1},{17,9},{25,17},{2,26},{10... | collective-permute-start | bytes 442376 | tf_op jit(solution)/shard_map/ppermute | solution.py:370
  26.2 5.7 %copy-start.19 = (bf16[64,1152]{1,0:T(8,128)(2,1)}, bf16[64,1152]{1,0:T(8,128)(2,1)S(1)}, u32[]{:S(2)}) copy-start(bf16[64,1152]{1,0:T(8,128)(2,1)S(1)} %collective-permute-done.1.refs_1_) | copy-start | bytes 442372
  35.3 6.5 %collective-permute-start.4 = (bf16[4,64,1152]{2,1,0:T(8,128)(2,1)}, bf16[4,64,1152]{2,1,0:T(8,128)(2,1)S(1)}, u32[]{:S(2)}, u32[]{:S(2)}) collective-permute-start(bf16[4,64,1152]{2,1,0:T(8,128)(2,1)} %shard_map.164), channel_id=1, source_target_pairs={{0,1},{1,0},{2,3},{3,2},{4,5},{5,4},{6,7},{7,6},{8,9},{9,8},{10,11... | collective-permute-start | bytes 1769480 | tf_op jit(solution)/shard_map/ppermute | solution.py:747
  41.8 0.9 copy-start
  45.6 11.9 %collective-permute-start.6 = (bf16[512,512]{1,0:T(8,128)(2,1)}, bf16[512,512]{1,0:T(8,128)(2,1)S(1)}, u32[]{:S(2)}, u32[]{:S(2)}) collective-permute-start(bf16[512,512]{1,0:T(8,128)(2,1)} %shard_map.167), channel_id=1, source_target_pairs={{0,8},{25,17},{2,10},{27,19},{4,12},{29,21},{6,14},{31,23}} | collective-permute-start | bytes 1572872 | tf_op jit(solution)/shard_map/ppermute | solution.py:826
  53.6 12.2 %collective-permute-start.10 = (bf16[512,512]{1,0:T(8,128)(2,1)}, bf16[512,512]{1,0:T(8,128)(2,1)S(1)}, u32[]{:S(2)}, u32[]{:S(2)}) collective-permute-start(bf16[512,512]{1,0:T(8,128)(2,1)} %shard_map.172), channel_id=1, source_target_pairs={{0,8},{25,17},{2,10},{27,19},{4,12},{29,21},{6,14},{31,23}} | collective-permute-start | bytes 1572872 | tf_op jit(solution)/shard_map/ppermute | solution.py:826
  57.5 0.8 copy-start.17
  61.5 11.3 %collective-permute-start.7 = (bf16[512,512]{1,0:T(8,128)(2,1)}, bf16[512,512]{1,0:T(8,128)(2,1)S(1)}, u32[]{:S(2)}, u32[]{:S(2)}) collective-permute-start(bf16[512,512]{1,0:T(8,128)(2,1)} %shard_map.168), channel_id=1, source_target_pairs={{0,8},{25,17},{8,16},{17,9},{2,10},{27,19},{10,18},{19,11},{4,12},... | collective-permute-start | bytes 1572872 | tf_op jit(solution)/shard_map/ppermute | solution.py:826
  65.8 0.8 copy-start.16
  69.8 11.3 %collective-permute-start.11 = (bf16[512,512]{1,0:T(8,128)(2,1)}, bf16[512,512]{1,0:T(8,128)(2,1)S(1)}, u32[]{:S(2)}, u32[]{:S(2)}) collective-permute-start(bf16[512,512]{1,0:T(8,128)(2,1)} %shard_map.173), channel_id=1, source_target_pairs={{0,8},{25,17},{8,16},{17,9},{2,10},{27,19},{10,18},{19,11},{4,12},... | collective-permute-start | bytes 1572872 | tf_op jit(solution)/shard_map/ppermute | solution.py:826
  76.8 25.6 %collective-permute-start.8 = (bf16[512,512]{1,0:T(8,128)(2,1)}, bf16[512,512]{1,0:T(8,128)(2,1)S(1)}, u32[]{:S(2)}, u32[]{:S(2)}) collective-permute-start(bf16[512,512]{1,0:T(8,128)(2,1)} %shard_map.169), channel_id=1, source_target_pairs={{0,8},{25,17},{8,16},{17,9},{16,24},{9,1},{2,10},{27,19},{10,18},{... | collective-permute-start | bytes 1572872 | tf_op jit(solution)/shard_map/ppermute | solution.py:826
  81.1 0.8 copy-start.6
  81.9 5.9 %copy-start.29 = (f32[16]{0:T(128)S(1)}, f32[16]{0:T(128)}, u32[]{:S(2)}) copy-start(f32[16]{0:T(128)} %param.30) | copy-start | bytes 196
  81.9 5.9 %copy-start.27 = (bf16[16,512]{1,0:T(8,128)(2,1)S(1)}, bf16[16,512]{1,0:T(8,128)(2,1)}, u32[]{:S(2)}) copy-start(bf16[16,512]{1,0:T(8,128)(2,1)} %param.26) | copy-start | bytes 49156
  81.9 5.9 %copy-start.28 = (f32[512]{0:T(512)S(1)}, f32[512]{0:T(512)}, u32[]{:S(2)}) copy-start(f32[512]{0:T(512)} %param.27) | copy-start | bytes 6148
  85.1 8.9 %collective-permute-start.12 = (bf16[512,512]{1,0:T(8,128)(2,1)}, bf16[512,512]{1,0:T(8,128)(2,1)S(1)}, u32[]{:S(2)}, u32[]{:S(2)}) collective-permute-start(bf16[512,512]{1,0:T(8,128)(2,1)} %shard_map.174), channel_id=1, source_target_pairs={{0,8},{25,17},{8,16},{17,9},{16,24},{9,1},{2,10},{27,19},{10,18},{... | collective-permute-start | bytes 1572872 | tf_op jit(solution)/shard_map/ppermute | solution.py:826
  87.9 18.5 %copy-start.26 = (f32[24,512]{1,0:T(8,128)}, f32[24,512]{1,0:T(8,128)S(1)}, u32[]{:S(2)}) copy-start(f32[24,512]{1,0:T(8,128)S(1)} %maximum_maximum_fusion.own_ref) | copy-start | bytes 147460
  87.9 1.3 collective-permute-start.15
  89.1 17.2 %copy-start.30 = (f32[24,512]{1,0:T(8,128)}, f32[24,512]{1,0:T(8,128)S(1)}, u32[]{:S(2)}) copy-start(f32[24,512]{1,0:T(8,128)S(1)} %collective-permute-done.15.other_ref) | copy-start | bytes 147460
  98.0 15.4 %collective-permute-start.13 = (bf16[512,512]{1,0:T(8,128)(2,1)}, bf16[512,512]{1,0:T(8,128)(2,1)S(1)}, u32[]{:S(2)}, u32[]{:S(2)}) collective-permute-start(bf16[512,512]{1,0:T(8,128)(2,1)} %shard_map.175.key_value_ref), channel_id=1, source_target_pairs={{0,8},{25,17},{8,16},{17,9},{16,24},{9,1},{2,10},{27,19},{10,18},{... | collective-permute-start | bytes 1572872 | tf_op jit(solution)/shard_map/ppermute | solution.py:826
  102.3 0.8 copy-start.7
  106.3 12.5 %collective-permute-start.9 = (bf16[512,512]{1,0:T(8,128)(2,1)}, bf16[512,512]{1,0:T(8,128)(2,1)S(1)}, u32[]{:S(2)}, u32[]{:S(2)}) collective-permute-start(bf16[512,512]{1,0:T(8,128)(2,1)} %shard_map.170.query_ref), channel_id=1, source_target_pairs={{8,16},{17,9},{16,24},{9,1},{10,18},{19,11},{18,26},{11,3},{12,20}... | collective-permute-start | bytes 1572872 | tf_op jit(solution)/shard_map/ppermute | solution.py:826
  112.0 24.3 %collective-permute-start.26 = (bf16[512,512]{1,0:T(8,128)(2,1)}, bf16[512,512]{1,0:T(8,128)(2,1)}, u32[]{:S(2)}, u32[]{:S(2)}) collective-permute-start(bf16[512,512]{1,0:T(8,128)(2,1)} %shard_map.183.refs_0_), channel_id=1, source_target_pairs={{1,9},{24,16},{3,11},{26,18},{5,13},{28,20},{7,15},{30,22}} | collective-permute-start | bytes 1572872 | tf_op jit(solution)/shard_map/ppermute | solution.py:870
  113.4 0.8 copy-start.15
  117.4 23.3 %collective-permute-start.14 = (bf16[512,512]{1,0:T(8,128)(2,1)}, bf16[512,512]{1,0:T(8,128)(2,1)}, u32[]{:S(2)}, u32[]{:S(2)}) collective-permute-start(bf16[512,512]{1,0:T(8,128)(2,1)} %shard_map.176.query_ref), channel_id=1, source_target_pairs={{8,16},{17,9},{16,24},{9,1},{10,18},{19,11},{18,26},{11,3},{12,20}... | collective-permute-start | bytes 1572872 | tf_op jit(solution)/shard_map/ppermute | solution.py:826
  118.9 26.5 %collective-permute-start.16 = (f32[4,128,256]{2,1,0:T(8,128)}, f32[4,128,256]{2,1,0:T(8,128)}, u32[]{:S(2)}, u32[]{:S(2)}) collective-permute-start(f32[4,128,256]{2,1,0:T(8,128)} %own_ref.1), channel_id=1, source_target_pairs={{0,1},{1,0},{2,3},{3,2},{4,5},{5,4},{6,7},{7,6},{8,9},{9,8},{10,11... | collective-permute-start | bytes 1572872 | tf_op jit(solution)/shard_map/ppermute | solution.py:747
  118.9 0.8 copy-start.14
  122.9 29.0 %collective-permute-start.20 = (bf16[512,512]{1,0:T(8,128)(2,1)}, bf16[512,512]{1,0:T(8,128)(2,1)}, u32[]{:S(2)}, u32[]{:S(2)}) collective-permute-start(bf16[512,512]{1,0:T(8,128)(2,1)} %shard_map.171.query_key_ref), channel_id=1, source_target_pairs={{16,24},{9,1},{18,26},{11,3},{20,28},{13,5},{22,30},{15,7}} | collective-permute-start | bytes 1572872 | tf_op jit(solution)/shard_map/ppermute | solution.py:826
  124.3 7.0 %copy-start.1 = (bf16[1024,1024]{1,0:T(8,128)(2,1)S(1)}, bf16[1024,1024]{1,0:T(8,128)(2,1)}, u32[]{:S(2)}) copy-start(bf16[1024,1024]{1,0:T(8,128)(2,1)} %refs_8_) | copy-start | bytes 6291460
  129.9 23.4 %collective-permute-start.29 = (bf16[512,512]{1,0:T(8,128)(2,1)}, bf16[512,512]{1,0:T(8,128)(2,1)}, u32[]{:S(2)}, u32[]{:S(2)}) collective-permute-start(bf16[512,512]{1,0:T(8,128)(2,1)} %shard_map.184.refs_4_), channel_id=1, source_target_pairs={{1,9},{24,16},{3,11},{26,18},{5,13},{28,20},{7,15},{30,22}} | collective-permute-start | bytes 1572872 | tf_op jit(solution)/shard_map/ppermute | solution.py:870
  136.3 38.3 %collective-permute-start.32 = (bf16[512,1024]{1,0:T(8,128)(2,1)S(1)}, bf16[512,1024]{1,0:T(8,128)(2,1)S(1)}, u32[]{:S(2)}, u32[]{:S(2)}) collective-permute-start(bf16[512,1024]{1,0:T(8,128)(2,1)S(1)} %constant_dynamic-slice_fusion), channel_id=1, source_target_pairs={{0,1},{1,0},{2,3},{3,2},{4,5},{5,4},{6,7},{7,6},{8,9},{9,8},{10,11... | collective-permute-start | bytes 3145736 | tf_op jit(solution)/shard_map/ppermute | solution.py:747
  140.7 15.2 %collective-permute-start.27 = (bf16[512,512]{1,0:T(8,128)(2,1)}, bf16[512,512]{1,0:T(8,128)(2,1)}, u32[]{:S(2)}, u32[]{:S(2)}) collective-permute-start(bf16[512,512]{1,0:T(8,128)(2,1)} %collective-permute-done.26.refs_1_), channel_id=1, source_target_pairs={{9,17},{16,8},{11,19},{18,10},{13,21},{20,12},{15,23},{22,14}} | collective-permute-start | bytes 1572872 | tf_op jit(solution)/shard_map/ppermute | solution.py:870
  145.4 6.4 %copy-start.11 = (bf16[512,512]{1,0:T(8,128)(2,1)S(1)}, bf16[512,512]{1,0:T(8,128)(2,1)}, u32[]{:S(2)}) copy-start(bf16[512,512]{1,0:T(8,128)(2,1)} %shard_map.177.value_ref) | copy-start | bytes 1572868
  145.4 9.4 %copy-start.2 = (bf16[1024,1024]{1,0:T(8,128)(2,1)S(1)}, bf16[1024,1024]{1,0:T(8,128)(2,1)}, u32[]{:S(2)}) copy-start(bf16[1024,1024]{1,0:T(8,128)(2,1)} %refs_8_.1) | copy-start | bytes 6291460
  150.3 8.9 %collective-permute-start.17 = (bf16[512,512]{1,0:T(8,128)(2,1)}, bf16[512,512]{1,0:T(8,128)(2,1)}, u32[]{:S(2)}, u32[]{:S(2)}) collective-permute-start(bf16[512,512]{1,0:T(8,128)(2,1)} %shard_map.179.refs_0_), channel_id=1, source_target_pairs={{1,9},{24,16},{3,11},{26,18},{5,13},{28,20},{7,15},{30,22}} | collective-permute-start | bytes 1572872 | tf_op jit(solution)/shard_map/ppermute | solution.py:870
  151.8 8.7 %collective-permute-start.21 = (bf16[512,512]{1,0:T(8,128)(2,1)S(1)}, bf16[512,512]{1,0:T(8,128)(2,1)}, u32[]{:S(2)}, u32[]{:S(2)}) collective-permute-start(bf16[512,512]{1,0:T(8,128)(2,1)S(1)} %copy-done.11), channel_id=1, source_target_pairs={{16,24},{9,1},{18,26},{11,3},{20,28},{13,5},{22,30},{15,7}} | collective-permute-start | bytes 1572872 | tf_op jit(solution)/shard_map/ppermute | solution.py:826
  153.3 8.7 %collective-permute-start.30 = (bf16[512,512]{1,0:T(8,128)(2,1)}, bf16[512,512]{1,0:T(8,128)(2,1)}, u32[]{:S(2)}, u32[]{:S(2)}) collective-permute-start(bf16[512,512]{1,0:T(8,128)(2,1)} %collective-permute-done.29.refs_5_), channel_id=1, source_target_pairs={{9,17},{16,8},{11,19},{18,10},{13,21},{20,12},{15,23},{22,14}} | collective-permute-start | bytes 1572872 | tf_op jit(solution)/shard_map/ppermute | solution.py:870
  155.9 28.9 %collective-permute-start.25 = (bf16[512,1024]{1,0:T(8,128)(2,1)}, bf16[512,1024]{1,0:T(8,128)(2,1)S(1)}, u32[]{:S(2)}, u32[]{:S(2)}) collective-permute-start(bf16[512,1024]{1,0:T(8,128)(2,1)} %constant_dynamic-slice_fusion.2), channel_id=1, source_target_pairs={{0,1},{1,0},{2,3},{3,2},{4,5},{5,4},{6,7},{7,6},{8,9},{9,8},{10,11... | collective-permute-start | bytes 3145736 | tf_op jit(solution)/shard_map/ppermute | solution.py:747
  159.2 16.0 %collective-permute-start.28 = (bf16[512,512]{1,0:T(8,128)(2,1)}, bf16[512,512]{1,0:T(8,128)(2,1)}, u32[]{:S(2)}, u32[]{:S(2)}) collective-permute-start(bf16[512,512]{1,0:T(8,128)(2,1)} %collective-permute-done.27.refs_2_), channel_id=1, source_target_pairs={{17,25},{8,0},{19,27},{10,2},{21,29},{12,4},{23,31},{14,6}} | collective-permute-start | bytes 1572872 | tf_op jit(solution)/shard_map/ppermute | solution.py:870
  160.5 15.4 %collective-permute-start.18 = (bf16[512,512]{1,0:T(8,128)(2,1)}, bf16[512,512]{1,0:T(8,128)(2,1)}, u32[]{:S(2)}, u32[]{:S(2)}) collective-permute-start(bf16[512,512]{1,0:T(8,128)(2,1)} %collective-permute-done.17.refs_1_), channel_id=1, source_target_pairs={{9,17},{16,8},{11,19},{18,10},{13,21},{20,12},{15,23},{22,14}} | collective-permute-start | bytes 1572872 | tf_op jit(solution)/shard_map/ppermute | solution.py:870
  162.0 15.4 %collective-permute-start.31 = (bf16[512,512]{1,0:T(8,128)(2,1)}, bf16[512,512]{1,0:T(8,128)(2,1)}, u32[]{:S(2)}, u32[]{:S(2)}) collective-permute-start(bf16[512,512]{1,0:T(8,128)(2,1)} %collective-permute-done.30.refs_6_), channel_id=1, source_target_pairs={{17,25},{8,0},{19,27},{10,2},{21,29},{12,4},{23,31},{14,6}} | collective-permute-start | bytes 1572872 | tf_op jit(solution)/shard_map/ppermute | solution.py:870
  174.5 4.2 %copy-start.3 = (bf16[512,1024]{1,0:T(8,128)(2,1)}, bf16[512,1024]{1,0:T(8,128)(2,1)S(1)}, u32[]{:S(2)}) copy-start(bf16[512,1024]{1,0:T(8,128)(2,1)S(1)} %collective-permute-done.32.refs_9_) | copy-start | bytes 3145732
  174.5 10.2 %collective-permute-start.22 = (bf16[512,512]{1,0:T(8,128)(2,1)}, bf16[512,512]{1,0:T(8,128)(2,1)S(1)}, u32[]{:S(2)}, u32[]{:S(2)}) collective-permute-start(bf16[512,512]{1,0:T(8,128)(2,1)} %shard_map.182.refs_4_), channel_id=1, source_target_pairs={{24,16},{1,9},{26,18},{3,11},{28,20},{5,13},{30,22},{7,15}} | collective-permute-start | bytes 1572872 | tf_op jit(solution)/shard_map/ppermute | solution.py:874
  175.2 9.6 %collective-permute-start.23 = (bf16[512,512]{1,0:T(8,128)(2,1)}, bf16[512,512]{1,0:T(8,128)(2,1)S(1)}, u32[]{:S(2)}, u32[]{:S(2)}) collective-permute-start(bf16[512,512]{1,0:T(8,128)(2,1)} %shard_map.182.refs_4_), channel_id=1, source_target_pairs={{24,8},{1,17},{26,10},{3,19},{28,12},{5,21},{30,14},{7,23}} | collective-permute-start | bytes 1572872 | tf_op jit(solution)/shard_map/ppermute | solution.py:874
  176.0 28.0 %collective-permute-start.24 = (bf16[512,512]{1,0:T(8,128)(2,1)}, bf16[512,512]{1,0:T(8,128)(2,1)S(1)}, u32[]{:S(2)}, u32[]{:S(2)}) collective-permute-start(bf16[512,512]{1,0:T(8,128)(2,1)} %shard_map.182.refs_4_), channel_id=1, source_target_pairs={{24,0},{1,25},{26,2},{3,27},{28,4},{5,29},{30,6},{7,31}} | collective-permute-start | bytes 1572872 | tf_op jit(solution)/shard_map/ppermute | solution.py:874
  177.5 26.5 %collective-permute-start.19 = (bf16[512,512]{1,0:T(8,128)(2,1)}, bf16[512,512]{1,0:T(8,128)(2,1)S(1)}, u32[]{:S(2)}, u32[]{:S(2)}) collective-permute-start(bf16[512,512]{1,0:T(8,128)(2,1)} %collective-permute-done.18.refs_2_), channel_id=1, source_target_pairs={{17,25},{8,0},{19,27},{10,2},{21,29},{12,4},{23,31},{14,6}} | collective-permute-start | bytes 1572872 | tf_op jit(solution)/shard_map/ppermute | solution.py:870
  184.8 19.2 %copy-start.4 = (bf16[512,1024]{1,0:T(8,128)(2,1)}, bf16[512,1024]{1,0:T(8,128)(2,1)S(1)}, u32[]{:S(2)}) copy-start(bf16[512,1024]{1,0:T(8,128)(2,1)S(1)} %collective-permute-done.25.refs_9_) | copy-start | bytes 3145732
  184.8 19.2 %copy-start.8 = (bf16[512,512]{1,0:T(8,128)(2,1)}, bf16[512,512]{1,0:T(8,128)(2,1)S(1)}, u32[]{:S(2)}) copy-start(bf16[512,512]{1,0:T(8,128)(2,1)S(1)} %collective-permute-done.22.refs_5_) | copy-start | bytes 1572868
  184.8 19.1 %copy-start.9 = (bf16[512,512]{1,0:T(8,128)(2,1)}, bf16[512,512]{1,0:T(8,128)(2,1)S(1)}, u32[]{:S(2)}) copy-start(bf16[512,512]{1,0:T(8,128)(2,1)S(1)} %collective-permute-done.23.refs_6_) | copy-start | bytes 1572868
  203.9 0.8 copy-start.10
  211.7 2.2 collective-permute-start.33
  213.9 0.8 copy-start.18
  216.8 8.5 %collective-permute-start.34 = (bf16[64,1024]{1,0:T(8,128)(2,1)}, bf16[64,1024]{1,0:T(8,128)(2,1)S(1)}, u32[]{:S(2)}, u32[]{:S(2)}) collective-permute-start(bf16[64,1024]{1,0:T(8,128)(2,1)} %get-tuple-element.54), channel_id=1, source_target_pairs={{0,8},{8,16},{16,24},{24,0},{1,9},{9,17},{17,25},{25,1},{2,10},{10... | collective-permute-start | bytes 393224 | tf_op jit(solution)/shard_map/ppermute | solution.py:370
  216.8 13.1 %collective-permute-start.35 = (bf16[64,1024]{1,0:T(8,128)(2,1)}, bf16[64,1024]{1,0:T(8,128)(2,1)S(1)}, u32[]{:S(2)}, u32[]{:S(2)}) collective-permute-start(bf16[64,1024]{1,0:T(8,128)(2,1)} %get-tuple-element.55), channel_id=1, source_target_pairs={{0,16},{8,24},{16,0},{24,8},{1,17},{9,25},{17,1},{25,9},{2,18},{10... | collective-permute-start | bytes 393224 | tf_op jit(solution)/shard_map/ppermute | solution.py:370
  217.1 12.8 %collective-permute-start.36 = (bf16[64,1024]{1,0:T(8,128)(2,1)}, bf16[64,1024]{1,0:T(8,128)(2,1)S(1)}, u32[]{:S(2)}, u32[]{:S(2)}) collective-permute-start(bf16[64,1024]{1,0:T(8,128)(2,1)} %get-tuple-element.56), channel_id=1, source_target_pairs={{0,24},{8,0},{16,8},{24,16},{1,25},{9,1},{17,9},{25,17},{2,26},{10... | collective-permute-start | bytes 393224 | tf_op jit(solution)/shard_map/ppermute | solution.py:370
  225.3 4.6 %copy-start.23 = (bf16[64,1024]{1,0:T(8,128)(2,1)}, bf16[64,1024]{1,0:T(8,128)(2,1)S(1)}, u32[]{:S(2)}) copy-start(bf16[64,1024]{1,0:T(8,128)(2,1)S(1)} %collective-permute-done.34.refs_1_) | copy-start | bytes 393220
  (8 other events, 5.8 us)

commit v3 on v2

--- a/solution.py
+++ b/solution.py
@@ -249,11 +249,11 @@
 BY_ROWS = (((0,), (0,)), ((), ()))
 
 
-def _call(kernel, out_shape, flops, moved, **kw):
+def _call(kernel, out_shape, flops, moved, grant=24, **kw):
     return pl.pallas_call(
         kernel,
         out_shape=out_shape,
-        compiler_params=pltpu.CompilerParams(vmem_limit_bytes=58 * 1024 * 1024),
+        compiler_params=pltpu.CompilerParams(vmem_limit_bytes=grant * 1024 * 1024),
         cost_estimate=pl.CostEstimate(flops=flops, bytes_accessed=moved, transcendentals=0),
         **kw,
     )
@@ -263,6 +263,23 @@
     return pltpu.PrefetchScalarGridSpec(
         num_scalar_prefetch=scalars, grid=grid, in_specs=in_specs, out_specs=out_specs, scratch_shapes=scratch
     )
+
+
+def message_kernel(place_ref, x_ref, fade_ref, out_ref):
+    rows, wide = out_ref.shape
+    half_model = x_ref.shape[1]
+    at = pl.ds(pl.multiple_of(place_ref[1] * rows, rows), rows)
+    out_ref[:, :half_model] = x_ref[at, :]
+    out_ref[:, half_model:] = jnp.concatenate(
+        [_parts(fade_ref[at, :]), jnp.zeros((rows, wide - half_model - 3 * fade_ref.shape[1]), jnp.float32)], axis=1
+    ).astype(out_ref.dtype)
+
+
+def _parts(value):
+    high = value.astype(jnp.bfloat16).astype(jnp.float32)
+    rest = value - high
+    middle = rest.astype(jnp.bfloat16).astype(jnp.float32)
+    return jnp.concatenate([high, middle, rest - middle], axis=1)
 
 
 def norm_kernel(place_ref, x_ref, fade_ref, mate_ref, gain_ref, down_ref, *out_refs):
@@ -271,7 +288,7 @@
     rows, wide = out_refs[0].shape
     half_model = x_ref.shape[1]
     cut = 2 * half_model // pieces
-    fades = fade_ref.shape[1]
+    fades = 3 * fade_ref.shape[1]
     own = x_ref[pl.ds(pl.multiple_of(me * rows, rows), rows), :].astype(jnp.float32)
     mate = mate_ref[:, :half_model].astype(jnp.float32)
     square = jnp.sum(own * own, axis=1, keepdims=True) + jnp.sum(mate * mate, axis=1, keepdims=True)
@@ -280,7 +297,9 @@
     for side, value in ((me, own), (1 - me, mate)):
         start = pl.multiple_of(side * half_model, half_model)
         normed = (value * scale * gain_ref[:, pl.ds(start, half_model)]).astype(jnp.bfloat16)
-        part = jnp.dot(normed, down_ref[pl.ds(start, half_model), :], preferred_element_type=jnp.float32)
+        part = lax.dot_general(
+            normed, down_ref[:, pl.ds(start, half_model)], BY_COLUMNS, preferred_element_type=jnp.float32
+        )
         low_rank = part if low_rank is None else low_rank + part
         for k in range(pieces // 2):
             away = lax.rem(side * (pieces // 2) + k - line + pieces, pieces)
@@ -290,13 +309,13 @@
                 def _():
                     out_ref[:, :cut] = normed[:, k * cut : (k + 1) * cut]
 
-    mine = fade_ref[pl.ds(pl.multiple_of(me * rows, rows), rows), :]
-    theirs = mate_ref[:, half_model : half_model + fades]
+    mine = _parts(fade_ref[pl.ds(pl.multiple_of(me * rows, rows), rows), :])
+    theirs = mate_ref[:, half_model : half_model + fades].astype(jnp.float32)
     tail = jnp.concatenate(
         [
             low_rank.astype(jnp.bfloat16).astype(jnp.float32),
-            jnp.where(me == 0, mine, theirs).astype(jnp.float32),
-            jnp.where(me == 0, theirs, mine).astype(jnp.float32),
+            jnp.where(me == 0, mine, theirs),
+            jnp.where(me == 0, theirs, mine),
             jnp.zeros((rows, wide - cut - low_rank.shape[1] - 2 * fades), jnp.float32),
         ],
         axis=1,
@@ -424,13 +443,14 @@
 
 def partial_kernel(index_ref, mine_ref, theirs_ref, own_ref, other_ref, *rest):
     out_ref = rest[-1]
-    width = own_ref.shape[-1]
     rows = mine_ref.shape[0]
-    for top, x_ref in enumerate((mine_ref, theirs_ref)):
-        for half, weight in enumerate((own_ref, other_ref)):
+    _, depth, width = own_ref.shape
+    for half, source in enumerate((own_ref, other_ref)):
+        weight = source[index_ref[0]]
+        for top, x_ref in enumerate((mine_ref, theirs_ref)):
             at = slice(top * rows, (top + 1) * rows)
             span = slice(half * width, (half + 1) * width)
-            total = jnp.dot(x_ref[...], weight[0], preferred_element_type=jnp.float32)
+            total = jnp.dot(x_ref[:, :depth], weight, preferred_element_type=jnp.float32)
             if len(rest) == 2:
                 total = total + rest[0][at, span].astype(jnp.float32)
             out_ref[at, span] = total.astype(out_ref.dtype)
@@ -440,21 +460,17 @@
     rows = mine.shape[0]
     _, depth, width = own.shape
     operands = [mine, theirs, own, other] + ([] if arrived is None else [arrived])
-    whole = pl.BlockSpec((2 * rows, 2 * width), lambda i, index: (0, 0))
-    tokens = pl.BlockSpec((rows, depth), lambda i, index: (0, 0))
-    block = pl.BlockSpec((1, depth, width), lambda i, index: (index[0], 0, 0))
     return _call(
         partial_kernel,
         jax.ShapeDtypeStruct((2 * rows, 2 * width), jnp.bfloat16),
-        8 * rows * depth * width,
+        160 * rows * depth * width,
         4 * depth * (rows + width),
-        grid_spec=_prefetch(
-            1, (1,), [tokens, tokens, block, block] + ([] if arrived is None else [whole]), whole
-        ),
+        in_specs=[SMEM] + [VMEM] * (len(operands)),
+        out_specs=VMEM,
     )(index, *operands)
 
 
-def decay_kernel(lin, rank, place_ref, mine_ref, theirs_ref, own_ref, other_ref, out_ref):
+def decay_kernel(lin, rank, place_ref, mine_ref, theirs_ref, own_ref, other_ref, *out_refs):
     me, side = place_ref[0], place_ref[1]
     rows = mine_ref.shape[0]
     features = LOOKUP_FEATURES
@@ -462,7 +478,7 @@
         lax.broadcasted_iota(jnp.int32, (SPAN, SPAN), 0) >= lax.broadcasted_iota(jnp.int32, (SPAN, SPAN), 1)
     ).astype(jnp.bfloat16)
     for top, tail_ref in enumerate((mine_ref, theirs_ref)):
-        tail = tail_ref[...]
+        tail = tail_ref[:, tail_ref.shape[1] - features :]
         low_rank = tail[:, :rank]
         parts = [
             tail[:, rank + k * 2 * lin : rank + (k + 1) * 2 * lin].astype(jnp.float32) for k in range(6)
@@ -482,7 +498,8 @@
                 rest = step - high.astype(jnp.float32)
                 middle = rest.astype(jnp.bfloat16)
                 low = (rest - middle.astype(jnp.float32)).astype(jnp.bfloat16)
-                column = (2 * head + owner) * features
+                column = owner * features
+                out_ref = out_refs[head]
                 for span in range(rows // SPAN):
                     cut = slice(span * SPAN, (span + 1) * SPAN)
                     out_ref[top * rows + span * SPAN : top * rows + (span + 1) * SPAN, column : column + features] = (
@@ -493,19 +510,13 @@
 
 
 def decay_sums(place, lin, rank, mine, theirs, own, other):
-    rows, wide = mine.shape
-    lanes = LOOKUP_FEATURES
-    tail = pl.BlockSpec((rows, lanes), lambda i, place: (0, wide // lanes - 1))
-    whole = lambda shape: pl.BlockSpec(shape, lambda i, place: (0, 0))
-    out = (2 * rows, 2 * lin * LOOKUP_FEATURES)
     return _call(
         functools.partial(decay_kernel, lin, rank),
-        jax.ShapeDtypeStruct(out, jnp.float32),
+        [jax.ShapeDtypeStruct((2 * mine.shape[0], 2 * LOOKUP_FEATURES), jnp.float32)] * lin,
         10**9,
         2**20,
-        grid_spec=_prefetch(
-            1, (1,), [tail, tail, whole(own.shape), whole(other.shape)], whole(out)
-        ),
+        in_specs=[SMEM] + [VMEM] * 4,
+        out_specs=[VMEM] * lin,
     )(place, mine, theirs, own, other)
 
 
@@ -547,20 +558,13 @@
 
 
 def linear_heads(place, lin, head, half, query_key, value, running, own, other, gain):
-    rows, width = query_key.shape
-    whole = lambda a: pl.BlockSpec(a.shape, lambda i, place: (0,) * a.ndim)
-    block = pl.BlockSpec((rows, 2 * LOOKUP_FEATURES), lambda i, place: (0, head))
     return _call(
         functools.partial(linear_kernel, lin, head, half),
-        jax.ShapeDtypeStruct((rows, width), jnp.bfloat16),
+        jax.ShapeDtypeStruct(query_key.shape, jnp.bfloat16),
         2 * 10**9,
         2**21,
-        grid_spec=_prefetch(
-            1,
-            (1,),
-            [whole(query_key), whole(value), block, whole(own), whole(other), whole(gain)],
-            pl.BlockSpec((rows, width), lambda i, place: (0, 0)),
-        ),
+        in_specs=[SMEM] + [VMEM] * 6,
+        out_specs=VMEM,
     )(place, query_key, value, running, own, other, gain)
 
 
@@ -744,15 +748,20 @@
     query_heads = window_query_weight.shape[1] // HD // 2
     groups = query_heads // key_heads
     rank = decay_down_factor.shape[1]
-    swap = lambda value: lax.ppermute(value, "tp", SWAP)
-
-    high = lax.reduce_precision(extra_fading_exponent, 8, 7)
-    rest = extra_fading_exponent - high
-    middle = lax.reduce_precision(rest, 8, 7)
-    fade = jnp.concatenate([high, middle, rest - middle], axis=1).astype(bf16)
-    message = jnp.concatenate([activations, fade], axis=1)
-    message = jnp.pad(message, ((0, 0), (0, LOOKUP_FEATURES - fade.shape[1])))
-    mate = swap(lax.dynamic_slice_in_dim(message, far * half, half, axis=0))
+
+    def swap(value):
+        return lax.ppermute(value, "tp", SWAP)
+
+
+    message = _call(
+        message_kernel,
+        jax.ShapeDtypeStruct((half, half_model + LOOKUP_FEATURES), bf16),
+        10**8,
+        2**20,
+        in_specs=[SMEM, VMEM, VMEM],
+        out_specs=VMEM,
+    )(place, activations, extra_fading_exponent)
+    mate = swap(message)
     wide = 2 * half_model // peers + LOOKUP_FEATURES
     outgoing = _call(
         norm_kernel,
@@ -761,7 +770,7 @@
         2**21,
         in_specs=[SMEM] + [VMEM] * 5,
         out_specs=[VMEM] * peers,
-    )(place, activations, fade, mate, input_norm_gain.reshape(1, -1), decay_down_factor)
+    )(place, activations, extra_fading_exponent, mate, input_norm_gain.reshape(1, -1), decay_down_factor.T)
 
     (
         outgoing,
@@ -854,7 +863,7 @@
                 half,
                 finals[first],
                 finals[first + 1],
-                running,
+                running[head],
                 starting_state,
                 other_state,
                 linear_head_gain.reshape(1, DV),
@@ -862,24 +871,41 @@
         )
 
     pieces = len(attended)
-    held = []
-    for piece in range(pieces):
-        seen = [attended[piece]]
-        for hop in range(hops):
-            if piece < pieces - 1:
-                seen.append(lax.ppermute(seen[-1], ("sp", "tp"), _pairs(peers, [hop], 1)))
-            else:
-                last = hops - hop
-                straight = [(hops * 2, (hops - last) * 2), (1, last * 2 + 1)]
-                seen.insert(1, lax.ppermute(seen[0], ("sp", "tp"), straight))
-        held.append(seen)
-    table = lambda count: tuple(tuple(range(k * peers, (k + 1) * peers)) for k in range(count))
-    flat = lambda lists: [value for seen in lists for value in seen]
+    chained = pieces - 1
+    passed, back = [], None
+    for step in range(chained + hops):
+        if step == 0:
+            now = attended[0]
+        elif step < chained:
+            now = jnp.where(depth == hops, attended[step], back)
+        else:
+            now = back
+        passed.append(now)
+        depths = [d for d in range(hops) if 0 <= step - d < chained]
+        if depths:
+            back = lax.ppermute(now, ("sp", "tp"), _pairs(peers, depths, 1))
+    straight = [attended[-1]]
+    for far_hop in range(hops, 0, -1):
+        pairs = [(hops * 2, (hops - far_hop) * 2), (1, far_hop * 2 + 1)]
+        straight.insert(1, lax.ppermute(attended[-1], ("sp", "tp"), pairs))
     (terms,) = output_sum(
-        place, flat(held[:key_heads]), table(key_heads), window_output_weight, other_window, None, False
-    )
+        place,
+        passed[: key_heads + hops],
+        tuple(tuple(range(k, k + peers)) for k in range(key_heads)),
+        window_output_weight,
+        other_window,
+        None,
+        False,
+    )
+    late = passed[key_heads:]
     kept, given = output_sum(
-        place, flat(held[key_heads:]), table(lin), linear_output_weight, other_linear, terms, True
+        place,
+        late + straight,
+        tuple(tuple(range(k, k + peers)) for k in range(lin - 1)) + (tuple(len(late) + k for k in range(peers)),),
+        linear_output_weight,
+        other_linear,
+        terms,
+        True,
     )
 
     return spread(place, to_offsets(join(place, kept, swap(given), peers)))

time: 234 us -> 204 us (0.87)
  Pallas kernels: 100 us -> 75 us
  starting transfers between devices: 62.6 us -> 48.2 us
  waiting for transfers between devices: 48.6 us -> 60.5 us
  other arithmetic: 2.8 us -> 0.44 us
    ppermute x20 -> x16, waiting for transfers between devices: 22.5 us -> 40.1 us  [the longest x5 19.1 us: resident(): back = lax.ppermute(now, ('sp', 'tp'), _pairs(peers, depths, 1))]
    ppermute x20 -> x16, starting transfers between devices: 23.8 us -> 9.78 us  [the longest x5 5.41 us: resident(): back = lax.ppermute(now, ('sp', 'tp'), _pairs(peers, depths, 1))]
    pallas_call x2, Pallas kernels: 13 us -> 5.63 us  [pack_items(): _call(functools.partial(pack_kernel, key_heads), jax.ShapeDtypeStruct((co...]
    pallas_call x2, Pallas kernels: 12.2 us -> 6.28 us  [output_sum(): _call(functools.partial(output_kernel, sources), [jax.ShapeDtypeStruct((r...]
    pallas_call x2, Pallas kernels: 9.81 us -> 5.68 us  [linear_heads(): _call(functools.partial(linear_kernel, lin, head, half), jax.ShapeDtypeSt...]
    ppermute x11, waiting for transfers between devices: 8.18 us -> 4.58 us  [resident(): arrived[step] = lax.ppermute(value, ('sp', 'tp'), _pairs(peers, depths, 0))]
    pallas_call x2, Pallas kernels: 9.89 us -> 6.84 us  [window_heads(): _call(functools.partial(window_kernel, group, half), jax.ShapeDtypeStruct...]
    unnamed x72 -> x47, local copies, waits for them, and re-layouts: 14.5 us -> 13.2 us
  transfers between devices with their start and end apart: 37 -> 33, of which waited for: 11 -> 13; matrix products, arithmetic and copies ran while one was open for 2% -> 3% of each run, Pallas kernels for 33% -> 31%
where the time goes in v3:
time: 204 us; the launch traced here: 203 us
  Pallas kernels  75 us (37%)
  waiting for transfers between devices  60.5 us (30%)
  starting transfers between devices  48.2 us (24%)
  local copies, waits for them, and re-layouts  18.3 us (9%)
    pallas_call x13, Pallas kernels, partial_sum(): _call(partial_kernel, jax.ShapeDtypeStruct((2 * rows, 2 * width), jnp.bfl...  40.7 us
    ppermute x11, starting transfers between devices, resident(): arrived[step] = lax.ppermute(value, ('sp', 'tp'), _pairs(peers, depths, 0))  27.9 us
    ppermute x5, waiting for transfers between devices, resident(): back = lax.ppermute(now, ('sp', 'tp'), _pairs(peers, depths, 1))  19.1 us
    ppermute x3, waiting for transfers between devices, resident(): straight.insert(1, lax.ppermute(attended[-1], ('sp', 'tp'), pairs))  17.9 us
    ppermute x6, waiting for transfers between devices, to_offsets(): lax.ppermute(parts[k], 'sp', [(i, (i + k) % peers) for i in range(peers)])  15.8 us
    unnamed x47, local copies, waits for them, and re-layouts  13.2 us
    ppermute x6, starting transfers between devices, to_offsets(): lax.ppermute(parts[k], 'sp', [(i, (i + k) % peers) for i in range(peers)])  10.5 us
    pallas_call x2, Pallas kernels, window_heads(): _call(functools.partial(window_kernel, group, half), jax.ShapeDtypeStruct...  6.84 us
  transfers between devices with their start and end apart: 33, of which 13 were waited for; matrix products, arithmetic and copies ran while one was open for 3% of the time, Pallas kernels for 31%

profile of v3, /device:TPU:0, one launch (start us, length us, event | category | flops | bytes accessed | tf_op | source)
XLA Modules:
  0.0 203.0 jit_solution(12942482646096605981)
XLA Ops:
  0.9 1.0 copy-done.15
  3.1 1.2 collective-permute-done.mate_ref
  4.3 0.9 copy-done.17
  5.9 2.0 shard_map.164
  7.9 1.2 copy-done.5
  9.2 1.2 copy-done.7
  10.4 1.0 copy-done.11
  11.4 1.0 copy-done.13
  12.5 4.0 %shard_map.167 = bf16[7,1024,256]{2,1,0:T(8,128)(2,1)} custom-call(s32[1]{0:T(128)} %bitcast.side_ref, bf16[1024,1024]{1,0:T(8,128)(2,1)S(1)} %copy-done, bf16[1024,256]{1,0:T(8,128)(2,1)S(1)} %copy-done.11, bf16[1024,256]{1,0:T(8,128)(2,1)S(1)} %copy-done.13, bf16[1024,512]{1,0:T(8,128)(2,1)S(1)} %copy-done.5, bf16[1024,512]{1,0:T(8,128)(2,1)S(1)} %copy-done.7, ...), custom_call_target="tpu_custom_call" | custom-call | flops 1000000000 | bytes 7340032 | tf_op jit(solution)/shard_map/pallas_call | solution.py:430
  17.1 2.7 %collective-permute-start.1 = (bf16[64,1152]{1,0:T(8,128)(2,1)}, bf16[64,1152]{1,0:T(8,128)(2,1)S(1)}, u32[]{:S(2)}, u32[]{:S(2)}) collective-permute-start(bf16[64,1152]{1,0:T(8,128)(2,1)} %get-tuple-element.38), channel_id=1, source_target_pairs={{0,8},{8,16},{16,24},{24,0},{1,9},{9,17},{17,25},{25,1},{2,10},{10... | collective-permute-start | bytes 442376 | tf_op jit(solution)/shard_map/ppermute | solution.py:389
  19.8 2.6 %collective-permute-start.2 = (bf16[64,1152]{1,0:T(8,128)(2,1)}, bf16[64,1152]{1,0:T(8,128)(2,1)S(1)}, u32[]{:S(2)}, u32[]{:S(2)}) collective-permute-start(bf16[64,1152]{1,0:T(8,128)(2,1)} %get-tuple-element.39), channel_id=1, source_target_pairs={{0,16},{8,24},{16,0},{24,8},{1,17},{9,25},{17,1},{25,9},{2,18},{10... | collective-permute-start | bytes 442376 | tf_op jit(solution)/shard_map/ppermute | solution.py:389
  22.4 1.3 collective-permute-start.3
  23.9 2.3 %constant_dynamic-slice_fusion.1 = bf16[512,1024]{1,0:T(8,128)(2,1)} fusion(bf16[1024,1024]{1,0:T(8,128)(2,1)} %refs_8_, s32[]{:T(128)S(6)} %select_n.29), kind=kLoop, calls=%fused_computation.7 | loop fusion | bytes 2097156 | tf_op jit(solution)/shard_map/dynamic_slice | solution.py:820
  26.9 6.0 %collective-permute-done.2.refs_2_ = bf16[64,1152]{1,0:T(8,128)(2,1)S(1)} collective-permute-done((bf16[64,1152]{1,0:T(8,128)(2,1)}, bf16[64,1152]{1,0:T(8,128)(2,1)S(1)}, u32[]{:S(2)}, u32[]{:S(2)}) %collective-permute-start.2) | collective-permute-done | bytes 147488 | tf_op jit(solution)/shard_map/ppermute | solution.py:389
  32.8 1.4 shard_map.165
  34.9 2.4 %constant_dynamic-slice_fusion = bf16[512,1024]{1,0:T(8,128)(2,1)} fusion(bf16[1024,1024]{1,0:T(8,128)(2,1)} %refs_5_, s32[]{:T(128)S(6)} %select_n.29), kind=kLoop, calls=%fused_computation.6 | loop fusion | bytes 2097156 | tf_op jit(solution)/shard_map/dynamic_slice | solution.py:822
  37.3 1.2 copy-done.8
  38.6 1.0 copy-done.12
  39.6 1.0 copy-done.14
  40.6 1.6 shard_map.166.own_ref
  42.3 1.9 copy-done.9
  44.4 3.8 %shard_map.179 = (f32[512,256]{1,0:T(8,128)S(1)}, f32[512,256]{1,0:T(8,128)S(1)}) custom-call(s32[4]{0:T(128)S(1)} %pad_add_fusion.place_ref, bf16[256,1152]{1,0:T(8,128)(2,1)} %bitcast.7.mine_ref, bf16[256,1152]{1,0:T(8,128)(2,1)} %bitcast.8.theirs_ref, f32[24,512]{1,0:T(8,128)S(1)} %maximum_maximum_fusion.own_ref, ...), custom_call_target="tpu_custom_call" | custom-call | flops 1000000000 | bytes 1048576 | tf_op jit(solution)/shard_map/pallas_call | solution.py:513
  48.2 3.1 %shard_map.173 = bf16[512,512]{1,0:T(8,128)(2,1)S(1)} custom-call(s32[1]{0:T(128)} %bitcast.18.index_ref, bf16[256,1152]{1,0:T(8,128)(2,1)} %bitcast.7.mine_ref, bf16[256,1152]{1,0:T(8,128)(2,1)} %bitcast.8.theirs_ref, bf16[7,1024,256]{2,1,0:T(8,128)(2,1)S(1)} %copy-done.10, bf16[7,1024,256]{2,1,0:T(8,128)(2,1)} %collective-permute-done.5.other_ref), custom_call_target="tpu_custom_call" | custom-call | flops 10737418240 | bytes 2097152 | tf_op jit(solution)/shard_map/pallas_call | solution.py:463
  51.3 5.6 %collective-permute-start.10 = (bf16[512,512]{1,0:T(8,128)(2,1)S(1)}, bf16[512,512]{1,0:T(8,128)(2,1)S(1)}, u32[]{:S(2)}, u32[]{:S(2)}) collective-permute-start(bf16[512,512]{1,0:T(8,128)(2,1)S(1)} %shard_map.173), channel_id=1, source_target_pairs={{0,8},{25,17},{2,10},{27,19},{4,12},{29,21},{6,14},{31,23}} | collective-permute-start | bytes 1572872 | tf_op jit(solution)/shard_map/ppermute | solution.py:835
  56.9 3.1 %shard_map.168 = bf16[512,512]{1,0:T(8,128)(2,1)S(1)} custom-call(s32[1]{0:T(128)} %bitcast.12.index_ref, bf16[256,1152]{1,0:T(8,128)(2,1)} %bitcast.7.mine_ref, bf16[256,1152]{1,0:T(8,128)(2,1)} %bitcast.8.theirs_ref, bf16[7,1024,256]{2,1,0:T(8,128)(2,1)S(1)} %copy-done.10, bf16[7,1024,256]{2,1,0:T(8,128)(2,1)} %collective-permute-done.5.other_ref), custom_call_target="tpu_custom_call" | custom-call | flops 10737418240 | bytes 2097152 | tf_op jit(solution)/shard_map/pallas_call | solution.py:463
  60.0 1.3 collective-permute-start.6
  61.4 2.2 %collective-permute-done.10.rest_0_ = bf16[512,512]{1,0:T(8,128)(2,1)S(1)} collective-permute-done((bf16[512,512]{1,0:T(8,128)(2,1)S(1)}, bf16[512,512]{1,0:T(8,128)(2,1)S(1)}, u32[]{:S(2)}, u32[]{:S(2)}) %collective-permute-start.10) | collective-permute-done | bytes 524320 | tf_op jit(solution)/shard_map/ppermute | solution.py:835
  63.6 3.1 %shard_map.174 = bf16[512,512]{1,0:T(8,128)(2,1)S(1)} custom-call(s32[1]{0:T(128)} %bitcast.17.index_ref, bf16[256,1152]{1,0:T(8,128)(2,1)} %bitcast.7.mine_ref, bf16[256,1152]{1,0:T(8,128)(2,1)} %bitcast.8.theirs_ref, bf16[7,1024,256]{2,1,0:T(8,128)(2,1)S(1)} %copy-done.10, bf16[7,1024,256]{2,1,0:T(8,128)(2,1)} %collective-permute-done.5.other_ref, ...), custom_call_target="tpu_custom_call" | custom-call | flops 10737418240 | bytes 2097152 | tf_op jit(solution)/shard_map/pallas_call | solution.py:463
  66.7 4.4 %collective-permute-start.11 = (bf16[512,512]{1,0:T(8,128)(2,1)S(1)}, bf16[512,512]{1,0:T(8,128)(2,1)S(1)}, u32[]{:S(2)}, u32[]{:S(2)}) collective-permute-start(bf16[512,512]{1,0:T(8,128)(2,1)S(1)} %shard_map.174), channel_id=1, source_target_pairs={{0,8},{25,17},{8,16},{17,9},{2,10},{27,19},{10,18},{19,11},{4,12},... | collective-permute-start | bytes 1572872 | tf_op jit(solution)/shard_map/ppermute | solution.py:835
  71.1 3.1 %shard_map.169 = bf16[512,512]{1,0:T(8,128)(2,1)S(1)} custom-call(s32[1]{0:T(128)} %bitcast.11.index_ref, bf16[256,1152]{1,0:T(8,128)(2,1)} %bitcast.7.mine_ref, bf16[256,1152]{1,0:T(8,128)(2,1)} %bitcast.8.theirs_ref, bf16[7,1024,256]{2,1,0:T(8,128)(2,1)S(1)} %copy-done.10, bf16[7,1024,256]{2,1,0:T(8,128)(2,1)} %collective-permute-done.5.other_ref, ...), custom_call_target="tpu_custom_call" | custom-call | flops 10737418240 | bytes 2097152 | tf_op jit(solution)/shard_map/pallas_call | solution.py:463
  74.3 2.5 %collective-permute-start.7 = (bf16[512,512]{1,0:T(8,128)(2,1)S(1)}, bf16[512,512]{1,0:T(8,128)(2,1)S(1)}, u32[]{:S(2)}, u32[]{:S(2)}) collective-permute-start(bf16[512,512]{1,0:T(8,128)(2,1)S(1)} %shard_map.169), channel_id=1, source_target_pairs={{0,8},{25,17},{8,16},{17,9},{2,10},{27,19},{10,18},{19,11},{4,12},... | collective-permute-start | bytes 1572872 | tf_op jit(solution)/shard_map/ppermute | solution.py:835
  76.7 1.0 collective-permute-done.11.rest_0_
  77.8 3.1 %shard_map.175 = bf16[512,512]{1,0:T(8,128)(2,1)S(1)} custom-call(s32[1]{0:T(128)} %bitcast.16.index_ref, bf16[256,1152]{1,0:T(8,128)(2,1)} %bitcast.7.mine_ref, bf16[256,1152]{1,0:T(8,128)(2,1)} %bitcast.8.theirs_ref, bf16[7,1024,256]{2,1,0:T(8,128)(2,1)S(1)} %copy-done.10, bf16[7,1024,256]{2,1,0:T(8,128)(2,1)} %collective-permute-done.5.other_ref, ...), custom_call_target="tpu_custom_call" | custom-call | flops 10737418240 | bytes 2097152 | tf_op jit(solution)/shard_map/pallas_call | solution.py:463
  80.9 4.4 %collective-permute-start.12 = (bf16[512,512]{1,0:T(8,128)(2,1)S(1)}, bf16[512,512]{1,0:T(8,128)(2,1)S(1)}, u32[]{:S(2)}, u32[]{:S(2)}) collective-permute-start(bf16[512,512]{1,0:T(8,128)(2,1)S(1)} %shard_map.175), channel_id=1, source_target_pairs={{0,8},{25,17},{8,16},{17,9},{16,24},{9,1},{2,10},{27,19},{10,18},{... | collective-permute-start | bytes 1572872 | tf_op jit(solution)/shard_map/ppermute | solution.py:835
  85.3 3.1 %shard_map.170 = bf16[512,512]{1,0:T(8,128)(2,1)S(1)} custom-call(s32[1]{0:T(128)} %bitcast.10.index_ref, bf16[256,1152]{1,0:T(8,128)(2,1)} %bitcast.7.mine_ref, bf16[256,1152]{1,0:T(8,128)(2,1)} %bitcast.8.theirs_ref, bf16[7,1024,256]{2,1,0:T(8,128)(2,1)S(1)} %copy-done.10, bf16[7,1024,256]{2,1,0:T(8,128)(2,1)} %collective-permute-done.5.other_ref, ...), custom_call_target="tpu_custom_call" | custom-call | flops 10737418240 | bytes 2097152 | tf_op jit(solution)/shard_map/pallas_call | solution.py:463
  88.5 2.5 %collective-permute-start.8 = (bf16[512,512]{1,0:T(8,128)(2,1)S(1)}, bf16[512,512]{1,0:T(8,128)(2,1)S(1)}, u32[]{:S(2)}, u32[]{:S(2)}) collective-permute-start(bf16[512,512]{1,0:T(8,128)(2,1)S(1)} %shard_map.170), channel_id=1, source_target_pairs={{0,8},{25,17},{8,16},{17,9},{16,24},{9,1},{2,10},{27,19},{10,18},{... | collective-permute-start | bytes 1572872 | tf_op jit(solution)/shard_map/ppermute | solution.py:835
  90.9 1.0 collective-permute-done.12.rest_0_
  92.0 3.1 %shard_map.176.key_value_ref = bf16[512,512]{1,0:T(8,128)(2,1)S(1)} custom-call(s32[1]{0:T(128)} %bitcast.15.index_ref, bf16[256,1152]{1,0:T(8,128)(2,1)} %bitcast.7.mine_ref, bf16[256,1152]{1,0:T(8,128)(2,1)} %bitcast.8.theirs_ref, bf16[7,1024,256]{2,1,0:T(8,128)(2,1)S(1)} %copy-done.10, bf16[7,1024,256]{2,1,0:T(8,128)(2,1)} %collective-permute-done.5.other_ref, ...), custom_call_target="tpu_custom_call" | custom-call | flops 10737418240 | bytes 2097152 | tf_op jit(solution)/shard_map/pallas_call | solution.py:463
  95.1 4.4 %collective-permute-start.13 = (bf16[512,512]{1,0:T(8,128)(2,1)S(1)}, bf16[512,512]{1,0:T(8,128)(2,1)S(1)}, u32[]{:S(2)}, u32[]{:S(2)}) collective-permute-start(bf16[512,512]{1,0:T(8,128)(2,1)S(1)} %shard_map.176.key_value_ref), channel_id=1, source_target_pairs={{0,8},{25,17},{8,16},{17,9},{16,24},{9,1},{2,10},{27,19},{10,18},{... | collective-permute-start | bytes 1572872 | tf_op jit(solution)/shard_map/ppermute | solution.py:835
  99.5 3.1 %shard_map.171.query_ref = bf16[512,512]{1,0:T(8,128)(2,1)S(1)} custom-call(s32[1]{0:T(128)} %bitcast.9.index_ref, bf16[256,1152]{1,0:T(8,128)(2,1)} %bitcast.7.mine_ref, bf16[256,1152]{1,0:T(8,128)(2,1)} %bitcast.8.theirs_ref, bf16[7,1024,256]{2,1,0:T(8,128)(2,1)S(1)} %copy-done.10, bf16[7,1024,256]{2,1,0:T(8,128)(2,1)} %collective-permute-done.5.other_ref, ...), custom_call_target="tpu_custom_call" | custom-call | flops 10737418240 | bytes 2097152 | tf_op jit(solution)/shard_map/pallas_call | solution.py:463
  103.4 2.9 %shard_map.182.refs_0_ = bf16[512,512]{1,0:T(8,128)(2,1)S(1)} custom-call(s32[4]{0:T(128)S(1)} %pad_add_fusion.place_ref, f32[2,4]{1,0:T(2,128)S(1)} %get-tuple-element.63.slope_ref, f32[2,4]{1,0:T(2,128)S(1)} %bitcast.27, bf16[512,512]{1,0:T(8,128)(2,1)S(1)} %shard_map.176.key_value_ref, bf16[512,512]{1,0:T(8,128)(2,1)S(1)} %shard_map.171.query_ref), custom_call_target="tpu_custom_call" | custom-call | flops 2000000000 | bytes 2097152 | tf_op jit(solution)/shard_map/pallas_call | solution.py:641
  106.6 0.9 collective-permute-start.17
  107.5 3.1 %shard_map.177.query_ref = bf16[512,512]{1,0:T(8,128)(2,1)S(1)} custom-call(s32[1]{0:T(128)} %bitcast.14.index_ref, bf16[256,1152]{1,0:T(8,128)(2,1)} %bitcast.7.mine_ref, bf16[256,1152]{1,0:T(8,128)(2,1)} %bitcast.8.theirs_ref, bf16[7,1024,256]{2,1,0:T(8,128)(2,1)S(1)} %copy-done.10, bf16[7,1024,256]{2,1,0:T(8,128)(2,1)} %collective-permute-done.5.other_ref, ...), custom_call_target="tpu_custom_call" | custom-call | flops 10737418240 | bytes 2097152 | tf_op jit(solution)/shard_map/pallas_call | solution.py:463
  110.6 3.9 %shard_map.181 = bf16[512,512]{1,0:T(8,128)(2,1)S(1)} custom-call(s32[4]{0:T(128)S(1)} %pad_add_fusion.place_ref, f32[2,4]{1,0:T(2,128)S(1)} %get-tuple-element.64.slope_ref, f32[2,4]{1,0:T(2,128)S(1)} %bitcast.26, bf16[512,512]{1,0:T(8,128)(2,1)S(1)} %shard_map.176.key_value_ref, bf16[512,512]{1,0:T(8,128)(2,1)S(1)} %shard_map.177.query_ref), custom_call_target="tpu_custom_call" | custom-call | flops 2000000000 | bytes 2097152 | tf_op jit(solution)/shard_map/pallas_call | solution.py:641
  116.0 3.1 %shard_map.172.query_key_ref = bf16[512,512]{1,0:T(8,128)(2,1)S(1)} custom-call(s32[1]{0:T(128)} %bitcast.4.index_ref, bf16[256,1152]{1,0:T(8,128)(2,1)} %bitcast.7.mine_ref, bf16[256,1152]{1,0:T(8,128)(2,1)} %bitcast.8.theirs_ref, bf16[7,1024,256]{2,1,0:T(8,128)(2,1)S(1)} %copy-done.10, bf16[7,1024,256]{2,1,0:T(8,128)(2,1)} %collective-permute-done.5.other_ref, ...), custom_call_target="tpu_custom_call" | custom-call | flops 10737418240 | bytes 2097152 | tf_op jit(solution)/shard_map/pallas_call | solution.py:463
  119.9 3.2 %shard_map.178.value_ref = bf16[512,512]{1,0:T(8,128)(2,1)S(1)} custom-call(s32[1]{0:T(128)} %bitcast.13.index_ref, bf16[256,1152]{1,0:T(8,128)(2,1)} %bitcast.7.mine_ref, bf16[256,1152]{1,0:T(8,128)(2,1)} %bitcast.8.theirs_ref, bf16[7,1024,256]{2,1,0:T(8,128)(2,1)S(1)} %copy-done.10, bf16[7,1024,256]{2,1,0:T(8,128)(2,1)} %collective-permute-done.5.other_ref, ...), custom_call_target="tpu_custom_call" | custom-call | flops 10737418240 | bytes 2097152 | tf_op jit(solution)/shard_map/pallas_call | solution.py:463
  123.8 2.8 %shard_map.180 = bf16[512,512]{1,0:T(8,128)(2,1)S(1)} custom-call(s32[4]{0:T(128)S(1)} %pad_add_fusion.place_ref, bf16[512,512]{1,0:T(8,128)(2,1)S(1)} %shard_map.172.query_key_ref, bf16[512,512]{1,0:T(8,128)(2,1)S(1)} %shard_map.178.value_ref, f32[512,256]{1,0:T(8,128)S(1)} %get-tuple-element.50.running_ref, f32[4,128,256]{2,1,0:T(8,128)S(1)} %copy-done.16, ...), custom_call_target="tpu_custom_call" | custom-call | flops 2000000000 | bytes 2097152 | tf_op jit(solution)/shard_map/pallas_call | solution.py:561
  126.6 1.3 collective-permute-start.19
  127.9 3.1 %shard_map.183.query_key_ref = bf16[512,512]{1,0:T(8,128)(2,1)S(1)} custom-call(s32[1]{0:T(128)} %bitcast.24.index_ref, bf16[256,1152]{1,0:T(8,128)(2,1)} %bitcast.7.mine_ref, bf16[256,1152]{1,0:T(8,128)(2,1)} %bitcast.8.theirs_ref, bf16[7,1024,256]{2,1,0:T(8,128)(2,1)S(1)} %copy-done.10, bf16[7,1024,256]{2,1,0:T(8,128)(2,1)} %collective-permute-done.5.other_ref, ...), custom_call_target="tpu_custom_call" | custom-call | flops 10737418240 | bytes 2097152 | tf_op jit(solution)/shard_map/pallas_call | solution.py:463
  131.1 16.5 %collective-permute-done.19.refs_3_.refs_1_ = bf16[512,512]{1,0:T(8,128)(2,1)S(1)} collective-permute-done((bf16[512,512]{1,0:T(8,128)(2,1)S(1)}, bf16[512,512]{1,0:T(8,128)(2,1)S(1)}, u32[]{:S(2)}, u32[]{:S(2)}) %collective-permute-start.19) | collective-permute-done | bytes 524320 | tf_op jit(solution)/shard_map/ppermute | solution.py:886
  147.6 1.3 collective-permute-start.20
  148.9 3.1 %shard_map.184.value_ref = bf16[512,512]{1,0:T(8,128)(2,1)S(1)} custom-call(s32[1]{0:T(128)} %bitcast.25.index_ref, bf16[256,1152]{1,0:T(8,128)(2,1)} %bitcast.7.mine_ref, bf16[256,1152]{1,0:T(8,128)(2,1)} %bitcast.8.theirs_ref, bf16[7,1024,256]{2,1,0:T(8,128)(2,1)S(1)} %copy-done.10, bf16[7,1024,256]{2,1,0:T(8,128)(2,1)} %collective-permute-done.5.other_ref, ...), custom_call_target="tpu_custom_call" | custom-call | flops 10737418240 | bytes 2097152 | tf_op jit(solution)/shard_map/pallas_call | solution.py:463
  152.1 2.9 %shard_map.185.refs_4_ = bf16[512,512]{1,0:T(8,128)(2,1)S(1)} custom-call(s32[4]{0:T(128)S(1)} %pad_add_fusion.place_ref, bf16[512,512]{1,0:T(8,128)(2,1)S(1)} %shard_map.183.query_key_ref, bf16[512,512]{1,0:T(8,128)(2,1)S(1)} %shard_map.184.value_ref, f32[512,256]{1,0:T(8,128)S(1)} %get-tuple-element.52.running_ref, f32[4,128,256]{2,1,0:T(8,128)S(1)} %copy-done.16, ...), custom_call_target="tpu_custom_call" | custom-call | flops 2000000000 | bytes 2097152 | tf_op jit(solution)/shard_map/pallas_call | solution.py:561
  156.5 1.3 collective-permute-start.26
  157.8 2.6 %collective-permute-done.20.refs_4_.refs_2_ = bf16[512,512]{1,0:T(8,128)(2,1)S(1)} collective-permute-done((bf16[512,512]{1,0:T(8,128)(2,1)S(1)}, bf16[512,512]{1,0:T(8,128)(2,1)S(1)}, u32[]{:S(2)}, u32[]{:S(2)}) %collective-permute-start.20) | collective-permute-done | bytes 524320 | tf_op jit(solution)/shard_map/ppermute | solution.py:886
  160.4 1.3 collective-permute-start.21
  161.7 3.1 %shard_map.186.refs_10_ = f32[512,1024]{1,0:T(8,128)S(1)} custom-call(s32[4]{0:T(128)S(1)} %pad_add_fusion.place_ref, bf16[512,512]{1,0:T(8,128)(2,1)S(1)} %shard_map.182.refs_0_, bf16[512,512]{1,0:T(8,128)(2,1)S(1)} %broadcast_select_fusion.1.refs_1_, bf16[512,512]{1,0:T(8,128)(2,1)S(1)} %broadcast_select_fusion.refs_2_.refs_0_, ...), custom_call_target="tpu_custom_call" | custom-call | flops 1073741824 | bytes 4194304 | tf_op jit(solution)/shard_map/pallas_call | solution.py:698
  164.9 17.9 %collective-permute-done.26.refs_7_ = bf16[512,512]{1,0:T(8,128)(2,1)S(1)} collective-permute-done((bf16[512,512]{1,0:T(8,128)(2,1)S(1)}, bf16[512,512]{1,0:T(8,128)(2,1)S(1)}, u32[]{:S(2)}, u32[]{:S(2)}) %collective-permute-start.26) | collective-permute-done | bytes 524320 | tf_op jit(solution)/shard_map/ppermute | solution.py:890
  182.7 3.2 %shard_map.187 = (bf16[256,1024]{1,0:T(8,128)(2,1)S(1)}, bf16[256,1024]{1,0:T(8,128)(2,1)S(1)}) custom-call(s32[4]{0:T(128)S(1)} %pad_add_fusion.place_ref, bf16[512,512]{1,0:T(8,128)(2,1)S(1)} %broadcast_select_fusion.refs_2_.refs_0_, bf16[512,512]{1,0:T(8,128)(2,1)S(1)} %collective-permute-done.19.refs_3_.refs_1_, ...), custom_call_target="tpu_custom_call" | custom-call | flops 1073741824 | bytes 4194304 | tf_op jit(solution)/shard_map/pallas_call | solution.py:698
  186.0 1.9 collective-permute-done.29.given_ref
  188.7 3.7 %collective-permute-start.32 = (bf16[64,1024]{1,0:T(8,128)(2,1)S(1)}, bf16[64,1024]{1,0:T(8,128)(2,1)S(1)}, u32[]{:S(2)}, u32[]{:S(2)}) collective-permute-start(bf16[64,1024]{1,0:T(8,128)(2,1)S(1)} %get-tuple-element.60), channel_id=1, source_target_pairs={{0,24},{8,0},{16,8},{24,16},{1,25},{9,1},{17,9},{25,17},{2,26},{10... | collective-permute-start | bytes 393224 | tf_op jit(solution)/shard_map/ppermute | solution.py:389
  192.4 4.5 %collective-permute-done.30.refs_1_ = bf16[64,1024]{1,0:T(8,128)(2,1)S(1)} collective-permute-done((bf16[64,1024]{1,0:T(8,128)(2,1)S(1)}, bf16[64,1024]{1,0:T(8,128)(2,1)S(1)}, u32[]{:S(2)}, u32[]{:S(2)}) %collective-permute-start.30) | collective-permute-done | bytes 131104 | tf_op jit(solution)/shard_map/ppermute | solution.py:389
  196.9 4.7 %collective-permute-done.31.refs_2_ = bf16[64,1024]{1,0:T(8,128)(2,1)S(1)} collective-permute-done((bf16[64,1024]{1,0:T(8,128)(2,1)S(1)}, bf16[64,1024]{1,0:T(8,128)(2,1)S(1)}, u32[]{:S(2)}, u32[]{:S(2)}) %collective-permute-start.31) | collective-permute-done | bytes 131104 | tf_op jit(solution)/shard_map/ppermute | solution.py:389
  201.6 1.4 shard_map.189
  (97 shorter events, 11.5 us)
Async XLA Ops:
  0.9 1.0 copy-start.15
  1.9 6.0 %copy-start = (bf16[1024,1024]{1,0:T(8,128)(2,1)S(1)}, bf16[1024,1024]{1,0:T(8,128)(2,1)}, u32[]{:S(2)}) copy-start(bf16[1024,1024]{1,0:T(8,128)(2,1)} %wq.1) | copy-start | bytes 6291460
  1.9 6.0 %copy-start.1 = (bf16[1024,1024]{1,0:T(8,128)(2,1)S(1)}, bf16[1024,1024]{1,0:T(8,128)(2,1)}, u32[]{:S(2)}) copy-start(bf16[1024,1024]{1,0:T(8,128)(2,1)} %lv.1) | copy-start | bytes 6291460
  2.6 1.7 collective-permute-start
  4.3 0.9 copy-start.17
  5.2 0.7 copy-start.18
  7.9 1.2 copy-start.5
  9.2 1.2 copy-start.7
  10.4 1.0 copy-start.11
  11.4 1.0 copy-start.13
  12.5 11.3 %copy-start.22 = (f32[16]{0:T(128)S(1)}, f32[16]{0:T(128)}, u32[]{:S(2)}) copy-start(f32[16]{0:T(128)} %param.30) | copy-start | bytes 196
  12.5 11.3 %copy-start.20 = (bf16[16,512]{1,0:T(8,128)(2,1)S(1)}, bf16[16,512]{1,0:T(8,128)(2,1)}, u32[]{:S(2)}) copy-start(bf16[16,512]{1,0:T(8,128)(2,1)} %param.26) | copy-start | bytes 49156
  12.5 11.3 %copy-start.21 = (f32[512]{0:T(512)S(1)}, f32[512]{0:T(512)}, u32[]{:S(2)}) copy-start(f32[512]{0:T(512)} %param.27) | copy-start | bytes 6148
  16.5 31.6 %collective-permute-start.5 = (bf16[7,1024,256]{2,1,0:T(8,128)(2,1)}, bf16[7,1024,256]{2,1,0:T(8,128)(2,1)}, u32[]{:S(2)}, u32[]{:S(2)}) collective-permute-start(bf16[7,1024,256]{2,1,0:T(8,128)(2,1)} %shard_map.167), channel_id=1, source_target_pairs={{0,1},{1,0},{2,3},{3,2},{4,5},{5,4},{6,7},{7,6},{8,9},{9,8},{10,11... | collective-permute-start | bytes 11010056 | tf_op jit(solution)/shard_map/ppermute | solution.py:753
  17.1 9.7 %collective-permute-start.1 = (bf16[64,1152]{1,0:T(8,128)(2,1)}, bf16[64,1152]{1,0:T(8,128)(2,1)S(1)}, u32[]{:S(2)}, u32[]{:S(2)}) collective-permute-start(bf16[64,1152]{1,0:T(8,128)(2,1)} %get-tuple-element.38), channel_id=1, source_target_pairs={{0,8},{8,16},{16,24},{24,0},{1,9},{9,17},{17,25},{25,1},{2,10},{10... | collective-permute-start | bytes 442376 | tf_op jit(solution)/shard_map/ppermute | solution.py:389
  19.8 13.0 %collective-permute-start.2 = (bf16[64,1152]{1,0:T(8,128)(2,1)}, bf16[64,1152]{1,0:T(8,128)(2,1)S(1)}, u32[]{:S(2)}, u32[]{:S(2)}) collective-permute-start(bf16[64,1152]{1,0:T(8,128)(2,1)} %get-tuple-element.39), channel_id=1, source_target_pairs={{0,16},{8,24},{16,0},{24,8},{1,17},{9,25},{17,1},{25,9},{2,18},{10... | collective-permute-start | bytes 442376 | tf_op jit(solution)/shard_map/ppermute | solution.py:389
  22.4 10.4 %collective-permute-start.3 = (bf16[64,1152]{1,0:T(8,128)(2,1)S(1)}, bf16[64,1152]{1,0:T(8,128)(2,1)S(1)}, u32[]{:S(2)}, u32[]{:S(2)}) collective-permute-start(bf16[64,1152]{1,0:T(8,128)(2,1)S(1)} %get-tuple-element.40), channel_id=1, source_target_pairs={{0,24},{8,0},{16,8},{24,16},{1,25},{9,1},{17,9},{25,17},{2,26},{10... | collective-permute-start | bytes 442376 | tf_op jit(solution)/shard_map/ppermute | solution.py:389
  23.9 20.3 %collective-permute-start.15 = (f32[24,512]{1,0:T(8,128)S(1)}, f32[24,512]{1,0:T(8,128)S(1)}, u32[]{:S(2)}, u32[]{:S(2)}) collective-permute-start(f32[24,512]{1,0:T(8,128)S(1)} %maximum_maximum_fusion.own_ref), channel_id=1, source_target_pairs={{0,1},{1,0},{2,3},{3,2},{4,5},{5,4},{6,7},{7,6},{8,9},{9,8},{10,11... | collective-permute-start | bytes 147464 | tf_op jit(solution)/shard_map/ppermute | solution.py:753
  26.2 11.1 %copy-start.6 = (bf16[1024,512]{1,0:T(8,128)(2,1)S(1)}, bf16[1024,512]{1,0:T(8,128)(2,1)}, u32[]{:S(2)}) copy-start(bf16[1024,512]{1,0:T(8,128)(2,1)} %lq.1) | copy-start | bytes 3145732
  26.9 96.2 %collective-permute-start.16 = (f32[4,128,256]{2,1,0:T(8,128)}, f32[4,128,256]{2,1,0:T(8,128)}, u32[]{:S(2)}, u32[]{:S(2)}) collective-permute-start(f32[4,128,256]{2,1,0:T(8,128)} %own_ref.1), channel_id=1, source_target_pairs={{0,1},{1,0},{2,3},{3,2},{4,5},{5,4},{6,7},{7,6},{8,9},{9,8},{10,11... | collective-permute-start | bytes 1572872 | tf_op jit(solution)/shard_map/ppermute | solution.py:753
  34.3 10.1 %collective-permute-start.4 = (bf16[4,64,1152]{2,1,0:T(8,128)(2,1)}, bf16[4,64,1152]{2,1,0:T(8,128)(2,1)}, u32[]{:S(2)}, u32[]{:S(2)}) collective-permute-start(bf16[4,64,1152]{2,1,0:T(8,128)(2,1)} %shard_map.165), channel_id=1, source_target_pairs={{0,1},{1,0},{2,3},{3,2},{4,5},{5,4},{6,7},{7,6},{8,9},{9,8},{10,11... | collective-permute-start | bytes 1769480 | tf_op jit(solution)/shard_map/ppermute | solution.py:753
  34.4 2.9 %copy-start.2 = (bf16[1024,1024]{1,0:T(8,128)(2,1)S(1)}, bf16[1024,1024]{1,0:T(8,128)(2,1)}, u32[]{:S(2)}) copy-start(bf16[1024,1024]{1,0:T(8,128)(2,1)} %lv.1) | copy-start | bytes 6291460
  34.4 130.4 %collective-permute-start.27 = (bf16[512,1024]{1,0:T(8,128)(2,1)}, bf16[512,1024]{1,0:T(8,128)(2,1)}, u32[]{:S(2)}, u32[]{:S(2)}) collective-permute-start(bf16[512,1024]{1,0:T(8,128)(2,1)} %constant_dynamic-slice_fusion.1), channel_id=1, source_target_pairs={{0,1},{1,0},{2,3},{3,2},{4,5},{5,4},{6,7},{7,6},{8,9},{9,8},{10,11... | collective-permute-start | bytes 3145736 | tf_op jit(solution)/shard_map/ppermute | solution.py:753
  37.3 1.2 copy-start.8
  38.6 1.0 copy-start.12
  39.6 1.0 copy-start.14
  42.3 1.9 copy-start.9
  44.1 112.4 %collective-permute-start.28 = (bf16[512,1024]{1,0:T(8,128)(2,1)}, bf16[512,1024]{1,0:T(8,128)(2,1)}, u32[]{:S(2)}, u32[]{:S(2)}) collective-permute-start(bf16[512,1024]{1,0:T(8,128)(2,1)} %constant_dynamic-slice_fusion), channel_id=1, source_target_pairs={{0,1},{1,0},{2,3},{3,2},{4,5},{5,4},{6,7},{7,6},{8,9},{9,8},{10,11... | collective-permute-start | bytes 3145736 | tf_op jit(solution)/shard_map/ppermute | solution.py:753
  44.3 3.8 %copy-start.10 = (bf16[7,1024,256]{2,1,0:T(8,128)(2,1)S(1)}, bf16[7,1024,256]{2,1,0:T(8,128)(2,1)}, u32[]{:S(2)}) copy-start(bf16[7,1024,256]{2,1,0:T(8,128)(2,1)} %copy-done.9) | copy-start | bytes 11010052
  51.3 12.3 %collective-permute-start.10 = (bf16[512,512]{1,0:T(8,128)(2,1)S(1)}, bf16[512,512]{1,0:T(8,128)(2,1)S(1)}, u32[]{:S(2)}, u32[]{:S(2)}) collective-permute-start(bf16[512,512]{1,0:T(8,128)(2,1)S(1)} %shard_map.173), channel_id=1, source_target_pairs={{0,8},{25,17},{2,10},{27,19},{4,12},{29,21},{6,14},{31,23}} | collective-permute-start | bytes 1572872 | tf_op jit(solution)/shard_map/ppermute | solution.py:835
  60.0 11.1 %collective-permute-start.6 = (bf16[512,512]{1,0:T(8,128)(2,1)S(1)}, bf16[512,512]{1,0:T(8,128)(2,1)S(1)}, u32[]{:S(2)}, u32[]{:S(2)}) collective-permute-start(bf16[512,512]{1,0:T(8,128)(2,1)S(1)} %shard_map.168), channel_id=1, source_target_pairs={{0,8},{25,17},{2,10},{27,19},{4,12},{29,21},{6,14},{31,23}} | collective-permute-start | bytes 1572872 | tf_op jit(solution)/shard_map/ppermute | solution.py:835
  66.7 11.1 %collective-permute-start.11 = (bf16[512,512]{1,0:T(8,128)(2,1)S(1)}, bf16[512,512]{1,0:T(8,128)(2,1)S(1)}, u32[]{:S(2)}, u32[]{:S(2)}) collective-permute-start(bf16[512,512]{1,0:T(8,128)(2,1)S(1)} %shard_map.174), channel_id=1, source_target_pairs={{0,8},{25,17},{8,16},{17,9},{2,10},{27,19},{10,18},{19,11},{4,12},... | collective-permute-start | bytes 1572872 | tf_op jit(solution)/shard_map/ppermute | solution.py:835
  74.3 11.1 %collective-permute-start.7 = (bf16[512,512]{1,0:T(8,128)(2,1)S(1)}, bf16[512,512]{1,0:T(8,128)(2,1)S(1)}, u32[]{:S(2)}, u32[]{:S(2)}) collective-permute-start(bf16[512,512]{1,0:T(8,128)(2,1)S(1)} %shard_map.169), channel_id=1, source_target_pairs={{0,8},{25,17},{8,16},{17,9},{2,10},{27,19},{10,18},{19,11},{4,12},... | collective-permute-start | bytes 1572872 | tf_op jit(solution)/shard_map/ppermute | solution.py:835
  80.9 11.1 %collective-permute-start.12 = (bf16[512,512]{1,0:T(8,128)(2,1)S(1)}, bf16[512,512]{1,0:T(8,128)(2,1)S(1)}, u32[]{:S(2)}, u32[]{:S(2)}) collective-permute-start(bf16[512,512]{1,0:T(8,128)(2,1)S(1)} %shard_map.175), channel_id=1, source_target_pairs={{0,8},{25,17},{8,16},{17,9},{16,24},{9,1},{2,10},{27,19},{10,18},{... | collective-permute-start | bytes 1572872 | tf_op jit(solution)/shard_map/ppermute | solution.py:835
  88.5 11.1 %collective-permute-start.8 = (bf16[512,512]{1,0:T(8,128)(2,1)S(1)}, bf16[512,512]{1,0:T(8,128)(2,1)S(1)}, u32[]{:S(2)}, u32[]{:S(2)}) collective-permute-start(bf16[512,512]{1,0:T(8,128)(2,1)S(1)} %shard_map.170), channel_id=1, source_target_pairs={{0,8},{25,17},{8,16},{17,9},{16,24},{9,1},{2,10},{27,19},{10,18},{... | collective-permute-start | bytes 1572872 | tf_op jit(solution)/shard_map/ppermute | solution.py:835
  95.1 11.5 %collective-permute-start.13 = (bf16[512,512]{1,0:T(8,128)(2,1)S(1)}, bf16[512,512]{1,0:T(8,128)(2,1)S(1)}, u32[]{:S(2)}, u32[]{:S(2)}) collective-permute-start(bf16[512,512]{1,0:T(8,128)(2,1)S(1)} %shard_map.176.key_value_ref), channel_id=1, source_target_pairs={{0,8},{25,17},{8,16},{17,9},{16,24},{9,1},{2,10},{27,19},{10,18},{... | collective-permute-start | bytes 1572872 | tf_op jit(solution)/shard_map/ppermute | solution.py:835
  102.7 12.6 %collective-permute-start.9 = (bf16[512,512]{1,0:T(8,128)(2,1)S(1)}, bf16[512,512]{1,0:T(8,128)(2,1)S(1)}, u32[]{:S(2)}, u32[]{:S(2)}) collective-permute-start(bf16[512,512]{1,0:T(8,128)(2,1)S(1)} %shard_map.171.query_ref), channel_id=1, source_target_pairs={{8,16},{17,9},{16,24},{9,1},{10,18},{19,11},{18,26},{11,3},{12,20}... | collective-permute-start | bytes 1572872 | tf_op jit(solution)/shard_map/ppermute | solution.py:835
  106.6 7.9 %collective-permute-start.17 = (bf16[512,512]{1,0:T(8,128)(2,1)S(1)}, bf16[512,512]{1,0:T(8,128)(2,1)S(1)}, u32[]{:S(2)}, u32[]{:S(2)}) collective-permute-start(bf16[512,512]{1,0:T(8,128)(2,1)S(1)} %shard_map.182.refs_0_), channel_id=1, source_target_pairs={{1,9},{24,16},{3,11},{26,18},{5,13},{28,20},{7,15},{30,22}} | collective-permute-start | bytes 1572872 | tf_op jit(solution)/shard_map/ppermute | solution.py:886
  114.5 4.6 %collective-permute-start.14 = (bf16[512,512]{1,0:T(8,128)(2,1)S(1)}, bf16[512,512]{1,0:T(8,128)(2,1)S(1)}, u32[]{:S(2)}, u32[]{:S(2)}) collective-permute-start(bf16[512,512]{1,0:T(8,128)(2,1)S(1)} %shard_map.177.query_ref), channel_id=1, source_target_pairs={{8,16},{17,9},{16,24},{9,1},{10,18},{19,11},{18,26},{11,3},{12,20}... | collective-permute-start | bytes 1572872 | tf_op jit(solution)/shard_map/ppermute | solution.py:835
  115.3 11.3 %collective-permute-start.18 = (bf16[512,512]{1,0:T(8,128)(2,1)S(1)}, bf16[512,512]{1,0:T(8,128)(2,1)S(1)}, u32[]{:S(2)}, u32[]{:S(2)}) collective-permute-start(bf16[512,512]{1,0:T(8,128)(2,1)S(1)} %broadcast_select_fusion.1.refs_1_), channel_id=1, source_target_pairs={{1,9},{24,16},{9,17},{16,8},{3,11},{26,18},{11,19},{18,10},{5,13},... | collective-permute-start | bytes 1572872 | tf_op jit(solution)/shard_map/ppermute | solution.py:886
  119.2 8.8 %collective-permute-start.22 = (bf16[512,512]{1,0:T(8,128)(2,1)S(1)}, bf16[512,512]{1,0:T(8,128)(2,1)S(1)}, u32[]{:S(2)}, u32[]{:S(2)}) collective-permute-start(bf16[512,512]{1,0:T(8,128)(2,1)S(1)} %shard_map.172.query_key_ref), channel_id=1, source_target_pairs={{16,24},{9,1},{18,26},{11,3},{20,28},{13,5},{22,30},{15,7}} | collective-permute-start | bytes 1572872 | tf_op jit(solution)/shard_map/ppermute | solution.py:835
  119.9 3.9 %copy-start.16 = (f32[4,128,256]{2,1,0:T(8,128)S(1)}, f32[4,128,256]{2,1,0:T(8,128)}, u32[]{:S(2)}) copy-start(f32[4,128,256]{2,1,0:T(8,128)} %own_ref.1) | copy-start | bytes 1572868
  119.9 3.9 %copy-start.19 = (f32[256]{0:T(256)S(1)}, f32[256]{0:T(256)}, u32[]{:S(2)}) copy-start(f32[256]{0:T(256)} %param.31) | copy-start | bytes 3076
  123.1 25.9 %collective-permute-start.23 = (bf16[512,512]{1,0:T(8,128)(2,1)S(1)}, bf16[512,512]{1,0:T(8,128)(2,1)S(1)}, u32[]{:S(2)}, u32[]{:S(2)}) collective-permute-start(bf16[512,512]{1,0:T(8,128)(2,1)S(1)} %shard_map.178.value_ref), channel_id=1, source_target_pairs={{16,24},{9,1},{18,26},{11,3},{20,28},{13,5},{22,30},{15,7}} | collective-permute-start | bytes 1572872 | tf_op jit(solution)/shard_map/ppermute | solution.py:835
  126.6 21.0 %collective-permute-start.19 = (bf16[512,512]{1,0:T(8,128)(2,1)S(1)}, bf16[512,512]{1,0:T(8,128)(2,1)S(1)}, u32[]{:S(2)}, u32[]{:S(2)}) collective-permute-start(bf16[512,512]{1,0:T(8,128)(2,1)S(1)} %broadcast_select_fusion.refs_2_.refs_0_), channel_id=1, source_target_pairs={{1,9},{24,16},{9,17},{16,8},{17,25},{8,0},{3,11},{26,18},{11,19},{... | collective-permute-start | bytes 1572872 | tf_op jit(solution)/shard_map/ppermute | solution.py:886
  147.6 12.8 %collective-permute-start.20 = (bf16[512,512]{1,0:T(8,128)(2,1)S(1)}, bf16[512,512]{1,0:T(8,128)(2,1)S(1)}, u32[]{:S(2)}, u32[]{:S(2)}) collective-permute-start(bf16[512,512]{1,0:T(8,128)(2,1)S(1)} %collective-permute-done.19.refs_3_.refs_1_), channel_id=1, source_target_pairs={{9,17},{16,8},{17,25},{8,0},{11,19},{18,10},{19,27},{10,2},{13,21}... | collective-permute-start | bytes 1572872 | tf_op jit(solution)/shard_map/ppermute | solution.py:886
  152.1 9.6 %copy-start.4 = (bf16[1024,1024]{1,0:T(8,128)(2,1)S(1)}, bf16[1024,1024]{1,0:T(8,128)(2,1)}, u32[]{:S(2)}) copy-start(bf16[1024,1024]{1,0:T(8,128)(2,1)} %refs_5_) | copy-start | bytes 6291460
  155.0 27.7 %copy-start.3 = (bf16[1024,1024]{1,0:T(8,128)(2,1)S(1)}, bf16[1024,1024]{1,0:T(8,128)(2,1)}, u32[]{:S(2)}) copy-start(bf16[1024,1024]{1,0:T(8,128)(2,1)} %refs_8_) | copy-start | bytes 6291460
  155.0 9.8 %collective-permute-start.24 = (bf16[512,512]{1,0:T(8,128)(2,1)S(1)}, bf16[512,512]{1,0:T(8,128)(2,1)S(1)}, u32[]{:S(2)}, u32[]{:S(2)}) collective-permute-start(bf16[512,512]{1,0:T(8,128)(2,1)S(1)} %shard_map.185.refs_4_), channel_id=1, source_target_pairs={{24,16},{1,9},{26,18},{3,11},{28,20},{5,13},{30,22},{7,15}} | collective-permute-start | bytes 1572872 | tf_op jit(solution)/shard_map/ppermute | solution.py:890
  155.8 9.0 %collective-permute-start.25 = (bf16[512,512]{1,0:T(8,128)(2,1)S(1)}, bf16[512,512]{1,0:T(8,128)(2,1)S(1)}, u32[]{:S(2)}, u32[]{:S(2)}) collective-permute-start(bf16[512,512]{1,0:T(8,128)(2,1)S(1)} %shard_map.185.refs_4_), channel_id=1, source_target_pairs={{24,8},{1,17},{26,10},{3,19},{28,12},{5,21},{30,14},{7,23}} | collective-permute-start | bytes 1572872 | tf_op jit(solution)/shard_map/ppermute | solution.py:890
  156.5 26.2 %collective-permute-start.26 = (bf16[512,512]{1,0:T(8,128)(2,1)S(1)}, bf16[512,512]{1,0:T(8,128)(2,1)S(1)}, u32[]{:S(2)}, u32[]{:S(2)}) collective-permute-start(bf16[512,512]{1,0:T(8,128)(2,1)S(1)} %shard_map.185.refs_4_), channel_id=1, source_target_pairs={{24,0},{1,25},{26,2},{3,27},{28,4},{5,29},{30,6},{7,31}} | collective-permute-start | bytes 1572872 | tf_op jit(solution)/shard_map/ppermute | solution.py:890
  160.4 22.3 %collective-permute-start.21 = (bf16[512,512]{1,0:T(8,128)(2,1)S(1)}, bf16[512,512]{1,0:T(8,128)(2,1)S(1)}, u32[]{:S(2)}, u32[]{:S(2)}) collective-permute-start(bf16[512,512]{1,0:T(8,128)(2,1)S(1)} %collective-permute-done.20.refs_4_.refs_2_), channel_id=1, source_target_pairs={{17,25},{8,0},{19,27},{10,2},{21,29},{12,4},{23,31},{14,6}} | collective-permute-start | bytes 1572872 | tf_op jit(solution)/shard_map/ppermute | solution.py:886
  185.9 2.0 collective-permute-start.29
  188.6 8.4 %collective-permute-start.30 = (bf16[64,1024]{1,0:T(8,128)(2,1)S(1)}, bf16[64,1024]{1,0:T(8,128)(2,1)S(1)}, u32[]{:S(2)}, u32[]{:S(2)}) collective-permute-start(bf16[64,1024]{1,0:T(8,128)(2,1)S(1)} %get-tuple-element.58), channel_id=1, source_target_pairs={{0,8},{8,16},{16,24},{24,0},{1,9},{9,17},{17,25},{25,1},{2,10},{10... | collective-permute-start | bytes 393224 | tf_op jit(solution)/shard_map/ppermute | solution.py:389
  188.6 13.0 %collective-permute-start.31 = (bf16[64,1024]{1,0:T(8,128)(2,1)S(1)}, bf16[64,1024]{1,0:T(8,128)(2,1)S(1)}, u32[]{:S(2)}, u32[]{:S(2)}) collective-permute-start(bf16[64,1024]{1,0:T(8,128)(2,1)S(1)} %get-tuple-element.59), channel_id=1, source_target_pairs={{0,16},{8,24},{16,0},{24,8},{1,17},{9,25},{17,1},{25,9},{2,18},{10... | collective-permute-start | bytes 393224 | tf_op jit(solution)/shard_map/ppermute | solution.py:389
  188.7 12.9 %collective-permute-start.32 = (bf16[64,1024]{1,0:T(8,128)(2,1)S(1)}, bf16[64,1024]{1,0:T(8,128)(2,1)S(1)}, u32[]{:S(2)}, u32[]{:S(2)}) collective-permute-start(bf16[64,1024]{1,0:T(8,128)(2,1)S(1)} %get-tuple-element.60), channel_id=1, source_target_pairs={{0,24},{8,0},{16,8},{24,16},{1,25},{9,1},{17,9},{25,17},{2,26},{10... | collective-permute-start | bytes 393224 | tf_op jit(solution)/shard_map/ppermute | solution.py:389

commit v4 on v3

--- a/solution.py
+++ b/solution.py
@@ -390,13 +390,13 @@
     return out
 
 
-def pack_kernel(key_heads, side_ref, wq, wk, wv, lq, lk, lv, out_ref):
+def pack_kernel(key_heads, lin, side_ref, wq, wk, wv, lq, lk, lv, out_ref):
     step = pl.program_id(0)
     half = out_ref.shape[2] // 2
     keys_and_values = step == 0
     queries = (step > 0) & (step <= key_heads)
-    head_items = (step > key_heads) & ((step - key_heads) % 2 == 1)
-    head_values = (step > key_heads) & ((step - key_heads) % 2 == 0)
+    head_items = (step > key_heads) & (step <= key_heads + lin)
+    head_values = step > key_heads + lin
 
     @pl.when(keys_and_values)
     def _():
@@ -425,12 +425,12 @@
     query = pl.BlockSpec(
         (depth, width), lambda i, side: (0, side[0] * key_heads + jnp.clip(i - 1, 0, key_heads - 1))
     )
-    head = lambda i, side: (0, side[0] * lin + jnp.clip((i - 1 - key_heads) // 2, 0, lin - 1))
-    narrow, full = pl.BlockSpec((depth, width // 2), head), pl.BlockSpec((depth, width), head)
+    head = lambda past: lambda i, side: (0, side[0] * lin + jnp.clip(i - 1 - key_heads - past, 0, lin - 1))
+    narrow, full = pl.BlockSpec((depth, width // 2), head(0)), pl.BlockSpec((depth, width), head(lin))
     return _call(
-        functools.partial(pack_kernel, key_heads),
+        functools.partial(pack_kernel, key_heads, lin),
         jax.ShapeDtypeStruct((count, depth, width), jnp.bfloat16),
-        10**9,
+        10**11,
         4 * count * depth * width,
         grid_spec=_prefetch(
             1,
@@ -442,16 +442,20 @@
 
 
 def partial_kernel(index_ref, mine_ref, theirs_ref, own_ref, other_ref, *rest):
-    out_ref = rest[-1]
+    out_ref, weight, arrival = rest[-3:]
     rows = mine_ref.shape[0]
-    _, depth, width = own_ref.shape
-    for half, source in enumerate((own_ref, other_ref)):
-        weight = source[index_ref[0]]
+    depth, width = weight.shape
+    copy = pltpu.make_async_copy(other_ref.at[index_ref[0]], weight, arrival)
+    copy.start()
+    for half in range(2):
+        if half == 1:
+            copy.wait()
         for top, x_ref in enumerate((mine_ref, theirs_ref)):
             at = slice(top * rows, (top + 1) * rows)
             span = slice(half * width, (half + 1) * width)
-            total = jnp.dot(x_ref[:, :depth], weight, preferred_element_type=jnp.float32)
-            if len(rest) == 2:
+            matrix = own_ref[index_ref[0]] if half == 0 else weight[...]
+            total = jnp.dot(x_ref[:, :depth], matrix, preferred_element_type=jnp.float32)
+            if len(rest) == 4:
                 total = total + rest[0][at, span].astype(jnp.float32)
             out_ref[at, span] = total.astype(out_ref.dtype)
 
@@ -465,8 +469,9 @@
         jax.ShapeDtypeStruct((2 * rows, 2 * width), jnp.bfloat16),
         160 * rows * depth * width,
         4 * depth * (rows + width),
-        in_specs=[SMEM] + [VMEM] * (len(operands)),
+        in_specs=[SMEM, VMEM, VMEM, VMEM, ANY] + [VMEM] * (len(operands) - 4),
         out_specs=VMEM,
+        scratch_shapes=[pltpu.VMEM((depth, width), jnp.bfloat16), pltpu.SemaphoreType.DMA],
     )(index, *operands)
 
 
@@ -520,7 +525,7 @@
     )(place, mine, theirs, own, other)
 
 
-def linear_kernel(lin, head, half, place_ref, query_key_ref, value_ref, running_ref, own_ref, other_ref, gain_ref, out_ref):
+def linear_kernel(lin, head, half, place_ref, query_key_ref, value_ref, rest_ref, running_ref, own_ref, other_ref, gain_ref, out_ref):
     me, side = place_ref[0], place_ref[1]
     rows, width = query_key_ref.shape
     features = LOOKUP_FEATURES
@@ -539,7 +544,10 @@
             running = running_ref[at, owner * features : (owner + 1) * features]
             query = query_key_ref[at, base : base + features].astype(jnp.float32)
             key = query_key_ref[at, base + features : base + 2 * features].astype(jnp.float32)
-            value = value_ref[at, base : base + values]
+            value = (
+                value_ref[at, base : base + values].astype(jnp.float32)
+                + rest_ref[at, base : base + values].astype(jnp.float32)
+            ).astype(jnp.bfloat16)
             end = running[SPAN - 1 : SPAN]
             scaled = (query * features ** (-0.5) * jnp.exp(running)).astype(jnp.bfloat16)
             inverse = (key * jnp.exp(-running)).astype(jnp.bfloat16)
@@ -557,15 +565,15 @@
             out_ref[at, base : base + values] = (raw * scale * gain_ref[...]).astype(out_ref.dtype)
 
 
-def linear_heads(place, lin, head, half, query_key, value, running, own, other, gain):
+def linear_heads(place, lin, head, half, query_key, value, rest, running, own, other, gain):
     return _call(
         functools.partial(linear_kernel, lin, head, half),
         jax.ShapeDtypeStruct(query_key.shape, jnp.bfloat16),
         2 * 10**9,
         2**21,
-        in_specs=[SMEM] + [VMEM] * 6,
+        in_specs=[SMEM] + [VMEM] * 7,
         out_specs=VMEM,
-    )(place, query_key, value, running, own, other, gain)
+    )(place, query_key, value, rest, running, own, other, gain)
 
 
 def window_kernel(group, half, place_ref, slope_ref, sink_ref, key_value_ref, query_ref, out_ref):
@@ -817,24 +825,32 @@
     other_small = swap(own_small)
     other_state = swap(starting_state)
     lines = linear_output_weight.shape[0] // 2
-    other_linear = swap(lax.dynamic_slice_in_dim(linear_output_weight, near * lines, lines, axis=0))
+    other_linear = lax.dynamic_slice_in_dim(linear_output_weight, near * lines, lines, axis=0)
+    other_linear = swap(other_linear)
     lines = window_output_weight.shape[0] // 2
-    other_window = swap(lax.dynamic_slice_in_dim(window_output_weight, near * lines, lines, axis=0))
+    other_window = lax.dynamic_slice_in_dim(window_output_weight, near * lines, lines, axis=0)
+    other_window = swap(other_window)
 
     incoming = collect(place, incoming)
     mine = incoming.reshape(peers * half, wide)
     theirs = swap(incoming).reshape(peers * half, wide)
 
     count = 1 + key_heads + 2 * lin
-    arrived, finals = {}, []
-    for step in range(count + 2 * hops):
-        index = jnp.clip(step - 2 * depth, 0, count - 1).astype(jnp.int32).reshape(1)
+    chained = count - lin
+    arrived, sums, direct = {}, [], []
+    for step in range(chained + 2 * hops):
+        turn = step - 2 * depth
+        index = jnp.where(turn >= 0, turn, count + turn)
+        index = jnp.clip(index, 0, count - 1).astype(jnp.int32).reshape(1)
         value = partial_sum(index, mine, theirs, own_in, other_in, arrived.get(step - 2))
-        depths = [d for d in range(hops) if 0 <= step - 2 * d < count]
+        sums.append(value)
+        if chained <= step < count:
+            pairs = [(0, hops * 2), (hops * 2 + 1, 1)]
+            direct.append(lax.ppermute(value, ("sp", "tp"), pairs))
+        depths = [d for d in range(hops) if 0 <= step - 2 * d < chained or (d and -lin <= step - 2 * d < 0)]
         if depths:
             arrived[step] = lax.ppermute(value, ("sp", "tp"), _pairs(peers, depths, 0))
-        if step >= 2 * hops:
-            finals.append(value)
+    finals = sums[2 * hops :]
 
     running = decay_sums(place, lin, rank, mine, theirs, own_small, other_small)
     sinks = jnp.stack(
@@ -854,15 +870,15 @@
             window_heads(place, group, half, slopes, sinks[:, group], finals[0], finals[1 + group])
         )
     for head in range(lin):
-        first = 1 + key_heads + 2 * head
         attended.append(
             linear_heads(
                 place,
                 lin,
                 head,
                 half,
-                finals[first],
-                finals[first + 1],
+                finals[1 + key_heads + head],
+                sums[2 * (hops - 1) + head],
+                direct[head],
                 running[head],
                 starting_state,
                 other_state,
@@ -871,41 +887,24 @@
         )
 
     pieces = len(attended)
-    chained = pieces - 1
-    passed, back = [], None
-    for step in range(chained + hops):
-        if step == 0:
-            now = attended[0]
-        elif step < chained:
-            now = jnp.where(depth == hops, attended[step], back)
-        else:
-            now = back
-        passed.append(now)
-        depths = [d for d in range(hops) if 0 <= step - d < chained]
-        if depths:
-            back = lax.ppermute(now, ("sp", "tp"), _pairs(peers, depths, 1))
-    straight = [attended[-1]]
-    for far_hop in range(hops, 0, -1):
-        pairs = [(hops * 2, (hops - far_hop) * 2), (1, far_hop * 2 + 1)]
-        straight.insert(1, lax.ppermute(attended[-1], ("sp", "tp"), pairs))
+    held = []
+    for piece in range(pieces):
+        seen = [attended[piece]]
+        for hop in range(hops):
+            if piece < pieces - 1:
+                seen.append(lax.ppermute(seen[-1], ("sp", "tp"), _pairs(peers, [hop], 1)))
+            else:
+                last = hops - hop
+                pairs = [(hops * 2, (hops - last) * 2), (1, last * 2 + 1)]
+                seen.insert(1, lax.ppermute(seen[0], ("sp", "tp"), pairs))
+        held.append(seen)
+    table = lambda count: tuple(tuple(range(k * peers, (k + 1) * peers)) for k in range(count))
+    flat = lambda lists: [value for seen in lists for value in seen]
     (terms,) = output_sum(
-        place,
-        passed[: key_heads + hops],
-        tuple(tuple(range(k, k + peers)) for k in range(key_heads)),
-        window_output_weight,
-        other_window,
-        None,
-        False,
-    )
-    late = passed[key_heads:]
+        place, flat(held[:key_heads]), table(key_heads), window_output_weight, other_window, None, False
+    )
     kept, given = output_sum(
-        place,
-        late + straight,
-        tuple(tuple(range(k, k + peers)) for k in range(lin - 1)) + (tuple(len(late) + k for k in range(peers)),),
-        linear_output_weight,
-        other_linear,
-        terms,
-        True,
+        place, flat(held[key_heads:]), table(lin), linear_output_weight, other_linear, terms, True
     )
 
     return spread(place, to_offsets(join(place, kept, swap(given), peers)))

time: 204 us -> 185 us (0.907)
  Pallas kernels: 75 us -> 52.8 us
  starting transfers between devices: 48.2 us -> 69.8 us
  waiting for transfers between devices: 60.5 us -> 45.8 us
  local copies, waits for them, and re-layouts: 18.3 us -> 14.5 us
    pallas_call x13 -> x11, Pallas kernels: 40.7 us -> 20.2 us  [partial_sum(): _call(partial_kernel, jax.ShapeDtypeStruct((2 * rows, 2 * width), jnp.bfl...]
    ppermute x8 -> x14, starting transfers between devices: 8.22 us -> 23.1 us  [the longest x9 12 us: resident(): seen.append(lax.ppermute(seen[-1], ('sp', 'tp'), _pairs(peers, [hop], 1)))]
    ppermute x8, starting transfers between devices: 1.56 us -> 13.9 us  [swap(): return lax.ppermute(value, 'tp', SWAP)]
    ppermute x8 -> x14, waiting for transfers between devices: 37 us -> 27.8 us  [the longest x3 17.7 us: resident(): seen.insert(1, lax.ppermute(seen[0], ('sp', 'tp'), pairs))]
    ppermute x6, waiting for transfers between devices: 15.8 us -> 9.17 us  [to_offsets(): lax.ppermute(parts[k], 'sp', [(i, (i + k) % peers) for i in range(peers)])]
    ppermute x11 -> x9, starting transfers between devices: 27.9 us -> 22 us  [resident(): arrived[step] = lax.ppermute(value, ('sp', 'tp'), _pairs(peers, depths, 0))]
    pallas_call x2, Pallas kernels: 6.28 us -> 3.89 us  [output_sum(): _call(functools.partial(output_kernel, sources), [jax.ShapeDtypeStruct((r...]
    dynamic_slice x1, local copies, waits for them, and re-layouts: 2.39 us -> 0.08 us  [resident(): lax.dynamic_slice_in_dim(window_output_weight, near * lines, lines, axis=0)]
  transfers between devices with their start and end apart: 33 -> 37, of which waited for: 13 -> 11; matrix products, arithmetic and copies ran while one was open for 3% -> 1% of each run, Pallas kernels for 31% -> 25%
where the time goes in v4:
time: 185 us; the launch traced here: 184 us
  starting transfers between devices  69.8 us (38%)
  Pallas kernels  52.8 us (29%)
  waiting for transfers between devices  45.8 us (25%)
  local copies, waits for them, and re-layouts  14.5 us (8%)
    ppermute x9, starting transfers between devices, resident(): arrived[step] = lax.ppermute(value, ('sp', 'tp'), _pairs(peers, depths, 0))  22 us
    pallas_call x11, Pallas kernels, partial_sum(): _call(partial_kernel, jax.ShapeDtypeStruct((2 * rows, 2 * width), jnp.bfl...  20.2 us
    ppermute x3, waiting for transfers between devices, resident(): seen.insert(1, lax.ppermute(seen[0], ('sp', 'tp'), pairs))  17.7 us
    ppermute x8, starting transfers between devices, swap(): return lax.ppermute(value, 'tp', SWAP)  13.9 us
    unnamed x65, local copies, waits for them, and re-layouts  12.1 us
    ppermute x9, starting transfers between devices, resident(): seen.append(lax.ppermute(seen[-1], ('sp', 'tp'), _pairs(peers, [hop], 1)))  12 us
    ppermute x6, starting transfers between devices, to_offsets(): lax.ppermute(parts[k], 'sp', [(i, (i + k) % peers) for i in range(peers)])  10.7 us
    ppermute x9, waiting for transfers between devices, resident(): seen.append(lax.ppermute(seen[-1], ('sp', 'tp'), _pairs(peers, [hop], 1)))  10.1 us
  transfers between devices with their start and end apart: 37, of which 11 were waited for; matrix products, arithmetic and copies ran while one was open for 1% of the time, Pallas kernels for 25%

profile of v4, /device:TPU:0, one launch (start us, length us, event | category | flops | bytes accessed | tf_op | source)
XLA Modules:
  0.0 183.9 jit_solution(4673224806202329883)
XLA Ops:
  0.9 1.0 copy-done.4
  4.3 1.0 copy-done.5
  5.3 0.9 copy-done.20
  7.0 2.0 %shard_map.164 = (bf16[64,1152]{1,0:T(8,128)(2,1)S(1)}, bf16[64,1152]{1,0:T(8,128)(2,1)}, bf16[64,1152]{1,0:T(8,128)(2,1)}, bf16[64,1152]{1,0:T(8,128)(2,1)}) custom-call(s32[4]{0:T(128)S(1)} %pad_add_fusion.place_ref, bf16[128,2048]{1,0:T(8,128)(2,1)S(1)} %copy-done.5, f32[128,4]{1,0:T(8,128)S(1)} %copy.19.fade_ref, ...), custom_call_target="tpu_custom_call" | custom-call | flops 1000000000 | bytes 2097152 | tf_op jit(solution)/shard_map/pallas_call | solution.py:774
  9.0 2.9 %collective-permute-start.1 = (bf16[64,1152]{1,0:T(8,128)(2,1)}, bf16[64,1152]{1,0:T(8,128)(2,1)}, u32[]{:S(2)}, u32[]{:S(2)}) collective-permute-start(bf16[64,1152]{1,0:T(8,128)(2,1)} %get-tuple-element.38), channel_id=1, source_target_pairs={{0,8},{8,16},{16,24},{24,0},{1,9},{9,17},{17,25},{25,1},{2,10},{10... | collective-permute-start | bytes 442376 | tf_op jit(solution)/shard_map/ppermute | solution.py:389
  11.9 2.6 %collective-permute-start.2 = (bf16[64,1152]{1,0:T(8,128)(2,1)}, bf16[64,1152]{1,0:T(8,128)(2,1)}, u32[]{:S(2)}, u32[]{:S(2)}) collective-permute-start(bf16[64,1152]{1,0:T(8,128)(2,1)} %get-tuple-element.39), channel_id=1, source_target_pairs={{0,16},{8,24},{16,0},{24,8},{1,17},{9,25},{17,1},{25,9},{2,18},{10... | collective-permute-start | bytes 442376 | tf_op jit(solution)/shard_map/ppermute | solution.py:389
  14.5 1.4 collective-permute-start.3
  15.9 1.6 copy-done.9
  17.5 1.2 copy-done.11
  18.7 3.9 %shard_map.167 = bf16[7,1024,256]{2,1,0:T(8,128)(2,1)} custom-call(s32[1]{0:T(128)} %bitcast.side_ref, bf16[1024,1024]{1,0:T(8,128)(2,1)S(1)} %copy-done.8, bf16[1024,256]{1,0:T(8,128)(2,1)S(1)} %copy-done.14, bf16[1024,256]{1,0:T(8,128)(2,1)S(1)} %copy-done.15, bf16[1024,512]{1,0:T(8,128)(2,1)S(1)} %copy-done.10, bf16[1024,512]{1,0:T(8,128)(2,1)S(1)} %copy-done.11, ...), custom_call_target="tpu_custom_call" | custom-call | flops 99999997952 | bytes 7340032 | tf_op jit(solution)/shard_map/pallas_call | solution.py:430
  22.8 1.6 shard_map.166.own_ref
  24.4 1.8 copy-done.25
  26.2 1.1 shard_map.165
  28.6 1.6 collective-permute-done.13.other_ref
  30.5 2.9 %shard_map.176 = (f32[512,256]{1,0:T(8,128)S(1)}, f32[512,256]{1,0:T(8,128)S(1)}) custom-call(s32[4]{0:T(128)S(1)} %pad_add_fusion.place_ref, bf16[256,1152]{1,0:T(8,128)(2,1)S(1)} %bitcast.24, bf16[256,1152]{1,0:T(8,128)(2,1)S(1)} %bitcast.38, f32[24,512]{1,0:T(8,128)S(1)} %maximum_maximum_fusion.own_ref, f32[24,512]{1,0:T(8,128)S(1)} %collective-permute-done.13.other_ref), custom_call_target="tpu_custom_call" | custom-call | flops 1000000000 | bytes 1048576 | tf_op jit(solution)/shard_map/pallas_call | solution.py:518
  34.2 1.7 shard_map.173
  35.9 3.4 %collective-permute-start.10 = (bf16[512,512]{1,0:T(8,128)(2,1)S(1)}, bf16[512,512]{1,0:T(8,128)(2,1)S(1)}, u32[]{:S(2)}, u32[]{:S(2)}) collective-permute-start(bf16[512,512]{1,0:T(8,128)(2,1)S(1)} %shard_map.173), channel_id=1, source_target_pairs={{0,8},{25,17},{8,16},{17,9},{2,10},{27,19},{10,18},{19,11},{4,12},... | collective-permute-start | bytes 1572872 | tf_op jit(solution)/shard_map/ppermute | solution.py:852
  39.3 1.7 shard_map.168
  41.0 1.9 %collective-permute-start.6 = (bf16[512,512]{1,0:T(8,128)(2,1)S(1)}, bf16[512,512]{1,0:T(8,128)(2,1)S(1)}, u32[]{:S(2)}, u32[]{:S(2)}) collective-permute-start(bf16[512,512]{1,0:T(8,128)(2,1)S(1)} %shard_map.168), channel_id=1, source_target_pairs={{0,8},{25,17},{8,16},{17,9},{2,10},{27,19},{10,18},{19,11},{4,12},... | collective-permute-start | bytes 1572872 | tf_op jit(solution)/shard_map/ppermute | solution.py:852
  43.0 3.0 %collective-permute-done.10.rest_0_ = bf16[512,512]{1,0:T(8,128)(2,1)S(1)} collective-permute-done((bf16[512,512]{1,0:T(8,128)(2,1)S(1)}, bf16[512,512]{1,0:T(8,128)(2,1)S(1)}, u32[]{:S(2)}, u32[]{:S(2)}) %collective-permute-start.10) | collective-permute-done | bytes 524320 | tf_op jit(solution)/shard_map/ppermute | solution.py:852
  46.0 1.5 shard_map.174
  47.5 4.4 %collective-permute-start.11 = (bf16[512,512]{1,0:T(8,128)(2,1)S(1)}, bf16[512,512]{1,0:T(8,128)(2,1)S(1)}, u32[]{:S(2)}, u32[]{:S(2)}) collective-permute-start(bf16[512,512]{1,0:T(8,128)(2,1)S(1)} %shard_map.174), channel_id=1, source_target_pairs={{0,8},{25,17},{8,16},{17,9},{16,24},{9,1},{2,10},{27,19},{10,18},{... | collective-permute-start | bytes 1572872 | tf_op jit(solution)/shard_map/ppermute | solution.py:852
  51.9 1.5 shard_map.169
  53.5 4.1 %collective-permute-start.7 = (bf16[512,512]{1,0:T(8,128)(2,1)S(1)}, bf16[512,512]{1,0:T(8,128)(2,1)S(1)}, u32[]{:S(2)}, u32[]{:S(2)}) collective-permute-start(bf16[512,512]{1,0:T(8,128)(2,1)S(1)} %shard_map.169), channel_id=1, source_target_pairs={{0,8},{25,17},{8,16},{17,9},{16,24},{9,1},{2,10},{27,19},{10,18},{... | collective-permute-start | bytes 1572872 | tf_op jit(solution)/shard_map/ppermute | solution.py:852
  57.5 1.0 collective-permute-done.11.rest_0_
  58.6 1.5 shard_map.175.value_ref
  60.1 4.4 %collective-permute-start.18 = (bf16[512,512]{1,0:T(8,128)(2,1)S(1)}, bf16[512,512]{1,0:T(8,128)(2,1)S(1)}, u32[]{:S(2)}, u32[]{:S(2)}) collective-permute-start(bf16[512,512]{1,0:T(8,128)(2,1)S(1)} %shard_map.175.value_ref), channel_id=1, source_target_pairs={{0,8},{25,17},{8,16},{17,9},{16,24},{9,1},{2,10},{27,19},{10,18},{... | collective-permute-start | bytes 1572872 | tf_op jit(solution)/shard_map/ppermute | solution.py:852
  64.5 1.5 shard_map.170.value_ref
  66.8 3.6 %collective-permute-start.12 = (bf16[512,512]{1,0:T(8,128)(2,1)S(1)}, bf16[512,512]{1,0:T(8,128)(2,1)S(1)}, u32[]{:S(2)}, u32[]{:S(2)}) collective-permute-start(bf16[512,512]{1,0:T(8,128)(2,1)S(1)} %shard_map.170.value_ref), channel_id=1, source_target_pairs={{0,24},{25,1},{2,26},{27,3},{4,28},{29,5},{6,30},{31,7}} | collective-permute-start | bytes 1572872 | tf_op jit(solution)/shard_map/ppermute | solution.py:849
  71.2 2.4 %shard_map.178.key_value_ref = bf16[512,512]{1,0:T(8,128)(2,1)} custom-call(s32[1]{0:T(128)} %bitcast.21.index_ref, bf16[256,1152]{1,0:T(8,128)(2,1)S(1)} %bitcast.31, bf16[256,1152]{1,0:T(8,128)(2,1)S(1)} %bitcast.45, bf16[7,1024,256]{2,1,0:T(8,128)(2,1)S(1)} %copy-done.26, bf16[7,1024,256]{2,1,0:T(8,128)(2,1)} %collective-permute-done.5.other_ref, ...), custom_call_target="tpu_custom_call" | custom-call | flops 10737418240 | bytes 2097152 | tf_op jit(solution)/shard_map/pallas_call | solution.py:467
  74.3 4.7 %collective-permute-start.21 = (bf16[512,512]{1,0:T(8,128)(2,1)}, bf16[512,512]{1,0:T(8,128)(2,1)}, u32[]{:S(2)}, u32[]{:S(2)}) collective-permute-start(bf16[512,512]{1,0:T(8,128)(2,1)} %shard_map.178.key_value_ref), channel_id=1, source_target_pairs={{0,24},{25,1},{2,26},{27,3},{4,28},{29,5},{6,30},{31,7}} | collective-permute-start | bytes 1572872 | tf_op jit(solution)/shard_map/ppermute | solution.py:849
  79.1 1.5 shard_map.171.query_ref
  80.6 0.9 collective-permute-start.9
  81.5 3.4 %shard_map.182.refs_0_ = bf16[512,512]{1,0:T(8,128)(2,1)S(1)} custom-call(s32[4]{0:T(128)S(1)} %pad_add_fusion.place_ref, f32[2,4]{1,0:T(2,128)S(1)} %get-tuple-element.64.slope_ref, f32[2,4]{1,0:T(2,128)S(1)} %bitcast.37, bf16[512,512]{1,0:T(8,128)(2,1)} %shard_map.178.key_value_ref, bf16[512,512]{1,0:T(8,128)(2,1)S(1)} %shard_map.171.query_ref), custom_call_target="tpu_custom_call" | custom-call | flops 2000000000 | bytes 2097152 | tf_op jit(solution)/shard_map/pallas_call | solution.py:649
  84.9 1.5 collective-permute-start.26
  86.3 2.4 %shard_map.179.query_ref = bf16[512,512]{1,0:T(8,128)(2,1)} custom-call(s32[1]{0:T(128)} %bitcast.20.index_ref, bf16[256,1152]{1,0:T(8,128)(2,1)S(1)} %bitcast.33, bf16[256,1152]{1,0:T(8,128)(2,1)S(1)} %bitcast.47, bf16[7,1024,256]{2,1,0:T(8,128)(2,1)S(1)} %copy-done.26, bf16[7,1024,256]{2,1,0:T(8,128)(2,1)} %collective-permute-done.5.other_ref, ...), custom_call_target="tpu_custom_call" | custom-call | flops 10737418240 | bytes 2097152 | tf_op jit(solution)/shard_map/pallas_call | solution.py:467
  88.8 4.6 %shard_map.183.refs_4_ = bf16[512,512]{1,0:T(8,128)(2,1)S(1)} custom-call(s32[4]{0:T(128)S(1)} %pad_add_fusion.place_ref, f32[2,4]{1,0:T(2,128)S(1)} %get-tuple-element.63.slope_ref, f32[2,4]{1,0:T(2,128)S(1)} %bitcast.36, bf16[512,512]{1,0:T(8,128)(2,1)} %shard_map.178.key_value_ref, bf16[512,512]{1,0:T(8,128)(2,1)} %shard_map.179.query_ref), custom_call_target="tpu_custom_call" | custom-call | flops 2000000000 | bytes 2097152 | tf_op jit(solution)/shard_map/pallas_call | solution.py:649
  93.4 1.5 collective-permute-start.29
  94.9 1.5 shard_map.172.query_key_ref
  96.5 3.6 %shard_map.177.refs_0_ = bf16[512,512]{1,0:T(8,128)(2,1)} custom-call(s32[4]{0:T(128)S(1)} %pad_add_fusion.place_ref, bf16[512,512]{1,0:T(8,128)(2,1)S(1)} %shard_map.172.query_key_ref, bf16[512,512]{1,0:T(8,128)(2,1)S(1)} %shard_map.175.value_ref, bf16[512,512]{1,0:T(8,128)(2,1)S(1)} %collective-permute-done.12.rest_ref, ...), custom_call_target="tpu_custom_call" | custom-call | flops 2000000000 | bytes 2097152 | tf_op jit(solution)/shard_map/pallas_call | solution.py:569
  100.0 1.6 collective-permute-start.15
  101.6 1.5 collective-permute-start.20
  103.1 1.5 collective-permute-start.27
  104.5 1.5 collective-permute-start.30
  106.0 1.4 constant_dynamic-slice_fusion.2
  107.5 12.1 %collective-permute-start.25 = (bf16[512,1024]{1,0:T(8,128)(2,1)S(1)}, bf16[512,1024]{1,0:T(8,128)(2,1)S(1)}, u32[]{:S(2)}, u32[]{:S(2)}) collective-permute-start(bf16[512,1024]{1,0:T(8,128)(2,1)S(1)} %constant_dynamic-slice_fusion.2), channel_id=1, source_target_pairs={{0,1},{1,0},{2,3},{3,2},{4,5},{5,4},{6,7},{7,6},{8,9},{9,8},{10,11... | collective-permute-start | bytes 3145736 | tf_op jit(solution)/shard_map/ppermute | solution.py:761
  120.4 1.3 collective-permute-start.28
  121.7 1.3 collective-permute-start.31
  123.0 2.0 %copy-done.27 = bf16[7,1024,256]{2,1,0:T(8,128)(2,1)S(1)} copy-done((bf16[7,1024,256]{2,1,0:T(8,128)(2,1)S(1)}, bf16[7,1024,256]{2,1,0:T(8,128)(2,1)}, u32[]{:S(2)}) %copy-start.27) | copy-done | bytes 3670040
  125.1 2.9 %shard_map.180.query_key_ref = bf16[512,512]{1,0:T(8,128)(2,1)S(1)} custom-call(s32[1]{0:T(128)} %bitcast.19.index_ref, bf16[256,1152]{1,0:T(8,128)(2,1)S(1)} %bitcast.35, bf16[256,1152]{1,0:T(8,128)(2,1)S(1)} %bitcast.49, bf16[7,1024,256]{2,1,0:T(8,128)(2,1)S(1)} %copy-done.27, bf16[7,1024,256]{2,1,0:T(8,128)(2,1)} %collective-permute-done.5.other_ref, ...), custom_call_target="tpu_custom_call" | custom-call | flops 10737418240 | bytes 2097152 | tf_op jit(solution)/shard_map/pallas_call | solution.py:467
  128.0 3.0 %shard_map.181.refs_4_ = bf16[512,512]{1,0:T(8,128)(2,1)S(1)} custom-call(s32[4]{0:T(128)S(1)} %copy-done.7, bf16[512,512]{1,0:T(8,128)(2,1)S(1)} %shard_map.180.query_key_ref, bf16[512,512]{1,0:T(8,128)(2,1)S(1)} %copy-done.19, bf16[512,512]{1,0:T(8,128)(2,1)} %collective-permute-done.21.rest_ref, f32[512,256]{1,0:T(8,128)S(1)} %copy-done.24, ...), custom_call_target="tpu_custom_call" | custom-call | flops 2000000000 | bytes 2097152 | tf_op jit(solution)/shard_map/pallas_call | solution.py:569
  132.5 5.8 %collective-permute-done.28.refs_3_ = bf16[512,512]{1,0:T(8,128)(2,1)S(1)} collective-permute-done((bf16[512,512]{1,0:T(8,128)(2,1)}, bf16[512,512]{1,0:T(8,128)(2,1)S(1)}, u32[]{:S(2)}, u32[]{:S(2)}) %collective-permute-start.28) | collective-permute-done | bytes 524320 | tf_op jit(solution)/shard_map/ppermute | solution.py:895
  138.3 1.3 collective-permute-start.24
  139.6 4.3 %collective-permute-done.31.refs_7_ = bf16[512,512]{1,0:T(8,128)(2,1)S(1)} collective-permute-done((bf16[512,512]{1,0:T(8,128)(2,1)}, bf16[512,512]{1,0:T(8,128)(2,1)S(1)}, u32[]{:S(2)}, u32[]{:S(2)}) %collective-permute-start.31) | collective-permute-done | bytes 524320 | tf_op jit(solution)/shard_map/ppermute | solution.py:895
  143.9 1.3 collective-permute-start.17
  145.2 1.9 %shard_map.184.refs_10_ = f32[512,1024]{1,0:T(8,128)S(1)} custom-call(s32[4]{0:T(128)S(1)} %copy-done.7, bf16[512,512]{1,0:T(8,128)(2,1)S(1)} %shard_map.182.refs_0_, bf16[512,512]{1,0:T(8,128)(2,1)} %collective-permute-done.26.refs_1_, bf16[512,512]{1,0:T(8,128)(2,1)} %collective-permute-done.27.refs_2_, ...), custom_call_target="tpu_custom_call" | custom-call | flops 1073741824 | bytes 4194304 | tf_op jit(solution)/shard_map/pallas_call | solution.py:706
  147.2 17.7 %collective-permute-done.24.refs_7_ = bf16[512,512]{1,0:T(8,128)(2,1)S(1)} collective-permute-done((bf16[512,512]{1,0:T(8,128)(2,1)S(1)}, bf16[512,512]{1,0:T(8,128)(2,1)S(1)}, u32[]{:S(2)}, u32[]{:S(2)}) %collective-permute-start.24) | collective-permute-done | bytes 524320 | tf_op jit(solution)/shard_map/ppermute | solution.py:899
  164.8 2.0 %shard_map.185 = (bf16[256,1024]{1,0:T(8,128)(2,1)S(1)}, bf16[256,1024]{1,0:T(8,128)(2,1)S(1)}) custom-call(s32[4]{0:T(128)S(1)} %copy-done.7, bf16[512,512]{1,0:T(8,128)(2,1)} %shard_map.177.refs_0_, bf16[512,512]{1,0:T(8,128)(2,1)} %collective-permute-done.15.refs_1_, bf16[512,512]{1,0:T(8,128)(2,1)S(1)} %collective-permute-done.16.refs_2_, ...), custom_call_target="tpu_custom_call" | custom-call | flops 1073741824 | bytes 4194304 | tf_op jit(solution)/shard_map/pallas_call | solution.py:706
  166.9 1.9 %collective-permute-done.33.given_ref = bf16[256,1024]{1,0:T(8,128)(2,1)S(1)} collective-permute-done((bf16[256,1024]{1,0:T(8,128)(2,1)S(1)}, bf16[256,1024]{1,0:T(8,128)(2,1)S(1)}, u32[]{:S(2)}, u32[]{:S(2)}) %collective-permute-start.33) | collective-permute-done | bytes 524320 | tf_op jit(solution)/shard_map/ppermute | solution.py:761
  169.6 1.0 collective-permute-start.35
  170.6 2.8 %collective-permute-start.36 = (bf16[64,1024]{1,0:T(8,128)(2,1)S(1)}, bf16[64,1024]{1,0:T(8,128)(2,1)S(1)}, u32[]{:S(2)}, u32[]{:S(2)}) collective-permute-start(bf16[64,1024]{1,0:T(8,128)(2,1)S(1)} %get-tuple-element.60), channel_id=1, source_target_pairs={{0,24},{8,0},{16,8},{24,16},{1,25},{9,1},{17,9},{25,17},{2,26},{10... | collective-permute-start | bytes 393224 | tf_op jit(solution)/shard_map/ppermute | solution.py:389
  173.4 4.5 %collective-permute-done.34.refs_1_ = bf16[64,1024]{1,0:T(8,128)(2,1)S(1)} collective-permute-done((bf16[64,1024]{1,0:T(8,128)(2,1)S(1)}, bf16[64,1024]{1,0:T(8,128)(2,1)S(1)}, u32[]{:S(2)}, u32[]{:S(2)}) %collective-permute-start.34) | collective-permute-done | bytes 131104 | tf_op jit(solution)/shard_map/ppermute | solution.py:389
  177.8 4.7 %collective-permute-done.35.refs_2_ = bf16[64,1024]{1,0:T(8,128)(2,1)S(1)} collective-permute-done((bf16[64,1024]{1,0:T(8,128)(2,1)S(1)}, bf16[64,1024]{1,0:T(8,128)(2,1)S(1)}, u32[]{:S(2)}, u32[]{:S(2)}) %collective-permute-start.35) | collective-permute-done | bytes 131104 | tf_op jit(solution)/shard_map/ppermute | solution.py:389
  182.5 1.4 shard_map.187
  (119 shorter events, 11.8 us)
Async XLA Ops:
  1.9 94.5 %copy-start.6 = (s32[4]{0:T(128)}, s32[4]{0:T(128)S(1)}, u32[]{:S(2)}) copy-start(s32[4]{0:T(128)S(1)} %pad_add_fusion.place_ref) | copy-start | bytes 52
  1.9 14.0 %copy-start.14 = (bf16[1024,256]{1,0:T(8,128)(2,1)S(1)}, bf16[1024,256]{1,0:T(8,128)(2,1)}, u32[]{:S(2)}) copy-start(bf16[1024,256]{1,0:T(8,128)(2,1)} %wk.1) | copy-start | bytes 1572868
  2.6 1.7 collective-permute-start
  7.0 8.9 %copy-start.8 = (bf16[1024,1024]{1,0:T(8,128)(2,1)S(1)}, bf16[1024,1024]{1,0:T(8,128)(2,1)}, u32[]{:S(2)}) copy-start(bf16[1024,1024]{1,0:T(8,128)(2,1)} %wq.1) | copy-start | bytes 6291460
  7.0 8.9 %copy-start.10 = (bf16[1024,512]{1,0:T(8,128)(2,1)S(1)}, bf16[1024,512]{1,0:T(8,128)(2,1)}, u32[]{:S(2)}) copy-start(bf16[1024,512]{1,0:T(8,128)(2,1)} %lq.1) | copy-start | bytes 3145732
  7.0 8.9 %copy-start.15 = (bf16[1024,256]{1,0:T(8,128)(2,1)S(1)}, bf16[1024,256]{1,0:T(8,128)(2,1)}, u32[]{:S(2)}) copy-start(bf16[1024,256]{1,0:T(8,128)(2,1)} %wv.1) | copy-start | bytes 1572868
  9.0 17.2 %collective-permute-start.1 = (bf16[64,1152]{1,0:T(8,128)(2,1)}, bf16[64,1152]{1,0:T(8,128)(2,1)}, u32[]{:S(2)}, u32[]{:S(2)}) collective-permute-start(bf16[64,1152]{1,0:T(8,128)(2,1)} %get-tuple-element.38), channel_id=1, source_target_pairs={{0,8},{8,16},{16,24},{24,0},{1,9},{9,17},{17,25},{25,1},{2,10},{10... | collective-permute-start | bytes 442376 | tf_op jit(solution)/shard_map/ppermute | solution.py:389
  11.9 14.3 %collective-permute-start.2 = (bf16[64,1152]{1,0:T(8,128)(2,1)}, bf16[64,1152]{1,0:T(8,128)(2,1)}, u32[]{:S(2)}, u32[]{:S(2)}) collective-permute-start(bf16[64,1152]{1,0:T(8,128)(2,1)} %get-tuple-element.39), channel_id=1, source_target_pairs={{0,16},{8,24},{16,0},{24,8},{1,17},{9,25},{17,1},{25,9},{2,18},{10... | collective-permute-start | bytes 442376 | tf_op jit(solution)/shard_map/ppermute | solution.py:389
  14.5 11.7 %collective-permute-start.3 = (bf16[64,1152]{1,0:T(8,128)(2,1)}, bf16[64,1152]{1,0:T(8,128)(2,1)}, u32[]{:S(2)}, u32[]{:S(2)}) collective-permute-start(bf16[64,1152]{1,0:T(8,128)(2,1)} %get-tuple-element.40), channel_id=1, source_target_pairs={{0,24},{8,0},{16,8},{24,16},{1,25},{9,1},{17,9},{25,17},{2,26},{10... | collective-permute-start | bytes 442376 | tf_op jit(solution)/shard_map/ppermute | solution.py:389
  15.9 1.6 copy-start.9
  17.5 1.2 copy-start.11
  22.6 3.5 %copy-start.31 = (f32[16]{0:T(128)S(1)}, f32[16]{0:T(128)}, u32[]{:S(2)}) copy-start(f32[16]{0:T(128)} %param.30) | copy-start | bytes 196
  22.7 3.5 %copy-start.28 = (bf16[16,512]{1,0:T(8,128)(2,1)S(1)}, bf16[16,512]{1,0:T(8,128)(2,1)}, u32[]{:S(2)}) copy-start(bf16[16,512]{1,0:T(8,128)(2,1)} %param.26) | copy-start | bytes 49156
  22.7 5.2 %copy-start.29 = (f32[512]{0:T(512)S(1)}, f32[512]{0:T(512)}, u32[]{:S(2)}) copy-start(f32[512]{0:T(512)} %param.27) | copy-start | bytes 6148
  22.7 5.2 %copy-start.30 = (f32[24]{0:T(128)S(1)}, f32[24]{0:T(128)}, u32[]{:S(2)}) copy-start(f32[24]{0:T(128)} %pad.12.clone) | copy-start | bytes 292
  22.7 5.4 %copy-start.16 = (f32[4,128,256]{2,1,0:T(8,128)S(1)}, f32[4,128,256]{2,1,0:T(8,128)}, u32[]{:S(2)}) copy-start(f32[4,128,256]{2,1,0:T(8,128)} %own_ref.1) | copy-start | bytes 1572868
  22.7 11.6 %collective-permute-start.5 = (bf16[7,1024,256]{2,1,0:T(8,128)(2,1)}, bf16[7,1024,256]{2,1,0:T(8,128)(2,1)}, u32[]{:S(2)}, u32[]{:S(2)}) collective-permute-start(bf16[7,1024,256]{2,1,0:T(8,128)(2,1)} %shard_map.167), channel_id=1, source_target_pairs={{0,1},{1,0},{2,3},{3,2},{4,5},{5,4},{6,7},{7,6},{8,9},{9,8},{10,11... | collective-permute-start | bytes 11010056 | tf_op jit(solution)/shard_map/ppermute | solution.py:761
  24.4 1.8 copy-start.25
  27.4 3.1 %collective-permute-start.4 = (bf16[4,64,1152]{2,1,0:T(8,128)(2,1)S(1)}, bf16[4,64,1152]{2,1,0:T(8,128)(2,1)S(1)}, u32[]{:S(2)}, u32[]{:S(2)}) collective-permute-start(bf16[4,64,1152]{2,1,0:T(8,128)(2,1)S(1)} %shard_map.165), channel_id=1, source_target_pairs={{0,1},{1,0},{2,3},{3,2},{4,5},{5,4},{6,7},{7,6},{8,9},{9,8},{10,11... | collective-permute-start | bytes 1769480 | tf_op jit(solution)/shard_map/ppermute | solution.py:761
  28.0 2.3 %collective-permute-start.13 = (f32[24,512]{1,0:T(8,128)S(1)}, f32[24,512]{1,0:T(8,128)S(1)}, u32[]{:S(2)}, u32[]{:S(2)}) collective-permute-start(f32[24,512]{1,0:T(8,128)S(1)} %maximum_maximum_fusion.own_ref), channel_id=1, source_target_pairs={{0,1},{1,0},{2,3},{3,2},{4,5},{5,4},{6,7},{7,6},{8,9},{9,8},{10,11... | collective-permute-start | bytes 147464 | tf_op jit(solution)/shard_map/ppermute | solution.py:761
  28.0 68.4 %collective-permute-start.14 = (f32[4,128,256]{2,1,0:T(8,128)S(1)}, f32[4,128,256]{2,1,0:T(8,128)}, u32[]{:S(2)}, u32[]{:S(2)}) collective-permute-start(f32[4,128,256]{2,1,0:T(8,128)S(1)} %copy-done.16), channel_id=1, source_target_pairs={{0,1},{1,0},{2,3},{3,2},{4,5},{5,4},{6,7},{7,6},{8,9},{9,8},{10,11... | collective-permute-start | bytes 1572872 | tf_op jit(solution)/shard_map/ppermute | solution.py:761
  30.5 3.8 %copy-start.26 = (bf16[7,1024,256]{2,1,0:T(8,128)(2,1)S(1)}, bf16[7,1024,256]{2,1,0:T(8,128)(2,1)}, u32[]{:S(2)}) copy-start(bf16[7,1024,256]{2,1,0:T(8,128)(2,1)} %copy-done.25) | copy-start | bytes 11010052
  30.5 64.4 %copy-start.12 = (bf16[4,64,1152]{2,1,0:T(8,128)(2,1)}, bf16[4,64,1152]{2,1,0:T(8,128)(2,1)S(1)}, u32[]{:S(2)}) copy-start(bf16[4,64,1152]{2,1,0:T(8,128)(2,1)S(1)} %collective-permute-done.4) | copy-start | bytes 1769476
  35.9 10.1 %collective-permute-start.10 = (bf16[512,512]{1,0:T(8,128)(2,1)S(1)}, bf16[512,512]{1,0:T(8,128)(2,1)S(1)}, u32[]{:S(2)}, u32[]{:S(2)}) collective-permute-start(bf16[512,512]{1,0:T(8,128)(2,1)S(1)} %shard_map.173), channel_id=1, source_target_pairs={{0,8},{25,17},{8,16},{17,9},{2,10},{27,19},{10,18},{19,11},{4,12},... | collective-permute-start | bytes 1572872 | tf_op jit(solution)/shard_map/ppermute | solution.py:852
  41.0 10.9 %collective-permute-start.6 = (bf16[512,512]{1,0:T(8,128)(2,1)S(1)}, bf16[512,512]{1,0:T(8,128)(2,1)S(1)}, u32[]{:S(2)}, u32[]{:S(2)}) collective-permute-start(bf16[512,512]{1,0:T(8,128)(2,1)S(1)} %shard_map.168), channel_id=1, source_target_pairs={{0,8},{25,17},{8,16},{17,9},{2,10},{27,19},{10,18},{19,11},{4,12},... | collective-permute-start | bytes 1572872 | tf_op jit(solution)/shard_map/ppermute | solution.py:852
  47.5 11.1 %collective-permute-start.11 = (bf16[512,512]{1,0:T(8,128)(2,1)S(1)}, bf16[512,512]{1,0:T(8,128)(2,1)S(1)}, u32[]{:S(2)}, u32[]{:S(2)}) collective-permute-start(bf16[512,512]{1,0:T(8,128)(2,1)S(1)} %shard_map.174), channel_id=1, source_target_pairs={{0,8},{25,17},{8,16},{17,9},{16,24},{9,1},{2,10},{27,19},{10,18},{... | collective-permute-start | bytes 1572872 | tf_op jit(solution)/shard_map/ppermute | solution.py:852
  53.5 11.1 %collective-permute-start.7 = (bf16[512,512]{1,0:T(8,128)(2,1)S(1)}, bf16[512,512]{1,0:T(8,128)(2,1)S(1)}, u32[]{:S(2)}, u32[]{:S(2)}) collective-permute-start(bf16[512,512]{1,0:T(8,128)(2,1)S(1)} %shard_map.169), channel_id=1, source_target_pairs={{0,8},{25,17},{8,16},{17,9},{16,24},{9,1},{2,10},{27,19},{10,18},{... | collective-permute-start | bytes 1572872 | tf_op jit(solution)/shard_map/ppermute | solution.py:852
  60.1 11.1 %collective-permute-start.18 = (bf16[512,512]{1,0:T(8,128)(2,1)S(1)}, bf16[512,512]{1,0:T(8,128)(2,1)S(1)}, u32[]{:S(2)}, u32[]{:S(2)}) collective-permute-start(bf16[512,512]{1,0:T(8,128)(2,1)S(1)} %shard_map.175.value_ref), channel_id=1, source_target_pairs={{0,8},{25,17},{8,16},{17,9},{16,24},{9,1},{2,10},{27,19},{10,18},{... | collective-permute-start | bytes 1572872 | tf_op jit(solution)/shard_map/ppermute | solution.py:852
  66.1 7.6 %copy-start.18 = (bf16[512,512]{1,0:T(8,128)(2,1)}, bf16[512,512]{1,0:T(8,128)(2,1)S(1)}, u32[]{:S(2)}) copy-start(bf16[512,512]{1,0:T(8,128)(2,1)S(1)} %shard_map.170.value_ref) | copy-start | bytes 1572868
  66.1 13.0 %collective-permute-start.8 = (bf16[512,512]{1,0:T(8,128)(2,1)S(1)}, bf16[512,512]{1,0:T(8,128)(2,1)S(1)}, u32[]{:S(2)}, u32[]{:S(2)}) collective-permute-start(bf16[512,512]{1,0:T(8,128)(2,1)S(1)} %shard_map.170.value_ref), channel_id=1, source_target_pairs={{8,16},{17,9},{16,24},{9,1},{10,18},{19,11},{18,26},{11,3},{12,20}... | collective-permute-start | bytes 1572872 | tf_op jit(solution)/shard_map/ppermute | solution.py:852
  66.8 29.7 %collective-permute-start.12 = (bf16[512,512]{1,0:T(8,128)(2,1)S(1)}, bf16[512,512]{1,0:T(8,128)(2,1)S(1)}, u32[]{:S(2)}, u32[]{:S(2)}) collective-permute-start(bf16[512,512]{1,0:T(8,128)(2,1)S(1)} %shard_map.170.value_ref), channel_id=1, source_target_pairs={{0,24},{25,1},{2,26},{27,3},{4,28},{29,5},{6,30},{31,7}} | collective-permute-start | bytes 1572872 | tf_op jit(solution)/shard_map/ppermute | solution.py:849
  73.6 11.2 %collective-permute-start.19 = (bf16[512,512]{1,0:T(8,128)(2,1)}, bf16[512,512]{1,0:T(8,128)(2,1)S(1)}, u32[]{:S(2)}, u32[]{:S(2)}) collective-permute-start(bf16[512,512]{1,0:T(8,128)(2,1)} %shard_map.178.key_value_ref), channel_id=1, source_target_pairs={{8,16},{17,9},{16,24},{9,1},{10,18},{19,11},{18,26},{11,3},{12,20}... | collective-permute-start | bytes 1572872 | tf_op jit(solution)/shard_map/ppermute | solution.py:852
  74.3 33.1 %collective-permute-start.21 = (bf16[512,512]{1,0:T(8,128)(2,1)}, bf16[512,512]{1,0:T(8,128)(2,1)}, u32[]{:S(2)}, u32[]{:S(2)}) collective-permute-start(bf16[512,512]{1,0:T(8,128)(2,1)} %shard_map.178.key_value_ref), channel_id=1, source_target_pairs={{0,24},{25,1},{2,26},{27,3},{4,28},{29,5},{6,30},{31,7}} | collective-permute-start | bytes 1572872 | tf_op jit(solution)/shard_map/ppermute | solution.py:849
  80.6 12.8 %collective-permute-start.9 = (bf16[512,512]{1,0:T(8,128)(2,1)S(1)}, bf16[512,512]{1,0:T(8,128)(2,1)S(1)}, u32[]{:S(2)}, u32[]{:S(2)}) collective-permute-start(bf16[512,512]{1,0:T(8,128)(2,1)S(1)} %shard_map.171.query_ref), channel_id=1, source_target_pairs={{16,24},{9,1},{18,26},{11,3},{20,28},{13,5},{22,30},{15,7}} | collective-permute-start | bytes 1572872 | tf_op jit(solution)/shard_map/ppermute | solution.py:852
  84.9 18.2 %collective-permute-start.26 = (bf16[512,512]{1,0:T(8,128)(2,1)S(1)}, bf16[512,512]{1,0:T(8,128)(2,1)}, u32[]{:S(2)}, u32[]{:S(2)}) collective-permute-start(bf16[512,512]{1,0:T(8,128)(2,1)S(1)} %shard_map.182.refs_0_), channel_id=1, source_target_pairs={{1,9},{24,16},{3,11},{26,18},{5,13},{28,20},{7,15},{30,22}} | collective-permute-start | bytes 1572872 | tf_op jit(solution)/shard_map/ppermute | solution.py:895
  93.4 3.0 %copy-start.2 = (bf16[512,512]{1,0:T(8,128)(2,1)}, bf16[512,512]{1,0:T(8,128)(2,1)S(1)}, u32[]{:S(2)}) copy-start(bf16[512,512]{1,0:T(8,128)(2,1)S(1)} %shard_map.183.refs_4_) | copy-start | bytes 1572868
  93.4 11.2 %collective-permute-start.29 = (bf16[512,512]{1,0:T(8,128)(2,1)S(1)}, bf16[512,512]{1,0:T(8,128)(2,1)}, u32[]{:S(2)}, u32[]{:S(2)}) collective-permute-start(bf16[512,512]{1,0:T(8,128)(2,1)S(1)} %shard_map.183.refs_4_), channel_id=1, source_target_pairs={{1,9},{24,16},{3,11},{26,18},{5,13},{28,20},{7,15},{30,22}} | collective-permute-start | bytes 1572872 | tf_op jit(solution)/shard_map/ppermute | solution.py:895
  94.9 1.6 copy-start.22
  100.0 7.4 %copy-start = (bf16[1024,1024]{1,0:T(8,128)(2,1)S(1)}, bf16[1024,1024]{1,0:T(8,128)(2,1)}, u32[]{:S(2)}) copy-start(bf16[1024,1024]{1,0:T(8,128)(2,1)} %refs_8_) | copy-start | bytes 6291460
  100.0 19.6 %collective-permute-start.15 = (bf16[512,512]{1,0:T(8,128)(2,1)}, bf16[512,512]{1,0:T(8,128)(2,1)}, u32[]{:S(2)}, u32[]{:S(2)}) collective-permute-start(bf16[512,512]{1,0:T(8,128)(2,1)} %shard_map.177.refs_0_), channel_id=1, source_target_pairs={{1,9},{24,16},{3,11},{26,18},{5,13},{28,20},{7,15},{30,22}} | collective-permute-start | bytes 1572872 | tf_op jit(solution)/shard_map/ppermute | solution.py:895
  101.6 18.1 %collective-permute-start.20 = (bf16[512,512]{1,0:T(8,128)(2,1)}, bf16[512,512]{1,0:T(8,128)(2,1)}, u32[]{:S(2)}, u32[]{:S(2)}) collective-permute-start(bf16[512,512]{1,0:T(8,128)(2,1)} %shard_map.179.query_ref), channel_id=1, source_target_pairs={{16,24},{9,1},{18,26},{11,3},{20,28},{13,5},{22,30},{15,7}} | collective-permute-start | bytes 1572872 | tf_op jit(solution)/shard_map/ppermute | solution.py:852
  103.1 17.3 %collective-permute-start.27 = (bf16[512,512]{1,0:T(8,128)(2,1)}, bf16[512,512]{1,0:T(8,128)(2,1)}, u32[]{:S(2)}, u32[]{:S(2)}) collective-permute-start(bf16[512,512]{1,0:T(8,128)(2,1)} %collective-permute-done.26.refs_1_), channel_id=1, source_target_pairs={{9,17},{16,8},{11,19},{18,10},{13,21},{20,12},{15,23},{22,14}} | collective-permute-start | bytes 1572872 | tf_op jit(solution)/shard_map/ppermute | solution.py:895
  104.5 17.1 %collective-permute-start.30 = (bf16[512,512]{1,0:T(8,128)(2,1)}, bf16[512,512]{1,0:T(8,128)(2,1)}, u32[]{:S(2)}, u32[]{:S(2)}) collective-permute-start(bf16[512,512]{1,0:T(8,128)(2,1)} %collective-permute-done.29.refs_5_), channel_id=1, source_target_pairs={{9,17},{16,8},{11,19},{18,10},{13,21},{20,12},{15,23},{22,14}} | collective-permute-start | bytes 1572872 | tf_op jit(solution)/shard_map/ppermute | solution.py:895
  106.0 17.0 %copy-start.13 = (bf16[4,64,1152]{2,1,0:T(8,128)(2,1)S(1)}, bf16[4,64,1152]{2,1,0:T(8,128)(2,1)}, u32[]{:S(2)}) copy-start(bf16[4,64,1152]{2,1,0:T(8,128)(2,1)} %copy-done.12) | copy-start | bytes 1769476
  107.5 39.7 %collective-permute-start.25 = (bf16[512,1024]{1,0:T(8,128)(2,1)S(1)}, bf16[512,1024]{1,0:T(8,128)(2,1)S(1)}, u32[]{:S(2)}, u32[]{:S(2)}) collective-permute-start(bf16[512,1024]{1,0:T(8,128)(2,1)S(1)} %constant_dynamic-slice_fusion.2), channel_id=1, source_target_pairs={{0,1},{1,0},{2,3},{3,2},{4,5},{5,4},{6,7},{7,6},{8,9},{9,8},{10,11... | collective-permute-start | bytes 3145736 | tf_op jit(solution)/shard_map/ppermute | solution.py:761
  119.6 11.4 %collective-permute-start.32 = (bf16[512,1024]{1,0:T(8,128)(2,1)S(1)}, bf16[512,1024]{1,0:T(8,128)(2,1)S(1)}, u32[]{:S(2)}, u32[]{:S(2)}) collective-permute-start(bf16[512,1024]{1,0:T(8,128)(2,1)S(1)} %constant_dynamic-slice_fusion), channel_id=1, source_target_pairs={{0,1},{1,0},{2,3},{3,2},{4,5},{5,4},{6,7},{7,6},{8,9},{9,8},{10,11... | collective-permute-start | bytes 3145736 | tf_op jit(solution)/shard_map/ppermute | solution.py:761
  119.7 12.1 %collective-permute-start.16 = (bf16[512,512]{1,0:T(8,128)(2,1)}, bf16[512,512]{1,0:T(8,128)(2,1)S(1)}, u32[]{:S(2)}, u32[]{:S(2)}) collective-permute-start(bf16[512,512]{1,0:T(8,128)(2,1)} %collective-permute-done.15.refs_1_), channel_id=1, source_target_pairs={{9,17},{16,8},{11,19},{18,10},{13,21},{20,12},{15,23},{22,14}} | collective-permute-start | bytes 1572872 | tf_op jit(solution)/shard_map/ppermute | solution.py:895
  120.4 17.9 %collective-permute-start.28 = (bf16[512,512]{1,0:T(8,128)(2,1)}, bf16[512,512]{1,0:T(8,128)(2,1)S(1)}, u32[]{:S(2)}, u32[]{:S(2)}) collective-permute-start(bf16[512,512]{1,0:T(8,128)(2,1)} %collective-permute-done.27.refs_2_), channel_id=1, source_target_pairs={{17,25},{8,0},{19,27},{10,2},{21,29},{12,4},{23,31},{14,6}} | collective-permute-start | bytes 1572872 | tf_op jit(solution)/shard_map/ppermute | solution.py:895
  121.7 22.2 %collective-permute-start.31 = (bf16[512,512]{1,0:T(8,128)(2,1)}, bf16[512,512]{1,0:T(8,128)(2,1)S(1)}, u32[]{:S(2)}, u32[]{:S(2)}) collective-permute-start(bf16[512,512]{1,0:T(8,128)(2,1)} %collective-permute-done.30.refs_6_), channel_id=1, source_target_pairs={{17,25},{8,0},{19,27},{10,2},{21,29},{12,4},{23,31},{14,6}} | collective-permute-start | bytes 1572872 | tf_op jit(solution)/shard_map/ppermute | solution.py:895
  123.0 2.0 %copy-start.27 = (bf16[7,1024,256]{2,1,0:T(8,128)(2,1)S(1)}, bf16[7,1024,256]{2,1,0:T(8,128)(2,1)}, u32[]{:S(2)}) copy-start(bf16[7,1024,256]{2,1,0:T(8,128)(2,1)} %copy-done.25) | copy-start | bytes 11010052
  125.0 2.9 %copy-start.7 = (s32[4]{0:T(128)S(1)}, s32[4]{0:T(128)}, u32[]{:S(2)}) copy-start(s32[4]{0:T(128)} %copy-done.6) | copy-start | bytes 52
  125.0 2.9 %copy-start.17 = (f32[4,128,256]{2,1,0:T(8,128)S(1)}, f32[4,128,256]{2,1,0:T(8,128)}, u32[]{:S(2)}) copy-start(f32[4,128,256]{2,1,0:T(8,128)} %own_ref.1) | copy-start | bytes 1572868
  125.0 2.9 %copy-start.19 = (bf16[512,512]{1,0:T(8,128)(2,1)S(1)}, bf16[512,512]{1,0:T(8,128)(2,1)}, u32[]{:S(2)}) copy-start(bf16[512,512]{1,0:T(8,128)(2,1)} %copy-done.18) | copy-start | bytes 1572868
  125.1 2.9 %copy-start.24 = (f32[512,256]{1,0:T(8,128)S(1)}, f32[512,256]{1,0:T(8,128)}, u32[]{:S(2)}) copy-start(f32[512,256]{1,0:T(8,128)} %copy-done.23) | copy-start | bytes 1572868
  128.0 17.3 %copy-start.3 = (bf16[512,512]{1,0:T(8,128)(2,1)S(1)}, bf16[512,512]{1,0:T(8,128)(2,1)}, u32[]{:S(2)}) copy-start(bf16[512,512]{1,0:T(8,128)(2,1)} %copy-done.2) | copy-start | bytes 1572868
  131.0 33.9 %copy-start.1 = (bf16[1024,1024]{1,0:T(8,128)(2,1)S(1)}, bf16[1024,1024]{1,0:T(8,128)(2,1)}, u32[]{:S(2)}) copy-start(bf16[1024,1024]{1,0:T(8,128)(2,1)} %refs_8_.1) | copy-start | bytes 6291460
  131.0 16.2 %collective-permute-start.22 = (bf16[512,512]{1,0:T(8,128)(2,1)S(1)}, bf16[512,512]{1,0:T(8,128)(2,1)S(1)}, u32[]{:S(2)}, u32[]{:S(2)}) collective-permute-start(bf16[512,512]{1,0:T(8,128)(2,1)S(1)} %shard_map.181.refs_4_), channel_id=1, source_target_pairs={{24,16},{1,9},{26,18},{3,11},{28,20},{5,13},{30,22},{7,15}} | collective-permute-start | bytes 1572872 | tf_op jit(solution)/shard_map/ppermute | solution.py:899
  131.8 15.3 %collective-permute-start.23 = (bf16[512,512]{1,0:T(8,128)(2,1)S(1)}, bf16[512,512]{1,0:T(8,128)(2,1)S(1)}, u32[]{:S(2)}, u32[]{:S(2)}) collective-permute-start(bf16[512,512]{1,0:T(8,128)(2,1)S(1)} %shard_map.181.refs_4_), channel_id=1, source_target_pairs={{24,8},{1,17},{26,10},{3,19},{28,12},{5,21},{30,14},{7,23}} | collective-permute-start | bytes 1572872 | tf_op jit(solution)/shard_map/ppermute | solution.py:899
  138.3 26.5 %collective-permute-start.24 = (bf16[512,512]{1,0:T(8,128)(2,1)S(1)}, bf16[512,512]{1,0:T(8,128)(2,1)S(1)}, u32[]{:S(2)}, u32[]{:S(2)}) collective-permute-start(bf16[512,512]{1,0:T(8,128)(2,1)S(1)} %shard_map.181.refs_4_), channel_id=1, source_target_pairs={{24,0},{1,25},{26,2},{3,27},{28,4},{5,29},{30,6},{7,31}} | collective-permute-start | bytes 1572872 | tf_op jit(solution)/shard_map/ppermute | solution.py:899
  143.9 20.9 %collective-permute-start.17 = (bf16[512,512]{1,0:T(8,128)(2,1)S(1)}, bf16[512,512]{1,0:T(8,128)(2,1)S(1)}, u32[]{:S(2)}, u32[]{:S(2)}) collective-permute-start(bf16[512,512]{1,0:T(8,128)(2,1)S(1)} %collective-permute-done.16.refs_2_), channel_id=1, source_target_pairs={{17,25},{8,0},{19,27},{10,2},{21,29},{12,4},{23,31},{14,6}} | collective-permute-start | bytes 1572872 | tf_op jit(solution)/shard_map/ppermute | solution.py:895
  166.8 2.0 %collective-permute-start.33 = (bf16[256,1024]{1,0:T(8,128)(2,1)S(1)}, bf16[256,1024]{1,0:T(8,128)(2,1)S(1)}, u32[]{:S(2)}, u32[]{:S(2)}) collective-permute-start(bf16[256,1024]{1,0:T(8,128)(2,1)S(1)} %get-tuple-element.56), channel_id=1, source_target_pairs={{0,1},{1,0},{2,3},{3,2},{4,5},{5,4},{6,7},{7,6},{8,9},{9,8},{10,11... | collective-permute-start | bytes 1572872 | tf_op jit(solution)/shard_map/ppermute | solution.py:761
  169.5 8.4 %collective-permute-start.34 = (bf16[64,1024]{1,0:T(8,128)(2,1)S(1)}, bf16[64,1024]{1,0:T(8,128)(2,1)S(1)}, u32[]{:S(2)}, u32[]{:S(2)}) collective-permute-start(bf16[64,1024]{1,0:T(8,128)(2,1)S(1)} %get-tuple-element.58), channel_id=1, source_target_pairs={{0,8},{8,16},{16,24},{24,0},{1,9},{9,17},{17,25},{25,1},{2,10},{10... | collective-permute-start | bytes 393224 | tf_op jit(solution)/shard_map/ppermute | solution.py:389
  169.6 13.0 %collective-permute-start.35 = (bf16[64,1024]{1,0:T(8,128)(2,1)S(1)}, bf16[64,1024]{1,0:T(8,128)(2,1)S(1)}, u32[]{:S(2)}, u32[]{:S(2)}) collective-permute-start(bf16[64,1024]{1,0:T(8,128)(2,1)S(1)} %get-tuple-element.59), channel_id=1, source_target_pairs={{0,16},{8,24},{16,0},{24,8},{1,17},{9,25},{17,1},{25,9},{2,18},{10... | collective-permute-start | bytes 393224 | tf_op jit(solution)/shard_map/ppermute | solution.py:389
  170.6 11.9 %collective-permute-start.36 = (bf16[64,1024]{1,0:T(8,128)(2,1)S(1)}, bf16[64,1024]{1,0:T(8,128)(2,1)S(1)}, u32[]{:S(2)}, u32[]{:S(2)}) collective-permute-start(bf16[64,1024]{1,0:T(8,128)(2,1)S(1)} %get-tuple-element.60), channel_id=1, source_target_pairs={{0,24},{8,0},{16,8},{24,16},{1,25},{9,1},{17,9},{25,17},{2,26},{10... | collective-permute-start | bytes 393224 | tf_op jit(solution)/shard_map/ppermute | solution.py:389
  (5 other events, 4.5 us)

commit v5 on v4

--- a/solution.py
+++ b/solution.py
@@ -390,13 +390,13 @@
     return out
 
 
-def pack_kernel(key_heads, lin, side_ref, wq, wk, wv, lq, lk, lv, out_ref):
+def pack_kernel(key_heads, side_ref, wq, wk, wv, lq, lk, lv, out_ref):
     step = pl.program_id(0)
     half = out_ref.shape[2] // 2
     keys_and_values = step == 0
     queries = (step > 0) & (step <= key_heads)
-    head_items = (step > key_heads) & (step <= key_heads + lin)
-    head_values = step > key_heads + lin
+    head_items = (step > key_heads) & ((step - key_heads) % 2 == 1)
+    head_values = (step > key_heads) & ((step - key_heads) % 2 == 0)
 
     @pl.when(keys_and_values)
     def _():
@@ -425,10 +425,10 @@
     query = pl.BlockSpec(
         (depth, width), lambda i, side: (0, side[0] * key_heads + jnp.clip(i - 1, 0, key_heads - 1))
     )
-    head = lambda past: lambda i, side: (0, side[0] * lin + jnp.clip(i - 1 - key_heads - past, 0, lin - 1))
-    narrow, full = pl.BlockSpec((depth, width // 2), head(0)), pl.BlockSpec((depth, width), head(lin))
+    head = lambda i, side: (0, side[0] * lin + jnp.clip((i - 1 - key_heads) // 2, 0, lin - 1))
+    narrow, full = pl.BlockSpec((depth, width // 2), head), pl.BlockSpec((depth, width), head)
     return _call(
-        functools.partial(pack_kernel, key_heads, lin),
+        functools.partial(pack_kernel, key_heads),
         jax.ShapeDtypeStruct((count, depth, width), jnp.bfloat16),
         10**11,
         4 * count * depth * width,
@@ -525,7 +525,7 @@
     )(place, mine, theirs, own, other)
 
 
-def linear_kernel(lin, head, half, place_ref, query_key_ref, value_ref, rest_ref, running_ref, own_ref, other_ref, gain_ref, out_ref):
+def linear_kernel(lin, head, half, place_ref, query_key_ref, value_ref, running_ref, own_ref, other_ref, gain_ref, out_ref):
     me, side = place_ref[0], place_ref[1]
     rows, width = query_key_ref.shape
     features = LOOKUP_FEATURES
@@ -544,10 +544,7 @@
             running = running_ref[at, owner * features : (owner + 1) * features]
             query = query_key_ref[at, base : base + features].astype(jnp.float32)
             key = query_key_ref[at, base + features : base + 2 * features].astype(jnp.float32)
-            value = (
-                value_ref[at, base : base + values].astype(jnp.float32)
-                + rest_ref[at, base : base + values].astype(jnp.float32)
-            ).astype(jnp.bfloat16)
+            value = value_ref[at, base : base + values]
             end = running[SPAN - 1 : SPAN]
             scaled = (query * features ** (-0.5) * jnp.exp(running)).astype(jnp.bfloat16)
             inverse = (key * jnp.exp(-running)).astype(jnp.bfloat16)
@@ -565,15 +562,15 @@
             out_ref[at, base : base + values] = (raw * scale * gain_ref[...]).astype(out_ref.dtype)
 
 
-def linear_heads(place, lin, head, half, query_key, value, rest, running, own, other, gain):
+def linear_heads(place, lin, head, half, query_key, value, running, own, other, gain):
     return _call(
         functools.partial(linear_kernel, lin, head, half),
         jax.ShapeDtypeStruct(query_key.shape, jnp.bfloat16),
         2 * 10**9,
         2**21,
-        in_specs=[SMEM] + [VMEM] * 7,
+        in_specs=[SMEM] + [VMEM] * 6,
         out_specs=VMEM,
-    )(place, query_key, value, rest, running, own, other, gain)
+    )(place, query_key, value, running, own, other, gain)
 
 
 def window_kernel(group, half, place_ref, slope_ref, sink_ref, key_value_ref, query_ref, out_ref):
@@ -764,7 +761,7 @@
     message = _call(
         message_kernel,
         jax.ShapeDtypeStruct((half, half_model + LOOKUP_FEATURES), bf16),
-        10**8,
+        10**11,
         2**20,
         in_specs=[SMEM, VMEM, VMEM],
         out_specs=VMEM,
@@ -774,7 +771,7 @@
     outgoing = _call(
         norm_kernel,
         [jax.ShapeDtypeStruct((half, wide), bf16)] * peers,
-        10**9,
+        10**11,
         2**21,
         in_specs=[SMEM] + [VMEM] * 5,
         out_specs=[VMEM] * peers,
@@ -836,21 +833,15 @@
     theirs = swap(incoming).reshape(peers * half, wide)
 
     count = 1 + key_heads + 2 * lin
-    chained = count - lin
-    arrived, sums, direct = {}, [], []
-    for step in range(chained + 2 * hops):
-        turn = step - 2 * depth
-        index = jnp.where(turn >= 0, turn, count + turn)
-        index = jnp.clip(index, 0, count - 1).astype(jnp.int32).reshape(1)
+    arrived, finals = {}, []
+    for step in range(count + 2 * hops):
+        index = jnp.clip(step - 2 * depth, 0, count - 1).astype(jnp.int32).reshape(1)
         value = partial_sum(index, mine, theirs, own_in, other_in, arrived.get(step - 2))
-        sums.append(value)
-        if chained <= step < count:
-            pairs = [(0, hops * 2), (hops * 2 + 1, 1)]
-            direct.append(lax.ppermute(value, ("sp", "tp"), pairs))
-        depths = [d for d in range(hops) if 0 <= step - 2 * d < chained or (d and -lin <= step - 2 * d < 0)]
+        depths = [d for d in range(hops) if 0 <= step - 2 * d < count]
         if depths:
             arrived[step] = lax.ppermute(value, ("sp", "tp"), _pairs(peers, depths, 0))
-    finals = sums[2 * hops :]
+        if step >= 2 * hops:
+            finals.append(value)
 
     running = decay_sums(place, lin, rank, mine, theirs, own_small, other_small)
     sinks = jnp.stack(
@@ -876,9 +867,8 @@
                 lin,
                 head,
                 half,
-                finals[1 + key_heads + head],
-                sums[2 * (hops - 1) + head],
-                direct[head],
+                finals[1 + key_heads + 2 * head],
+                finals[2 + key_heads + 2 * head],
                 running[head],
                 starting_state,
                 other_state,

time: 185 us -> 174 us (0.941)
  waiting for transfers between devices: 45.8 us -> 54.5 us
  local copies, waits for them, and re-layouts: 14.5 us -> 5.8 us
  starting transfers between devices: 69.8 us -> 61.3 us
  Pallas kernels: 52.8 us -> 49.8 us
    ppermute x9 -> x11, starting transfers between devices: 22 us -> 31.3 us  [resident(): arrived[step] = lax.ppermute(value, ('sp', 'tp'), _pairs(peers, depths, 0))]
    ppermute x6, waiting for transfers between devices: 9.17 us -> 17.9 us  [to_offsets(): lax.ppermute(parts[k], 'sp', [(i, (i + k) % peers) for i in range(peers)])]
    unnamed x65 -> x49, local copies, waits for them, and re-layouts: 12.1 us -> 3.63 us
    ppermute x2 -> x0, starting transfers between devices: 8.31 us -> none  [resident(): direct.append(lax.ppermute(value, ('sp', 'tp'), pairs))]
    ppermute x8, starting transfers between devices: 13.9 us -> 8.63 us  [swap(): return lax.ppermute(value, 'tp', SWAP)]
    ppermute x9, starting transfers between devices: 12 us -> 8.02 us  [resident(): seen.append(lax.ppermute(seen[-1], ('sp', 'tp'), _pairs(peers, [hop], 1)))]
    ppermute x9 -> x11, waiting for transfers between devices: 4.9 us -> 6.95 us  [resident(): arrived[step] = lax.ppermute(value, ('sp', 'tp'), _pairs(peers, depths, 0))]
    pallas_call x2, Pallas kernels: 6.54 us -> 4.5 us  [linear_heads(): _call(functools.partial(linear_kernel, lin, head, half), jax.ShapeDtypeSt...]
  transfers between devices with their start and end apart: 37 -> 37, of which waited for: 11 -> 13; matrix products, arithmetic and copies ran while one was open for 1% -> 1% of each run, Pallas kernels for 25% -> 22%
where the time goes in v5:
time: 174 us; the launch traced here: 172 us
  starting transfers between devices  61.3 us (35%)
  waiting for transfers between devices  54.5 us (31%)
  Pallas kernels  49.8 us (29%)
  local copies, waits for them, and re-layouts  5.8 us (3%)
    ppermute x11, starting transfers between devices, resident(): arrived[step] = lax.ppermute(value, ('sp', 'tp'), _pairs(peers, depths, 0))  31.3 us
    pallas_call x13, Pallas kernels, partial_sum(): _call(partial_kernel, jax.ShapeDtypeStruct((2 * rows, 2 * width), jnp.bfl...  20 us
    ppermute x6, waiting for transfers between devices, to_offsets(): lax.ppermute(parts[k], 'sp', [(i, (i + k) % peers) for i in range(peers)])  17.9 us
    ppermute x3, waiting for transfers between devices, resident(): seen.insert(1, lax.ppermute(seen[0], ('sp', 'tp'), pairs))  17.3 us
    ppermute x6, starting transfers between devices, to_offsets(): lax.ppermute(parts[k], 'sp', [(i, (i + k) % peers) for i in range(peers)])  10.5 us
    ppermute x9, waiting for transfers between devices, resident(): seen.append(lax.ppermute(seen[-1], ('sp', 'tp'), _pairs(peers, [hop], 1)))  10.1 us
    ppermute x8, starting transfers between devices, swap(): return lax.ppermute(value, 'tp', SWAP)  8.63 us
    ppermute x9, starting transfers between devices, resident(): seen.append(lax.ppermute(seen[-1], ('sp', 'tp'), _pairs(peers, [hop], 1)))  8.02 us
  transfers between devices with their start and end apart: 37, of which 13 were waited for; matrix products, arithmetic and copies ran while one was open for 1% of the time, Pallas kernels for 22%

profile of v5, /device:TPU:0, one launch (start us, length us, event | category | flops | bytes accessed | tf_op | source)
XLA Modules:
  0.0 172.5 jit_solution(11571437311396570105)
XLA Ops:
  0.0 0.8 copy.19.fade_ref
  0.9 1.0 copy-done.10
  4.4 1.3 shard_map.164
  7.4 4.1 %shard_map.167 = bf16[7,1024,256]{2,1,0:T(8,128)(2,1)} custom-call(s32[1]{0:T(128)} %bitcast.side_ref, bf16[1024,1024]{1,0:T(8,128)(2,1)S(1)} %copy-done.6, bf16[1024,256]{1,0:T(8,128)(2,1)S(1)} %copy-done.12, bf16[1024,256]{1,0:T(8,128)(2,1)S(1)} %copy-done.13, bf16[1024,512]{1,0:T(8,128)(2,1)S(1)} %copy-done.8, bf16[1024,512]{1,0:T(8,128)(2,1)S(1)} %copy-done.9, ...), custom_call_target="tpu_custom_call" | custom-call | flops 99999997952 | bytes 7340032 | tf_op jit(solution)/shard_map/pallas_call | solution.py:430
  12.0 1.6 shard_map.166.own_ref
  13.6 2.7 %collective-permute-start.1 = (bf16[64,1152]{1,0:T(8,128)(2,1)S(1)}, bf16[64,1152]{1,0:T(8,128)(2,1)S(1)}, u32[]{:S(2)}, u32[]{:S(2)}) collective-permute-start(bf16[64,1152]{1,0:T(8,128)(2,1)S(1)} %get-tuple-element.38), channel_id=1, source_target_pairs={{0,8},{8,16},{16,24},{24,0},{1,9},{9,17},{17,25},{25,1},{2,10},{10... | collective-permute-start | bytes 442376 | tf_op jit(solution)/shard_map/ppermute | solution.py:389
  16.3 2.6 %collective-permute-start.2 = (bf16[64,1152]{1,0:T(8,128)(2,1)S(1)}, bf16[64,1152]{1,0:T(8,128)(2,1)S(1)}, u32[]{:S(2)}, u32[]{:S(2)}) collective-permute-start(bf16[64,1152]{1,0:T(8,128)(2,1)S(1)} %get-tuple-element.39), channel_id=1, source_target_pairs={{0,16},{8,24},{16,0},{24,8},{1,17},{9,25},{17,1},{25,9},{2,18},{10... | collective-permute-start | bytes 442376 | tf_op jit(solution)/shard_map/ppermute | solution.py:389
  18.9 1.3 collective-permute-start.3
  20.4 2.7 %collective-permute-done.1.refs_1_ = bf16[64,1152]{1,0:T(8,128)(2,1)S(1)} collective-permute-done((bf16[64,1152]{1,0:T(8,128)(2,1)S(1)}, bf16[64,1152]{1,0:T(8,128)(2,1)S(1)}, u32[]{:S(2)}, u32[]{:S(2)}) %collective-permute-start.1) | collective-permute-done | bytes 147488 | tf_op jit(solution)/shard_map/ppermute | solution.py:389
  23.2 6.0 %collective-permute-done.2.refs_2_ = bf16[64,1152]{1,0:T(8,128)(2,1)S(1)} collective-permute-done((bf16[64,1152]{1,0:T(8,128)(2,1)S(1)}, bf16[64,1152]{1,0:T(8,128)(2,1)S(1)}, u32[]{:S(2)}, u32[]{:S(2)}) %collective-permute-start.2) | collective-permute-done | bytes 147488 | tf_op jit(solution)/shard_map/ppermute | solution.py:389
  29.9 1.1 constant_dynamic-slice_fusion.2
  31.9 2.9 %shard_map.179 = (f32[512,256]{1,0:T(8,128)S(1)}, f32[512,256]{1,0:T(8,128)S(1)}) custom-call(s32[4]{0:T(128)S(1)} %copy-done.5, bf16[256,1152]{1,0:T(8,128)(2,1)S(1)} %bitcast.26, bf16[256,1152]{1,0:T(8,128)(2,1)S(1)} %bitcast.42, f32[24,512]{1,0:T(8,128)S(1)} %maximum_maximum_fusion.own_ref, f32[24,512]{1,0:T(8,128)S(1)} %collective-permute-done.15.other_ref), custom_call_target="tpu_custom_call" | custom-call | flops 1000000000 | bytes 1048576 | tf_op jit(solution)/shard_map/pallas_call | solution.py:518
  34.8 1.7 shard_map.173
  36.5 5.6 %collective-permute-start.10 = (bf16[512,512]{1,0:T(8,128)(2,1)S(1)}, bf16[512,512]{1,0:T(8,128)(2,1)S(1)}, u32[]{:S(2)}, u32[]{:S(2)}) collective-permute-start(bf16[512,512]{1,0:T(8,128)(2,1)S(1)} %shard_map.173), channel_id=1, source_target_pairs={{0,8},{25,17},{2,10},{27,19},{4,12},{29,21},{6,14},{31,23}} | collective-permute-start | bytes 1572872 | tf_op jit(solution)/shard_map/ppermute | solution.py:842
  42.1 1.7 shard_map.168
  43.8 1.3 collective-permute-start.6
  45.1 3.6 %collective-permute-done.10.rest_0_ = bf16[512,512]{1,0:T(8,128)(2,1)S(1)} collective-permute-done((bf16[512,512]{1,0:T(8,128)(2,1)S(1)}, bf16[512,512]{1,0:T(8,128)(2,1)S(1)}, u32[]{:S(2)}, u32[]{:S(2)}) %collective-permute-start.10) | collective-permute-done | bytes 524320 | tf_op jit(solution)/shard_map/ppermute | solution.py:842
  48.8 1.5 shard_map.174
  50.3 4.4 %collective-permute-start.11 = (bf16[512,512]{1,0:T(8,128)(2,1)S(1)}, bf16[512,512]{1,0:T(8,128)(2,1)S(1)}, u32[]{:S(2)}, u32[]{:S(2)}) collective-permute-start(bf16[512,512]{1,0:T(8,128)(2,1)S(1)} %shard_map.174), channel_id=1, source_target_pairs={{0,8},{25,17},{8,16},{17,9},{2,10},{27,19},{10,18},{19,11},{4,12},... | collective-permute-start | bytes 1572872 | tf_op jit(solution)/shard_map/ppermute | solution.py:842
  54.7 1.5 shard_map.169
  56.2 4.1 %collective-permute-start.7 = (bf16[512,512]{1,0:T(8,128)(2,1)S(1)}, bf16[512,512]{1,0:T(8,128)(2,1)S(1)}, u32[]{:S(2)}, u32[]{:S(2)}) collective-permute-start(bf16[512,512]{1,0:T(8,128)(2,1)S(1)} %shard_map.169), channel_id=1, source_target_pairs={{0,8},{25,17},{8,16},{17,9},{2,10},{27,19},{10,18},{19,11},{4,12},... | collective-permute-start | bytes 1572872 | tf_op jit(solution)/shard_map/ppermute | solution.py:842
  60.3 1.0 collective-permute-done.11.rest_0_
  61.4 1.5 shard_map.175
  62.9 4.4 %collective-permute-start.12 = (bf16[512,512]{1,0:T(8,128)(2,1)S(1)}, bf16[512,512]{1,0:T(8,128)(2,1)S(1)}, u32[]{:S(2)}, u32[]{:S(2)}) collective-permute-start(bf16[512,512]{1,0:T(8,128)(2,1)S(1)} %shard_map.175), channel_id=1, source_target_pairs={{0,8},{25,17},{8,16},{17,9},{16,24},{9,1},{2,10},{27,19},{10,18},{... | collective-permute-start | bytes 1572872 | tf_op jit(solution)/shard_map/ppermute | solution.py:842
  67.3 1.5 shard_map.170
  68.8 4.1 %collective-permute-start.8 = (bf16[512,512]{1,0:T(8,128)(2,1)S(1)}, bf16[512,512]{1,0:T(8,128)(2,1)S(1)}, u32[]{:S(2)}, u32[]{:S(2)}) collective-permute-start(bf16[512,512]{1,0:T(8,128)(2,1)S(1)} %shard_map.170), channel_id=1, source_target_pairs={{0,8},{25,17},{8,16},{17,9},{16,24},{9,1},{2,10},{27,19},{10,18},{... | collective-permute-start | bytes 1572872 | tf_op jit(solution)/shard_map/ppermute | solution.py:842
  72.9 1.0 collective-permute-done.12.rest_0_
  73.9 1.5 shard_map.176.key_value_ref
  75.5 4.4 %collective-permute-start.13 = (bf16[512,512]{1,0:T(8,128)(2,1)S(1)}, bf16[512,512]{1,0:T(8,128)(2,1)S(1)}, u32[]{:S(2)}, u32[]{:S(2)}) collective-permute-start(bf16[512,512]{1,0:T(8,128)(2,1)S(1)} %shard_map.176.key_value_ref), channel_id=1, source_target_pairs={{0,8},{25,17},{8,16},{17,9},{16,24},{9,1},{2,10},{27,19},{10,18},{... | collective-permute-start | bytes 1572872 | tf_op jit(solution)/shard_map/ppermute | solution.py:842
  79.9 1.5 shard_map.171.query_ref
  81.4 0.9 collective-permute-start.9
  82.3 2.9 %shard_map.184.refs_0_ = bf16[512,512]{1,0:T(8,128)(2,1)S(1)} custom-call(s32[4]{0:T(128)S(1)} %copy-done.5, f32[2,4]{1,0:T(2,128)S(1)} %get-tuple-element.64.slope_ref, f32[2,4]{1,0:T(2,128)S(1)} %bitcast.41, bf16[512,512]{1,0:T(8,128)(2,1)S(1)} %shard_map.176.key_value_ref, bf16[512,512]{1,0:T(8,128)(2,1)S(1)} %shard_map.171.query_ref), custom_call_target="tpu_custom_call" | custom-call | flops 2000000000 | bytes 2097152 | tf_op jit(solution)/shard_map/pallas_call | solution.py:646
  85.2 0.7 collective-permute-start.26
  85.9 1.2 collective-permute-done.13.rest_0_
  87.2 1.5 shard_map.177.query_ref
  88.7 0.7 collective-permute-start.14
  89.4 1.5 shard_map.172.query_key_ref
  90.9 0.7 collective-permute-start.20
  91.6 3.9 %shard_map.185.refs_4_ = bf16[512,512]{1,0:T(8,128)(2,1)S(1)} custom-call(s32[4]{0:T(128)S(1)} %copy-done.5, f32[2,4]{1,0:T(2,128)S(1)} %get-tuple-element.63.slope_ref, f32[2,4]{1,0:T(2,128)S(1)} %bitcast.40, bf16[512,512]{1,0:T(8,128)(2,1)S(1)} %shard_map.176.key_value_ref, bf16[512,512]{1,0:T(8,128)(2,1)S(1)} %shard_map.177.query_ref), custom_call_target="tpu_custom_call" | custom-call | flops 2000000000 | bytes 2097152 | tf_op jit(solution)/shard_map/pallas_call | solution.py:646
  95.6 0.7 collective-permute-start.29
  96.3 0.7 collective-permute-start.27
  97.0 1.5 shard_map.178.value_ref
  99.2 2.3 %shard_map.180.refs_0_ = bf16[512,512]{1,0:T(8,128)(2,1)S(1)} custom-call(s32[4]{0:T(128)S(1)} %copy-done.5, bf16[512,512]{1,0:T(8,128)(2,1)S(1)} %shard_map.172.query_key_ref, bf16[512,512]{1,0:T(8,128)(2,1)S(1)} %shard_map.178.value_ref, f32[512,256]{1,0:T(8,128)S(1)} %get-tuple-element.50.running_ref, f32[4,128,256]{2,1,0:T(8,128)S(1)} %copy-done.14, ...), custom_call_target="tpu_custom_call" | custom-call | flops 2000000000 | bytes 2097152 | tf_op jit(solution)/shard_map/pallas_call | solution.py:566
  101.5 0.7 collective-permute-start.17
  102.9 1.5 shard_map.181.query_key_ref
  104.5 7.0 %collective-permute-start.32 = (bf16[512,1024]{1,0:T(8,128)(2,1)S(1)}, bf16[512,1024]{1,0:T(8,128)(2,1)S(1)}, u32[]{:S(2)}, u32[]{:S(2)}) collective-permute-start(bf16[512,1024]{1,0:T(8,128)(2,1)S(1)} %constant_dynamic-slice_fusion), channel_id=1, source_target_pairs={{0,1},{1,0},{2,3},{3,2},{4,5},{5,4},{6,7},{7,6},{8,9},{9,8},{10,11... | collective-permute-start | bytes 3145736 | tf_op jit(solution)/shard_map/ppermute | solution.py:758
  111.4 1.3 collective-permute-start.28
  112.7 0.7 collective-permute-start.18
  113.5 1.3 collective-permute-start.31
  114.8 1.5 shard_map.182.value_ref
  116.3 2.3 %shard_map.183.refs_4_ = bf16[512,512]{1,0:T(8,128)(2,1)S(1)} custom-call(s32[4]{0:T(128)S(1)} %copy-done.5, bf16[512,512]{1,0:T(8,128)(2,1)S(1)} %shard_map.181.query_key_ref, bf16[512,512]{1,0:T(8,128)(2,1)S(1)} %shard_map.182.value_ref, f32[512,256]{1,0:T(8,128)S(1)} %get-tuple-element.52.running_ref, f32[4,128,256]{2,1,0:T(8,128)S(1)} %copy-done.14, ...), custom_call_target="tpu_custom_call" | custom-call | flops 2000000000 | bytes 2097152 | tf_op jit(solution)/shard_map/pallas_call | solution.py:566
  118.6 0.8 collective-permute-start.22
  119.4 3.1 %collective-permute-done.28.refs_3_ = bf16[512,512]{1,0:T(8,128)(2,1)S(1)} collective-permute-done((bf16[512,512]{1,0:T(8,128)(2,1)S(1)}, bf16[512,512]{1,0:T(8,128)(2,1)S(1)}, u32[]{:S(2)}, u32[]{:S(2)}) %collective-permute-start.28) | collective-permute-done | bytes 524320 | tf_op jit(solution)/shard_map/ppermute | solution.py:885
  123.2 1.3 collective-permute-start.24
  124.5 6.9 %collective-permute-done.31.refs_7_ = bf16[512,512]{1,0:T(8,128)(2,1)S(1)} collective-permute-done((bf16[512,512]{1,0:T(8,128)(2,1)S(1)}, bf16[512,512]{1,0:T(8,128)(2,1)S(1)}, u32[]{:S(2)}, u32[]{:S(2)}) %collective-permute-start.31) | collective-permute-done | bytes 524320 | tf_op jit(solution)/shard_map/ppermute | solution.py:885
  131.4 1.3 collective-permute-start.19
  132.7 2.1 %shard_map.186.refs_10_ = f32[512,1024]{1,0:T(8,128)S(1)} custom-call(s32[4]{0:T(128)S(1)} %copy-done.5, bf16[512,512]{1,0:T(8,128)(2,1)S(1)} %shard_map.184.refs_0_, bf16[512,512]{1,0:T(8,128)(2,1)S(1)} %collective-permute-done.26.refs_1_, bf16[512,512]{1,0:T(8,128)(2,1)S(1)} %collective-permute-done.27.refs_2_, ...), custom_call_target="tpu_custom_call" | custom-call | flops 1073741824 | bytes 4194304 | tf_op jit(solution)/shard_map/pallas_call | solution.py:703
  134.9 17.3 %collective-permute-done.24.refs_7_ = bf16[512,512]{1,0:T(8,128)(2,1)S(1)} collective-permute-done((bf16[512,512]{1,0:T(8,128)(2,1)S(1)}, bf16[512,512]{1,0:T(8,128)(2,1)S(1)}, u32[]{:S(2)}, u32[]{:S(2)}) %collective-permute-start.24) | collective-permute-done | bytes 524320 | tf_op jit(solution)/shard_map/ppermute | solution.py:889
  152.2 3.2 %shard_map.187 = (bf16[256,1024]{1,0:T(8,128)(2,1)S(1)}, bf16[256,1024]{1,0:T(8,128)(2,1)S(1)}) custom-call(s32[4]{0:T(128)S(1)} %copy-done.5, bf16[512,512]{1,0:T(8,128)(2,1)S(1)} %shard_map.180.refs_0_, bf16[512,512]{1,0:T(8,128)(2,1)S(1)} %collective-permute-done.17.refs_1_, bf16[512,512]{1,0:T(8,128)(2,1)S(1)} %collective-permute-done.18.refs_2_, ...), custom_call_target="tpu_custom_call" | custom-call | flops 1073741824 | bytes 4194304 | tf_op jit(solution)/shard_map/pallas_call | solution.py:703
  155.5 1.9 %collective-permute-done.33.given_ref = bf16[256,1024]{1,0:T(8,128)(2,1)S(1)} collective-permute-done((bf16[256,1024]{1,0:T(8,128)(2,1)S(1)}, bf16[256,1024]{1,0:T(8,128)(2,1)S(1)}, u32[]{:S(2)}, u32[]{:S(2)}) %collective-permute-start.33) | collective-permute-done | bytes 524320 | tf_op jit(solution)/shard_map/ppermute | solution.py:758
  158.2 3.7 %collective-permute-start.36 = (bf16[64,1024]{1,0:T(8,128)(2,1)S(1)}, bf16[64,1024]{1,0:T(8,128)(2,1)S(1)}, u32[]{:S(2)}, u32[]{:S(2)}) collective-permute-start(bf16[64,1024]{1,0:T(8,128)(2,1)S(1)} %get-tuple-element.60), channel_id=1, source_target_pairs={{0,24},{8,0},{16,8},{24,16},{1,25},{9,1},{17,9},{25,17},{2,26},{10... | collective-permute-start | bytes 393224 | tf_op jit(solution)/shard_map/ppermute | solution.py:389
  161.9 4.5 %collective-permute-done.34.refs_1_ = bf16[64,1024]{1,0:T(8,128)(2,1)S(1)} collective-permute-done((bf16[64,1024]{1,0:T(8,128)(2,1)S(1)}, bf16[64,1024]{1,0:T(8,128)(2,1)S(1)}, u32[]{:S(2)}, u32[]{:S(2)}) %collective-permute-start.34) | collective-permute-done | bytes 131104 | tf_op jit(solution)/shard_map/ppermute | solution.py:389
  166.4 4.7 %collective-permute-done.35.refs_2_ = bf16[64,1024]{1,0:T(8,128)(2,1)S(1)} collective-permute-done((bf16[64,1024]{1,0:T(8,128)(2,1)S(1)}, bf16[64,1024]{1,0:T(8,128)(2,1)S(1)}, u32[]{:S(2)}, u32[]{:S(2)}) %collective-permute-start.35) | collective-permute-done | bytes 131104 | tf_op jit(solution)/shard_map/ppermute | solution.py:389
  171.1 1.4 shard_map.189
  (105 shorter events, 9.4 us)
Async XLA Ops:
  0.9 1.0 copy-start.10
  1.9 2.4 %copy-start.4 = (s32[4]{0:T(128)}, s32[4]{0:T(128)S(1)}, u32[]{:S(2)}) copy-start(s32[4]{0:T(128)S(1)} %pad_add_fusion.place_ref) | copy-start | bytes 52
  1.9 2.4 %copy-start.11 = (bf16[128,2048]{1,0:T(8,128)(2,1)S(1)}, bf16[128,2048]{1,0:T(8,128)(2,1)}, u32[]{:S(2)}) copy-start(bf16[128,2048]{1,0:T(8,128)(2,1)} %x_ref.3) | copy-start | bytes 1572868
  1.9 2.4 %copy-start.15 = (bf16[4096,16]{0,1:T(8,128)(2,1)S(1)}, bf16[4096,16]{0,1:T(8,128)(2,1)}, u32[]{:S(2)}) copy-start(bf16[4096,16]{0,1:T(8,128)(2,1)} %param.25) | copy-start | bytes 393220
  1.9 2.4 %copy-start.16 = (f32[4096]{0:T(1024)S(1)}, f32[4096]{0:T(1024)}, u32[]{:S(2)}) copy-start(f32[4096]{0:T(1024)} %param.18) | copy-start | bytes 49156
  2.6 1.7 %collective-permute-start = (bf16[64,2176]{1,0:T(8,128)(2,1)S(1)}, bf16[64,2176]{1,0:T(8,128)(2,1)S(1)}, u32[]{:S(2)}, u32[]{:S(2)}) collective-permute-start(bf16[64,2176]{1,0:T(8,128)(2,1)S(1)} %shard_map.163), channel_id=1, source_target_pairs={{0,1},{1,0},{2,3},{3,2},{4,5},{5,4},{6,7},{7,6},{8,9},{9,8},{10,11... | collective-permute-start | bytes 835592 | tf_op jit(solution)/shard_map/ppermute | solution.py:758
  4.3 1.6 copy-start.6
  4.3 2.2 %copy-start.7 = (bf16[1024,1024]{1,0:T(8,128)(2,1)S(1)}, bf16[1024,1024]{1,0:T(8,128)(2,1)}, u32[]{:S(2)}) copy-start(bf16[1024,1024]{1,0:T(8,128)(2,1)} %lv.1) | copy-start | bytes 6291460
  4.3 2.5 %copy-start.8 = (bf16[1024,512]{1,0:T(8,128)(2,1)S(1)}, bf16[1024,512]{1,0:T(8,128)(2,1)}, u32[]{:S(2)}) copy-start(bf16[1024,512]{1,0:T(8,128)(2,1)} %lq.1) | copy-start | bytes 3145732
  4.4 2.8 %copy-start.9 = (bf16[1024,512]{1,0:T(8,128)(2,1)S(1)}, bf16[1024,512]{1,0:T(8,128)(2,1)}, u32[]{:S(2)}) copy-start(bf16[1024,512]{1,0:T(8,128)(2,1)} %lk.1) | copy-start | bytes 3145732
  4.4 2.9 %copy-start.12 = (bf16[1024,256]{1,0:T(8,128)(2,1)S(1)}, bf16[1024,256]{1,0:T(8,128)(2,1)}, u32[]{:S(2)}) copy-start(bf16[1024,256]{1,0:T(8,128)(2,1)} %wk.1) | copy-start | bytes 1572868
  4.4 3.0 %copy-start.13 = (bf16[1024,256]{1,0:T(8,128)(2,1)S(1)}, bf16[1024,256]{1,0:T(8,128)(2,1)}, u32[]{:S(2)}) copy-start(bf16[1024,256]{1,0:T(8,128)(2,1)} %wv.1) | copy-start | bytes 1572868
  11.5 8.8 %copy-start.23 = (f32[16]{0:T(128)S(1)}, f32[16]{0:T(128)}, u32[]{:S(2)}) copy-start(f32[16]{0:T(128)} %param.30) | copy-start | bytes 196
  11.5 8.8 %copy-start.20 = (bf16[16,512]{1,0:T(8,128)(2,1)S(1)}, bf16[16,512]{1,0:T(8,128)(2,1)}, u32[]{:S(2)}) copy-start(bf16[16,512]{1,0:T(8,128)(2,1)} %param.26) | copy-start | bytes 49156
  11.5 8.8 %copy-start.21 = (f32[512]{0:T(512)S(1)}, f32[512]{0:T(512)}, u32[]{:S(2)}) copy-start(f32[512]{0:T(512)} %param.27) | copy-start | bytes 6148
  11.5 8.8 %copy-start.22 = (f32[24]{0:T(128)S(1)}, f32[24]{0:T(128)}, u32[]{:S(2)}) copy-start(f32[24]{0:T(128)} %pad.12.clone) | copy-start | bytes 292
  11.5 11.7 %copy-start.14 = (f32[4,128,256]{2,1,0:T(8,128)S(1)}, f32[4,128,256]{2,1,0:T(8,128)}, u32[]{:S(2)}) copy-start(f32[4,128,256]{2,1,0:T(8,128)} %own_ref.1) | copy-start | bytes 1572868
  11.5 17.7 %copy-start.5 = (s32[4]{0:T(128)S(1)}, s32[4]{0:T(128)}, u32[]{:S(2)}) copy-start(s32[4]{0:T(128)} %copy-done.4) | copy-start | bytes 52
  11.5 18.3 %copy-start.2 = (bf16[1024,1024]{1,0:T(8,128)(2,1)S(1)}, bf16[1024,1024]{1,0:T(8,128)(2,1)}, u32[]{:S(2)}) copy-start(bf16[1024,1024]{1,0:T(8,128)(2,1)} %refs_8_.1) | copy-start | bytes 6291460
  11.5 23.3 %collective-permute-start.5 = (bf16[7,1024,256]{2,1,0:T(8,128)(2,1)}, bf16[7,1024,256]{2,1,0:T(8,128)(2,1)}, u32[]{:S(2)}, u32[]{:S(2)}) collective-permute-start(bf16[7,1024,256]{2,1,0:T(8,128)(2,1)} %shard_map.167), channel_id=1, source_target_pairs={{0,1},{1,0},{2,3},{3,2},{4,5},{5,4},{6,7},{7,6},{8,9},{9,8},{10,11... | collective-permute-start | bytes 11010056 | tf_op jit(solution)/shard_map/ppermute | solution.py:758
  13.6 17.9 %copy-start.18 = (bf16[7,1024,256]{2,1,0:T(8,128)(2,1)}, bf16[7,1024,256]{2,1,0:T(8,128)(2,1)S(1)}, u32[]{:S(2)}) copy-start(bf16[7,1024,256]{2,1,0:T(8,128)(2,1)S(1)} %shard_map.166.own_ref) | copy-start | bytes 11010052
  13.6 17.8 %copy-start = (bf16[1024,1024]{1,0:T(8,128)(2,1)S(1)}, bf16[1024,1024]{1,0:T(8,128)(2,1)}, u32[]{:S(2)}) copy-start(bf16[1024,1024]{1,0:T(8,128)(2,1)} %refs_8_) | copy-start | bytes 6291460
  13.6 9.6 %collective-permute-start.1 = (bf16[64,1152]{1,0:T(8,128)(2,1)S(1)}, bf16[64,1152]{1,0:T(8,128)(2,1)S(1)}, u32[]{:S(2)}, u32[]{:S(2)}) collective-permute-start(bf16[64,1152]{1,0:T(8,128)(2,1)S(1)} %get-tuple-element.38), channel_id=1, source_target_pairs={{0,8},{8,16},{16,24},{24,0},{1,9},{9,17},{17,25},{25,1},{2,10},{10... | collective-permute-start | bytes 442376 | tf_op jit(solution)/shard_map/ppermute | solution.py:389
  16.3 12.8 %collective-permute-start.2 = (bf16[64,1152]{1,0:T(8,128)(2,1)S(1)}, bf16[64,1152]{1,0:T(8,128)(2,1)S(1)}, u32[]{:S(2)}, u32[]{:S(2)}) collective-permute-start(bf16[64,1152]{1,0:T(8,128)(2,1)S(1)} %get-tuple-element.39), channel_id=1, source_target_pairs={{0,16},{8,24},{16,0},{24,8},{1,17},{9,25},{17,1},{25,9},{2,18},{10... | collective-permute-start | bytes 442376 | tf_op jit(solution)/shard_map/ppermute | solution.py:389
  18.9 10.2 %collective-permute-start.3 = (bf16[64,1152]{1,0:T(8,128)(2,1)S(1)}, bf16[64,1152]{1,0:T(8,128)(2,1)S(1)}, u32[]{:S(2)}, u32[]{:S(2)}) collective-permute-start(bf16[64,1152]{1,0:T(8,128)(2,1)S(1)} %get-tuple-element.40), channel_id=1, source_target_pairs={{0,24},{8,0},{16,8},{24,16},{1,25},{9,1},{17,9},{25,17},{2,26},{10... | collective-permute-start | bytes 442376 | tf_op jit(solution)/shard_map/ppermute | solution.py:389
  20.4 11.3 %collective-permute-start.15 = (f32[24,512]{1,0:T(8,128)S(1)}, f32[24,512]{1,0:T(8,128)S(1)}, u32[]{:S(2)}, u32[]{:S(2)}) collective-permute-start(f32[24,512]{1,0:T(8,128)S(1)} %maximum_maximum_fusion.own_ref), channel_id=1, source_target_pairs={{0,1},{1,0},{2,3},{3,2},{4,5},{5,4},{6,7},{7,6},{8,9},{9,8},{10,11... | collective-permute-start | bytes 147464 | tf_op jit(solution)/shard_map/ppermute | solution.py:758
  23.2 75.4 %collective-permute-start.16 = (f32[4,128,256]{2,1,0:T(8,128)S(1)}, f32[4,128,256]{2,1,0:T(8,128)S(1)}, u32[]{:S(2)}, u32[]{:S(2)}) collective-permute-start(f32[4,128,256]{2,1,0:T(8,128)S(1)} %copy-done.14), channel_id=1, source_target_pairs={{0,1},{1,0},{2,3},{3,2},{4,5},{5,4},{6,7},{7,6},{8,9},{9,8},{10,11... | collective-permute-start | bytes 1572872 | tf_op jit(solution)/shard_map/ppermute | solution.py:758
  29.8 2.1 %collective-permute-start.4 = (bf16[4,64,1152]{2,1,0:T(8,128)(2,1)S(1)}, bf16[4,64,1152]{2,1,0:T(8,128)(2,1)S(1)}, u32[]{:S(2)}, u32[]{:S(2)}) collective-permute-start(bf16[4,64,1152]{2,1,0:T(8,128)(2,1)S(1)} %shard_map.165), channel_id=1, source_target_pairs={{0,1},{1,0},{2,3},{3,2},{4,5},{5,4},{6,7},{7,6},{8,9},{9,8},{10,11... | collective-permute-start | bytes 1769480 | tf_op jit(solution)/shard_map/ppermute | solution.py:758
  30.9 103.9 %collective-permute-start.25 = (bf16[512,1024]{1,0:T(8,128)(2,1)}, bf16[512,1024]{1,0:T(8,128)(2,1)}, u32[]{:S(2)}, u32[]{:S(2)}) collective-permute-start(bf16[512,1024]{1,0:T(8,128)(2,1)} %constant_dynamic-slice_fusion.2), channel_id=1, source_target_pairs={{0,1},{1,0},{2,3},{3,2},{4,5},{5,4},{6,7},{7,6},{8,9},{9,8},{10,11... | collective-permute-start | bytes 3145736 | tf_op jit(solution)/shard_map/ppermute | solution.py:758
  31.9 3.0 %copy-start.19 = (bf16[7,1024,256]{2,1,0:T(8,128)(2,1)S(1)}, bf16[7,1024,256]{2,1,0:T(8,128)(2,1)}, u32[]{:S(2)}) copy-start(bf16[7,1024,256]{2,1,0:T(8,128)(2,1)} %copy-done.18) | copy-start | bytes 11010052
  36.5 12.2 %collective-permute-start.10 = (bf16[512,512]{1,0:T(8,128)(2,1)S(1)}, bf16[512,512]{1,0:T(8,128)(2,1)S(1)}, u32[]{:S(2)}, u32[]{:S(2)}) collective-permute-start(bf16[512,512]{1,0:T(8,128)(2,1)S(1)} %shard_map.173), channel_id=1, source_target_pairs={{0,8},{25,17},{2,10},{27,19},{4,12},{29,21},{6,14},{31,23}} | collective-permute-start | bytes 1572872 | tf_op jit(solution)/shard_map/ppermute | solution.py:842
  43.8 10.9 %collective-permute-start.6 = (bf16[512,512]{1,0:T(8,128)(2,1)S(1)}, bf16[512,512]{1,0:T(8,128)(2,1)S(1)}, u32[]{:S(2)}, u32[]{:S(2)}) collective-permute-start(bf16[512,512]{1,0:T(8,128)(2,1)S(1)} %shard_map.168), channel_id=1, source_target_pairs={{0,8},{25,17},{2,10},{27,19},{4,12},{29,21},{6,14},{31,23}} | collective-permute-start | bytes 1572872 | tf_op jit(solution)/shard_map/ppermute | solution.py:842
  50.3 11.1 %collective-permute-start.11 = (bf16[512,512]{1,0:T(8,128)(2,1)S(1)}, bf16[512,512]{1,0:T(8,128)(2,1)S(1)}, u32[]{:S(2)}, u32[]{:S(2)}) collective-permute-start(bf16[512,512]{1,0:T(8,128)(2,1)S(1)} %shard_map.174), channel_id=1, source_target_pairs={{0,8},{25,17},{8,16},{17,9},{2,10},{27,19},{10,18},{19,11},{4,12},... | collective-permute-start | bytes 1572872 | tf_op jit(solution)/shard_map/ppermute | solution.py:842
  56.2 11.1 %collective-permute-start.7 = (bf16[512,512]{1,0:T(8,128)(2,1)S(1)}, bf16[512,512]{1,0:T(8,128)(2,1)S(1)}, u32[]{:S(2)}, u32[]{:S(2)}) collective-permute-start(bf16[512,512]{1,0:T(8,128)(2,1)S(1)} %shard_map.169), channel_id=1, source_target_pairs={{0,8},{25,17},{8,16},{17,9},{2,10},{27,19},{10,18},{19,11},{4,12},... | collective-permute-start | bytes 1572872 | tf_op jit(solution)/shard_map/ppermute | solution.py:842
  62.9 11.1 %collective-permute-start.12 = (bf16[512,512]{1,0:T(8,128)(2,1)S(1)}, bf16[512,512]{1,0:T(8,128)(2,1)S(1)}, u32[]{:S(2)}, u32[]{:S(2)}) collective-permute-start(bf16[512,512]{1,0:T(8,128)(2,1)S(1)} %shard_map.175), channel_id=1, source_target_pairs={{0,8},{25,17},{8,16},{17,9},{16,24},{9,1},{2,10},{27,19},{10,18},{... | collective-permute-start | bytes 1572872 | tf_op jit(solution)/shard_map/ppermute | solution.py:842
  68.8 11.1 %collective-permute-start.8 = (bf16[512,512]{1,0:T(8,128)(2,1)S(1)}, bf16[512,512]{1,0:T(8,128)(2,1)S(1)}, u32[]{:S(2)}, u32[]{:S(2)}) collective-permute-start(bf16[512,512]{1,0:T(8,128)(2,1)S(1)} %shard_map.170), channel_id=1, source_target_pairs={{0,8},{25,17},{8,16},{17,9},{16,24},{9,1},{2,10},{27,19},{10,18},{... | collective-permute-start | bytes 1572872 | tf_op jit(solution)/shard_map/ppermute | solution.py:842
  75.5 11.7 %collective-permute-start.13 = (bf16[512,512]{1,0:T(8,128)(2,1)S(1)}, bf16[512,512]{1,0:T(8,128)(2,1)S(1)}, u32[]{:S(2)}, u32[]{:S(2)}) collective-permute-start(bf16[512,512]{1,0:T(8,128)(2,1)S(1)} %shard_map.176.key_value_ref), channel_id=1, source_target_pairs={{0,8},{25,17},{8,16},{17,9},{16,24},{9,1},{2,10},{27,19},{10,18},{... | collective-permute-start | bytes 1572872 | tf_op jit(solution)/shard_map/ppermute | solution.py:842
  81.4 8.0 %collective-permute-start.9 = (bf16[512,512]{1,0:T(8,128)(2,1)S(1)}, bf16[512,512]{1,0:T(8,128)(2,1)S(1)}, u32[]{:S(2)}, u32[]{:S(2)}) collective-permute-start(bf16[512,512]{1,0:T(8,128)(2,1)S(1)} %shard_map.171.query_ref), channel_id=1, source_target_pairs={{8,16},{17,9},{16,24},{9,1},{10,18},{19,11},{18,26},{11,3},{12,20}... | collective-permute-start | bytes 1572872 | tf_op jit(solution)/shard_map/ppermute | solution.py:842
  85.2 10.3 %collective-permute-start.26 = (bf16[512,512]{1,0:T(8,128)(2,1)S(1)}, bf16[512,512]{1,0:T(8,128)(2,1)S(1)}, u32[]{:S(2)}, u32[]{:S(2)}) collective-permute-start(bf16[512,512]{1,0:T(8,128)(2,1)S(1)} %shard_map.184.refs_0_), channel_id=1, source_target_pairs={{1,9},{24,16},{3,11},{26,18},{5,13},{28,20},{7,15},{30,22}} | collective-permute-start | bytes 1572872 | tf_op jit(solution)/shard_map/ppermute | solution.py:885
  88.7 7.6 %collective-permute-start.14 = (bf16[512,512]{1,0:T(8,128)(2,1)S(1)}, bf16[512,512]{1,0:T(8,128)(2,1)S(1)}, u32[]{:S(2)}, u32[]{:S(2)}) collective-permute-start(bf16[512,512]{1,0:T(8,128)(2,1)S(1)} %shard_map.177.query_ref), channel_id=1, source_target_pairs={{8,16},{17,9},{16,24},{9,1},{10,18},{19,11},{18,26},{11,3},{12,20}... | collective-permute-start | bytes 1572872 | tf_op jit(solution)/shard_map/ppermute | solution.py:842
  90.9 10.6 %collective-permute-start.20 = (bf16[512,512]{1,0:T(8,128)(2,1)S(1)}, bf16[512,512]{1,0:T(8,128)(2,1)S(1)}, u32[]{:S(2)}, u32[]{:S(2)}) collective-permute-start(bf16[512,512]{1,0:T(8,128)(2,1)S(1)} %shard_map.172.query_key_ref), channel_id=1, source_target_pairs={{16,24},{9,1},{18,26},{11,3},{20,28},{13,5},{22,30},{15,7}} | collective-permute-start | bytes 1572872 | tf_op jit(solution)/shard_map/ppermute | solution.py:842
  95.6 6.6 %collective-permute-start.29 = (bf16[512,512]{1,0:T(8,128)(2,1)S(1)}, bf16[512,512]{1,0:T(8,128)(2,1)S(1)}, u32[]{:S(2)}, u32[]{:S(2)}) collective-permute-start(bf16[512,512]{1,0:T(8,128)(2,1)S(1)} %shard_map.185.refs_4_), channel_id=1, source_target_pairs={{1,9},{24,16},{3,11},{26,18},{5,13},{28,20},{7,15},{30,22}} | collective-permute-start | bytes 1572872 | tf_op jit(solution)/shard_map/ppermute | solution.py:885
  96.3 8.2 %collective-permute-start.27 = (bf16[512,512]{1,0:T(8,128)(2,1)S(1)}, bf16[512,512]{1,0:T(8,128)(2,1)S(1)}, u32[]{:S(2)}, u32[]{:S(2)}) collective-permute-start(bf16[512,512]{1,0:T(8,128)(2,1)S(1)} %collective-permute-done.26.refs_1_), channel_id=1, source_target_pairs={{9,17},{16,8},{11,19},{18,10},{13,21},{20,12},{15,23},{22,14}} | collective-permute-start | bytes 1572872 | tf_op jit(solution)/shard_map/ppermute | solution.py:885
  97.0 2.2 %copy-start.17 = (f32[256]{0:T(256)S(1)}, f32[256]{0:T(256)}, u32[]{:S(2)}) copy-start(f32[256]{0:T(256)} %param.31) | copy-start | bytes 3076
  98.5 14.2 %collective-permute-start.21 = (bf16[512,512]{1,0:T(8,128)(2,1)S(1)}, bf16[512,512]{1,0:T(8,128)(2,1)S(1)}, u32[]{:S(2)}, u32[]{:S(2)}) collective-permute-start(bf16[512,512]{1,0:T(8,128)(2,1)S(1)} %shard_map.178.value_ref), channel_id=1, source_target_pairs={{16,24},{9,1},{18,26},{11,3},{20,28},{13,5},{22,30},{15,7}} | collective-permute-start | bytes 1572872 | tf_op jit(solution)/shard_map/ppermute | solution.py:842
  101.5 9.9 %collective-permute-start.17 = (bf16[512,512]{1,0:T(8,128)(2,1)S(1)}, bf16[512,512]{1,0:T(8,128)(2,1)S(1)}, u32[]{:S(2)}, u32[]{:S(2)}) collective-permute-start(bf16[512,512]{1,0:T(8,128)(2,1)S(1)} %shard_map.180.refs_0_), channel_id=1, source_target_pairs={{1,9},{24,16},{3,11},{26,18},{5,13},{28,20},{7,15},{30,22}} | collective-permute-start | bytes 1572872 | tf_op jit(solution)/shard_map/ppermute | solution.py:885
  102.2 11.2 %collective-permute-start.30 = (bf16[512,512]{1,0:T(8,128)(2,1)S(1)}, bf16[512,512]{1,0:T(8,128)(2,1)S(1)}, u32[]{:S(2)}, u32[]{:S(2)}) collective-permute-start(bf16[512,512]{1,0:T(8,128)(2,1)S(1)} %collective-permute-done.29.refs_5_), channel_id=1, source_target_pairs={{9,17},{16,8},{11,19},{18,10},{13,21},{20,12},{15,23},{22,14}} | collective-permute-start | bytes 1572872 | tf_op jit(solution)/shard_map/ppermute | solution.py:885
  104.5 14.1 %collective-permute-start.32 = (bf16[512,1024]{1,0:T(8,128)(2,1)S(1)}, bf16[512,1024]{1,0:T(8,128)(2,1)S(1)}, u32[]{:S(2)}, u32[]{:S(2)}) collective-permute-start(bf16[512,1024]{1,0:T(8,128)(2,1)S(1)} %constant_dynamic-slice_fusion), channel_id=1, source_target_pairs={{0,1},{1,0},{2,3},{3,2},{4,5},{5,4},{6,7},{7,6},{8,9},{9,8},{10,11... | collective-permute-start | bytes 3145736 | tf_op jit(solution)/shard_map/ppermute | solution.py:758
  111.4 11.1 %collective-permute-start.28 = (bf16[512,512]{1,0:T(8,128)(2,1)S(1)}, bf16[512,512]{1,0:T(8,128)(2,1)S(1)}, u32[]{:S(2)}, u32[]{:S(2)}) collective-permute-start(bf16[512,512]{1,0:T(8,128)(2,1)S(1)} %collective-permute-done.27.refs_2_), channel_id=1, source_target_pairs={{17,25},{8,0},{19,27},{10,2},{21,29},{12,4},{23,31},{14,6}} | collective-permute-start | bytes 1572872 | tf_op jit(solution)/shard_map/ppermute | solution.py:885
  112.7 10.5 %collective-permute-start.18 = (bf16[512,512]{1,0:T(8,128)(2,1)S(1)}, bf16[512,512]{1,0:T(8,128)(2,1)S(1)}, u32[]{:S(2)}, u32[]{:S(2)}) collective-permute-start(bf16[512,512]{1,0:T(8,128)(2,1)S(1)} %collective-permute-done.17.refs_1_), channel_id=1, source_target_pairs={{9,17},{16,8},{11,19},{18,10},{13,21},{20,12},{15,23},{22,14}} | collective-permute-start | bytes 1572872 | tf_op jit(solution)/shard_map/ppermute | solution.py:885
  113.5 18.0 %collective-permute-start.31 = (bf16[512,512]{1,0:T(8,128)(2,1)S(1)}, bf16[512,512]{1,0:T(8,128)(2,1)S(1)}, u32[]{:S(2)}, u32[]{:S(2)}) collective-permute-start(bf16[512,512]{1,0:T(8,128)(2,1)S(1)} %collective-permute-done.30.refs_6_), channel_id=1, source_target_pairs={{17,25},{8,0},{19,27},{10,2},{21,29},{12,4},{23,31},{14,6}} | collective-permute-start | bytes 1572872 | tf_op jit(solution)/shard_map/ppermute | solution.py:885
  116.3 16.5 %copy-start.1 = (bf16[1024,1024]{1,0:T(8,128)(2,1)S(1)}, bf16[1024,1024]{1,0:T(8,128)(2,1)}, u32[]{:S(2)}) copy-start(bf16[1024,1024]{1,0:T(8,128)(2,1)} %refs_8_) | copy-start | bytes 6291460
  118.5 33.7 %copy-start.3 = (bf16[1024,1024]{1,0:T(8,128)(2,1)S(1)}, bf16[1024,1024]{1,0:T(8,128)(2,1)}, u32[]{:S(2)}) copy-start(bf16[1024,1024]{1,0:T(8,128)(2,1)} %refs_8_.1) | copy-start | bytes 6291460
  118.6 16.3 %collective-permute-start.22 = (bf16[512,512]{1,0:T(8,128)(2,1)S(1)}, bf16[512,512]{1,0:T(8,128)(2,1)S(1)}, u32[]{:S(2)}, u32[]{:S(2)}) collective-permute-start(bf16[512,512]{1,0:T(8,128)(2,1)S(1)} %shard_map.183.refs_4_), channel_id=1, source_target_pairs={{24,16},{1,9},{26,18},{3,11},{28,20},{5,13},{30,22},{7,15}} | collective-permute-start | bytes 1572872 | tf_op jit(solution)/shard_map/ppermute | solution.py:889
  122.5 12.4 %collective-permute-start.23 = (bf16[512,512]{1,0:T(8,128)(2,1)S(1)}, bf16[512,512]{1,0:T(8,128)(2,1)S(1)}, u32[]{:S(2)}, u32[]{:S(2)}) collective-permute-start(bf16[512,512]{1,0:T(8,128)(2,1)S(1)} %shard_map.183.refs_4_), channel_id=1, source_target_pairs={{24,8},{1,17},{26,10},{3,19},{28,12},{5,21},{30,14},{7,23}} | collective-permute-start | bytes 1572872 | tf_op jit(solution)/shard_map/ppermute | solution.py:889
  123.2 29.0 %collective-permute-start.24 = (bf16[512,512]{1,0:T(8,128)(2,1)S(1)}, bf16[512,512]{1,0:T(8,128)(2,1)S(1)}, u32[]{:S(2)}, u32[]{:S(2)}) collective-permute-start(bf16[512,512]{1,0:T(8,128)(2,1)S(1)} %shard_map.183.refs_4_), channel_id=1, source_target_pairs={{24,0},{1,25},{26,2},{3,27},{28,4},{5,29},{30,6},{7,31}} | collective-permute-start | bytes 1572872 | tf_op jit(solution)/shard_map/ppermute | solution.py:889
  131.4 20.8 %collective-permute-start.19 = (bf16[512,512]{1,0:T(8,128)(2,1)S(1)}, bf16[512,512]{1,0:T(8,128)(2,1)S(1)}, u32[]{:S(2)}, u32[]{:S(2)}) collective-permute-start(bf16[512,512]{1,0:T(8,128)(2,1)S(1)} %collective-permute-done.18.refs_2_), channel_id=1, source_target_pairs={{17,25},{8,0},{19,27},{10,2},{21,29},{12,4},{23,31},{14,6}} | collective-permute-start | bytes 1572872 | tf_op jit(solution)/shard_map/ppermute | solution.py:885
  155.4 2.0 %collective-permute-start.33 = (bf16[256,1024]{1,0:T(8,128)(2,1)S(1)}, bf16[256,1024]{1,0:T(8,128)(2,1)S(1)}, u32[]{:S(2)}, u32[]{:S(2)}) collective-permute-start(bf16[256,1024]{1,0:T(8,128)(2,1)S(1)} %get-tuple-element.56), channel_id=1, source_target_pairs={{0,1},{1,0},{2,3},{3,2},{4,5},{5,4},{6,7},{7,6},{8,9},{9,8},{10,11... | collective-permute-start | bytes 1572872 | tf_op jit(solution)/shard_map/ppermute | solution.py:758
  158.0 8.4 %collective-permute-start.34 = (bf16[64,1024]{1,0:T(8,128)(2,1)S(1)}, bf16[64,1024]{1,0:T(8,128)(2,1)S(1)}, u32[]{:S(2)}, u32[]{:S(2)}) collective-permute-start(bf16[64,1024]{1,0:T(8,128)(2,1)S(1)} %get-tuple-element.58), channel_id=1, source_target_pairs={{0,8},{8,16},{16,24},{24,0},{1,9},{9,17},{17,25},{25,1},{2,10},{10... | collective-permute-start | bytes 393224 | tf_op jit(solution)/shard_map/ppermute | solution.py:389
  158.1 13.0 %collective-permute-start.35 = (bf16[64,1024]{1,0:T(8,128)(2,1)S(1)}, bf16[64,1024]{1,0:T(8,128)(2,1)S(1)}, u32[]{:S(2)}, u32[]{:S(2)}) collective-permute-start(bf16[64,1024]{1,0:T(8,128)(2,1)S(1)} %get-tuple-element.59), channel_id=1, source_target_pairs={{0,16},{8,24},{16,0},{24,8},{1,17},{9,25},{17,1},{25,9},{2,18},{10... | collective-permute-start | bytes 393224 | tf_op jit(solution)/shard_map/ppermute | solution.py:389
  158.2 12.9 %collective-permute-start.36 = (bf16[64,1024]{1,0:T(8,128)(2,1)S(1)}, bf16[64,1024]{1,0:T(8,128)(2,1)S(1)}, u32[]{:S(2)}, u32[]{:S(2)}) collective-permute-start(bf16[64,1024]{1,0:T(8,128)(2,1)S(1)} %get-tuple-element.60), channel_id=1, source_target_pairs={{0,24},{8,0},{16,8},{24,16},{1,25},{9,1},{17,9},{25,17},{2,26},{10... | collective-permute-start | bytes 393224 | tf_op jit(solution)/shard_map/ppermute | solution.py:389

commit v6 on v5

--- a/solution.py
+++ b/solution.py
@@ -881,12 +881,10 @@
     for piece in range(pieces):
         seen = [attended[piece]]
         for hop in range(hops):
-            if piece < pieces - 1:
+            if piece == pieces - 1 and 0 < hop == hops - 1:
+                seen.append(lax.ppermute(seen[0], ("sp", "tp"), [(hops * 2, 0), (1, hops * 2 + 1)]))
+            else:
                 seen.append(lax.ppermute(seen[-1], ("sp", "tp"), _pairs(peers, [hop], 1)))
-            else:
-                last = hops - hop
-                pairs = [(hops * 2, (hops - last) * 2), (1, last * 2 + 1)]
-                seen.insert(1, lax.ppermute(seen[0], ("sp", "tp"), pairs))
         held.append(seen)
     table = lambda count: tuple(tuple(range(k * peers, (k + 1) * peers)) for k in range(count))
     flat = lambda lists: [value for seen in lists for value in seen]

time: 174 us -> 174 us (level)
    ppermute x9 -> x11, waiting for transfers between devices: 10.1 us -> 27.6 us  [resident(): seen.append(lax.ppermute(seen[-1], ('sp', 'tp'), _pairs(peers, [hop], 1)))]
    ppermute x3 -> x1, waiting for transfers between devices: 17.3 us -> 0.01 us  [resident(): lax.ppermute(seen[0], ('sp', 'tp'), [(hops * 2, 0), (1, hops * 2 + 1)])]
    ppermute x9 -> x11, starting transfers between devices: 8.02 us -> 9.55 us  [resident(): seen.append(lax.ppermute(seen[-1], ('sp', 'tp'), _pairs(peers, [hop], 1)))]
where the time goes in v6:
time: 174 us; the launch traced here: 173 us
  starting transfers between devices  61.3 us (35%)
  waiting for transfers between devices  54.8 us (31%)
  Pallas kernels  49.8 us (29%)
  local copies, waits for them, and re-layouts  5.8 us (3%)
    ppermute x11, starting transfers between devices, resident(): arrived[step] = lax.ppermute(value, ('sp', 'tp'), _pairs(peers, depths, 0))  31.3 us
    ppermute x11, waiting for transfers between devices, resident(): seen.append(lax.ppermute(seen[-1], ('sp', 'tp'), _pairs(peers, [hop], 1)))  27.6 us
    pallas_call x13, Pallas kernels, partial_sum(): _call(partial_kernel, jax.ShapeDtypeStruct((2 * rows, 2 * width), jnp.bfl...  20 us
    ppermute x6, waiting for transfers between devices, to_offsets(): lax.ppermute(parts[k], 'sp', [(i, (i + k) % peers) for i in range(peers)])  18 us
    ppermute x6, starting transfers between devices, to_offsets(): lax.ppermute(parts[k], 'sp', [(i, (i + k) % peers) for i in range(peers)])  10.6 us
    ppermute x11, starting transfers between devices, resident(): seen.append(lax.ppermute(seen[-1], ('sp', 'tp'), _pairs(peers, [hop], 1)))  9.55 us
    ppermute x8, starting transfers between devices, swap(): return lax.ppermute(value, 'tp', SWAP)  8.63 us
    ppermute x11, waiting for transfers between devices, resident(): arrived[step] = lax.ppermute(value, ('sp', 'tp'), _pairs(peers, depths, 0))  6.95 us
  transfers between devices with their start and end apart: 37, of which 13 were waited for; matrix products, arithmetic and copies ran while one was open for 1% of the time, Pallas kernels for 22%

profile of v6, /device:TPU:0, one launch (start us, length us, event | category | flops | bytes accessed | tf_op | source)
XLA Modules:
  0.0 172.8 jit_solution(17164673544013363199)
XLA Ops:
  0.0 0.8 copy.19.fade_ref
  0.9 1.0 copy-done.10
  4.4 1.3 shard_map.164
  7.4 4.1 %shard_map.167 = bf16[7,1024,256]{2,1,0:T(8,128)(2,1)} custom-call(s32[1]{0:T(128)} %bitcast.side_ref, bf16[1024,1024]{1,0:T(8,128)(2,1)S(1)} %copy-done.6, bf16[1024,256]{1,0:T(8,128)(2,1)S(1)} %copy-done.12, bf16[1024,256]{1,0:T(8,128)(2,1)S(1)} %copy-done.13, bf16[1024,512]{1,0:T(8,128)(2,1)S(1)} %copy-done.8, bf16[1024,512]{1,0:T(8,128)(2,1)S(1)} %copy-done.9, ...), custom_call_target="tpu_custom_call" | custom-call | flops 99999997952 | bytes 7340032 | tf_op jit(solution)/shard_map/pallas_call | solution.py:430
  12.0 1.6 shard_map.166.own_ref
  13.6 2.7 %collective-permute-start.1 = (bf16[64,1152]{1,0:T(8,128)(2,1)S(1)}, bf16[64,1152]{1,0:T(8,128)(2,1)S(1)}, u32[]{:S(2)}, u32[]{:S(2)}) collective-permute-start(bf16[64,1152]{1,0:T(8,128)(2,1)S(1)} %get-tuple-element.38), channel_id=1, source_target_pairs={{0,8},{8,16},{16,24},{24,0},{1,9},{9,17},{17,25},{25,1},{2,10},{10... | collective-permute-start | bytes 442376 | tf_op jit(solution)/shard_map/ppermute | solution.py:389
  16.3 2.6 %collective-permute-start.2 = (bf16[64,1152]{1,0:T(8,128)(2,1)S(1)}, bf16[64,1152]{1,0:T(8,128)(2,1)S(1)}, u32[]{:S(2)}, u32[]{:S(2)}) collective-permute-start(bf16[64,1152]{1,0:T(8,128)(2,1)S(1)} %get-tuple-element.39), channel_id=1, source_target_pairs={{0,16},{8,24},{16,0},{24,8},{1,17},{9,25},{17,1},{25,9},{2,18},{10... | collective-permute-start | bytes 442376 | tf_op jit(solution)/shard_map/ppermute | solution.py:389
  18.9 1.3 collective-permute-start.3
  20.4 2.7 %collective-permute-done.1.refs_1_ = bf16[64,1152]{1,0:T(8,128)(2,1)S(1)} collective-permute-done((bf16[64,1152]{1,0:T(8,128)(2,1)S(1)}, bf16[64,1152]{1,0:T(8,128)(2,1)S(1)}, u32[]{:S(2)}, u32[]{:S(2)}) %collective-permute-start.1) | collective-permute-done | bytes 147488 | tf_op jit(solution)/shard_map/ppermute | solution.py:389
  23.2 6.0 %collective-permute-done.2.refs_2_ = bf16[64,1152]{1,0:T(8,128)(2,1)S(1)} collective-permute-done((bf16[64,1152]{1,0:T(8,128)(2,1)S(1)}, bf16[64,1152]{1,0:T(8,128)(2,1)S(1)}, u32[]{:S(2)}, u32[]{:S(2)}) %collective-permute-start.2) | collective-permute-done | bytes 147488 | tf_op jit(solution)/shard_map/ppermute | solution.py:389
  29.9 1.1 constant_dynamic-slice_fusion.2
  31.9 2.9 %shard_map.179 = (f32[512,256]{1,0:T(8,128)S(1)}, f32[512,256]{1,0:T(8,128)S(1)}) custom-call(s32[4]{0:T(128)S(1)} %copy-done.5, bf16[256,1152]{1,0:T(8,128)(2,1)S(1)} %bitcast.26, bf16[256,1152]{1,0:T(8,128)(2,1)S(1)} %bitcast.42, f32[24,512]{1,0:T(8,128)S(1)} %maximum_maximum_fusion.own_ref, f32[24,512]{1,0:T(8,128)S(1)} %collective-permute-done.15.other_ref), custom_call_target="tpu_custom_call" | custom-call | flops 1000000000 | bytes 1048576 | tf_op jit(solution)/shard_map/pallas_call | solution.py:518
  34.8 1.7 shard_map.173
  36.5 5.6 %collective-permute-start.10 = (bf16[512,512]{1,0:T(8,128)(2,1)S(1)}, bf16[512,512]{1,0:T(8,128)(2,1)S(1)}, u32[]{:S(2)}, u32[]{:S(2)}) collective-permute-start(bf16[512,512]{1,0:T(8,128)(2,1)S(1)} %shard_map.173), channel_id=1, source_target_pairs={{0,8},{25,17},{2,10},{27,19},{4,12},{29,21},{6,14},{31,23}} | collective-permute-start | bytes 1572872 | tf_op jit(solution)/shard_map/ppermute | solution.py:842
  42.1 1.7 shard_map.168
  43.8 1.3 collective-permute-start.6
  45.1 3.6 %collective-permute-done.10.rest_0_ = bf16[512,512]{1,0:T(8,128)(2,1)S(1)} collective-permute-done((bf16[512,512]{1,0:T(8,128)(2,1)S(1)}, bf16[512,512]{1,0:T(8,128)(2,1)S(1)}, u32[]{:S(2)}, u32[]{:S(2)}) %collective-permute-start.10) | collective-permute-done | bytes 524320 | tf_op jit(solution)/shard_map/ppermute | solution.py:842
  48.8 1.5 shard_map.174
  50.3 4.4 %collective-permute-start.11 = (bf16[512,512]{1,0:T(8,128)(2,1)S(1)}, bf16[512,512]{1,0:T(8,128)(2,1)S(1)}, u32[]{:S(2)}, u32[]{:S(2)}) collective-permute-start(bf16[512,512]{1,0:T(8,128)(2,1)S(1)} %shard_map.174), channel_id=1, source_target_pairs={{0,8},{25,17},{8,16},{17,9},{2,10},{27,19},{10,18},{19,11},{4,12},... | collective-permute-start | bytes 1572872 | tf_op jit(solution)/shard_map/ppermute | solution.py:842
  54.7 1.5 shard_map.169
  56.2 4.1 %collective-permute-start.7 = (bf16[512,512]{1,0:T(8,128)(2,1)S(1)}, bf16[512,512]{1,0:T(8,128)(2,1)S(1)}, u32[]{:S(2)}, u32[]{:S(2)}) collective-permute-start(bf16[512,512]{1,0:T(8,128)(2,1)S(1)} %shard_map.169), channel_id=1, source_target_pairs={{0,8},{25,17},{8,16},{17,9},{2,10},{27,19},{10,18},{19,11},{4,12},... | collective-permute-start | bytes 1572872 | tf_op jit(solution)/shard_map/ppermute | solution.py:842
  60.3 1.0 collective-permute-done.11.rest_0_
  61.4 1.5 shard_map.175
  62.9 4.4 %collective-permute-start.12 = (bf16[512,512]{1,0:T(8,128)(2,1)S(1)}, bf16[512,512]{1,0:T(8,128)(2,1)S(1)}, u32[]{:S(2)}, u32[]{:S(2)}) collective-permute-start(bf16[512,512]{1,0:T(8,128)(2,1)S(1)} %shard_map.175), channel_id=1, source_target_pairs={{0,8},{25,17},{8,16},{17,9},{16,24},{9,1},{2,10},{27,19},{10,18},{... | collective-permute-start | bytes 1572872 | tf_op jit(solution)/shard_map/ppermute | solution.py:842
  67.3 1.5 shard_map.170
  68.8 4.1 %collective-permute-start.8 = (bf16[512,512]{1,0:T(8,128)(2,1)S(1)}, bf16[512,512]{1,0:T(8,128)(2,1)S(1)}, u32[]{:S(2)}, u32[]{:S(2)}) collective-permute-start(bf16[512,512]{1,0:T(8,128)(2,1)S(1)} %shard_map.170), channel_id=1, source_target_pairs={{0,8},{25,17},{8,16},{17,9},{16,24},{9,1},{2,10},{27,19},{10,18},{... | collective-permute-start | bytes 1572872 | tf_op jit(solution)/shard_map/ppermute | solution.py:842
  72.9 1.0 collective-permute-done.12.rest_0_
  73.9 1.5 shard_map.176.key_value_ref
  75.5 4.4 %collective-permute-start.13 = (bf16[512,512]{1,0:T(8,128)(2,1)S(1)}, bf16[512,512]{1,0:T(8,128)(2,1)S(1)}, u32[]{:S(2)}, u32[]{:S(2)}) collective-permute-start(bf16[512,512]{1,0:T(8,128)(2,1)S(1)} %shard_map.176.key_value_ref), channel_id=1, source_target_pairs={{0,8},{25,17},{8,16},{17,9},{16,24},{9,1},{2,10},{27,19},{10,18},{... | collective-permute-start | bytes 1572872 | tf_op jit(solution)/shard_map/ppermute | solution.py:842
  79.9 1.5 shard_map.171.query_ref
  81.4 0.9 collective-permute-start.9
  82.3 2.9 %shard_map.184.refs_0_ = bf16[512,512]{1,0:T(8,128)(2,1)S(1)} custom-call(s32[4]{0:T(128)S(1)} %copy-done.5, f32[2,4]{1,0:T(2,128)S(1)} %get-tuple-element.64.slope_ref, f32[2,4]{1,0:T(2,128)S(1)} %bitcast.41, bf16[512,512]{1,0:T(8,128)(2,1)S(1)} %shard_map.176.key_value_ref, bf16[512,512]{1,0:T(8,128)(2,1)S(1)} %shard_map.171.query_ref), custom_call_target="tpu_custom_call" | custom-call | flops 2000000000 | bytes 2097152 | tf_op jit(solution)/shard_map/pallas_call | solution.py:646
  85.2 0.7 collective-permute-start.26
  85.9 1.2 collective-permute-done.13.rest_0_
  87.2 1.5 shard_map.177.query_ref
  88.7 0.7 collective-permute-start.14
  89.4 1.5 shard_map.172.query_key_ref
  90.9 0.7 collective-permute-start.20
  91.6 3.9 %shard_map.185.refs_4_ = bf16[512,512]{1,0:T(8,128)(2,1)S(1)} custom-call(s32[4]{0:T(128)S(1)} %copy-done.5, f32[2,4]{1,0:T(2,128)S(1)} %get-tuple-element.63.slope_ref, f32[2,4]{1,0:T(2,128)S(1)} %bitcast.40, bf16[512,512]{1,0:T(8,128)(2,1)S(1)} %shard_map.176.key_value_ref, bf16[512,512]{1,0:T(8,128)(2,1)S(1)} %shard_map.177.query_ref), custom_call_target="tpu_custom_call" | custom-call | flops 2000000000 | bytes 2097152 | tf_op jit(solution)/shard_map/pallas_call | solution.py:646
  95.6 0.7 collective-permute-start.29
  97.0 1.5 shard_map.178.value_ref
  99.2 2.3 %shard_map.180.refs_0_ = bf16[512,512]{1,0:T(8,128)(2,1)S(1)} custom-call(s32[4]{0:T(128)S(1)} %copy-done.5, bf16[512,512]{1,0:T(8,128)(2,1)S(1)} %shard_map.172.query_key_ref, bf16[512,512]{1,0:T(8,128)(2,1)S(1)} %shard_map.178.value_ref, f32[512,256]{1,0:T(8,128)S(1)} %get-tuple-element.50.running_ref, f32[4,128,256]{2,1,0:T(8,128)S(1)} %copy-done.14, ...), custom_call_target="tpu_custom_call" | custom-call | flops 2000000000 | bytes 2097152 | tf_op jit(solution)/shard_map/pallas_call | solution.py:566
  101.5 0.7 collective-permute-start.17
  102.2 1.5 shard_map.181.query_key_ref
  103.7 7.0 %collective-permute-start.32 = (bf16[512,1024]{1,0:T(8,128)(2,1)S(1)}, bf16[512,1024]{1,0:T(8,128)(2,1)S(1)}, u32[]{:S(2)}, u32[]{:S(2)}) collective-permute-start(bf16[512,1024]{1,0:T(8,128)(2,1)S(1)} %constant_dynamic-slice_fusion), channel_id=1, source_target_pairs={{0,1},{1,0},{2,3},{3,2},{4,5},{5,4},{6,7},{7,6},{8,9},{9,8},{10,11... | collective-permute-start | bytes 3145736 | tf_op jit(solution)/shard_map/ppermute | solution.py:758
  110.7 1.3 collective-permute-start.28
  112.7 0.7 collective-permute-start.18
  113.4 1.5 shard_map.182.value_ref
  115.0 2.3 %shard_map.183.refs_4_ = bf16[512,512]{1,0:T(8,128)(2,1)S(1)} custom-call(s32[4]{0:T(128)S(1)} %copy-done.5, bf16[512,512]{1,0:T(8,128)(2,1)S(1)} %shard_map.181.query_key_ref, bf16[512,512]{1,0:T(8,128)(2,1)S(1)} %shard_map.182.value_ref, f32[512,256]{1,0:T(8,128)S(1)} %get-tuple-element.52.running_ref, f32[4,128,256]{2,1,0:T(8,128)S(1)} %copy-done.14, ...), custom_call_target="tpu_custom_call" | custom-call | flops 2000000000 | bytes 2097152 | tf_op jit(solution)/shard_map/pallas_call | solution.py:566
  117.3 0.8 collective-permute-start.22
  118.1 1.3 collective-permute-start.31
  119.4 2.4 %collective-permute-done.28.refs_3_ = bf16[512,512]{1,0:T(8,128)(2,1)S(1)} collective-permute-done((bf16[512,512]{1,0:T(8,128)(2,1)S(1)}, bf16[512,512]{1,0:T(8,128)(2,1)S(1)}, u32[]{:S(2)}, u32[]{:S(2)}) %collective-permute-start.28) | collective-permute-done | bytes 524320 | tf_op jit(solution)/shard_map/ppermute | solution.py:887
  121.8 1.3 collective-permute-start.24
  123.1 1.3 collective-permute-start.19
  124.4 0.7 collective-permute-start.23
  125.1 21.7 %collective-permute-done.31.refs_7_ = bf16[512,512]{1,0:T(8,128)(2,1)S(1)} collective-permute-done((bf16[512,512]{1,0:T(8,128)(2,1)S(1)}, bf16[512,512]{1,0:T(8,128)(2,1)S(1)}, u32[]{:S(2)}, u32[]{:S(2)}) %collective-permute-start.31) | collective-permute-done | bytes 524320 | tf_op jit(solution)/shard_map/ppermute | solution.py:887
  146.8 2.1 %shard_map.186.refs_10_ = f32[512,1024]{1,0:T(8,128)S(1)} custom-call(s32[4]{0:T(128)S(1)} %copy-done.5, bf16[512,512]{1,0:T(8,128)(2,1)S(1)} %shard_map.184.refs_0_, bf16[512,512]{1,0:T(8,128)(2,1)S(1)} %collective-permute-done.26.refs_1_, bf16[512,512]{1,0:T(8,128)(2,1)S(1)} %collective-permute-done.27.refs_2_, ...), custom_call_target="tpu_custom_call" | custom-call | flops 1073741824 | bytes 4194304 | tf_op jit(solution)/shard_map/pallas_call | solution.py:703
  149.0 3.4 %collective-permute-done.19.refs_3_ = bf16[512,512]{1,0:T(8,128)(2,1)S(1)} collective-permute-done((bf16[512,512]{1,0:T(8,128)(2,1)S(1)}, bf16[512,512]{1,0:T(8,128)(2,1)S(1)}, u32[]{:S(2)}, u32[]{:S(2)}) %collective-permute-start.19) | collective-permute-done | bytes 524320 | tf_op jit(solution)/shard_map/ppermute | solution.py:887
  152.4 3.2 %shard_map.187 = (bf16[256,1024]{1,0:T(8,128)(2,1)S(1)}, bf16[256,1024]{1,0:T(8,128)(2,1)S(1)}) custom-call(s32[4]{0:T(128)S(1)} %copy-done.5, bf16[512,512]{1,0:T(8,128)(2,1)S(1)} %shard_map.180.refs_0_, bf16[512,512]{1,0:T(8,128)(2,1)S(1)} %collective-permute-done.17.refs_1_, bf16[512,512]{1,0:T(8,128)(2,1)S(1)} %collective-permute-done.18.refs_2_, ...), custom_call_target="tpu_custom_call" | custom-call | flops 1073741824 | bytes 4194304 | tf_op jit(solution)/shard_map/pallas_call | solution.py:703
  155.7 1.9 %collective-permute-done.33.given_ref = bf16[256,1024]{1,0:T(8,128)(2,1)S(1)} collective-permute-done((bf16[256,1024]{1,0:T(8,128)(2,1)S(1)}, bf16[256,1024]{1,0:T(8,128)(2,1)S(1)}, u32[]{:S(2)}, u32[]{:S(2)}) %collective-permute-start.33) | collective-permute-done | bytes 524320 | tf_op jit(solution)/shard_map/ppermute | solution.py:758
  158.6 3.5 %collective-permute-start.36 = (bf16[64,1024]{1,0:T(8,128)(2,1)S(1)}, bf16[64,1024]{1,0:T(8,128)(2,1)S(1)}, u32[]{:S(2)}, u32[]{:S(2)}) collective-permute-start(bf16[64,1024]{1,0:T(8,128)(2,1)S(1)} %get-tuple-element.60), channel_id=1, source_target_pairs={{0,24},{8,0},{16,8},{24,16},{1,25},{9,1},{17,9},{25,17},{2,26},{10... | collective-permute-start | bytes 393224 | tf_op jit(solution)/shard_map/ppermute | solution.py:389
  162.1 4.5 %collective-permute-done.34.refs_1_ = bf16[64,1024]{1,0:T(8,128)(2,1)S(1)} collective-permute-done((bf16[64,1024]{1,0:T(8,128)(2,1)S(1)}, bf16[64,1024]{1,0:T(8,128)(2,1)S(1)}, u32[]{:S(2)}, u32[]{:S(2)}) %collective-permute-start.34) | collective-permute-done | bytes 131104 | tf_op jit(solution)/shard_map/ppermute | solution.py:389
  166.6 4.8 %collective-permute-done.35.refs_2_ = bf16[64,1024]{1,0:T(8,128)(2,1)S(1)} collective-permute-done((bf16[64,1024]{1,0:T(8,128)(2,1)S(1)}, bf16[64,1024]{1,0:T(8,128)(2,1)S(1)}, u32[]{:S(2)}, u32[]{:S(2)}) %collective-permute-start.35) | collective-permute-done | bytes 131104 | tf_op jit(solution)/shard_map/ppermute | solution.py:389
  171.4 1.4 shard_map.189
  (105 shorter events, 9.6 us)
Async XLA Ops:
  0.9 1.0 copy-start.10
  1.9 2.4 %copy-start.4 = (s32[4]{0:T(128)}, s32[4]{0:T(128)S(1)}, u32[]{:S(2)}) copy-start(s32[4]{0:T(128)S(1)} %pad_add_fusion.place_ref) | copy-start | bytes 52
  1.9 2.4 %copy-start.11 = (bf16[128,2048]{1,0:T(8,128)(2,1)S(1)}, bf16[128,2048]{1,0:T(8,128)(2,1)}, u32[]{:S(2)}) copy-start(bf16[128,2048]{1,0:T(8,128)(2,1)} %x_ref.3) | copy-start | bytes 1572868
  1.9 2.4 %copy-start.15 = (bf16[4096,16]{0,1:T(8,128)(2,1)S(1)}, bf16[4096,16]{0,1:T(8,128)(2,1)}, u32[]{:S(2)}) copy-start(bf16[4096,16]{0,1:T(8,128)(2,1)} %param.25) | copy-start | bytes 393220
  1.9 2.4 %copy-start.16 = (f32[4096]{0:T(1024)S(1)}, f32[4096]{0:T(1024)}, u32[]{:S(2)}) copy-start(f32[4096]{0:T(1024)} %param.18) | copy-start | bytes 49156
  2.6 1.7 %collective-permute-start = (bf16[64,2176]{1,0:T(8,128)(2,1)S(1)}, bf16[64,2176]{1,0:T(8,128)(2,1)S(1)}, u32[]{:S(2)}, u32[]{:S(2)}) collective-permute-start(bf16[64,2176]{1,0:T(8,128)(2,1)S(1)} %shard_map.163), channel_id=1, source_target_pairs={{0,1},{1,0},{2,3},{3,2},{4,5},{5,4},{6,7},{7,6},{8,9},{9,8},{10,11... | collective-permute-start | bytes 835592 | tf_op jit(solution)/shard_map/ppermute | solution.py:758
  4.3 1.6 copy-start.6
  4.3 2.2 %copy-start.7 = (bf16[1024,1024]{1,0:T(8,128)(2,1)S(1)}, bf16[1024,1024]{1,0:T(8,128)(2,1)}, u32[]{:S(2)}) copy-start(bf16[1024,1024]{1,0:T(8,128)(2,1)} %lv.1) | copy-start | bytes 6291460
  4.3 2.5 %copy-start.8 = (bf16[1024,512]{1,0:T(8,128)(2,1)S(1)}, bf16[1024,512]{1,0:T(8,128)(2,1)}, u32[]{:S(2)}) copy-start(bf16[1024,512]{1,0:T(8,128)(2,1)} %lq.1) | copy-start | bytes 3145732
  4.4 2.8 %copy-start.9 = (bf16[1024,512]{1,0:T(8,128)(2,1)S(1)}, bf16[1024,512]{1,0:T(8,128)(2,1)}, u32[]{:S(2)}) copy-start(bf16[1024,512]{1,0:T(8,128)(2,1)} %lk.1) | copy-start | bytes 3145732
  4.4 2.9 %copy-start.12 = (bf16[1024,256]{1,0:T(8,128)(2,1)S(1)}, bf16[1024,256]{1,0:T(8,128)(2,1)}, u32[]{:S(2)}) copy-start(bf16[1024,256]{1,0:T(8,128)(2,1)} %wk.1) | copy-start | bytes 1572868
  4.4 3.0 %copy-start.13 = (bf16[1024,256]{1,0:T(8,128)(2,1)S(1)}, bf16[1024,256]{1,0:T(8,128)(2,1)}, u32[]{:S(2)}) copy-start(bf16[1024,256]{1,0:T(8,128)(2,1)} %wv.1) | copy-start | bytes 1572868
  11.5 8.8 %copy-start.23 = (f32[16]{0:T(128)S(1)}, f32[16]{0:T(128)}, u32[]{:S(2)}) copy-start(f32[16]{0:T(128)} %param.30) | copy-start | bytes 196
  11.5 8.8 %copy-start.20 = (bf16[16,512]{1,0:T(8,128)(2,1)S(1)}, bf16[16,512]{1,0:T(8,128)(2,1)}, u32[]{:S(2)}) copy-start(bf16[16,512]{1,0:T(8,128)(2,1)} %param.26) | copy-start | bytes 49156
  11.5 8.8 %copy-start.21 = (f32[512]{0:T(512)S(1)}, f32[512]{0:T(512)}, u32[]{:S(2)}) copy-start(f32[512]{0:T(512)} %param.27) | copy-start | bytes 6148
  11.5 8.8 %copy-start.22 = (f32[24]{0:T(128)S(1)}, f32[24]{0:T(128)}, u32[]{:S(2)}) copy-start(f32[24]{0:T(128)} %pad.12.clone) | copy-start | bytes 292
  11.5 11.7 %copy-start.14 = (f32[4,128,256]{2,1,0:T(8,128)S(1)}, f32[4,128,256]{2,1,0:T(8,128)}, u32[]{:S(2)}) copy-start(f32[4,128,256]{2,1,0:T(8,128)} %own_ref.1) | copy-start | bytes 1572868
  11.5 17.7 %copy-start.5 = (s32[4]{0:T(128)S(1)}, s32[4]{0:T(128)}, u32[]{:S(2)}) copy-start(s32[4]{0:T(128)} %copy-done.4) | copy-start | bytes 52
  11.5 18.3 %copy-start.2 = (bf16[1024,1024]{1,0:T(8,128)(2,1)S(1)}, bf16[1024,1024]{1,0:T(8,128)(2,1)}, u32[]{:S(2)}) copy-start(bf16[1024,1024]{1,0:T(8,128)(2,1)} %refs_8_.1) | copy-start | bytes 6291460
  11.5 23.3 %collective-permute-start.5 = (bf16[7,1024,256]{2,1,0:T(8,128)(2,1)}, bf16[7,1024,256]{2,1,0:T(8,128)(2,1)}, u32[]{:S(2)}, u32[]{:S(2)}) collective-permute-start(bf16[7,1024,256]{2,1,0:T(8,128)(2,1)} %shard_map.167), channel_id=1, source_target_pairs={{0,1},{1,0},{2,3},{3,2},{4,5},{5,4},{6,7},{7,6},{8,9},{9,8},{10,11... | collective-permute-start | bytes 11010056 | tf_op jit(solution)/shard_map/ppermute | solution.py:758
  13.6 17.9 %copy-start.18 = (bf16[7,1024,256]{2,1,0:T(8,128)(2,1)}, bf16[7,1024,256]{2,1,0:T(8,128)(2,1)S(1)}, u32[]{:S(2)}) copy-start(bf16[7,1024,256]{2,1,0:T(8,128)(2,1)S(1)} %shard_map.166.own_ref) | copy-start | bytes 11010052
  13.6 17.8 %copy-start = (bf16[1024,1024]{1,0:T(8,128)(2,1)S(1)}, bf16[1024,1024]{1,0:T(8,128)(2,1)}, u32[]{:S(2)}) copy-start(bf16[1024,1024]{1,0:T(8,128)(2,1)} %refs_8_) | copy-start | bytes 6291460
  13.6 9.6 %collective-permute-start.1 = (bf16[64,1152]{1,0:T(8,128)(2,1)S(1)}, bf16[64,1152]{1,0:T(8,128)(2,1)S(1)}, u32[]{:S(2)}, u32[]{:S(2)}) collective-permute-start(bf16[64,1152]{1,0:T(8,128)(2,1)S(1)} %get-tuple-element.38), channel_id=1, source_target_pairs={{0,8},{8,16},{16,24},{24,0},{1,9},{9,17},{17,25},{25,1},{2,10},{10... | collective-permute-start | bytes 442376 | tf_op jit(solution)/shard_map/ppermute | solution.py:389
  16.3 12.8 %collective-permute-start.2 = (bf16[64,1152]{1,0:T(8,128)(2,1)S(1)}, bf16[64,1152]{1,0:T(8,128)(2,1)S(1)}, u32[]{:S(2)}, u32[]{:S(2)}) collective-permute-start(bf16[64,1152]{1,0:T(8,128)(2,1)S(1)} %get-tuple-element.39), channel_id=1, source_target_pairs={{0,16},{8,24},{16,0},{24,8},{1,17},{9,25},{17,1},{25,9},{2,18},{10... | collective-permute-start | bytes 442376 | tf_op jit(solution)/shard_map/ppermute | solution.py:389
  18.9 10.2 %collective-permute-start.3 = (bf16[64,1152]{1,0:T(8,128)(2,1)S(1)}, bf16[64,1152]{1,0:T(8,128)(2,1)S(1)}, u32[]{:S(2)}, u32[]{:S(2)}) collective-permute-start(bf16[64,1152]{1,0:T(8,128)(2,1)S(1)} %get-tuple-element.40), channel_id=1, source_target_pairs={{0,24},{8,0},{16,8},{24,16},{1,25},{9,1},{17,9},{25,17},{2,26},{10... | collective-permute-start | bytes 442376 | tf_op jit(solution)/shard_map/ppermute | solution.py:389
  20.4 11.3 %collective-permute-start.15 = (f32[24,512]{1,0:T(8,128)S(1)}, f32[24,512]{1,0:T(8,128)S(1)}, u32[]{:S(2)}, u32[]{:S(2)}) collective-permute-start(f32[24,512]{1,0:T(8,128)S(1)} %maximum_maximum_fusion.own_ref), channel_id=1, source_target_pairs={{0,1},{1,0},{2,3},{3,2},{4,5},{5,4},{6,7},{7,6},{8,9},{9,8},{10,11... | collective-permute-start | bytes 147464 | tf_op jit(solution)/shard_map/ppermute | solution.py:758
  23.2 75.4 %collective-permute-start.16 = (f32[4,128,256]{2,1,0:T(8,128)S(1)}, f32[4,128,256]{2,1,0:T(8,128)S(1)}, u32[]{:S(2)}, u32[]{:S(2)}) collective-permute-start(f32[4,128,256]{2,1,0:T(8,128)S(1)} %copy-done.14), channel_id=1, source_target_pairs={{0,1},{1,0},{2,3},{3,2},{4,5},{5,4},{6,7},{7,6},{8,9},{9,8},{10,11... | collective-permute-start | bytes 1572872 | tf_op jit(solution)/shard_map/ppermute | solution.py:758
  29.8 2.1 %collective-permute-start.4 = (bf16[4,64,1152]{2,1,0:T(8,128)(2,1)S(1)}, bf16[4,64,1152]{2,1,0:T(8,128)(2,1)S(1)}, u32[]{:S(2)}, u32[]{:S(2)}) collective-permute-start(bf16[4,64,1152]{2,1,0:T(8,128)(2,1)S(1)} %shard_map.165), channel_id=1, source_target_pairs={{0,1},{1,0},{2,3},{3,2},{4,5},{5,4},{6,7},{7,6},{8,9},{9,8},{10,11... | collective-permute-start | bytes 1769480 | tf_op jit(solution)/shard_map/ppermute | solution.py:758
  30.9 118.0 %collective-permute-start.25 = (bf16[512,1024]{1,0:T(8,128)(2,1)}, bf16[512,1024]{1,0:T(8,128)(2,1)}, u32[]{:S(2)}, u32[]{:S(2)}) collective-permute-start(bf16[512,1024]{1,0:T(8,128)(2,1)} %constant_dynamic-slice_fusion.2), channel_id=1, source_target_pairs={{0,1},{1,0},{2,3},{3,2},{4,5},{5,4},{6,7},{7,6},{8,9},{9,8},{10,11... | collective-permute-start | bytes 3145736 | tf_op jit(solution)/shard_map/ppermute | solution.py:758
  31.9 3.0 %copy-start.19 = (bf16[7,1024,256]{2,1,0:T(8,128)(2,1)S(1)}, bf16[7,1024,256]{2,1,0:T(8,128)(2,1)}, u32[]{:S(2)}) copy-start(bf16[7,1024,256]{2,1,0:T(8,128)(2,1)} %copy-done.18) | copy-start | bytes 11010052
  36.5 12.2 %collective-permute-start.10 = (bf16[512,512]{1,0:T(8,128)(2,1)S(1)}, bf16[512,512]{1,0:T(8,128)(2,1)S(1)}, u32[]{:S(2)}, u32[]{:S(2)}) collective-permute-start(bf16[512,512]{1,0:T(8,128)(2,1)S(1)} %shard_map.173), channel_id=1, source_target_pairs={{0,8},{25,17},{2,10},{27,19},{4,12},{29,21},{6,14},{31,23}} | collective-permute-start | bytes 1572872 | tf_op jit(solution)/shard_map/ppermute | solution.py:842
  43.8 10.9 %collective-permute-start.6 = (bf16[512,512]{1,0:T(8,128)(2,1)S(1)}, bf16[512,512]{1,0:T(8,128)(2,1)S(1)}, u32[]{:S(2)}, u32[]{:S(2)}) collective-permute-start(bf16[512,512]{1,0:T(8,128)(2,1)S(1)} %shard_map.168), channel_id=1, source_target_pairs={{0,8},{25,17},{2,10},{27,19},{4,12},{29,21},{6,14},{31,23}} | collective-permute-start | bytes 1572872 | tf_op jit(solution)/shard_map/ppermute | solution.py:842
  50.3 11.1 %collective-permute-start.11 = (bf16[512,512]{1,0:T(8,128)(2,1)S(1)}, bf16[512,512]{1,0:T(8,128)(2,1)S(1)}, u32[]{:S(2)}, u32[]{:S(2)}) collective-permute-start(bf16[512,512]{1,0:T(8,128)(2,1)S(1)} %shard_map.174), channel_id=1, source_target_pairs={{0,8},{25,17},{8,16},{17,9},{2,10},{27,19},{10,18},{19,11},{4,12},... | collective-permute-start | bytes 1572872 | tf_op jit(solution)/shard_map/ppermute | solution.py:842
  56.2 11.1 %collective-permute-start.7 = (bf16[512,512]{1,0:T(8,128)(2,1)S(1)}, bf16[512,512]{1,0:T(8,128)(2,1)S(1)}, u32[]{:S(2)}, u32[]{:S(2)}) collective-permute-start(bf16[512,512]{1,0:T(8,128)(2,1)S(1)} %shard_map.169), channel_id=1, source_target_pairs={{0,8},{25,17},{8,16},{17,9},{2,10},{27,19},{10,18},{19,11},{4,12},... | collective-permute-start | bytes 1572872 | tf_op jit(solution)/shard_map/ppermute | solution.py:842
  62.9 11.1 %collective-permute-start.12 = (bf16[512,512]{1,0:T(8,128)(2,1)S(1)}, bf16[512,512]{1,0:T(8,128)(2,1)S(1)}, u32[]{:S(2)}, u32[]{:S(2)}) collective-permute-start(bf16[512,512]{1,0:T(8,128)(2,1)S(1)} %shard_map.175), channel_id=1, source_target_pairs={{0,8},{25,17},{8,16},{17,9},{16,24},{9,1},{2,10},{27,19},{10,18},{... | collective-permute-start | bytes 1572872 | tf_op jit(solution)/shard_map/ppermute | solution.py:842
  68.8 11.1 %collective-permute-start.8 = (bf16[512,512]{1,0:T(8,128)(2,1)S(1)}, bf16[512,512]{1,0:T(8,128)(2,1)S(1)}, u32[]{:S(2)}, u32[]{:S(2)}) collective-permute-start(bf16[512,512]{1,0:T(8,128)(2,1)S(1)} %shard_map.170), channel_id=1, source_target_pairs={{0,8},{25,17},{8,16},{17,9},{16,24},{9,1},{2,10},{27,19},{10,18},{... | collective-permute-start | bytes 1572872 | tf_op jit(solution)/shard_map/ppermute | solution.py:842
  75.5 11.7 %collective-permute-start.13 = (bf16[512,512]{1,0:T(8,128)(2,1)S(1)}, bf16[512,512]{1,0:T(8,128)(2,1)S(1)}, u32[]{:S(2)}, u32[]{:S(2)}) collective-permute-start(bf16[512,512]{1,0:T(8,128)(2,1)S(1)} %shard_map.176.key_value_ref), channel_id=1, source_target_pairs={{0,8},{25,17},{8,16},{17,9},{16,24},{9,1},{2,10},{27,19},{10,18},{... | collective-permute-start | bytes 1572872 | tf_op jit(solution)/shard_map/ppermute | solution.py:842
  81.4 8.0 %collective-permute-start.9 = (bf16[512,512]{1,0:T(8,128)(2,1)S(1)}, bf16[512,512]{1,0:T(8,128)(2,1)S(1)}, u32[]{:S(2)}, u32[]{:S(2)}) collective-permute-start(bf16[512,512]{1,0:T(8,128)(2,1)S(1)} %shard_map.171.query_ref), channel_id=1, source_target_pairs={{8,16},{17,9},{16,24},{9,1},{10,18},{19,11},{18,26},{11,3},{12,20}... | collective-permute-start | bytes 1572872 | tf_op jit(solution)/shard_map/ppermute | solution.py:842
  85.2 10.3 %collective-permute-start.26 = (bf16[512,512]{1,0:T(8,128)(2,1)S(1)}, bf16[512,512]{1,0:T(8,128)(2,1)S(1)}, u32[]{:S(2)}, u32[]{:S(2)}) collective-permute-start(bf16[512,512]{1,0:T(8,128)(2,1)S(1)} %shard_map.184.refs_0_), channel_id=1, source_target_pairs={{1,9},{24,16},{3,11},{26,18},{5,13},{28,20},{7,15},{30,22}} | collective-permute-start | bytes 1572872 | tf_op jit(solution)/shard_map/ppermute | solution.py:887
  88.7 7.6 %collective-permute-start.14 = (bf16[512,512]{1,0:T(8,128)(2,1)S(1)}, bf16[512,512]{1,0:T(8,128)(2,1)S(1)}, u32[]{:S(2)}, u32[]{:S(2)}) collective-permute-start(bf16[512,512]{1,0:T(8,128)(2,1)S(1)} %shard_map.177.query_ref), channel_id=1, source_target_pairs={{8,16},{17,9},{16,24},{9,1},{10,18},{19,11},{18,26},{11,3},{12,20}... | collective-permute-start | bytes 1572872 | tf_op jit(solution)/shard_map/ppermute | solution.py:842
  90.9 10.6 %collective-permute-start.20 = (bf16[512,512]{1,0:T(8,128)(2,1)S(1)}, bf16[512,512]{1,0:T(8,128)(2,1)S(1)}, u32[]{:S(2)}, u32[]{:S(2)}) collective-permute-start(bf16[512,512]{1,0:T(8,128)(2,1)S(1)} %shard_map.172.query_key_ref), channel_id=1, source_target_pairs={{16,24},{9,1},{18,26},{11,3},{20,28},{13,5},{22,30},{15,7}} | collective-permute-start | bytes 1572872 | tf_op jit(solution)/shard_map/ppermute | solution.py:842
  95.6 15.2 %collective-permute-start.29 = (bf16[512,512]{1,0:T(8,128)(2,1)S(1)}, bf16[512,512]{1,0:T(8,128)(2,1)S(1)}, u32[]{:S(2)}, u32[]{:S(2)}) collective-permute-start(bf16[512,512]{1,0:T(8,128)(2,1)S(1)} %shard_map.185.refs_4_), channel_id=1, source_target_pairs={{1,9},{24,16},{3,11},{26,18},{5,13},{28,20},{7,15},{30,22}} | collective-permute-start | bytes 1572872 | tf_op jit(solution)/shard_map/ppermute | solution.py:887
  96.3 7.5 %collective-permute-start.27 = (bf16[512,512]{1,0:T(8,128)(2,1)S(1)}, bf16[512,512]{1,0:T(8,128)(2,1)S(1)}, u32[]{:S(2)}, u32[]{:S(2)}) collective-permute-start(bf16[512,512]{1,0:T(8,128)(2,1)S(1)} %collective-permute-done.26.refs_1_), channel_id=1, source_target_pairs={{9,17},{16,8},{11,19},{18,10},{13,21},{20,12},{15,23},{22,14}} | collective-permute-start | bytes 1572872 | tf_op jit(solution)/shard_map/ppermute | solution.py:887
  97.0 2.2 %copy-start.17 = (f32[256]{0:T(256)S(1)}, f32[256]{0:T(256)}, u32[]{:S(2)}) copy-start(f32[256]{0:T(256)} %param.31) | copy-start | bytes 3076
  98.5 14.2 %collective-permute-start.21 = (bf16[512,512]{1,0:T(8,128)(2,1)S(1)}, bf16[512,512]{1,0:T(8,128)(2,1)S(1)}, u32[]{:S(2)}, u32[]{:S(2)}) collective-permute-start(bf16[512,512]{1,0:T(8,128)(2,1)S(1)} %shard_map.178.value_ref), channel_id=1, source_target_pairs={{16,24},{9,1},{18,26},{11,3},{20,28},{13,5},{22,30},{15,7}} | collective-permute-start | bytes 1572872 | tf_op jit(solution)/shard_map/ppermute | solution.py:842
  101.5 10.5 %collective-permute-start.17 = (bf16[512,512]{1,0:T(8,128)(2,1)S(1)}, bf16[512,512]{1,0:T(8,128)(2,1)S(1)}, u32[]{:S(2)}, u32[]{:S(2)}) collective-permute-start(bf16[512,512]{1,0:T(8,128)(2,1)S(1)} %shard_map.180.refs_0_), channel_id=1, source_target_pairs={{1,9},{24,16},{3,11},{26,18},{5,13},{28,20},{7,15},{30,22}} | collective-permute-start | bytes 1572872 | tf_op jit(solution)/shard_map/ppermute | solution.py:887
  103.7 13.5 %collective-permute-start.32 = (bf16[512,1024]{1,0:T(8,128)(2,1)S(1)}, bf16[512,1024]{1,0:T(8,128)(2,1)S(1)}, u32[]{:S(2)}, u32[]{:S(2)}) collective-permute-start(bf16[512,1024]{1,0:T(8,128)(2,1)S(1)} %constant_dynamic-slice_fusion), channel_id=1, source_target_pairs={{0,1},{1,0},{2,3},{3,2},{4,5},{5,4},{6,7},{7,6},{8,9},{9,8},{10,11... | collective-permute-start | bytes 3145736 | tf_op jit(solution)/shard_map/ppermute | solution.py:758
  110.7 11.1 %collective-permute-start.28 = (bf16[512,512]{1,0:T(8,128)(2,1)S(1)}, bf16[512,512]{1,0:T(8,128)(2,1)S(1)}, u32[]{:S(2)}, u32[]{:S(2)}) collective-permute-start(bf16[512,512]{1,0:T(8,128)(2,1)S(1)} %collective-permute-done.27.refs_2_), channel_id=1, source_target_pairs={{17,25},{8,0},{19,27},{10,2},{21,29},{12,4},{23,31},{14,6}} | collective-permute-start | bytes 1572872 | tf_op jit(solution)/shard_map/ppermute | solution.py:887
  112.0 6.1 %collective-permute-start.30 = (bf16[512,512]{1,0:T(8,128)(2,1)S(1)}, bf16[512,512]{1,0:T(8,128)(2,1)S(1)}, u32[]{:S(2)}, u32[]{:S(2)}) collective-permute-start(bf16[512,512]{1,0:T(8,128)(2,1)S(1)} %collective-permute-done.29.refs_5_), channel_id=1, source_target_pairs={{9,17},{16,8},{11,19},{18,10},{13,21},{20,12},{15,23},{22,14}} | collective-permute-start | bytes 1572872 | tf_op jit(solution)/shard_map/ppermute | solution.py:887
  112.7 10.3 %collective-permute-start.18 = (bf16[512,512]{1,0:T(8,128)(2,1)S(1)}, bf16[512,512]{1,0:T(8,128)(2,1)S(1)}, u32[]{:S(2)}, u32[]{:S(2)}) collective-permute-start(bf16[512,512]{1,0:T(8,128)(2,1)S(1)} %collective-permute-done.17.refs_1_), channel_id=1, source_target_pairs={{9,17},{16,8},{11,19},{18,10},{13,21},{20,12},{15,23},{22,14}} | collective-permute-start | bytes 1572872 | tf_op jit(solution)/shard_map/ppermute | solution.py:887
  115.0 31.8 %copy-start.1 = (bf16[1024,1024]{1,0:T(8,128)(2,1)S(1)}, bf16[1024,1024]{1,0:T(8,128)(2,1)}, u32[]{:S(2)}) copy-start(bf16[1024,1024]{1,0:T(8,128)(2,1)} %refs_8_) | copy-start | bytes 6291460
  117.2 35.2 %copy-start.3 = (bf16[1024,1024]{1,0:T(8,128)(2,1)S(1)}, bf16[1024,1024]{1,0:T(8,128)(2,1)}, u32[]{:S(2)}) copy-start(bf16[1024,1024]{1,0:T(8,128)(2,1)} %refs_8_.1) | copy-start | bytes 6291460
  117.3 7.1 %collective-permute-start.22 = (bf16[512,512]{1,0:T(8,128)(2,1)S(1)}, bf16[512,512]{1,0:T(8,128)(2,1)S(1)}, u32[]{:S(2)}, u32[]{:S(2)}) collective-permute-start(bf16[512,512]{1,0:T(8,128)(2,1)S(1)} %shard_map.183.refs_4_), channel_id=1, source_target_pairs={{1,9},{24,16},{3,11},{26,18},{5,13},{28,20},{7,15},{30,22}} | collective-permute-start | bytes 1572872 | tf_op jit(solution)/shard_map/ppermute | solution.py:887
  118.1 28.7 %collective-permute-start.31 = (bf16[512,512]{1,0:T(8,128)(2,1)S(1)}, bf16[512,512]{1,0:T(8,128)(2,1)S(1)}, u32[]{:S(2)}, u32[]{:S(2)}) collective-permute-start(bf16[512,512]{1,0:T(8,128)(2,1)S(1)} %collective-permute-done.30.refs_6_), channel_id=1, source_target_pairs={{17,25},{8,0},{19,27},{10,2},{21,29},{12,4},{23,31},{14,6}} | collective-permute-start | bytes 1572872 | tf_op jit(solution)/shard_map/ppermute | solution.py:887
  121.8 27.2 %collective-permute-start.24 = (bf16[512,512]{1,0:T(8,128)(2,1)S(1)}, bf16[512,512]{1,0:T(8,128)(2,1)S(1)}, u32[]{:S(2)}, u32[]{:S(2)}) collective-permute-start(bf16[512,512]{1,0:T(8,128)(2,1)S(1)} %shard_map.183.refs_4_), channel_id=1, source_target_pairs={{24,0},{1,25},{26,2},{3,27},{28,4},{5,29},{30,6},{7,31}} | collective-permute-start | bytes 1572872 | tf_op jit(solution)/shard_map/ppermute | solution.py:885
  123.1 29.3 %collective-permute-start.19 = (bf16[512,512]{1,0:T(8,128)(2,1)S(1)}, bf16[512,512]{1,0:T(8,128)(2,1)S(1)}, u32[]{:S(2)}, u32[]{:S(2)}) collective-permute-start(bf16[512,512]{1,0:T(8,128)(2,1)S(1)} %collective-permute-done.18.refs_2_), channel_id=1, source_target_pairs={{17,25},{8,0},{19,27},{10,2},{21,29},{12,4},{23,31},{14,6}} | collective-permute-start | bytes 1572872 | tf_op jit(solution)/shard_map/ppermute | solution.py:887
  124.4 28.0 %collective-permute-start.23 = (bf16[512,512]{1,0:T(8,128)(2,1)S(1)}, bf16[512,512]{1,0:T(8,128)(2,1)S(1)}, u32[]{:S(2)}, u32[]{:S(2)}) collective-permute-start(bf16[512,512]{1,0:T(8,128)(2,1)S(1)} %collective-permute-done.22.refs_5_), channel_id=1, source_target_pairs={{9,17},{16,8},{11,19},{18,10},{13,21},{20,12},{15,23},{22,14}} | collective-permute-start | bytes 1572872 | tf_op jit(solution)/shard_map/ppermute | solution.py:887
  155.6 2.0 %collective-permute-start.33 = (bf16[256,1024]{1,0:T(8,128)(2,1)S(1)}, bf16[256,1024]{1,0:T(8,128)(2,1)S(1)}, u32[]{:S(2)}, u32[]{:S(2)}) collective-permute-start(bf16[256,1024]{1,0:T(8,128)(2,1)S(1)} %get-tuple-element.56), channel_id=1, source_target_pairs={{0,1},{1,0},{2,3},{3,2},{4,5},{5,4},{6,7},{7,6},{8,9},{9,8},{10,11... | collective-permute-start | bytes 1572872 | tf_op jit(solution)/shard_map/ppermute | solution.py:758
  158.3 8.4 %collective-permute-start.34 = (bf16[64,1024]{1,0:T(8,128)(2,1)S(1)}, bf16[64,1024]{1,0:T(8,128)(2,1)S(1)}, u32[]{:S(2)}, u32[]{:S(2)}) collective-permute-start(bf16[64,1024]{1,0:T(8,128)(2,1)S(1)} %get-tuple-element.58), channel_id=1, source_target_pairs={{0,8},{8,16},{16,24},{24,0},{1,9},{9,17},{17,25},{25,1},{2,10},{10... | collective-permute-start | bytes 393224 | tf_op jit(solution)/shard_map/ppermute | solution.py:389
  158.6 12.8 %collective-permute-start.35 = (bf16[64,1024]{1,0:T(8,128)(2,1)S(1)}, bf16[64,1024]{1,0:T(8,128)(2,1)S(1)}, u32[]{:S(2)}, u32[]{:S(2)}) collective-permute-start(bf16[64,1024]{1,0:T(8,128)(2,1)S(1)} %get-tuple-element.59), channel_id=1, source_target_pairs={{0,16},{8,24},{16,0},{24,8},{1,17},{9,25},{17,1},{25,9},{2,18},{10... | collective-permute-start | bytes 393224 | tf_op jit(solution)/shard_map/ppermute | solution.py:389
  158.6 12.8 %collective-permute-start.36 = (bf16[64,1024]{1,0:T(8,128)(2,1)S(1)}, bf16[64,1024]{1,0:T(8,128)(2,1)S(1)}, u32[]{:S(2)}, u32[]{:S(2)}) collective-permute-start(bf16[64,1024]{1,0:T(8,128)(2,1)S(1)} %get-tuple-element.60), channel_id=1, source_target_pairs={{0,24},{8,0},{16,8},{24,16},{1,25},{9,1},{17,9},{25,17},{2,26},{10... | collective-permute-start | bytes 393224 | tf_op jit(solution)/shard_map/ppermute | solution.py:389

commit v7 on v6

--- a/solution.py
+++ b/solution.py
@@ -271,8 +271,14 @@
     at = pl.ds(pl.multiple_of(place_ref[1] * rows, rows), rows)
     out_ref[:, :half_model] = x_ref[at, :]
     out_ref[:, half_model:] = jnp.concatenate(
-        [_parts(fade_ref[at, :]), jnp.zeros((rows, wide - half_model - 3 * fade_ref.shape[1]), jnp.float32)], axis=1
+        [_parts(_half(fade_ref, place_ref[1])), jnp.zeros((rows, wide - half_model - 3 * fade_ref.shape[0]), jnp.float32)], axis=1
     ).astype(out_ref.dtype)
+
+
+def _half(turned_ref, which):
+    value = turned_ref[...].T
+    rows = value.shape[0] // 2
+    return jnp.where(which == 0, value[:rows], value[rows:])
 
 
 def _parts(value):
@@ -288,7 +294,7 @@
     rows, wide = out_refs[0].shape
     half_model = x_ref.shape[1]
     cut = 2 * half_model // pieces
-    fades = 3 * fade_ref.shape[1]
+    fades = 3 * fade_ref.shape[0]
     own = x_ref[pl.ds(pl.multiple_of(me * rows, rows), rows), :].astype(jnp.float32)
     mate = mate_ref[:, :half_model].astype(jnp.float32)
     square = jnp.sum(own * own, axis=1, keepdims=True) + jnp.sum(mate * mate, axis=1, keepdims=True)
@@ -309,7 +315,7 @@
                 def _():
                     out_ref[:, :cut] = normed[:, k * cut : (k + 1) * cut]
 
-    mine = _parts(fade_ref[pl.ds(pl.multiple_of(me * rows, rows), rows), :])
+    mine = _parts(_half(fade_ref, me))
     theirs = mate_ref[:, half_model : half_model + fades].astype(jnp.float32)
     tail = jnp.concatenate(
         [
@@ -525,8 +531,9 @@
     )(place, mine, theirs, own, other)
 
 
-def linear_kernel(lin, head, half, place_ref, query_key_ref, value_ref, running_ref, own_ref, other_ref, gain_ref, out_ref):
+def linear_kernel(lin, head, half, place_ref, query_key_ref, value_ref, running_ref, own_ref, other_ref, gain_ref, *rest):
     me, side = place_ref[0], place_ref[1]
+    out_ref = rest[-1]
     rows, width = query_key_ref.shape
     features = LOOKUP_FEATURES
     values = width // 2
@@ -545,6 +552,9 @@
             query = query_key_ref[at, base : base + features].astype(jnp.float32)
             key = query_key_ref[at, base + features : base + 2 * features].astype(jnp.float32)
             value = value_ref[at, base : base + values]
+            if len(rest) == 2:
+                more = rest[0][at, base : base + values].astype(jnp.float32)
+                value = (value.astype(jnp.float32) + more).astype(jnp.bfloat16)
             end = running[SPAN - 1 : SPAN]
             scaled = (query * features ** (-0.5) * jnp.exp(running)).astype(jnp.bfloat16)
             inverse = (key * jnp.exp(-running)).astype(jnp.bfloat16)
@@ -562,15 +572,15 @@
             out_ref[at, base : base + values] = (raw * scale * gain_ref[...]).astype(out_ref.dtype)
 
 
-def linear_heads(place, lin, head, half, query_key, value, running, own, other, gain):
+def linear_heads(place, lin, head, half, query_key, value, running, own, other, gain, *more):
     return _call(
         functools.partial(linear_kernel, lin, head, half),
         jax.ShapeDtypeStruct(query_key.shape, jnp.bfloat16),
         2 * 10**9,
         2**21,
-        in_specs=[SMEM] + [VMEM] * 6,
+        in_specs=[SMEM] + [VMEM] * (6 + len(more)),
         out_specs=VMEM,
-    )(place, query_key, value, running, own, other, gain)
+    )(place, query_key, value, running, own, other, gain, *more)
 
 
 def window_kernel(group, half, place_ref, slope_ref, sink_ref, key_value_ref, query_ref, out_ref):
@@ -593,53 +603,60 @@
             out.append(pl.ds(pl.multiple_of(apart + device * half + inside % half, unit), unit))
         return out
 
+    lanes = lax.broadcasted_iota(jnp.int32, (WINDOW, pair), 1)
+    of_group = lanes // HD == group
+    first_half = lanes < HD
+    keep_present = present.astype(jnp.float32).astype(jnp.bfloat16)
+    keep_past = (1.0 - present.astype(jnp.float32)).astype(jnp.bfloat16)
+    turned = lambda value: jnp.concatenate([value[:, HD:], value[:, :HD]], axis=1)
+
     for owner in range(owners):
-        key_at = owner * 2 * pair + group * HD
-        value_at = key_at + pair
+        key_at = owner * 2 * pair
         base = owner * groups * HD
         biases = [slope_ref[owner, head] * distance for head in range(groups)]
         past_keys, past_values = None, None
         for block in range(rows // WINDOW):
             first = block == 0
             at = places(block)
-            keys = jnp.concatenate([key_value_ref[a, key_at : key_at + HD] for a in at], axis=0)
-            values = jnp.concatenate([key_value_ref[a, value_at : value_at + HD] for a in at], axis=0)
+            load = lambda ref, start: jnp.concatenate([ref[a, start : start + pair] for a in at], axis=0)
+            keys, values = load(key_value_ref, key_at), load(key_value_ref, key_at + pair)
             band_keys = keys if first else jnp.concatenate([past_keys, keys], axis=0)
             band_values = values if first else jnp.concatenate([past_values, values], axis=0)
             past_keys, past_values = keys, values
-            queries = jnp.concatenate(
-                [query_ref[a, base + head * HD : base + (head + 1) * HD] for head in range(groups) for a in at],
-                axis=0,
+            queries = []
+            for couple in range(groups // 2):
+                both = load(query_ref, base + couple * pair).astype(jnp.float32) * HD ** (-0.5)
+                swapped = turned(both)
+                ordered = (both, swapped) if group == 0 else (swapped, both)
+                queries += [jnp.where(of_group, value, 0.0).astype(jnp.bfloat16) for value in ordered]
+            scores = lax.dot_general(
+                jnp.concatenate(queries, axis=0), band_keys, BY_COLUMNS, preferred_element_type=jnp.float32
             )
-            scores = lax.dot_general(queries, band_keys, BY_COLUMNS, preferred_element_type=jnp.float32)
             probs = []
             for head in range(groups):
                 mine = scores[head * WINDOW : (head + 1) * WINDOW]
                 if first:
-                    weight = jnp.where(present, jnp.exp(mine * HD ** (-0.5) - biases[head]), 0.0)
+                    weight = jnp.where(present, jnp.exp(mine - biases[head]), 0.0)
                 else:
-                    score = jnp.where(present, mine[:, WINDOW:], mine[:, :WINDOW])
-                    weight = jnp.exp(score * HD ** (-0.5) - biases[head])
+                    weight = jnp.exp(jnp.where(present, mine[:, WINDOW:], mine[:, :WINDOW]) - biases[head])
                 total = jnp.sum(weight, axis=-1, keepdims=True) + sink_ref[owner, head]
-                share = weight / total
+                share = (weight / total).astype(jnp.bfloat16)
                 if first:
-                    probs.append(share.astype(jnp.bfloat16))
+                    probs.append(share)
                 else:
-                    probs.append(
-                        jnp.concatenate(
-                            [
-                                jnp.where(present, 0.0, share).astype(jnp.bfloat16),
-                                jnp.where(present, share, 0.0).astype(jnp.bfloat16),
-                            ],
-                            axis=1,
-                        )
-                    )
+                    probs.append(jnp.concatenate([share * keep_past, share * keep_present], axis=1))
             outs = jnp.dot(jnp.concatenate(probs, axis=0), band_values, preferred_element_type=jnp.float32)
-            joined = jnp.concatenate(
-                [outs[head * WINDOW : (head + 1) * WINDOW] for head in range(groups)], axis=1
-            ).astype(out_ref.dtype)
-            for piece, a in enumerate(at):
-                out_ref[a, base : base + groups * HD] = joined[piece * unit : (piece + 1) * unit]
+            for couple in range(groups // 2):
+                even = outs[2 * couple * WINDOW : (2 * couple + 1) * WINDOW]
+                odd = outs[(2 * couple + 1) * WINDOW : (2 * couple + 2) * WINDOW]
+                if group == 0:
+                    odd = turned(odd)
+                else:
+                    even = turned(even)
+                joined = jnp.where(first_half, even, odd).astype(out_ref.dtype)
+                start = base + couple * pair
+                for piece, a in enumerate(at):
+                    out_ref[a, start : start + pair] = joined[piece * unit : (piece + 1) * unit]
 
 
 def window_heads(place, group, half, slopes, sinks, key_value, query):
@@ -765,7 +782,7 @@
         2**20,
         in_specs=[SMEM, VMEM, VMEM],
         out_specs=VMEM,
-    )(place, activations, extra_fading_exponent)
+    )(place, activations, extra_fading_exponent.T)
     mate = swap(message)
     wide = 2 * half_model // peers + LOOKUP_FEATURES
     outgoing = _call(
@@ -775,7 +792,7 @@
         2**21,
         in_specs=[SMEM] + [VMEM] * 5,
         out_specs=[VMEM] * peers,
-    )(place, activations, extra_fading_exponent, mate, input_norm_gain.reshape(1, -1), decay_down_factor.T)
+    )(place, activations, extra_fading_exponent.T, mate, input_norm_gain.reshape(1, -1), decay_down_factor.T)
 
     (
         outgoing,
@@ -833,15 +850,23 @@
     theirs = swap(incoming).reshape(peers * half, wide)
 
     count = 1 + key_heads + 2 * lin
-    arrived, finals = {}, []
-    for step in range(count + 2 * hops):
-        index = jnp.clip(step - 2 * depth, 0, count - 1).astype(jnp.int32).reshape(1)
+    chained = count - 1 if hops > 1 else count
+    arrived, sums, straight = {}, [], []
+    for step in range(chained + 2 * hops):
+        turn = step - 2 * depth
+        index = jnp.clip(jnp.where(turn >= 0, turn, count - 1), 0, count - 1).astype(jnp.int32).reshape(1)
         value = partial_sum(index, mine, theirs, own_in, other_in, arrived.get(step - 2))
-        depths = [d for d in range(hops) if 0 <= step - 2 * d < count]
+        sums.append(value)
+        if step == chained and hops > 1:
+            straight.append(lax.ppermute(value, ("sp", "tp"), [(0, hops * 2), (hops * 2 + 1, 1)]))
+        depths = [
+            d for d in range(hops) if 0 <= step - 2 * d < chained or (chained < count and d and step - 2 * d == -2)
+        ]
         if depths:
             arrived[step] = lax.ppermute(value, ("sp", "tp"), _pairs(peers, depths, 0))
-        if step >= 2 * hops:
-            finals.append(value)
+    finals = sums[2 * hops :]
+    if straight:
+        finals.append(sums[2 * (hops - 1)])
 
     running = decay_sums(place, lin, rank, mine, theirs, own_small, other_small)
     sinks = jnp.stack(
@@ -873,6 +898,7 @@
                 starting_state,
                 other_state,
                 linear_head_gain.reshape(1, DV),
+                *(straight if head == lin - 1 else []),
             )
         )
 

time: 174 us -> 187 us (1.075)
  Pallas kernels: 49.8 us -> 63.4 us
  waiting for transfers between devices: 54.8 us -> 44.7 us
  starting transfers between devices: 61.3 us -> 67.1 us
  local copies, waits for them, and re-layouts: 5.8 us -> 8.55 us
    pallas_call x13 -> x12, Pallas kernels: 20 us -> 33 us  [partial_sum(): _call(partial_kernel, jax.ShapeDtypeStruct((2 * rows, 2 * width), jnp.bfl...]
    ppermute x8, starting transfers between devices: 8.63 us -> 15.7 us  [swap(): return lax.ppermute(value, 'tp', SWAP)]
    ppermute x11 -> x10, starting transfers between devices: 31.3 us -> 25 us  [resident(): arrived[step] = lax.ppermute(value, ('sp', 'tp'), _pairs(peers, depths, 0))]
    ppermute x11, waiting for transfers between devices: 27.6 us -> 21.3 us  [resident(): seen.append(lax.ppermute(seen[-1], ('sp', 'tp'), _pairs(peers, [hop], 1)))]
    ppermute x0 -> x1, starting transfers between devices: none -> 3.91 us  [resident(): lax.ppermute(value, ('sp', 'tp'), [(0, hops * 2), (hops * 2 + 1, 1)])]
    ppermute x11 -> x10, waiting for transfers between devices: 6.95 us -> 4.05 us  [resident(): arrived[step] = lax.ppermute(value, ('sp', 'tp'), _pairs(peers, depths, 0))]
    unnamed x49 -> x50, local copies, waits for them, and re-layouts: 3.63 us -> 5.4 us
  transfers between devices with their start and end apart: 37 -> 37, of which waited for: 13 -> 12; matrix products, arithmetic and copies ran while one was open for 1% -> 2% of each run, Pallas kernels for 22% -> 29%
where the time goes in v7:
time: 187 us; the launch traced here: 185 us
  starting transfers between devices  67.1 us (36%)
  Pallas kernels  63.4 us (34%)
  waiting for transfers between devices  44.7 us (24%)
  local copies, waits for them, and re-layouts  8.55 us (5%)
    pallas_call x12, Pallas kernels, partial_sum(): _call(partial_kernel, jax.ShapeDtypeStruct((2 * rows, 2 * width), jnp.bfl...  33 us
    ppermute x10, starting transfers between devices, resident(): arrived[step] = lax.ppermute(value, ('sp', 'tp'), _pairs(peers, depths, 0))  25 us
    ppermute x11, waiting for transfers between devices, resident(): seen.append(lax.ppermute(seen[-1], ('sp', 'tp'), _pairs(peers, [hop], 1)))  21.3 us
    ppermute x6, waiting for transfers between devices, to_offsets(): lax.ppermute(parts[k], 'sp', [(i, (i + k) % peers) for i in range(peers)])  17.1 us
    ppermute x8, starting transfers between devices, swap(): return lax.ppermute(value, 'tp', SWAP)  15.7 us
    ppermute x6, starting transfers between devices, to_offsets(): lax.ppermute(parts[k], 'sp', [(i, (i + k) % peers) for i in range(peers)])  11.7 us
    ppermute x11, starting transfers between devices, resident(): seen.append(lax.ppermute(seen[-1], ('sp', 'tp'), _pairs(peers, [hop], 1)))  9.54 us
    pallas_call x2, Pallas kernels, linear_heads(): _call(functools.partial(linear_kernel, lin, head, half), jax.ShapeDtypeSt...  5.85 us
  transfers between devices with their start and end apart: 37, of which 12 were waited for; matrix products, arithmetic and copies ran while one was open for 2% of the time, Pallas kernels for 29%

profile of v7, /device:TPU:0, one launch (start us, length us, event | category | flops | bytes accessed | tf_op | source)
XLA Modules:
  0.0 184.9 jit_solution(4919221002948005681)
XLA Ops:
  0.1 1.0 copy-done.9
  1.8 0.7 shard_map.163
  4.3 1.0 copy-done.10
  5.3 0.9 copy-done.13
  6.3 1.4 shard_map.164
  9.3 4.1 %shard_map.167 = bf16[7,1024,256]{2,1,0:T(8,128)(2,1)} custom-call(s32[1]{0:T(128)} %bitcast.side_ref, bf16[1024,1024]{1,0:T(8,128)(2,1)S(1)} %copy-done.5, bf16[1024,256]{1,0:T(8,128)(2,1)S(1)} %copy-done.11, bf16[1024,256]{1,0:T(8,128)(2,1)S(1)} %copy-done.12, bf16[1024,512]{1,0:T(8,128)(2,1)S(1)} %copy-done.7, bf16[1024,512]{1,0:T(8,128)(2,1)S(1)} %copy-done.8, ...), custom_call_target="tpu_custom_call" | custom-call | flops 99999997952 | bytes 7340032 | tf_op jit(solution)/shard_map/pallas_call | solution.py:436
  13.8 1.6 shard_map.166.own_ref
  15.5 2.7 %collective-permute-start.1 = (bf16[64,1152]{1,0:T(8,128)(2,1)S(1)}, bf16[64,1152]{1,0:T(8,128)(2,1)S(1)}, u32[]{:S(2)}, u32[]{:S(2)}) collective-permute-start(bf16[64,1152]{1,0:T(8,128)(2,1)S(1)} %get-tuple-element.38), channel_id=1, source_target_pairs={{0,8},{8,16},{16,24},{24,0},{1,9},{9,17},{17,25},{25,1},{2,10},{10... | collective-permute-start | bytes 442376 | tf_op jit(solution)/shard_map/ppermute | solution.py:395
  18.2 2.6 %collective-permute-start.2 = (bf16[64,1152]{1,0:T(8,128)(2,1)S(1)}, bf16[64,1152]{1,0:T(8,128)(2,1)S(1)}, u32[]{:S(2)}, u32[]{:S(2)}) collective-permute-start(bf16[64,1152]{1,0:T(8,128)(2,1)S(1)} %get-tuple-element.39), channel_id=1, source_target_pairs={{0,16},{8,24},{16,0},{24,8},{1,17},{9,25},{17,1},{25,9},{2,18},{10... | collective-permute-start | bytes 442376 | tf_op jit(solution)/shard_map/ppermute | solution.py:395
  20.8 1.3 collective-permute-start.3
  22.3 2.7 %collective-permute-done.1.refs_1_ = bf16[64,1152]{1,0:T(8,128)(2,1)S(1)} collective-permute-done((bf16[64,1152]{1,0:T(8,128)(2,1)S(1)}, bf16[64,1152]{1,0:T(8,128)(2,1)S(1)}, u32[]{:S(2)}, u32[]{:S(2)}) %collective-permute-start.1) | collective-permute-done | bytes 147488 | tf_op jit(solution)/shard_map/ppermute | solution.py:395
  25.0 6.0 %collective-permute-done.2.refs_2_ = bf16[64,1152]{1,0:T(8,128)(2,1)S(1)} collective-permute-done((bf16[64,1152]{1,0:T(8,128)(2,1)S(1)}, bf16[64,1152]{1,0:T(8,128)(2,1)S(1)}, u32[]{:S(2)}, u32[]{:S(2)}) %collective-permute-start.2) | collective-permute-done | bytes 147488 | tf_op jit(solution)/shard_map/ppermute | solution.py:395
  31.0 1.4 shard_map.165
  32.4 1.1 constant_dynamic-slice_fusion.2
  33.5 1.1 constant_dynamic-slice_fusion
  35.5 3.8 %shard_map.179 = (f32[512,256]{1,0:T(8,128)S(1)}, f32[512,256]{1,0:T(8,128)S(1)}) custom-call(s32[4]{0:T(128)S(1)} %copy-done.4, bf16[256,1152]{1,0:T(8,128)(2,1)} %bitcast.8.mine_ref, bf16[256,1152]{1,0:T(8,128)(2,1)} %bitcast.9.theirs_ref, f32[24,512]{1,0:T(8,128)S(1)} %maximum_maximum_fusion.own_ref, f32[24,512]{1,0:T(8,128)S(1)} %collective-permute-done.15.other_ref), custom_call_target="tpu_custom_call" | custom-call | flops 1000000000 | bytes 1048576 | tf_op jit(solution)/shard_map/pallas_call | solution.py:524
  39.3 2.7 %shard_map.173 = bf16[512,512]{1,0:T(8,128)(2,1)S(1)} custom-call(s32[1]{0:T(128)} %bitcast.19.index_ref, bf16[256,1152]{1,0:T(8,128)(2,1)} %bitcast.8.mine_ref, bf16[256,1152]{1,0:T(8,128)(2,1)} %bitcast.9.theirs_ref, bf16[7,1024,256]{2,1,0:T(8,128)(2,1)S(1)} %copy-done.19, bf16[7,1024,256]{2,1,0:T(8,128)(2,1)} %collective-permute-done.5.other_ref), custom_call_target="tpu_custom_call" | custom-call | flops 10737418240 | bytes 2097152 | tf_op jit(solution)/shard_map/pallas_call | solution.py:473
  42.0 5.6 %collective-permute-start.10 = (bf16[512,512]{1,0:T(8,128)(2,1)S(1)}, bf16[512,512]{1,0:T(8,128)(2,1)S(1)}, u32[]{:S(2)}, u32[]{:S(2)}) collective-permute-start(bf16[512,512]{1,0:T(8,128)(2,1)S(1)} %shard_map.173), channel_id=1, source_target_pairs={{0,8},{25,17},{8,16},{17,9},{2,10},{27,19},{10,18},{19,11},{4,12},... | collective-permute-start | bytes 1572872 | tf_op jit(solution)/shard_map/ppermute | solution.py:866
  47.6 2.7 %shard_map.168 = bf16[512,512]{1,0:T(8,128)(2,1)S(1)} custom-call(s32[1]{0:T(128)} %bitcast.13.index_ref, bf16[256,1152]{1,0:T(8,128)(2,1)} %bitcast.8.mine_ref, bf16[256,1152]{1,0:T(8,128)(2,1)} %bitcast.9.theirs_ref, bf16[7,1024,256]{2,1,0:T(8,128)(2,1)S(1)} %copy-done.19, bf16[7,1024,256]{2,1,0:T(8,128)(2,1)} %collective-permute-done.5.other_ref), custom_call_target="tpu_custom_call" | custom-call | flops 10737418240 | bytes 2097152 | tf_op jit(solution)/shard_map/pallas_call | solution.py:473
  50.3 1.9 %collective-permute-start.6 = (bf16[512,512]{1,0:T(8,128)(2,1)S(1)}, bf16[512,512]{1,0:T(8,128)(2,1)S(1)}, u32[]{:S(2)}, u32[]{:S(2)}) collective-permute-start(bf16[512,512]{1,0:T(8,128)(2,1)S(1)} %shard_map.168), channel_id=1, source_target_pairs={{0,8},{25,17},{2,10},{27,19},{4,12},{29,21},{6,14},{31,23}} | collective-permute-start | bytes 1572872 | tf_op jit(solution)/shard_map/ppermute | solution.py:866
  52.3 2.0 %collective-permute-done.10.rest_0_ = bf16[512,512]{1,0:T(8,128)(2,1)S(1)} collective-permute-done((bf16[512,512]{1,0:T(8,128)(2,1)S(1)}, bf16[512,512]{1,0:T(8,128)(2,1)S(1)}, u32[]{:S(2)}, u32[]{:S(2)}) %collective-permute-start.10) | collective-permute-done | bytes 524320 | tf_op jit(solution)/shard_map/ppermute | solution.py:866
  54.2 2.7 %shard_map.174 = bf16[512,512]{1,0:T(8,128)(2,1)S(1)} custom-call(s32[1]{0:T(128)} %bitcast.18.index_ref, bf16[256,1152]{1,0:T(8,128)(2,1)} %bitcast.8.mine_ref, bf16[256,1152]{1,0:T(8,128)(2,1)} %bitcast.9.theirs_ref, bf16[7,1024,256]{2,1,0:T(8,128)(2,1)S(1)} %copy-done.19, bf16[7,1024,256]{2,1,0:T(8,128)(2,1)} %collective-permute-done.5.other_ref, ...), custom_call_target="tpu_custom_call" | custom-call | flops 10737418240 | bytes 2097152 | tf_op jit(solution)/shard_map/pallas_call | solution.py:473
  57.0 4.4 %collective-permute-start.11 = (bf16[512,512]{1,0:T(8,128)(2,1)S(1)}, bf16[512,512]{1,0:T(8,128)(2,1)S(1)}, u32[]{:S(2)}, u32[]{:S(2)}) collective-permute-start(bf16[512,512]{1,0:T(8,128)(2,1)S(1)} %shard_map.174), channel_id=1, source_target_pairs={{0,8},{25,17},{8,16},{17,9},{16,24},{9,1},{2,10},{27,19},{10,18},{... | collective-permute-start | bytes 1572872 | tf_op jit(solution)/shard_map/ppermute | solution.py:866
  61.4 2.7 %shard_map.169 = bf16[512,512]{1,0:T(8,128)(2,1)S(1)} custom-call(s32[1]{0:T(128)} %bitcast.12.index_ref, bf16[256,1152]{1,0:T(8,128)(2,1)} %bitcast.8.mine_ref, bf16[256,1152]{1,0:T(8,128)(2,1)} %bitcast.9.theirs_ref, bf16[7,1024,256]{2,1,0:T(8,128)(2,1)S(1)} %copy-done.19, bf16[7,1024,256]{2,1,0:T(8,128)(2,1)} %collective-permute-done.5.other_ref, ...), custom_call_target="tpu_custom_call" | custom-call | flops 10737418240 | bytes 2097152 | tf_op jit(solution)/shard_map/pallas_call | solution.py:473
  64.2 2.8 %collective-permute-start.7 = (bf16[512,512]{1,0:T(8,128)(2,1)S(1)}, bf16[512,512]{1,0:T(8,128)(2,1)S(1)}, u32[]{:S(2)}, u32[]{:S(2)}) collective-permute-start(bf16[512,512]{1,0:T(8,128)(2,1)S(1)} %shard_map.169), channel_id=1, source_target_pairs={{0,8},{25,17},{8,16},{17,9},{2,10},{27,19},{10,18},{19,11},{4,12},... | collective-permute-start | bytes 1572872 | tf_op jit(solution)/shard_map/ppermute | solution.py:866
  67.0 1.0 collective-permute-done.11.rest_0_
  68.1 2.7 %shard_map.175.value_ref = bf16[512,512]{1,0:T(8,128)(2,1)S(1)} custom-call(s32[1]{0:T(128)} %bitcast.17.index_ref, bf16[256,1152]{1,0:T(8,128)(2,1)} %bitcast.8.mine_ref, bf16[256,1152]{1,0:T(8,128)(2,1)} %bitcast.9.theirs_ref, bf16[7,1024,256]{2,1,0:T(8,128)(2,1)S(1)} %copy-done.19, bf16[7,1024,256]{2,1,0:T(8,128)(2,1)} %collective-permute-done.5.other_ref, ...), custom_call_target="tpu_custom_call" | custom-call | flops 10737418240 | bytes 2097152 | tf_op jit(solution)/shard_map/pallas_call | solution.py:473
  70.8 4.4 %collective-permute-start.12 = (bf16[512,512]{1,0:T(8,128)(2,1)S(1)}, bf16[512,512]{1,0:T(8,128)(2,1)S(1)}, u32[]{:S(2)}, u32[]{:S(2)}) collective-permute-start(bf16[512,512]{1,0:T(8,128)(2,1)S(1)} %shard_map.175.value_ref), channel_id=1, source_target_pairs={{0,8},{25,17},{8,16},{17,9},{16,24},{9,1},{2,10},{27,19},{10,18},{... | collective-permute-start | bytes 1572872 | tf_op jit(solution)/shard_map/ppermute | solution.py:866
  75.3 2.7 %shard_map.170 = bf16[512,512]{1,0:T(8,128)(2,1)S(1)} custom-call(s32[1]{0:T(128)} %bitcast.11.index_ref, bf16[256,1152]{1,0:T(8,128)(2,1)} %bitcast.8.mine_ref, bf16[256,1152]{1,0:T(8,128)(2,1)} %bitcast.9.theirs_ref, bf16[7,1024,256]{2,1,0:T(8,128)(2,1)S(1)} %copy-done.19, bf16[7,1024,256]{2,1,0:T(8,128)(2,1)} %collective-permute-done.5.other_ref, ...), custom_call_target="tpu_custom_call" | custom-call | flops 10737418240 | bytes 2097152 | tf_op jit(solution)/shard_map/pallas_call | solution.py:473
  78.0 2.8 %collective-permute-start.8 = (bf16[512,512]{1,0:T(8,128)(2,1)S(1)}, bf16[512,512]{1,0:T(8,128)(2,1)S(1)}, u32[]{:S(2)}, u32[]{:S(2)}) collective-permute-start(bf16[512,512]{1,0:T(8,128)(2,1)S(1)} %shard_map.170), channel_id=1, source_target_pairs={{0,8},{25,17},{8,16},{17,9},{16,24},{9,1},{2,10},{27,19},{10,18},{... | collective-permute-start | bytes 1572872 | tf_op jit(solution)/shard_map/ppermute | solution.py:866
  80.9 1.0 collective-permute-done.12.rest_0_
  81.9 2.7 %shard_map.176.key_value_ref = bf16[512,512]{1,0:T(8,128)(2,1)S(1)} custom-call(s32[1]{0:T(128)} %bitcast.16.index_ref, bf16[256,1152]{1,0:T(8,128)(2,1)} %bitcast.8.mine_ref, bf16[256,1152]{1,0:T(8,128)(2,1)} %bitcast.9.theirs_ref, bf16[7,1024,256]{2,1,0:T(8,128)(2,1)S(1)} %copy-done.19, bf16[7,1024,256]{2,1,0:T(8,128)(2,1)} %collective-permute-done.5.other_ref, ...), custom_call_target="tpu_custom_call" | custom-call | flops 10737418240 | bytes 2097152 | tf_op jit(solution)/shard_map/pallas_call | solution.py:473
  84.7 0.7 collective-permute-start.13
  85.4 3.9 %collective-permute-start.21 = (bf16[512,512]{1,0:T(8,128)(2,1)S(1)}, bf16[512,512]{1,0:T(8,128)(2,1)S(1)}, u32[]{:S(2)}, u32[]{:S(2)}) collective-permute-start(bf16[512,512]{1,0:T(8,128)(2,1)S(1)} %shard_map.176.key_value_ref), channel_id=1, source_target_pairs={{0,24},{25,1},{2,26},{27,3},{4,28},{29,5},{6,30},{31,7}} | collective-permute-start | bytes 1572872 | tf_op jit(solution)/shard_map/ppermute | solution.py:861
  89.3 2.7 %shard_map.171.query_ref = bf16[512,512]{1,0:T(8,128)(2,1)S(1)} custom-call(s32[1]{0:T(128)} %bitcast.10.index_ref, bf16[256,1152]{1,0:T(8,128)(2,1)} %bitcast.8.mine_ref, bf16[256,1152]{1,0:T(8,128)(2,1)} %bitcast.9.theirs_ref, bf16[7,1024,256]{2,1,0:T(8,128)(2,1)S(1)} %copy-done.19, bf16[7,1024,256]{2,1,0:T(8,128)(2,1)} %collective-permute-done.5.other_ref, ...), custom_call_target="tpu_custom_call" | custom-call | flops 10737418240 | bytes 2097152 | tf_op jit(solution)/shard_map/pallas_call | solution.py:473
  92.0 0.9 collective-permute-start.9
  92.9 2.9 %shard_map.183.refs_0_ = bf16[512,512]{1,0:T(8,128)(2,1)S(1)} custom-call(s32[4]{0:T(128)S(1)} %copy-done.4, f32[2,4]{1,0:T(2,128)S(1)} %get-tuple-element.64.slope_ref, f32[2,4]{1,0:T(2,128)S(1)} %bitcast.27, bf16[512,512]{1,0:T(8,128)(2,1)S(1)} %shard_map.176.key_value_ref, bf16[512,512]{1,0:T(8,128)(2,1)S(1)} %shard_map.171.query_ref), custom_call_target="tpu_custom_call" | custom-call | flops 2000000000 | bytes 2097152 | tf_op jit(solution)/shard_map/pallas_call | solution.py:663
  95.9 0.7 collective-permute-start.26
  96.6 2.7 %shard_map.177.query_ref = bf16[512,512]{1,0:T(8,128)(2,1)S(1)} custom-call(s32[1]{0:T(128)} %bitcast.15.index_ref, bf16[256,1152]{1,0:T(8,128)(2,1)} %bitcast.8.mine_ref, bf16[256,1152]{1,0:T(8,128)(2,1)} %bitcast.9.theirs_ref, bf16[7,1024,256]{2,1,0:T(8,128)(2,1)S(1)} %copy-done.19, bf16[7,1024,256]{2,1,0:T(8,128)(2,1)} %collective-permute-done.5.other_ref, ...), custom_call_target="tpu_custom_call" | custom-call | flops 10737418240 | bytes 2097152 | tf_op jit(solution)/shard_map/pallas_call | solution.py:473
  99.3 0.7 collective-permute-start.14
  100.1 2.7 %shard_map.172.query_key_ref = bf16[512,512]{1,0:T(8,128)(2,1)S(1)} custom-call(s32[1]{0:T(128)} %bitcast.4.index_ref, bf16[256,1152]{1,0:T(8,128)(2,1)} %bitcast.8.mine_ref, bf16[256,1152]{1,0:T(8,128)(2,1)} %bitcast.9.theirs_ref, bf16[7,1024,256]{2,1,0:T(8,128)(2,1)S(1)} %copy-done.19, bf16[7,1024,256]{2,1,0:T(8,128)(2,1)} %collective-permute-done.5.other_ref, ...), custom_call_target="tpu_custom_call" | custom-call | flops 10737418240 | bytes 2097152 | tf_op jit(solution)/shard_map/pallas_call | solution.py:473
  102.8 2.8 %shard_map.184.refs_4_ = bf16[512,512]{1,0:T(8,128)(2,1)S(1)} custom-call(s32[4]{0:T(128)S(1)} %copy-done.4, f32[2,4]{1,0:T(2,128)S(1)} %get-tuple-element.63.slope_ref, f32[2,4]{1,0:T(2,128)S(1)} %bitcast.26, bf16[512,512]{1,0:T(8,128)(2,1)S(1)} %shard_map.176.key_value_ref, bf16[512,512]{1,0:T(8,128)(2,1)S(1)} %shard_map.177.query_ref), custom_call_target="tpu_custom_call" | custom-call | flops 2000000000 | bytes 2097152 | tf_op jit(solution)/shard_map/pallas_call | solution.py:663
  105.6 0.7 collective-permute-start.20
  106.3 2.7 %shard_map.178.value_ref = bf16[512,512]{1,0:T(8,128)(2,1)S(1)} custom-call(s32[1]{0:T(128)} %bitcast.14.index_ref, bf16[256,1152]{1,0:T(8,128)(2,1)} %bitcast.8.mine_ref, bf16[256,1152]{1,0:T(8,128)(2,1)} %bitcast.9.theirs_ref, bf16[7,1024,256]{2,1,0:T(8,128)(2,1)S(1)} %copy-done.19, bf16[7,1024,256]{2,1,0:T(8,128)(2,1)} %collective-permute-done.5.other_ref, ...), custom_call_target="tpu_custom_call" | custom-call | flops 10737418240 | bytes 2097152 | tf_op jit(solution)/shard_map/pallas_call | solution.py:473
  110.5 2.9 %shard_map.180.refs_0_ = bf16[512,512]{1,0:T(8,128)(2,1)S(1)} custom-call(s32[4]{0:T(128)S(1)} %copy-done.4, bf16[512,512]{1,0:T(8,128)(2,1)S(1)} %shard_map.172.query_key_ref, bf16[512,512]{1,0:T(8,128)(2,1)S(1)} %shard_map.178.value_ref, f32[512,256]{1,0:T(8,128)S(1)} %get-tuple-element.50.running_ref, f32[4,128,256]{2,1,0:T(8,128)} %own_ref.1, ...), custom_call_target="tpu_custom_call" | custom-call | flops 2000000000 | bytes 2097152 | tf_op jit(solution)/shard_map/pallas_call | solution.py:576
  114.2 2.8 %shard_map.181.query_key_ref = bf16[512,512]{1,0:T(8,128)(2,1)S(1)} custom-call(s32[1]{0:T(128)} %bitcast.23.index_ref, bf16[256,1152]{1,0:T(8,128)(2,1)} %bitcast.8.mine_ref, bf16[256,1152]{1,0:T(8,128)(2,1)} %bitcast.9.theirs_ref, bf16[7,1024,256]{2,1,0:T(8,128)(2,1)S(1)} %copy-done.19, bf16[7,1024,256]{2,1,0:T(8,128)(2,1)} %collective-permute-done.5.other_ref, ...), custom_call_target="tpu_custom_call" | custom-call | flops 10737418240 | bytes 2097152 | tf_op jit(solution)/shard_map/pallas_call | solution.py:473
  117.1 14.1 %collective-permute-start.25 = (bf16[512,1024]{1,0:T(8,128)(2,1)S(1)}, bf16[512,1024]{1,0:T(8,128)(2,1)S(1)}, u32[]{:S(2)}, u32[]{:S(2)}) collective-permute-start(bf16[512,1024]{1,0:T(8,128)(2,1)S(1)} %copy-done.20), channel_id=1, source_target_pairs={{0,1},{1,0},{2,3},{3,2},{4,5},{5,4},{6,7},{7,6},{8,9},{9,8},{10,11... | collective-permute-start | bytes 3145736 | tf_op jit(solution)/shard_map/ppermute | solution.py:775
  131.8 2.9 %shard_map.182.refs_4_ = bf16[512,512]{1,0:T(8,128)(2,1)S(1)} custom-call(s32[4]{0:T(128)S(1)} %copy-done.4, bf16[512,512]{1,0:T(8,128)(2,1)S(1)} %shard_map.181.query_key_ref, bf16[512,512]{1,0:T(8,128)(2,1)S(1)} %shard_map.175.value_ref, f32[512,256]{1,0:T(8,128)S(1)} %get-tuple-element.52.running_ref, f32[4,128,256]{2,1,0:T(8,128)} %own_ref.1, ...), custom_call_target="tpu_custom_call" | custom-call | flops 2000000000 | bytes 2097152 | tf_op jit(solution)/shard_map/pallas_call | solution.py:576
  134.8 0.8 collective-permute-start.22
  135.6 1.3 collective-permute-start.28
  137.7 1.3 collective-permute-start.31
  139.0 1.3 collective-permute-start.24
  140.3 6.4 %collective-permute-done.28.refs_3_ = bf16[512,512]{1,0:T(8,128)(2,1)S(1)} collective-permute-done((bf16[512,512]{1,0:T(8,128)(2,1)S(1)}, bf16[512,512]{1,0:T(8,128)(2,1)S(1)}, u32[]{:S(2)}, u32[]{:S(2)}) %collective-permute-start.28) | collective-permute-done | bytes 524320 | tf_op jit(solution)/shard_map/ppermute | solution.py:913
  147.4 1.3 collective-permute-start.19
  148.7 11.2 %collective-permute-done.31.refs_7_ = bf16[512,512]{1,0:T(8,128)(2,1)S(1)} collective-permute-done((bf16[512,512]{1,0:T(8,128)(2,1)S(1)}, bf16[512,512]{1,0:T(8,128)(2,1)S(1)}, u32[]{:S(2)}, u32[]{:S(2)}) %collective-permute-start.31) | collective-permute-done | bytes 524320 | tf_op jit(solution)/shard_map/ppermute | solution.py:913
  159.9 1.9 %shard_map.185.refs_10_ = f32[512,1024]{1,0:T(8,128)S(1)} custom-call(s32[4]{0:T(128)S(1)} %copy-done.4, bf16[512,512]{1,0:T(8,128)(2,1)S(1)} %shard_map.183.refs_0_, bf16[512,512]{1,0:T(8,128)(2,1)S(1)} %collective-permute-done.26.refs_1_, bf16[512,512]{1,0:T(8,128)(2,1)S(1)} %collective-permute-done.27.refs_2_, ...), custom_call_target="tpu_custom_call" | custom-call | flops 1073741824 | bytes 4194304 | tf_op jit(solution)/shard_map/pallas_call | solution.py:720
  161.8 3.7 %collective-permute-done.19.refs_3_ = bf16[512,512]{1,0:T(8,128)(2,1)S(1)} collective-permute-done((bf16[512,512]{1,0:T(8,128)(2,1)S(1)}, bf16[512,512]{1,0:T(8,128)(2,1)S(1)}, u32[]{:S(2)}, u32[]{:S(2)}) %collective-permute-start.19) | collective-permute-done | bytes 524320 | tf_op jit(solution)/shard_map/ppermute | solution.py:913
  165.5 1.9 %shard_map.186 = (bf16[256,1024]{1,0:T(8,128)(2,1)S(1)}, bf16[256,1024]{1,0:T(8,128)(2,1)S(1)}) custom-call(s32[4]{0:T(128)S(1)} %copy-done.4, bf16[512,512]{1,0:T(8,128)(2,1)S(1)} %shard_map.180.refs_0_, bf16[512,512]{1,0:T(8,128)(2,1)S(1)} %collective-permute-done.17.refs_1_, bf16[512,512]{1,0:T(8,128)(2,1)S(1)} %collective-permute-done.18.refs_2_, ...), custom_call_target="tpu_custom_call" | custom-call | flops 1073741824 | bytes 4194304 | tf_op jit(solution)/shard_map/pallas_call | solution.py:720
  167.5 1.9 %collective-permute-done.33.given_ref = bf16[256,1024]{1,0:T(8,128)(2,1)S(1)} collective-permute-done((bf16[256,1024]{1,0:T(8,128)(2,1)S(1)}, bf16[256,1024]{1,0:T(8,128)(2,1)S(1)}, u32[]{:S(2)}, u32[]{:S(2)}) %collective-permute-start.33) | collective-permute-done | bytes 524320 | tf_op jit(solution)/shard_map/ppermute | solution.py:775
  170.6 3.7 %collective-permute-start.35 = (bf16[64,1024]{1,0:T(8,128)(2,1)S(1)}, bf16[64,1024]{1,0:T(8,128)(2,1)S(1)}, u32[]{:S(2)}, u32[]{:S(2)}) collective-permute-start(bf16[64,1024]{1,0:T(8,128)(2,1)S(1)} %get-tuple-element.59), channel_id=1, source_target_pairs={{0,16},{8,24},{16,0},{24,8},{1,17},{9,25},{17,1},{25,9},{2,18},{10... | collective-permute-start | bytes 393224 | tf_op jit(solution)/shard_map/ppermute | solution.py:395
  174.4 0.7 collective-permute-start.36
  175.1 3.3 %collective-permute-done.34.refs_1_ = bf16[64,1024]{1,0:T(8,128)(2,1)S(1)} collective-permute-done((bf16[64,1024]{1,0:T(8,128)(2,1)S(1)}, bf16[64,1024]{1,0:T(8,128)(2,1)S(1)}, u32[]{:S(2)}, u32[]{:S(2)}) %collective-permute-start.34) | collective-permute-done | bytes 131104 | tf_op jit(solution)/shard_map/ppermute | solution.py:395
  178.4 5.1 %collective-permute-done.35.refs_2_ = bf16[64,1024]{1,0:T(8,128)(2,1)S(1)} collective-permute-done((bf16[64,1024]{1,0:T(8,128)(2,1)S(1)}, bf16[64,1024]{1,0:T(8,128)(2,1)S(1)}, u32[]{:S(2)}, u32[]{:S(2)}) %collective-permute-start.35) | collective-permute-done | bytes 131104 | tf_op jit(solution)/shard_map/ppermute | solution.py:395
  183.5 1.4 shard_map.188
  (105 shorter events, 11.1 us)
Async XLA Ops:
  0.1 4.2 %copy-start.3 = (s32[4]{0:T(128)}, s32[4]{0:T(128)S(1)}, u32[]{:S(2)}) copy-start(s32[4]{0:T(128)S(1)} %pad_add_fusion.place_ref) | copy-start | bytes 52
  0.1 1.0 copy-start.9
  1.1 0.7 copy-start.15
  1.8 2.5 %copy-start.14 = (f32[4096]{0:T(1024)S(1)}, f32[4096]{0:T(1024)}, u32[]{:S(2)}) copy-start(f32[4096]{0:T(1024)} %param.18) | copy-start | bytes 49156
  1.8 2.5 %copy-start.16 = (f32[128,4]{0,1:T(4,128)S(1)}, f32[128,4]{0,1:T(4,128)}, u32[]{:S(2)}) copy-start(f32[128,4]{0,1:T(4,128)} %param.28) | copy-start | bytes 6148
  2.5 1.7 collective-permute-start
  4.3 1.0 copy-start.10
  5.3 0.9 copy-start.13
  6.2 1.6 copy-start.5
  6.2 2.2 %copy-start.6 = (bf16[1024,1024]{1,0:T(8,128)(2,1)S(1)}, bf16[1024,1024]{1,0:T(8,128)(2,1)}, u32[]{:S(2)}) copy-start(bf16[1024,1024]{1,0:T(8,128)(2,1)} %lv.1) | copy-start | bytes 6291460
  6.2 2.5 %copy-start.7 = (bf16[1024,512]{1,0:T(8,128)(2,1)S(1)}, bf16[1024,512]{1,0:T(8,128)(2,1)}, u32[]{:S(2)}) copy-start(bf16[1024,512]{1,0:T(8,128)(2,1)} %lq.1) | copy-start | bytes 3145732
  6.2 2.8 %copy-start.8 = (bf16[1024,512]{1,0:T(8,128)(2,1)S(1)}, bf16[1024,512]{1,0:T(8,128)(2,1)}, u32[]{:S(2)}) copy-start(bf16[1024,512]{1,0:T(8,128)(2,1)} %lk.1) | copy-start | bytes 3145732
  6.2 2.9 %copy-start.11 = (bf16[1024,256]{1,0:T(8,128)(2,1)S(1)}, bf16[1024,256]{1,0:T(8,128)(2,1)}, u32[]{:S(2)}) copy-start(bf16[1024,256]{1,0:T(8,128)(2,1)} %wk.1) | copy-start | bytes 1572868
  6.3 3.0 %copy-start.12 = (bf16[1024,256]{1,0:T(8,128)(2,1)S(1)}, bf16[1024,256]{1,0:T(8,128)(2,1)}, u32[]{:S(2)}) copy-start(bf16[1024,256]{1,0:T(8,128)(2,1)} %wv.1) | copy-start | bytes 1572868
  13.4 8.8 %copy-start.24 = (f32[16]{0:T(128)S(1)}, f32[16]{0:T(128)}, u32[]{:S(2)}) copy-start(f32[16]{0:T(128)} %param.30) | copy-start | bytes 196
  13.4 8.8 %copy-start.21 = (bf16[16,512]{1,0:T(8,128)(2,1)S(1)}, bf16[16,512]{1,0:T(8,128)(2,1)}, u32[]{:S(2)}) copy-start(bf16[16,512]{1,0:T(8,128)(2,1)} %param.26) | copy-start | bytes 49156
  13.4 8.8 %copy-start.22 = (f32[512]{0:T(512)S(1)}, f32[512]{0:T(512)}, u32[]{:S(2)}) copy-start(f32[512]{0:T(512)} %param.27) | copy-start | bytes 6148
  13.4 8.8 %copy-start.23 = (f32[24]{0:T(128)S(1)}, f32[24]{0:T(128)}, u32[]{:S(2)}) copy-start(f32[24]{0:T(128)} %pad.12.clone) | copy-start | bytes 292
  13.4 17.7 %copy-start.4 = (s32[4]{0:T(128)S(1)}, s32[4]{0:T(128)}, u32[]{:S(2)}) copy-start(s32[4]{0:T(128)} %copy-done.3) | copy-start | bytes 52
  13.4 19.1 %copy-start.1 = (bf16[1024,1024]{1,0:T(8,128)(2,1)S(1)}, bf16[1024,1024]{1,0:T(8,128)(2,1)}, u32[]{:S(2)}) copy-start(bf16[1024,1024]{1,0:T(8,128)(2,1)} %refs_8_.1) | copy-start | bytes 6291460
  13.4 25.8 %collective-permute-start.5 = (bf16[7,1024,256]{2,1,0:T(8,128)(2,1)}, bf16[7,1024,256]{2,1,0:T(8,128)(2,1)}, u32[]{:S(2)}, u32[]{:S(2)}) collective-permute-start(bf16[7,1024,256]{2,1,0:T(8,128)(2,1)} %shard_map.167), channel_id=1, source_target_pairs={{0,1},{1,0},{2,3},{3,2},{4,5},{5,4},{6,7},{7,6},{8,9},{9,8},{10,11... | collective-permute-start | bytes 11010056 | tf_op jit(solution)/shard_map/ppermute | solution.py:775
  15.4 19.1 %copy-start.18 = (bf16[7,1024,256]{2,1,0:T(8,128)(2,1)}, bf16[7,1024,256]{2,1,0:T(8,128)(2,1)S(1)}, u32[]{:S(2)}) copy-start(bf16[7,1024,256]{2,1,0:T(8,128)(2,1)S(1)} %shard_map.166.own_ref) | copy-start | bytes 11010052
  15.5 18.0 %copy-start = (bf16[1024,1024]{1,0:T(8,128)(2,1)S(1)}, bf16[1024,1024]{1,0:T(8,128)(2,1)}, u32[]{:S(2)}) copy-start(bf16[1024,1024]{1,0:T(8,128)(2,1)} %refs_8_) | copy-start | bytes 6291460
  15.5 9.6 %collective-permute-start.1 = (bf16[64,1152]{1,0:T(8,128)(2,1)S(1)}, bf16[64,1152]{1,0:T(8,128)(2,1)S(1)}, u32[]{:S(2)}, u32[]{:S(2)}) collective-permute-start(bf16[64,1152]{1,0:T(8,128)(2,1)S(1)} %get-tuple-element.38), channel_id=1, source_target_pairs={{0,8},{8,16},{16,24},{24,0},{1,9},{9,17},{17,25},{25,1},{2,10},{10... | collective-permute-start | bytes 442376 | tf_op jit(solution)/shard_map/ppermute | solution.py:395
  18.2 12.8 %collective-permute-start.2 = (bf16[64,1152]{1,0:T(8,128)(2,1)S(1)}, bf16[64,1152]{1,0:T(8,128)(2,1)S(1)}, u32[]{:S(2)}, u32[]{:S(2)}) collective-permute-start(bf16[64,1152]{1,0:T(8,128)(2,1)S(1)} %get-tuple-element.39), channel_id=1, source_target_pairs={{0,16},{8,24},{16,0},{24,8},{1,17},{9,25},{17,1},{25,9},{2,18},{10... | collective-permute-start | bytes 442376 | tf_op jit(solution)/shard_map/ppermute | solution.py:395
  20.8 10.2 %collective-permute-start.3 = (bf16[64,1152]{1,0:T(8,128)(2,1)S(1)}, bf16[64,1152]{1,0:T(8,128)(2,1)S(1)}, u32[]{:S(2)}, u32[]{:S(2)}) collective-permute-start(bf16[64,1152]{1,0:T(8,128)(2,1)S(1)} %get-tuple-element.40), channel_id=1, source_target_pairs={{0,24},{8,0},{16,8},{24,16},{1,25},{9,1},{17,9},{25,17},{2,26},{10... | collective-permute-start | bytes 442376 | tf_op jit(solution)/shard_map/ppermute | solution.py:395
  22.3 13.0 %collective-permute-start.15 = (f32[24,512]{1,0:T(8,128)S(1)}, f32[24,512]{1,0:T(8,128)S(1)}, u32[]{:S(2)}, u32[]{:S(2)}) collective-permute-start(f32[24,512]{1,0:T(8,128)S(1)} %maximum_maximum_fusion.own_ref), channel_id=1, source_target_pairs={{0,1},{1,0},{2,3},{3,2},{4,5},{5,4},{6,7},{7,6},{8,9},{9,8},{10,11... | collective-permute-start | bytes 147464 | tf_op jit(solution)/shard_map/ppermute | solution.py:775
  25.0 84.1 %collective-permute-start.16 = (f32[4,128,256]{2,1,0:T(8,128)}, f32[4,128,256]{2,1,0:T(8,128)}, u32[]{:S(2)}, u32[]{:S(2)}) collective-permute-start(f32[4,128,256]{2,1,0:T(8,128)} %own_ref.1), channel_id=1, source_target_pairs={{0,1},{1,0},{2,3},{3,2},{4,5},{5,4},{6,7},{7,6},{8,9},{9,8},{10,11... | collective-permute-start | bytes 1572872 | tf_op jit(solution)/shard_map/ppermute | solution.py:775
  32.4 3.0 %collective-permute-start.4 = (bf16[4,64,1152]{2,1,0:T(8,128)(2,1)}, bf16[4,64,1152]{2,1,0:T(8,128)(2,1)}, u32[]{:S(2)}, u32[]{:S(2)}) collective-permute-start(bf16[4,64,1152]{2,1,0:T(8,128)(2,1)} %shard_map.165), channel_id=1, source_target_pairs={{0,1},{1,0},{2,3},{3,2},{4,5},{5,4},{6,7},{7,6},{8,9},{9,8},{10,11... | collective-permute-start | bytes 1769480 | tf_op jit(solution)/shard_map/ppermute | solution.py:775
  34.7 100.0 %collective-permute-start.32 = (bf16[512,1024]{1,0:T(8,128)(2,1)}, bf16[512,1024]{1,0:T(8,128)(2,1)S(1)}, u32[]{:S(2)}, u32[]{:S(2)}) collective-permute-start(bf16[512,1024]{1,0:T(8,128)(2,1)} %constant_dynamic-slice_fusion), channel_id=1, source_target_pairs={{0,1},{1,0},{2,3},{3,2},{4,5},{5,4},{6,7},{7,6},{8,9},{9,8},{10,11... | collective-permute-start | bytes 3145736 | tf_op jit(solution)/shard_map/ppermute | solution.py:775
  35.4 3.8 %copy-start.19 = (bf16[7,1024,256]{2,1,0:T(8,128)(2,1)S(1)}, bf16[7,1024,256]{2,1,0:T(8,128)(2,1)}, u32[]{:S(2)}) copy-start(bf16[7,1024,256]{2,1,0:T(8,128)(2,1)} %copy-done.18) | copy-start | bytes 11010052
  42.0 12.2 %collective-permute-start.10 = (bf16[512,512]{1,0:T(8,128)(2,1)S(1)}, bf16[512,512]{1,0:T(8,128)(2,1)S(1)}, u32[]{:S(2)}, u32[]{:S(2)}) collective-permute-start(bf16[512,512]{1,0:T(8,128)(2,1)S(1)} %shard_map.173), channel_id=1, source_target_pairs={{0,8},{25,17},{8,16},{17,9},{2,10},{27,19},{10,18},{19,11},{4,12},... | collective-permute-start | bytes 1572872 | tf_op jit(solution)/shard_map/ppermute | solution.py:866
  50.3 11.1 %collective-permute-start.6 = (bf16[512,512]{1,0:T(8,128)(2,1)S(1)}, bf16[512,512]{1,0:T(8,128)(2,1)S(1)}, u32[]{:S(2)}, u32[]{:S(2)}) collective-permute-start(bf16[512,512]{1,0:T(8,128)(2,1)S(1)} %shard_map.168), channel_id=1, source_target_pairs={{0,8},{25,17},{2,10},{27,19},{4,12},{29,21},{6,14},{31,23}} | collective-permute-start | bytes 1572872 | tf_op jit(solution)/shard_map/ppermute | solution.py:866
  57.0 11.1 %collective-permute-start.11 = (bf16[512,512]{1,0:T(8,128)(2,1)S(1)}, bf16[512,512]{1,0:T(8,128)(2,1)S(1)}, u32[]{:S(2)}, u32[]{:S(2)}) collective-permute-start(bf16[512,512]{1,0:T(8,128)(2,1)S(1)} %shard_map.174), channel_id=1, source_target_pairs={{0,8},{25,17},{8,16},{17,9},{16,24},{9,1},{2,10},{27,19},{10,18},{... | collective-permute-start | bytes 1572872 | tf_op jit(solution)/shard_map/ppermute | solution.py:866
  64.2 11.1 %collective-permute-start.7 = (bf16[512,512]{1,0:T(8,128)(2,1)S(1)}, bf16[512,512]{1,0:T(8,128)(2,1)S(1)}, u32[]{:S(2)}, u32[]{:S(2)}) collective-permute-start(bf16[512,512]{1,0:T(8,128)(2,1)S(1)} %shard_map.169), channel_id=1, source_target_pairs={{0,8},{25,17},{8,16},{17,9},{2,10},{27,19},{10,18},{19,11},{4,12},... | collective-permute-start | bytes 1572872 | tf_op jit(solution)/shard_map/ppermute | solution.py:866
  70.8 11.1 %collective-permute-start.12 = (bf16[512,512]{1,0:T(8,128)(2,1)S(1)}, bf16[512,512]{1,0:T(8,128)(2,1)S(1)}, u32[]{:S(2)}, u32[]{:S(2)}) collective-permute-start(bf16[512,512]{1,0:T(8,128)(2,1)S(1)} %shard_map.175.value_ref), channel_id=1, source_target_pairs={{0,8},{25,17},{8,16},{17,9},{16,24},{9,1},{2,10},{27,19},{10,18},{... | collective-permute-start | bytes 1572872 | tf_op jit(solution)/shard_map/ppermute | solution.py:866
  78.0 11.3 %collective-permute-start.8 = (bf16[512,512]{1,0:T(8,128)(2,1)S(1)}, bf16[512,512]{1,0:T(8,128)(2,1)S(1)}, u32[]{:S(2)}, u32[]{:S(2)}) collective-permute-start(bf16[512,512]{1,0:T(8,128)(2,1)S(1)} %shard_map.170), channel_id=1, source_target_pairs={{0,8},{25,17},{8,16},{17,9},{16,24},{9,1},{2,10},{27,19},{10,18},{... | collective-permute-start | bytes 1572872 | tf_op jit(solution)/shard_map/ppermute | solution.py:866
  84.7 11.2 %collective-permute-start.13 = (bf16[512,512]{1,0:T(8,128)(2,1)S(1)}, bf16[512,512]{1,0:T(8,128)(2,1)S(1)}, u32[]{:S(2)}, u32[]{:S(2)}) collective-permute-start(bf16[512,512]{1,0:T(8,128)(2,1)S(1)} %shard_map.176.key_value_ref), channel_id=1, source_target_pairs={{8,16},{17,9},{16,24},{9,1},{10,18},{19,11},{18,26},{11,3},{12,20}... | collective-permute-start | bytes 1572872 | tf_op jit(solution)/shard_map/ppermute | solution.py:866
  85.4 31.7 %collective-permute-start.21 = (bf16[512,512]{1,0:T(8,128)(2,1)S(1)}, bf16[512,512]{1,0:T(8,128)(2,1)S(1)}, u32[]{:S(2)}, u32[]{:S(2)}) collective-permute-start(bf16[512,512]{1,0:T(8,128)(2,1)S(1)} %shard_map.176.key_value_ref), channel_id=1, source_target_pairs={{0,24},{25,1},{2,26},{27,3},{4,28},{29,5},{6,30},{31,7}} | collective-permute-start | bytes 1572872 | tf_op jit(solution)/shard_map/ppermute | solution.py:861
  92.0 7.3 %collective-permute-start.9 = (bf16[512,512]{1,0:T(8,128)(2,1)S(1)}, bf16[512,512]{1,0:T(8,128)(2,1)S(1)}, u32[]{:S(2)}, u32[]{:S(2)}) collective-permute-start(bf16[512,512]{1,0:T(8,128)(2,1)S(1)} %shard_map.171.query_ref), channel_id=1, source_target_pairs={{8,16},{17,9},{16,24},{9,1},{10,18},{19,11},{18,26},{11,3},{12,20}... | collective-permute-start | bytes 1572872 | tf_op jit(solution)/shard_map/ppermute | solution.py:866
  95.9 13.9 %collective-permute-start.26 = (bf16[512,512]{1,0:T(8,128)(2,1)S(1)}, bf16[512,512]{1,0:T(8,128)(2,1)S(1)}, u32[]{:S(2)}, u32[]{:S(2)}) collective-permute-start(bf16[512,512]{1,0:T(8,128)(2,1)S(1)} %shard_map.183.refs_0_), channel_id=1, source_target_pairs={{1,9},{24,16},{3,11},{26,18},{5,13},{28,20},{7,15},{30,22}} | collective-permute-start | bytes 1572872 | tf_op jit(solution)/shard_map/ppermute | solution.py:913
  99.3 6.3 %collective-permute-start.14 = (bf16[512,512]{1,0:T(8,128)(2,1)S(1)}, bf16[512,512]{1,0:T(8,128)(2,1)S(1)}, u32[]{:S(2)}, u32[]{:S(2)}) collective-permute-start(bf16[512,512]{1,0:T(8,128)(2,1)S(1)} %shard_map.177.query_ref), channel_id=1, source_target_pairs={{16,24},{9,1},{18,26},{11,3},{20,28},{13,5},{22,30},{15,7}} | collective-permute-start | bytes 1572872 | tf_op jit(solution)/shard_map/ppermute | solution.py:866
  105.6 7.8 %collective-permute-start.20 = (bf16[512,512]{1,0:T(8,128)(2,1)S(1)}, bf16[512,512]{1,0:T(8,128)(2,1)S(1)}, u32[]{:S(2)}, u32[]{:S(2)}) collective-permute-start(bf16[512,512]{1,0:T(8,128)(2,1)S(1)} %shard_map.172.query_key_ref), channel_id=1, source_target_pairs={{16,24},{9,1},{18,26},{11,3},{20,28},{13,5},{22,30},{15,7}} | collective-permute-start | bytes 1572872 | tf_op jit(solution)/shard_map/ppermute | solution.py:866
  106.3 4.2 %copy-start.17 = (f32[256]{0:T(256)S(1)}, f32[256]{0:T(256)}, u32[]{:S(2)}) copy-start(f32[256]{0:T(256)} %param.31) | copy-start | bytes 3076
  109.1 22.0 %collective-permute-start.29 = (bf16[512,512]{1,0:T(8,128)(2,1)S(1)}, bf16[512,512]{1,0:T(8,128)(2,1)S(1)}, u32[]{:S(2)}, u32[]{:S(2)}) collective-permute-start(bf16[512,512]{1,0:T(8,128)(2,1)S(1)} %shard_map.184.refs_4_), channel_id=1, source_target_pairs={{1,9},{24,16},{3,11},{26,18},{5,13},{28,20},{7,15},{30,22}} | collective-permute-start | bytes 1572872 | tf_op jit(solution)/shard_map/ppermute | solution.py:913
  109.8 25.8 %collective-permute-start.27 = (bf16[512,512]{1,0:T(8,128)(2,1)S(1)}, bf16[512,512]{1,0:T(8,128)(2,1)S(1)}, u32[]{:S(2)}, u32[]{:S(2)}) collective-permute-start(bf16[512,512]{1,0:T(8,128)(2,1)S(1)} %collective-permute-done.26.refs_1_), channel_id=1, source_target_pairs={{9,17},{16,8},{11,19},{18,10},{13,21},{20,12},{15,23},{22,14}} | collective-permute-start | bytes 1572872 | tf_op jit(solution)/shard_map/ppermute | solution.py:913
  113.5 23.4 %collective-permute-start.17 = (bf16[512,512]{1,0:T(8,128)(2,1)S(1)}, bf16[512,512]{1,0:T(8,128)(2,1)S(1)}, u32[]{:S(2)}, u32[]{:S(2)}) collective-permute-start(bf16[512,512]{1,0:T(8,128)(2,1)S(1)} %shard_map.180.refs_0_), channel_id=1, source_target_pairs={{1,9},{24,16},{3,11},{26,18},{5,13},{28,20},{7,15},{30,22}} | collective-permute-start | bytes 1572872 | tf_op jit(solution)/shard_map/ppermute | solution.py:913
  114.2 2.9 %copy-start.20 = (bf16[512,1024]{1,0:T(8,128)(2,1)S(1)}, bf16[512,1024]{1,0:T(8,128)(2,1)}, u32[]{:S(2)}) copy-start(bf16[512,1024]{1,0:T(8,128)(2,1)} %constant_dynamic-slice_fusion.2) | copy-start | bytes 3145732
  117.1 44.8 %collective-permute-start.25 = (bf16[512,1024]{1,0:T(8,128)(2,1)S(1)}, bf16[512,1024]{1,0:T(8,128)(2,1)S(1)}, u32[]{:S(2)}, u32[]{:S(2)}) collective-permute-start(bf16[512,1024]{1,0:T(8,128)(2,1)S(1)} %copy-done.20), channel_id=1, source_target_pairs={{0,1},{1,0},{2,3},{3,2},{4,5},{5,4},{6,7},{7,6},{8,9},{9,8},{10,11... | collective-permute-start | bytes 3145736 | tf_op jit(solution)/shard_map/ppermute | solution.py:775
  131.2 6.5 %collective-permute-start.30 = (bf16[512,512]{1,0:T(8,128)(2,1)S(1)}, bf16[512,512]{1,0:T(8,128)(2,1)S(1)}, u32[]{:S(2)}, u32[]{:S(2)}) collective-permute-start(bf16[512,512]{1,0:T(8,128)(2,1)S(1)} %collective-permute-done.29.refs_5_), channel_id=1, source_target_pairs={{9,17},{16,8},{11,19},{18,10},{13,21},{20,12},{15,23},{22,14}} | collective-permute-start | bytes 1572872 | tf_op jit(solution)/shard_map/ppermute | solution.py:913
  134.8 30.7 %copy-start.2 = (bf16[1024,1024]{1,0:T(8,128)(2,1)S(1)}, bf16[1024,1024]{1,0:T(8,128)(2,1)}, u32[]{:S(2)}) copy-start(bf16[1024,1024]{1,0:T(8,128)(2,1)} %refs_8_.1) | copy-start | bytes 6291460
  134.8 4.2 %collective-permute-start.22 = (bf16[512,512]{1,0:T(8,128)(2,1)S(1)}, bf16[512,512]{1,0:T(8,128)(2,1)S(1)}, u32[]{:S(2)}, u32[]{:S(2)}) collective-permute-start(bf16[512,512]{1,0:T(8,128)(2,1)S(1)} %shard_map.182.refs_4_), channel_id=1, source_target_pairs={{1,9},{24,16},{3,11},{26,18},{5,13},{28,20},{7,15},{30,22}} | collective-permute-start | bytes 1572872 | tf_op jit(solution)/shard_map/ppermute | solution.py:913
  135.6 11.1 %collective-permute-start.28 = (bf16[512,512]{1,0:T(8,128)(2,1)S(1)}, bf16[512,512]{1,0:T(8,128)(2,1)S(1)}, u32[]{:S(2)}, u32[]{:S(2)}) collective-permute-start(bf16[512,512]{1,0:T(8,128)(2,1)S(1)} %collective-permute-done.27.refs_2_), channel_id=1, source_target_pairs={{17,25},{8,0},{19,27},{10,2},{21,29},{12,4},{23,31},{14,6}} | collective-permute-start | bytes 1572872 | tf_op jit(solution)/shard_map/ppermute | solution.py:913
  136.9 10.5 %collective-permute-start.18 = (bf16[512,512]{1,0:T(8,128)(2,1)S(1)}, bf16[512,512]{1,0:T(8,128)(2,1)S(1)}, u32[]{:S(2)}, u32[]{:S(2)}) collective-permute-start(bf16[512,512]{1,0:T(8,128)(2,1)S(1)} %collective-permute-done.17.refs_1_), channel_id=1, source_target_pairs={{9,17},{16,8},{11,19},{18,10},{13,21},{20,12},{15,23},{22,14}} | collective-permute-start | bytes 1572872 | tf_op jit(solution)/shard_map/ppermute | solution.py:913
  137.7 22.2 %collective-permute-start.31 = (bf16[512,512]{1,0:T(8,128)(2,1)S(1)}, bf16[512,512]{1,0:T(8,128)(2,1)S(1)}, u32[]{:S(2)}, u32[]{:S(2)}) collective-permute-start(bf16[512,512]{1,0:T(8,128)(2,1)S(1)} %collective-permute-done.30.refs_6_), channel_id=1, source_target_pairs={{17,25},{8,0},{19,27},{10,2},{21,29},{12,4},{23,31},{14,6}} | collective-permute-start | bytes 1572872 | tf_op jit(solution)/shard_map/ppermute | solution.py:913
  139.0 22.9 %collective-permute-start.24 = (bf16[512,512]{1,0:T(8,128)(2,1)S(1)}, bf16[512,512]{1,0:T(8,128)(2,1)S(1)}, u32[]{:S(2)}, u32[]{:S(2)}) collective-permute-start(bf16[512,512]{1,0:T(8,128)(2,1)S(1)} %shard_map.182.refs_4_), channel_id=1, source_target_pairs={{24,0},{1,25},{26,2},{3,27},{28,4},{5,29},{30,6},{7,31}} | collective-permute-start | bytes 1572872 | tf_op jit(solution)/shard_map/ppermute | solution.py:911
  146.7 15.1 %collective-permute-start.23 = (bf16[512,512]{1,0:T(8,128)(2,1)S(1)}, bf16[512,512]{1,0:T(8,128)(2,1)S(1)}, u32[]{:S(2)}, u32[]{:S(2)}) collective-permute-start(bf16[512,512]{1,0:T(8,128)(2,1)S(1)} %collective-permute-done.22.refs_5_), channel_id=1, source_target_pairs={{9,17},{16,8},{11,19},{18,10},{13,21},{20,12},{15,23},{22,14}} | collective-permute-start | bytes 1572872 | tf_op jit(solution)/shard_map/ppermute | solution.py:913
  147.4 18.1 %collective-permute-start.19 = (bf16[512,512]{1,0:T(8,128)(2,1)S(1)}, bf16[512,512]{1,0:T(8,128)(2,1)S(1)}, u32[]{:S(2)}, u32[]{:S(2)}) collective-permute-start(bf16[512,512]{1,0:T(8,128)(2,1)S(1)} %collective-permute-done.18.refs_2_), channel_id=1, source_target_pairs={{17,25},{8,0},{19,27},{10,2},{21,29},{12,4},{23,31},{14,6}} | collective-permute-start | bytes 1572872 | tf_op jit(solution)/shard_map/ppermute | solution.py:913
  167.5 2.0 %collective-permute-start.33 = (bf16[256,1024]{1,0:T(8,128)(2,1)S(1)}, bf16[256,1024]{1,0:T(8,128)(2,1)S(1)}, u32[]{:S(2)}, u32[]{:S(2)}) collective-permute-start(bf16[256,1024]{1,0:T(8,128)(2,1)S(1)} %get-tuple-element.56), channel_id=1, source_target_pairs={{0,1},{1,0},{2,3},{3,2},{4,5},{5,4},{6,7},{7,6},{8,9},{9,8},{10,11... | collective-permute-start | bytes 1572872 | tf_op jit(solution)/shard_map/ppermute | solution.py:775
  170.1 8.3 %collective-permute-start.34 = (bf16[64,1024]{1,0:T(8,128)(2,1)S(1)}, bf16[64,1024]{1,0:T(8,128)(2,1)S(1)}, u32[]{:S(2)}, u32[]{:S(2)}) collective-permute-start(bf16[64,1024]{1,0:T(8,128)(2,1)S(1)} %get-tuple-element.58), channel_id=1, source_target_pairs={{0,8},{8,16},{16,24},{24,0},{1,9},{9,17},{17,25},{25,1},{2,10},{10... | collective-permute-start | bytes 393224 | tf_op jit(solution)/shard_map/ppermute | solution.py:395
  170.6 12.9 %collective-permute-start.35 = (bf16[64,1024]{1,0:T(8,128)(2,1)S(1)}, bf16[64,1024]{1,0:T(8,128)(2,1)S(1)}, u32[]{:S(2)}, u32[]{:S(2)}) collective-permute-start(bf16[64,1024]{1,0:T(8,128)(2,1)S(1)} %get-tuple-element.59), channel_id=1, source_target_pairs={{0,16},{8,24},{16,0},{24,8},{1,17},{9,25},{17,1},{25,9},{2,18},{10... | collective-permute-start | bytes 393224 | tf_op jit(solution)/shard_map/ppermute | solution.py:395
  174.4 9.1 %collective-permute-start.36 = (bf16[64,1024]{1,0:T(8,128)(2,1)S(1)}, bf16[64,1024]{1,0:T(8,128)(2,1)S(1)}, u32[]{:S(2)}, u32[]{:S(2)}) collective-permute-start(bf16[64,1024]{1,0:T(8,128)(2,1)S(1)} %get-tuple-element.60), channel_id=1, source_target_pairs={{0,24},{8,0},{16,8},{24,16},{1,25},{9,1},{17,9},{25,17},{2,26},{10... | collective-permute-start | bytes 393224 | tf_op jit(solution)/shard_map/ppermute | solution.py:395

commit v8 on v7

--- a/solution.py
+++ b/solution.py
@@ -531,9 +531,8 @@
     )(place, mine, theirs, own, other)
 
 
-def linear_kernel(lin, head, half, place_ref, query_key_ref, value_ref, running_ref, own_ref, other_ref, gain_ref, *rest):
+def linear_kernel(lin, head, half, place_ref, query_key_ref, value_ref, running_ref, own_ref, other_ref, gain_ref, out_ref):
     me, side = place_ref[0], place_ref[1]
-    out_ref = rest[-1]
     rows, width = query_key_ref.shape
     features = LOOKUP_FEATURES
     values = width // 2
@@ -552,9 +551,6 @@
             query = query_key_ref[at, base : base + features].astype(jnp.float32)
             key = query_key_ref[at, base + features : base + 2 * features].astype(jnp.float32)
             value = value_ref[at, base : base + values]
-            if len(rest) == 2:
-                more = rest[0][at, base : base + values].astype(jnp.float32)
-                value = (value.astype(jnp.float32) + more).astype(jnp.bfloat16)
             end = running[SPAN - 1 : SPAN]
             scaled = (query * features ** (-0.5) * jnp.exp(running)).astype(jnp.bfloat16)
             inverse = (key * jnp.exp(-running)).astype(jnp.bfloat16)
@@ -572,15 +568,15 @@
             out_ref[at, base : base + values] = (raw * scale * gain_ref[...]).astype(out_ref.dtype)
 
 
-def linear_heads(place, lin, head, half, query_key, value, running, own, other, gain, *more):
+def linear_heads(place, lin, head, half, query_key, value, running, own, other, gain):
     return _call(
         functools.partial(linear_kernel, lin, head, half),
         jax.ShapeDtypeStruct(query_key.shape, jnp.bfloat16),
         2 * 10**9,
         2**21,
-        in_specs=[SMEM] + [VMEM] * (6 + len(more)),
+        in_specs=[SMEM] + [VMEM] * 6,
         out_specs=VMEM,
-    )(place, query_key, value, running, own, other, gain, *more)
+    )(place, query_key, value, running, own, other, gain)
 
 
 def window_kernel(group, half, place_ref, slope_ref, sink_ref, key_value_ref, query_ref, out_ref):
@@ -850,23 +846,15 @@
     theirs = swap(incoming).reshape(peers * half, wide)
 
     count = 1 + key_heads + 2 * lin
-    chained = count - 1 if hops > 1 else count
-    arrived, sums, straight = {}, [], []
-    for step in range(chained + 2 * hops):
-        turn = step - 2 * depth
-        index = jnp.clip(jnp.where(turn >= 0, turn, count - 1), 0, count - 1).astype(jnp.int32).reshape(1)
+    arrived, finals = {}, []
+    for step in range(count + 2 * hops):
+        index = jnp.clip(step - 2 * depth, 0, count - 1).astype(jnp.int32).reshape(1)
         value = partial_sum(index, mine, theirs, own_in, other_in, arrived.get(step - 2))
-        sums.append(value)
-        if step == chained and hops > 1:
-            straight.append(lax.ppermute(value, ("sp", "tp"), [(0, hops * 2), (hops * 2 + 1, 1)]))
-        depths = [
-            d for d in range(hops) if 0 <= step - 2 * d < chained or (chained < count and d and step - 2 * d == -2)
-        ]
+        depths = [d for d in range(hops) if 0 <= step - 2 * d < count]
         if depths:
             arrived[step] = lax.ppermute(value, ("sp", "tp"), _pairs(peers, depths, 0))
-    finals = sums[2 * hops :]
-    if straight:
-        finals.append(sums[2 * (hops - 1)])
+        if step >= 2 * hops:
+            finals.append(value)
 
     running = decay_sums(place, lin, rank, mine, theirs, own_small, other_small)
     sinks = jnp.stack(
@@ -898,7 +886,6 @@
                 starting_state,
                 other_state,
                 linear_head_gain.reshape(1, DV),
-                *(straight if head == lin - 1 else []),
             )
         )
 

time: 187 us -> 173 us (0.925)
  Pallas kernels: 63.4 us -> 48.6 us
  waiting for transfers between devices: 44.7 us -> 54.9 us
  starting transfers between devices: 67.1 us -> 61.4 us
  local copies, waits for them, and re-layouts: 8.55 us -> 5.62 us
    pallas_call x12 -> x13, Pallas kernels: 33 us -> 20 us  [partial_sum(): _call(partial_kernel, jax.ShapeDtypeStruct((2 * rows, 2 * width), jnp.bfl...]
    ppermute x8, starting transfers between devices: 15.7 us -> 8.69 us  [swap(): return lax.ppermute(value, 'tp', SWAP)]
    ppermute x11, waiting for transfers between devices: 21.3 us -> 27.8 us  [resident(): seen.append(lax.ppermute(seen[-1], ('sp', 'tp'), _pairs(peers, [hop], 1)))]
    ppermute x10 -> x11, starting transfers between devices: 25 us -> 31.3 us  [resident(): arrived[step] = lax.ppermute(value, ('sp', 'tp'), _pairs(peers, depths, 0))]
    ppermute x1 -> x0, starting transfers between devices: 3.91 us -> none  [resident(): lax.ppermute(value, ('sp', 'tp'), [(0, hops * 2), (hops * 2 + 1, 1)])]
    ppermute x10 -> x11, waiting for transfers between devices: 4.05 us -> 6.89 us  [resident(): arrived[step] = lax.ppermute(value, ('sp', 'tp'), _pairs(peers, depths, 0))]
    unnamed x50, local copies, waits for them, and re-layouts: 5.4 us -> 3.44 us
  transfers between devices with their start and end apart: 37 -> 37, of which waited for: 12 -> 13; matrix products, arithmetic and copies ran while one was open for 2% -> 1% of each run, Pallas kernels for 29% -> 22%
where the time goes in v8:
time: 173 us; the launch traced here: 172 us
  starting transfers between devices  61.4 us (35%)
  waiting for transfers between devices  54.9 us (32%)
  Pallas kernels  48.6 us (28%)
  local copies, waits for them, and re-layouts  5.62 us (3%)
    ppermute x11, starting transfers between devices, resident(): arrived[step] = lax.ppermute(value, ('sp', 'tp'), _pairs(peers, depths, 0))  31.3 us
    ppermute x11, waiting for transfers between devices, resident(): seen.append(lax.ppermute(seen[-1], ('sp', 'tp'), _pairs(peers, [hop], 1)))  27.8 us
    pallas_call x13, Pallas kernels, partial_sum(): _call(partial_kernel, jax.ShapeDtypeStruct((2 * rows, 2 * width), jnp.bfl...  20 us
    ppermute x6, waiting for transfers between devices, to_offsets(): lax.ppermute(parts[k], 'sp', [(i, (i + k) % peers) for i in range(peers)])  18 us
    ppermute x6, starting transfers between devices, to_offsets(): lax.ppermute(parts[k], 'sp', [(i, (i + k) % peers) for i in range(peers)])  10.6 us
    ppermute x11, starting transfers between devices, resident(): seen.append(lax.ppermute(seen[-1], ('sp', 'tp'), _pairs(peers, [hop], 1)))  9.55 us
    ppermute x8, starting transfers between devices, swap(): return lax.ppermute(value, 'tp', SWAP)  8.69 us
    ppermute x11, waiting for transfers between devices, resident(): arrived[step] = lax.ppermute(value, ('sp', 'tp'), _pairs(peers, depths, 0))  6.89 us
  transfers between devices with their start and end apart: 37, of which 13 were waited for; matrix products, arithmetic and copies ran while one was open for 1% of the time, Pallas kernels for 22%

profile of v8, /device:TPU:0, one launch (start us, length us, event | category | flops | bytes accessed | tf_op | source)
XLA Modules:
  0.0 171.6 jit_solution(1434660996237169381)
XLA Ops:
  0.1 1.0 copy-done.10
  1.8 0.7 shard_map.163
  4.4 1.4 shard_map.164
  7.4 4.1 %shard_map.167 = bf16[7,1024,256]{2,1,0:T(8,128)(2,1)} custom-call(s32[1]{0:T(128)} %bitcast.side_ref, bf16[1024,1024]{1,0:T(8,128)(2,1)S(1)} %copy-done.6, bf16[1024,256]{1,0:T(8,128)(2,1)S(1)} %copy-done.12, bf16[1024,256]{1,0:T(8,128)(2,1)S(1)} %copy-done.13, bf16[1024,512]{1,0:T(8,128)(2,1)S(1)} %copy-done.8, bf16[1024,512]{1,0:T(8,128)(2,1)S(1)} %copy-done.9, ...), custom_call_target="tpu_custom_call" | custom-call | flops 99999997952 | bytes 7340032 | tf_op jit(solution)/shard_map/pallas_call | solution.py:436
  11.9 1.6 shard_map.166.own_ref
  13.5 2.7 %collective-permute-start.1 = (bf16[64,1152]{1,0:T(8,128)(2,1)S(1)}, bf16[64,1152]{1,0:T(8,128)(2,1)S(1)}, u32[]{:S(2)}, u32[]{:S(2)}) collective-permute-start(bf16[64,1152]{1,0:T(8,128)(2,1)S(1)} %get-tuple-element.38), channel_id=1, source_target_pairs={{0,8},{8,16},{16,24},{24,0},{1,9},{9,17},{17,25},{25,1},{2,10},{10... | collective-permute-start | bytes 442376 | tf_op jit(solution)/shard_map/ppermute | solution.py:395
  16.3 2.6 %collective-permute-start.2 = (bf16[64,1152]{1,0:T(8,128)(2,1)S(1)}, bf16[64,1152]{1,0:T(8,128)(2,1)S(1)}, u32[]{:S(2)}, u32[]{:S(2)}) collective-permute-start(bf16[64,1152]{1,0:T(8,128)(2,1)S(1)} %get-tuple-element.39), channel_id=1, source_target_pairs={{0,16},{8,24},{16,0},{24,8},{1,17},{9,25},{17,1},{25,9},{2,18},{10... | collective-permute-start | bytes 442376 | tf_op jit(solution)/shard_map/ppermute | solution.py:395
  18.9 1.3 collective-permute-start.3
  20.4 2.7 %collective-permute-done.1.refs_1_ = bf16[64,1152]{1,0:T(8,128)(2,1)S(1)} collective-permute-done((bf16[64,1152]{1,0:T(8,128)(2,1)S(1)}, bf16[64,1152]{1,0:T(8,128)(2,1)S(1)}, u32[]{:S(2)}, u32[]{:S(2)}) %collective-permute-start.1) | collective-permute-done | bytes 147488 | tf_op jit(solution)/shard_map/ppermute | solution.py:395
  23.1 6.0 %collective-permute-done.2.refs_2_ = bf16[64,1152]{1,0:T(8,128)(2,1)S(1)} collective-permute-done((bf16[64,1152]{1,0:T(8,128)(2,1)S(1)}, bf16[64,1152]{1,0:T(8,128)(2,1)S(1)}, u32[]{:S(2)}, u32[]{:S(2)}) %collective-permute-start.2) | collective-permute-done | bytes 147488 | tf_op jit(solution)/shard_map/ppermute | solution.py:395
  29.8 1.1 constant_dynamic-slice_fusion.2
  31.8 2.9 %shard_map.179 = (f32[512,256]{1,0:T(8,128)S(1)}, f32[512,256]{1,0:T(8,128)S(1)}) custom-call(s32[4]{0:T(128)S(1)} %copy-done.5, bf16[256,1152]{1,0:T(8,128)(2,1)S(1)} %bitcast.27, bf16[256,1152]{1,0:T(8,128)(2,1)S(1)} %bitcast.43, f32[24,512]{1,0:T(8,128)S(1)} %maximum_maximum_fusion.own_ref, f32[24,512]{1,0:T(8,128)S(1)} %collective-permute-done.15.other_ref), custom_call_target="tpu_custom_call" | custom-call | flops 1000000000 | bytes 1048576 | tf_op jit(solution)/shard_map/pallas_call | solution.py:524
  34.8 1.7 shard_map.173
  36.5 5.6 %collective-permute-start.10 = (bf16[512,512]{1,0:T(8,128)(2,1)S(1)}, bf16[512,512]{1,0:T(8,128)(2,1)S(1)}, u32[]{:S(2)}, u32[]{:S(2)}) collective-permute-start(bf16[512,512]{1,0:T(8,128)(2,1)S(1)} %shard_map.173), channel_id=1, source_target_pairs={{0,8},{25,17},{2,10},{27,19},{4,12},{29,21},{6,14},{31,23}} | collective-permute-start | bytes 1572872 | tf_op jit(solution)/shard_map/ppermute | solution.py:855
  42.0 1.7 shard_map.168
  43.7 1.3 collective-permute-start.6
  45.1 3.6 %collective-permute-done.10.rest_0_ = bf16[512,512]{1,0:T(8,128)(2,1)S(1)} collective-permute-done((bf16[512,512]{1,0:T(8,128)(2,1)S(1)}, bf16[512,512]{1,0:T(8,128)(2,1)S(1)}, u32[]{:S(2)}, u32[]{:S(2)}) %collective-permute-start.10) | collective-permute-done | bytes 524320 | tf_op jit(solution)/shard_map/ppermute | solution.py:855
  48.7 1.5 shard_map.174
  50.2 4.4 %collective-permute-start.11 = (bf16[512,512]{1,0:T(8,128)(2,1)S(1)}, bf16[512,512]{1,0:T(8,128)(2,1)S(1)}, u32[]{:S(2)}, u32[]{:S(2)}) collective-permute-start(bf16[512,512]{1,0:T(8,128)(2,1)S(1)} %shard_map.174), channel_id=1, source_target_pairs={{0,8},{25,17},{8,16},{17,9},{2,10},{27,19},{10,18},{19,11},{4,12},... | collective-permute-start | bytes 1572872 | tf_op jit(solution)/shard_map/ppermute | solution.py:855
  54.7 1.5 shard_map.169
  56.2 4.1 %collective-permute-start.7 = (bf16[512,512]{1,0:T(8,128)(2,1)S(1)}, bf16[512,512]{1,0:T(8,128)(2,1)S(1)}, u32[]{:S(2)}, u32[]{:S(2)}) collective-permute-start(bf16[512,512]{1,0:T(8,128)(2,1)S(1)} %shard_map.169), channel_id=1, source_target_pairs={{0,8},{25,17},{8,16},{17,9},{2,10},{27,19},{10,18},{19,11},{4,12},... | collective-permute-start | bytes 1572872 | tf_op jit(solution)/shard_map/ppermute | solution.py:855
  60.3 1.0 collective-permute-done.11.rest_0_
  61.3 1.5 shard_map.175
  62.8 4.4 %collective-permute-start.12 = (bf16[512,512]{1,0:T(8,128)(2,1)S(1)}, bf16[512,512]{1,0:T(8,128)(2,1)S(1)}, u32[]{:S(2)}, u32[]{:S(2)}) collective-permute-start(bf16[512,512]{1,0:T(8,128)(2,1)S(1)} %shard_map.175), channel_id=1, source_target_pairs={{0,8},{25,17},{8,16},{17,9},{16,24},{9,1},{2,10},{27,19},{10,18},{... | collective-permute-start | bytes 1572872 | tf_op jit(solution)/shard_map/ppermute | solution.py:855
  67.2 1.5 shard_map.170
  68.8 4.1 %collective-permute-start.8 = (bf16[512,512]{1,0:T(8,128)(2,1)S(1)}, bf16[512,512]{1,0:T(8,128)(2,1)S(1)}, u32[]{:S(2)}, u32[]{:S(2)}) collective-permute-start(bf16[512,512]{1,0:T(8,128)(2,1)S(1)} %shard_map.170), channel_id=1, source_target_pairs={{0,8},{25,17},{8,16},{17,9},{16,24},{9,1},{2,10},{27,19},{10,18},{... | collective-permute-start | bytes 1572872 | tf_op jit(solution)/shard_map/ppermute | solution.py:855
  72.9 1.0 collective-permute-done.12.rest_0_
  73.9 1.5 shard_map.176.key_value_ref
  75.4 4.4 %collective-permute-start.13 = (bf16[512,512]{1,0:T(8,128)(2,1)S(1)}, bf16[512,512]{1,0:T(8,128)(2,1)S(1)}, u32[]{:S(2)}, u32[]{:S(2)}) collective-permute-start(bf16[512,512]{1,0:T(8,128)(2,1)S(1)} %shard_map.176.key_value_ref), channel_id=1, source_target_pairs={{0,8},{25,17},{8,16},{17,9},{16,24},{9,1},{2,10},{27,19},{10,18},{... | collective-permute-start | bytes 1572872 | tf_op jit(solution)/shard_map/ppermute | solution.py:855
  79.8 1.5 shard_map.171.query_ref
  81.4 0.9 collective-permute-start.9
  82.2 2.9 %shard_map.184.refs_0_ = bf16[512,512]{1,0:T(8,128)(2,1)S(1)} custom-call(s32[4]{0:T(128)S(1)} %copy-done.5, f32[2,4]{1,0:T(2,128)S(1)} %get-tuple-element.64.slope_ref, f32[2,4]{1,0:T(2,128)S(1)} %bitcast.42, bf16[512,512]{1,0:T(8,128)(2,1)S(1)} %shard_map.176.key_value_ref, bf16[512,512]{1,0:T(8,128)(2,1)S(1)} %shard_map.171.query_ref), custom_call_target="tpu_custom_call" | custom-call | flops 2000000000 | bytes 2097152 | tf_op jit(solution)/shard_map/pallas_call | solution.py:659
  85.2 0.7 collective-permute-start.26
  85.9 1.2 collective-permute-done.13.rest_0_
  87.1 1.5 shard_map.177.query_ref
  88.6 0.7 collective-permute-start.14
  89.3 1.5 shard_map.172.query_key_ref
  90.8 0.7 collective-permute-start.20
  91.5 2.8 %shard_map.185.refs_4_ = bf16[512,512]{1,0:T(8,128)(2,1)S(1)} custom-call(s32[4]{0:T(128)S(1)} %copy-done.5, f32[2,4]{1,0:T(2,128)S(1)} %get-tuple-element.63.slope_ref, f32[2,4]{1,0:T(2,128)S(1)} %bitcast.41, bf16[512,512]{1,0:T(8,128)(2,1)S(1)} %shard_map.176.key_value_ref, bf16[512,512]{1,0:T(8,128)(2,1)S(1)} %shard_map.177.query_ref), custom_call_target="tpu_custom_call" | custom-call | flops 2000000000 | bytes 2097152 | tf_op jit(solution)/shard_map/pallas_call | solution.py:659
  94.3 0.7 collective-permute-start.29
  95.1 0.7 collective-permute-start.27
  95.8 1.5 shard_map.178.value_ref
  98.0 2.3 %shard_map.180.refs_0_ = bf16[512,512]{1,0:T(8,128)(2,1)S(1)} custom-call(s32[4]{0:T(128)S(1)} %copy-done.5, bf16[512,512]{1,0:T(8,128)(2,1)S(1)} %shard_map.172.query_key_ref, bf16[512,512]{1,0:T(8,128)(2,1)S(1)} %shard_map.178.value_ref, f32[512,256]{1,0:T(8,128)S(1)} %get-tuple-element.50.running_ref, f32[4,128,256]{2,1,0:T(8,128)S(1)} %copy-done.14, ...), custom_call_target="tpu_custom_call" | custom-call | flops 2000000000 | bytes 2097152 | tf_op jit(solution)/shard_map/pallas_call | solution.py:572
  100.3 0.7 collective-permute-start.17
  101.0 1.5 shard_map.181.query_key_ref
  102.5 7.0 %collective-permute-start.32 = (bf16[512,1024]{1,0:T(8,128)(2,1)S(1)}, bf16[512,1024]{1,0:T(8,128)(2,1)S(1)}, u32[]{:S(2)}, u32[]{:S(2)}) collective-permute-start(bf16[512,1024]{1,0:T(8,128)(2,1)S(1)} %constant_dynamic-slice_fusion), channel_id=1, source_target_pairs={{0,1},{1,0},{2,3},{3,2},{4,5},{5,4},{6,7},{7,6},{8,9},{9,8},{10,11... | collective-permute-start | bytes 3145736 | tf_op jit(solution)/shard_map/ppermute | solution.py:771
  109.6 1.3 collective-permute-start.28
  111.6 0.7 collective-permute-start.18
  112.3 1.5 shard_map.182.value_ref
  113.8 2.3 %shard_map.183.refs_4_ = bf16[512,512]{1,0:T(8,128)(2,1)S(1)} custom-call(s32[4]{0:T(128)S(1)} %copy-done.5, bf16[512,512]{1,0:T(8,128)(2,1)S(1)} %shard_map.181.query_key_ref, bf16[512,512]{1,0:T(8,128)(2,1)S(1)} %shard_map.182.value_ref, f32[512,256]{1,0:T(8,128)S(1)} %get-tuple-element.52.running_ref, f32[4,128,256]{2,1,0:T(8,128)S(1)} %copy-done.14, ...), custom_call_target="tpu_custom_call" | custom-call | flops 2000000000 | bytes 2097152 | tf_op jit(solution)/shard_map/pallas_call | solution.py:572
  116.1 0.8 collective-permute-start.22
  116.9 1.3 collective-permute-start.31
  118.2 2.4 %collective-permute-done.28.refs_3_ = bf16[512,512]{1,0:T(8,128)(2,1)S(1)} collective-permute-done((bf16[512,512]{1,0:T(8,128)(2,1)S(1)}, bf16[512,512]{1,0:T(8,128)(2,1)S(1)}, u32[]{:S(2)}, u32[]{:S(2)}) %collective-permute-start.28) | collective-permute-done | bytes 524320 | tf_op jit(solution)/shard_map/ppermute | solution.py:900
  120.6 1.3 collective-permute-start.24
  121.9 1.3 collective-permute-start.19
  123.9 21.7 %collective-permute-done.31.refs_7_ = bf16[512,512]{1,0:T(8,128)(2,1)S(1)} collective-permute-done((bf16[512,512]{1,0:T(8,128)(2,1)S(1)}, bf16[512,512]{1,0:T(8,128)(2,1)S(1)}, u32[]{:S(2)}, u32[]{:S(2)}) %collective-permute-start.31) | collective-permute-done | bytes 524320 | tf_op jit(solution)/shard_map/ppermute | solution.py:900
  145.7 1.9 %shard_map.186.refs_10_ = f32[512,1024]{1,0:T(8,128)S(1)} custom-call(s32[4]{0:T(128)S(1)} %copy-done.5, bf16[512,512]{1,0:T(8,128)(2,1)S(1)} %shard_map.184.refs_0_, bf16[512,512]{1,0:T(8,128)(2,1)S(1)} %collective-permute-done.26.refs_1_, bf16[512,512]{1,0:T(8,128)(2,1)S(1)} %collective-permute-done.27.refs_2_, ...), custom_call_target="tpu_custom_call" | custom-call | flops 1073741824 | bytes 4194304 | tf_op jit(solution)/shard_map/pallas_call | solution.py:716
  147.6 3.7 %collective-permute-done.19.refs_3_ = bf16[512,512]{1,0:T(8,128)(2,1)S(1)} collective-permute-done((bf16[512,512]{1,0:T(8,128)(2,1)S(1)}, bf16[512,512]{1,0:T(8,128)(2,1)S(1)}, u32[]{:S(2)}, u32[]{:S(2)}) %collective-permute-start.19) | collective-permute-done | bytes 524320 | tf_op jit(solution)/shard_map/ppermute | solution.py:900
  151.3 3.2 %shard_map.187 = (bf16[256,1024]{1,0:T(8,128)(2,1)S(1)}, bf16[256,1024]{1,0:T(8,128)(2,1)S(1)}) custom-call(s32[4]{0:T(128)S(1)} %copy-done.5, bf16[512,512]{1,0:T(8,128)(2,1)S(1)} %shard_map.180.refs_0_, bf16[512,512]{1,0:T(8,128)(2,1)S(1)} %collective-permute-done.17.refs_1_, bf16[512,512]{1,0:T(8,128)(2,1)S(1)} %collective-permute-done.18.refs_2_, ...), custom_call_target="tpu_custom_call" | custom-call | flops 1073741824 | bytes 4194304 | tf_op jit(solution)/shard_map/pallas_call | solution.py:716
  154.5 1.9 %collective-permute-done.33.given_ref = bf16[256,1024]{1,0:T(8,128)(2,1)S(1)} collective-permute-done((bf16[256,1024]{1,0:T(8,128)(2,1)S(1)}, bf16[256,1024]{1,0:T(8,128)(2,1)S(1)}, u32[]{:S(2)}, u32[]{:S(2)}) %collective-permute-start.33) | collective-permute-done | bytes 524320 | tf_op jit(solution)/shard_map/ppermute | solution.py:771
  157.5 3.5 %collective-permute-start.36 = (bf16[64,1024]{1,0:T(8,128)(2,1)S(1)}, bf16[64,1024]{1,0:T(8,128)(2,1)S(1)}, u32[]{:S(2)}, u32[]{:S(2)}) collective-permute-start(bf16[64,1024]{1,0:T(8,128)(2,1)S(1)} %get-tuple-element.60), channel_id=1, source_target_pairs={{0,24},{8,0},{16,8},{24,16},{1,25},{9,1},{17,9},{25,17},{2,26},{10... | collective-permute-start | bytes 393224 | tf_op jit(solution)/shard_map/ppermute | solution.py:395
  161.0 4.5 %collective-permute-done.34.refs_1_ = bf16[64,1024]{1,0:T(8,128)(2,1)S(1)} collective-permute-done((bf16[64,1024]{1,0:T(8,128)(2,1)S(1)}, bf16[64,1024]{1,0:T(8,128)(2,1)S(1)}, u32[]{:S(2)}, u32[]{:S(2)}) %collective-permute-start.34) | collective-permute-done | bytes 131104 | tf_op jit(solution)/shard_map/ppermute | solution.py:395
  165.5 4.8 %collective-permute-done.35.refs_2_ = bf16[64,1024]{1,0:T(8,128)(2,1)S(1)} collective-permute-done((bf16[64,1024]{1,0:T(8,128)(2,1)S(1)}, bf16[64,1024]{1,0:T(8,128)(2,1)S(1)}, u32[]{:S(2)}, u32[]{:S(2)}) %collective-permute-start.35) | collective-permute-done | bytes 131104 | tf_op jit(solution)/shard_map/ppermute | solution.py:395
  170.2 1.4 shard_map.189
  (106 shorter events, 9.6 us)
Async XLA Ops:
  0.1 4.2 %copy-start.4 = (s32[4]{0:T(128)}, s32[4]{0:T(128)S(1)}, u32[]{:S(2)}) copy-start(s32[4]{0:T(128)S(1)} %pad_add_fusion.place_ref) | copy-start | bytes 52
  0.1 1.0 copy-start.10
  1.1 0.7 copy-start.17
  1.8 2.5 %copy-start.11 = (bf16[128,2048]{1,0:T(8,128)(2,1)S(1)}, bf16[128,2048]{1,0:T(8,128)(2,1)}, u32[]{:S(2)}) copy-start(bf16[128,2048]{1,0:T(8,128)(2,1)} %x_ref.3) | copy-start | bytes 1572868
  1.8 2.5 %copy-start.15 = (bf16[4096,16]{0,1:T(8,128)(2,1)S(1)}, bf16[4096,16]{0,1:T(8,128)(2,1)}, u32[]{:S(2)}) copy-start(bf16[4096,16]{0,1:T(8,128)(2,1)} %param.25) | copy-start | bytes 393220
  1.8 2.5 %copy-start.16 = (f32[4096]{0:T(1024)S(1)}, f32[4096]{0:T(1024)}, u32[]{:S(2)}) copy-start(f32[4096]{0:T(1024)} %param.18) | copy-start | bytes 49156
  2.5 1.7 %collective-permute-start = (bf16[64,2176]{1,0:T(8,128)(2,1)S(1)}, bf16[64,2176]{1,0:T(8,128)(2,1)S(1)}, u32[]{:S(2)}, u32[]{:S(2)}) collective-permute-start(bf16[64,2176]{1,0:T(8,128)(2,1)S(1)} %shard_map.163), channel_id=1, source_target_pairs={{0,1},{1,0},{2,3},{3,2},{4,5},{5,4},{6,7},{7,6},{8,9},{9,8},{10,11... | collective-permute-start | bytes 835592 | tf_op jit(solution)/shard_map/ppermute | solution.py:771
  4.3 1.6 copy-start.6
  4.3 2.2 %copy-start.7 = (bf16[1024,1024]{1,0:T(8,128)(2,1)S(1)}, bf16[1024,1024]{1,0:T(8,128)(2,1)}, u32[]{:S(2)}) copy-start(bf16[1024,1024]{1,0:T(8,128)(2,1)} %lv.1) | copy-start | bytes 6291460
  4.3 2.5 %copy-start.8 = (bf16[1024,512]{1,0:T(8,128)(2,1)S(1)}, bf16[1024,512]{1,0:T(8,128)(2,1)}, u32[]{:S(2)}) copy-start(bf16[1024,512]{1,0:T(8,128)(2,1)} %lq.1) | copy-start | bytes 3145732
  4.3 2.8 %copy-start.9 = (bf16[1024,512]{1,0:T(8,128)(2,1)S(1)}, bf16[1024,512]{1,0:T(8,128)(2,1)}, u32[]{:S(2)}) copy-start(bf16[1024,512]{1,0:T(8,128)(2,1)} %lk.1) | copy-start | bytes 3145732
  4.3 2.9 %copy-start.12 = (bf16[1024,256]{1,0:T(8,128)(2,1)S(1)}, bf16[1024,256]{1,0:T(8,128)(2,1)}, u32[]{:S(2)}) copy-start(bf16[1024,256]{1,0:T(8,128)(2,1)} %wk.1) | copy-start | bytes 1572868
  4.4 3.0 %copy-start.13 = (bf16[1024,256]{1,0:T(8,128)(2,1)S(1)}, bf16[1024,256]{1,0:T(8,128)(2,1)}, u32[]{:S(2)}) copy-start(bf16[1024,256]{1,0:T(8,128)(2,1)} %wv.1) | copy-start | bytes 1572868
  11.4 8.8 %copy-start.24 = (f32[16]{0:T(128)S(1)}, f32[16]{0:T(128)}, u32[]{:S(2)}) copy-start(f32[16]{0:T(128)} %param.30) | copy-start | bytes 196
  11.4 8.8 %copy-start.21 = (bf16[16,512]{1,0:T(8,128)(2,1)S(1)}, bf16[16,512]{1,0:T(8,128)(2,1)}, u32[]{:S(2)}) copy-start(bf16[16,512]{1,0:T(8,128)(2,1)} %param.26) | copy-start | bytes 49156
  11.4 8.8 %copy-start.22 = (f32[512]{0:T(512)S(1)}, f32[512]{0:T(512)}, u32[]{:S(2)}) copy-start(f32[512]{0:T(512)} %param.27) | copy-start | bytes 6148
  11.4 8.8 %copy-start.23 = (f32[24]{0:T(128)S(1)}, f32[24]{0:T(128)}, u32[]{:S(2)}) copy-start(f32[24]{0:T(128)} %pad.12.clone) | copy-start | bytes 292
  11.4 11.7 %copy-start.14 = (f32[4,128,256]{2,1,0:T(8,128)S(1)}, f32[4,128,256]{2,1,0:T(8,128)}, u32[]{:S(2)}) copy-start(f32[4,128,256]{2,1,0:T(8,128)} %own_ref.1) | copy-start | bytes 1572868
  11.4 17.7 %copy-start.5 = (s32[4]{0:T(128)S(1)}, s32[4]{0:T(128)}, u32[]{:S(2)}) copy-start(s32[4]{0:T(128)} %copy-done.4) | copy-start | bytes 52
  11.5 18.3 %copy-start.2 = (bf16[1024,1024]{1,0:T(8,128)(2,1)S(1)}, bf16[1024,1024]{1,0:T(8,128)(2,1)}, u32[]{:S(2)}) copy-start(bf16[1024,1024]{1,0:T(8,128)(2,1)} %refs_8_.1) | copy-start | bytes 6291460
  11.5 23.3 %collective-permute-start.5 = (bf16[7,1024,256]{2,1,0:T(8,128)(2,1)}, bf16[7,1024,256]{2,1,0:T(8,128)(2,1)}, u32[]{:S(2)}, u32[]{:S(2)}) collective-permute-start(bf16[7,1024,256]{2,1,0:T(8,128)(2,1)} %shard_map.167), channel_id=1, source_target_pairs={{0,1},{1,0},{2,3},{3,2},{4,5},{5,4},{6,7},{7,6},{8,9},{9,8},{10,11... | collective-permute-start | bytes 11010056 | tf_op jit(solution)/shard_map/ppermute | solution.py:771
  13.5 17.9 %copy-start.19 = (bf16[7,1024,256]{2,1,0:T(8,128)(2,1)}, bf16[7,1024,256]{2,1,0:T(8,128)(2,1)S(1)}, u32[]{:S(2)}) copy-start(bf16[7,1024,256]{2,1,0:T(8,128)(2,1)S(1)} %shard_map.166.own_ref) | copy-start | bytes 11010052
  13.5 17.8 %copy-start = (bf16[1024,1024]{1,0:T(8,128)(2,1)S(1)}, bf16[1024,1024]{1,0:T(8,128)(2,1)}, u32[]{:S(2)}) copy-start(bf16[1024,1024]{1,0:T(8,128)(2,1)} %refs_8_) | copy-start | bytes 6291460
  13.5 9.6 %collective-permute-start.1 = (bf16[64,1152]{1,0:T(8,128)(2,1)S(1)}, bf16[64,1152]{1,0:T(8,128)(2,1)S(1)}, u32[]{:S(2)}, u32[]{:S(2)}) collective-permute-start(bf16[64,1152]{1,0:T(8,128)(2,1)S(1)} %get-tuple-element.38), channel_id=1, source_target_pairs={{0,8},{8,16},{16,24},{24,0},{1,9},{9,17},{17,25},{25,1},{2,10},{10... | collective-permute-start | bytes 442376 | tf_op jit(solution)/shard_map/ppermute | solution.py:395
  16.3 12.8 %collective-permute-start.2 = (bf16[64,1152]{1,0:T(8,128)(2,1)S(1)}, bf16[64,1152]{1,0:T(8,128)(2,1)S(1)}, u32[]{:S(2)}, u32[]{:S(2)}) collective-permute-start(bf16[64,1152]{1,0:T(8,128)(2,1)S(1)} %get-tuple-element.39), channel_id=1, source_target_pairs={{0,16},{8,24},{16,0},{24,8},{1,17},{9,25},{17,1},{25,9},{2,18},{10... | collective-permute-start | bytes 442376 | tf_op jit(solution)/shard_map/ppermute | solution.py:395
  18.9 10.2 %collective-permute-start.3 = (bf16[64,1152]{1,0:T(8,128)(2,1)S(1)}, bf16[64,1152]{1,0:T(8,128)(2,1)S(1)}, u32[]{:S(2)}, u32[]{:S(2)}) collective-permute-start(bf16[64,1152]{1,0:T(8,128)(2,1)S(1)} %get-tuple-element.40), channel_id=1, source_target_pairs={{0,24},{8,0},{16,8},{24,16},{1,25},{9,1},{17,9},{25,17},{2,26},{10... | collective-permute-start | bytes 442376 | tf_op jit(solution)/shard_map/ppermute | solution.py:395
  20.3 11.3 %collective-permute-start.15 = (f32[24,512]{1,0:T(8,128)S(1)}, f32[24,512]{1,0:T(8,128)S(1)}, u32[]{:S(2)}, u32[]{:S(2)}) collective-permute-start(f32[24,512]{1,0:T(8,128)S(1)} %maximum_maximum_fusion.own_ref), channel_id=1, source_target_pairs={{0,1},{1,0},{2,3},{3,2},{4,5},{5,4},{6,7},{7,6},{8,9},{9,8},{10,11... | collective-permute-start | bytes 147464 | tf_op jit(solution)/shard_map/ppermute | solution.py:771
  23.1 74.2 %collective-permute-start.16 = (f32[4,128,256]{2,1,0:T(8,128)S(1)}, f32[4,128,256]{2,1,0:T(8,128)S(1)}, u32[]{:S(2)}, u32[]{:S(2)}) collective-permute-start(f32[4,128,256]{2,1,0:T(8,128)S(1)} %copy-done.14), channel_id=1, source_target_pairs={{0,1},{1,0},{2,3},{3,2},{4,5},{5,4},{6,7},{7,6},{8,9},{9,8},{10,11... | collective-permute-start | bytes 1572872 | tf_op jit(solution)/shard_map/ppermute | solution.py:771
  29.7 2.1 %collective-permute-start.4 = (bf16[4,64,1152]{2,1,0:T(8,128)(2,1)S(1)}, bf16[4,64,1152]{2,1,0:T(8,128)(2,1)S(1)}, u32[]{:S(2)}, u32[]{:S(2)}) collective-permute-start(bf16[4,64,1152]{2,1,0:T(8,128)(2,1)S(1)} %shard_map.165), channel_id=1, source_target_pairs={{0,1},{1,0},{2,3},{3,2},{4,5},{5,4},{6,7},{7,6},{8,9},{9,8},{10,11... | collective-permute-start | bytes 1769480 | tf_op jit(solution)/shard_map/ppermute | solution.py:771
  30.9 116.7 %collective-permute-start.25 = (bf16[512,1024]{1,0:T(8,128)(2,1)}, bf16[512,1024]{1,0:T(8,128)(2,1)}, u32[]{:S(2)}, u32[]{:S(2)}) collective-permute-start(bf16[512,1024]{1,0:T(8,128)(2,1)} %constant_dynamic-slice_fusion.2), channel_id=1, source_target_pairs={{0,1},{1,0},{2,3},{3,2},{4,5},{5,4},{6,7},{7,6},{8,9},{9,8},{10,11... | collective-permute-start | bytes 3145736 | tf_op jit(solution)/shard_map/ppermute | solution.py:771
  31.8 3.0 %copy-start.20 = (bf16[7,1024,256]{2,1,0:T(8,128)(2,1)S(1)}, bf16[7,1024,256]{2,1,0:T(8,128)(2,1)}, u32[]{:S(2)}) copy-start(bf16[7,1024,256]{2,1,0:T(8,128)(2,1)} %copy-done.19) | copy-start | bytes 11010052
  36.5 12.2 %collective-permute-start.10 = (bf16[512,512]{1,0:T(8,128)(2,1)S(1)}, bf16[512,512]{1,0:T(8,128)(2,1)S(1)}, u32[]{:S(2)}, u32[]{:S(2)}) collective-permute-start(bf16[512,512]{1,0:T(8,128)(2,1)S(1)} %shard_map.173), channel_id=1, source_target_pairs={{0,8},{25,17},{2,10},{27,19},{4,12},{29,21},{6,14},{31,23}} | collective-permute-start | bytes 1572872 | tf_op jit(solution)/shard_map/ppermute | solution.py:855
  43.7 10.9 %collective-permute-start.6 = (bf16[512,512]{1,0:T(8,128)(2,1)S(1)}, bf16[512,512]{1,0:T(8,128)(2,1)S(1)}, u32[]{:S(2)}, u32[]{:S(2)}) collective-permute-start(bf16[512,512]{1,0:T(8,128)(2,1)S(1)} %shard_map.168), channel_id=1, source_target_pairs={{0,8},{25,17},{2,10},{27,19},{4,12},{29,21},{6,14},{31,23}} | collective-permute-start | bytes 1572872 | tf_op jit(solution)/shard_map/ppermute | solution.py:855
  50.2 11.1 %collective-permute-start.11 = (bf16[512,512]{1,0:T(8,128)(2,1)S(1)}, bf16[512,512]{1,0:T(8,128)(2,1)S(1)}, u32[]{:S(2)}, u32[]{:S(2)}) collective-permute-start(bf16[512,512]{1,0:T(8,128)(2,1)S(1)} %shard_map.174), channel_id=1, source_target_pairs={{0,8},{25,17},{8,16},{17,9},{2,10},{27,19},{10,18},{19,11},{4,12},... | collective-permute-start | bytes 1572872 | tf_op jit(solution)/shard_map/ppermute | solution.py:855
  56.2 11.1 %collective-permute-start.7 = (bf16[512,512]{1,0:T(8,128)(2,1)S(1)}, bf16[512,512]{1,0:T(8,128)(2,1)S(1)}, u32[]{:S(2)}, u32[]{:S(2)}) collective-permute-start(bf16[512,512]{1,0:T(8,128)(2,1)S(1)} %shard_map.169), channel_id=1, source_target_pairs={{0,8},{25,17},{8,16},{17,9},{2,10},{27,19},{10,18},{19,11},{4,12},... | collective-permute-start | bytes 1572872 | tf_op jit(solution)/shard_map/ppermute | solution.py:855
  62.8 11.1 %collective-permute-start.12 = (bf16[512,512]{1,0:T(8,128)(2,1)S(1)}, bf16[512,512]{1,0:T(8,128)(2,1)S(1)}, u32[]{:S(2)}, u32[]{:S(2)}) collective-permute-start(bf16[512,512]{1,0:T(8,128)(2,1)S(1)} %shard_map.175), channel_id=1, source_target_pairs={{0,8},{25,17},{8,16},{17,9},{16,24},{9,1},{2,10},{27,19},{10,18},{... | collective-permute-start | bytes 1572872 | tf_op jit(solution)/shard_map/ppermute | solution.py:855
  68.8 11.1 %collective-permute-start.8 = (bf16[512,512]{1,0:T(8,128)(2,1)S(1)}, bf16[512,512]{1,0:T(8,128)(2,1)S(1)}, u32[]{:S(2)}, u32[]{:S(2)}) collective-permute-start(bf16[512,512]{1,0:T(8,128)(2,1)S(1)} %shard_map.170), channel_id=1, source_target_pairs={{0,8},{25,17},{8,16},{17,9},{16,24},{9,1},{2,10},{27,19},{10,18},{... | collective-permute-start | bytes 1572872 | tf_op jit(solution)/shard_map/ppermute | solution.py:855
  75.4 11.7 %collective-permute-start.13 = (bf16[512,512]{1,0:T(8,128)(2,1)S(1)}, bf16[512,512]{1,0:T(8,128)(2,1)S(1)}, u32[]{:S(2)}, u32[]{:S(2)}) collective-permute-start(bf16[512,512]{1,0:T(8,128)(2,1)S(1)} %shard_map.176.key_value_ref), channel_id=1, source_target_pairs={{0,8},{25,17},{8,16},{17,9},{16,24},{9,1},{2,10},{27,19},{10,18},{... | collective-permute-start | bytes 1572872 | tf_op jit(solution)/shard_map/ppermute | solution.py:855
  81.4 7.9 %collective-permute-start.9 = (bf16[512,512]{1,0:T(8,128)(2,1)S(1)}, bf16[512,512]{1,0:T(8,128)(2,1)S(1)}, u32[]{:S(2)}, u32[]{:S(2)}) collective-permute-start(bf16[512,512]{1,0:T(8,128)(2,1)S(1)} %shard_map.171.query_ref), channel_id=1, source_target_pairs={{8,16},{17,9},{16,24},{9,1},{10,18},{19,11},{18,26},{11,3},{12,20}... | collective-permute-start | bytes 1572872 | tf_op jit(solution)/shard_map/ppermute | solution.py:855
  85.2 9.2 %collective-permute-start.26 = (bf16[512,512]{1,0:T(8,128)(2,1)S(1)}, bf16[512,512]{1,0:T(8,128)(2,1)S(1)}, u32[]{:S(2)}, u32[]{:S(2)}) collective-permute-start(bf16[512,512]{1,0:T(8,128)(2,1)S(1)} %shard_map.184.refs_0_), channel_id=1, source_target_pairs={{1,9},{24,16},{3,11},{26,18},{5,13},{28,20},{7,15},{30,22}} | collective-permute-start | bytes 1572872 | tf_op jit(solution)/shard_map/ppermute | solution.py:900
  88.6 6.5 %collective-permute-start.14 = (bf16[512,512]{1,0:T(8,128)(2,1)S(1)}, bf16[512,512]{1,0:T(8,128)(2,1)S(1)}, u32[]{:S(2)}, u32[]{:S(2)}) collective-permute-start(bf16[512,512]{1,0:T(8,128)(2,1)S(1)} %shard_map.177.query_ref), channel_id=1, source_target_pairs={{8,16},{17,9},{16,24},{9,1},{10,18},{19,11},{18,26},{11,3},{12,20}... | collective-permute-start | bytes 1572872 | tf_op jit(solution)/shard_map/ppermute | solution.py:855
  90.8 9.5 %collective-permute-start.20 = (bf16[512,512]{1,0:T(8,128)(2,1)S(1)}, bf16[512,512]{1,0:T(8,128)(2,1)S(1)}, u32[]{:S(2)}, u32[]{:S(2)}) collective-permute-start(bf16[512,512]{1,0:T(8,128)(2,1)S(1)} %shard_map.172.query_key_ref), channel_id=1, source_target_pairs={{16,24},{9,1},{18,26},{11,3},{20,28},{13,5},{22,30},{15,7}} | collective-permute-start | bytes 1572872 | tf_op jit(solution)/shard_map/ppermute | solution.py:855
  94.3 15.2 %collective-permute-start.29 = (bf16[512,512]{1,0:T(8,128)(2,1)S(1)}, bf16[512,512]{1,0:T(8,128)(2,1)S(1)}, u32[]{:S(2)}, u32[]{:S(2)}) collective-permute-start(bf16[512,512]{1,0:T(8,128)(2,1)S(1)} %shard_map.185.refs_4_), channel_id=1, source_target_pairs={{1,9},{24,16},{3,11},{26,18},{5,13},{28,20},{7,15},{30,22}} | collective-permute-start | bytes 1572872 | tf_op jit(solution)/shard_map/ppermute | solution.py:900
  95.1 7.5 %collective-permute-start.27 = (bf16[512,512]{1,0:T(8,128)(2,1)S(1)}, bf16[512,512]{1,0:T(8,128)(2,1)S(1)}, u32[]{:S(2)}, u32[]{:S(2)}) collective-permute-start(bf16[512,512]{1,0:T(8,128)(2,1)S(1)} %collective-permute-done.26.refs_1_), channel_id=1, source_target_pairs={{9,17},{16,8},{11,19},{18,10},{13,21},{20,12},{15,23},{22,14}} | collective-permute-start | bytes 1572872 | tf_op jit(solution)/shard_map/ppermute | solution.py:900
  95.8 2.2 %copy-start.18 = (f32[256]{0:T(256)S(1)}, f32[256]{0:T(256)}, u32[]{:S(2)}) copy-start(f32[256]{0:T(256)} %param.31) | copy-start | bytes 3076
  97.3 14.3 %collective-permute-start.21 = (bf16[512,512]{1,0:T(8,128)(2,1)S(1)}, bf16[512,512]{1,0:T(8,128)(2,1)S(1)}, u32[]{:S(2)}, u32[]{:S(2)}) collective-permute-start(bf16[512,512]{1,0:T(8,128)(2,1)S(1)} %shard_map.178.value_ref), channel_id=1, source_target_pairs={{16,24},{9,1},{18,26},{11,3},{20,28},{13,5},{22,30},{15,7}} | collective-permute-start | bytes 1572872 | tf_op jit(solution)/shard_map/ppermute | solution.py:855
  100.3 10.6 %collective-permute-start.17 = (bf16[512,512]{1,0:T(8,128)(2,1)S(1)}, bf16[512,512]{1,0:T(8,128)(2,1)S(1)}, u32[]{:S(2)}, u32[]{:S(2)}) collective-permute-start(bf16[512,512]{1,0:T(8,128)(2,1)S(1)} %shard_map.180.refs_0_), channel_id=1, source_target_pairs={{1,9},{24,16},{3,11},{26,18},{5,13},{28,20},{7,15},{30,22}} | collective-permute-start | bytes 1572872 | tf_op jit(solution)/shard_map/ppermute | solution.py:900
  102.5 13.6 %collective-permute-start.32 = (bf16[512,1024]{1,0:T(8,128)(2,1)S(1)}, bf16[512,1024]{1,0:T(8,128)(2,1)S(1)}, u32[]{:S(2)}, u32[]{:S(2)}) collective-permute-start(bf16[512,1024]{1,0:T(8,128)(2,1)S(1)} %constant_dynamic-slice_fusion), channel_id=1, source_target_pairs={{0,1},{1,0},{2,3},{3,2},{4,5},{5,4},{6,7},{7,6},{8,9},{9,8},{10,11... | collective-permute-start | bytes 3145736 | tf_op jit(solution)/shard_map/ppermute | solution.py:771
  109.6 11.1 %collective-permute-start.28 = (bf16[512,512]{1,0:T(8,128)(2,1)S(1)}, bf16[512,512]{1,0:T(8,128)(2,1)S(1)}, u32[]{:S(2)}, u32[]{:S(2)}) collective-permute-start(bf16[512,512]{1,0:T(8,128)(2,1)S(1)} %collective-permute-done.27.refs_2_), channel_id=1, source_target_pairs={{17,25},{8,0},{19,27},{10,2},{21,29},{12,4},{23,31},{14,6}} | collective-permute-start | bytes 1572872 | tf_op jit(solution)/shard_map/ppermute | solution.py:900
  110.9 6.1 %collective-permute-start.30 = (bf16[512,512]{1,0:T(8,128)(2,1)S(1)}, bf16[512,512]{1,0:T(8,128)(2,1)S(1)}, u32[]{:S(2)}, u32[]{:S(2)}) collective-permute-start(bf16[512,512]{1,0:T(8,128)(2,1)S(1)} %collective-permute-done.29.refs_5_), channel_id=1, source_target_pairs={{9,17},{16,8},{11,19},{18,10},{13,21},{20,12},{15,23},{22,14}} | collective-permute-start | bytes 1572872 | tf_op jit(solution)/shard_map/ppermute | solution.py:900
  111.6 10.3 %collective-permute-start.18 = (bf16[512,512]{1,0:T(8,128)(2,1)S(1)}, bf16[512,512]{1,0:T(8,128)(2,1)S(1)}, u32[]{:S(2)}, u32[]{:S(2)}) collective-permute-start(bf16[512,512]{1,0:T(8,128)(2,1)S(1)} %collective-permute-done.17.refs_1_), channel_id=1, source_target_pairs={{9,17},{16,8},{11,19},{18,10},{13,21},{20,12},{15,23},{22,14}} | collective-permute-start | bytes 1572872 | tf_op jit(solution)/shard_map/ppermute | solution.py:900
  113.8 31.9 %copy-start.1 = (bf16[1024,1024]{1,0:T(8,128)(2,1)S(1)}, bf16[1024,1024]{1,0:T(8,128)(2,1)}, u32[]{:S(2)}) copy-start(bf16[1024,1024]{1,0:T(8,128)(2,1)} %refs_8_) | copy-start | bytes 6291460
  116.1 35.2 %copy-start.3 = (bf16[1024,1024]{1,0:T(8,128)(2,1)S(1)}, bf16[1024,1024]{1,0:T(8,128)(2,1)}, u32[]{:S(2)}) copy-start(bf16[1024,1024]{1,0:T(8,128)(2,1)} %refs_8_.1) | copy-start | bytes 6291460
  116.1 7.1 %collective-permute-start.22 = (bf16[512,512]{1,0:T(8,128)(2,1)S(1)}, bf16[512,512]{1,0:T(8,128)(2,1)S(1)}, u32[]{:S(2)}, u32[]{:S(2)}) collective-permute-start(bf16[512,512]{1,0:T(8,128)(2,1)S(1)} %shard_map.183.refs_4_), channel_id=1, source_target_pairs={{1,9},{24,16},{3,11},{26,18},{5,13},{28,20},{7,15},{30,22}} | collective-permute-start | bytes 1572872 | tf_op jit(solution)/shard_map/ppermute | solution.py:900
  116.9 28.7 %collective-permute-start.31 = (bf16[512,512]{1,0:T(8,128)(2,1)S(1)}, bf16[512,512]{1,0:T(8,128)(2,1)S(1)}, u32[]{:S(2)}, u32[]{:S(2)}) collective-permute-start(bf16[512,512]{1,0:T(8,128)(2,1)S(1)} %collective-permute-done.30.refs_6_), channel_id=1, source_target_pairs={{17,25},{8,0},{19,27},{10,2},{21,29},{12,4},{23,31},{14,6}} | collective-permute-start | bytes 1572872 | tf_op jit(solution)/shard_map/ppermute | solution.py:900
  120.6 27.0 %collective-permute-start.24 = (bf16[512,512]{1,0:T(8,128)(2,1)S(1)}, bf16[512,512]{1,0:T(8,128)(2,1)S(1)}, u32[]{:S(2)}, u32[]{:S(2)}) collective-permute-start(bf16[512,512]{1,0:T(8,128)(2,1)S(1)} %shard_map.183.refs_4_), channel_id=1, source_target_pairs={{24,0},{1,25},{26,2},{3,27},{28,4},{5,29},{30,6},{7,31}} | collective-permute-start | bytes 1572872 | tf_op jit(solution)/shard_map/ppermute | solution.py:898
  121.9 29.3 %collective-permute-start.19 = (bf16[512,512]{1,0:T(8,128)(2,1)S(1)}, bf16[512,512]{1,0:T(8,128)(2,1)S(1)}, u32[]{:S(2)}, u32[]{:S(2)}) collective-permute-start(bf16[512,512]{1,0:T(8,128)(2,1)S(1)} %collective-permute-done.18.refs_2_), channel_id=1, source_target_pairs={{17,25},{8,0},{19,27},{10,2},{21,29},{12,4},{23,31},{14,6}} | collective-permute-start | bytes 1572872 | tf_op jit(solution)/shard_map/ppermute | solution.py:900
  123.2 28.0 %collective-permute-start.23 = (bf16[512,512]{1,0:T(8,128)(2,1)S(1)}, bf16[512,512]{1,0:T(8,128)(2,1)S(1)}, u32[]{:S(2)}, u32[]{:S(2)}) collective-permute-start(bf16[512,512]{1,0:T(8,128)(2,1)S(1)} %collective-permute-done.22.refs_5_), channel_id=1, source_target_pairs={{9,17},{16,8},{11,19},{18,10},{13,21},{20,12},{15,23},{22,14}} | collective-permute-start | bytes 1572872 | tf_op jit(solution)/shard_map/ppermute | solution.py:900
  154.5 2.0 %collective-permute-start.33 = (bf16[256,1024]{1,0:T(8,128)(2,1)S(1)}, bf16[256,1024]{1,0:T(8,128)(2,1)S(1)}, u32[]{:S(2)}, u32[]{:S(2)}) collective-permute-start(bf16[256,1024]{1,0:T(8,128)(2,1)S(1)} %get-tuple-element.56), channel_id=1, source_target_pairs={{0,1},{1,0},{2,3},{3,2},{4,5},{5,4},{6,7},{7,6},{8,9},{9,8},{10,11... | collective-permute-start | bytes 1572872 | tf_op jit(solution)/shard_map/ppermute | solution.py:771
  157.1 8.4 %collective-permute-start.34 = (bf16[64,1024]{1,0:T(8,128)(2,1)S(1)}, bf16[64,1024]{1,0:T(8,128)(2,1)S(1)}, u32[]{:S(2)}, u32[]{:S(2)}) collective-permute-start(bf16[64,1024]{1,0:T(8,128)(2,1)S(1)} %get-tuple-element.58), channel_id=1, source_target_pairs={{0,8},{8,16},{16,24},{24,0},{1,9},{9,17},{17,25},{25,1},{2,10},{10... | collective-permute-start | bytes 393224 | tf_op jit(solution)/shard_map/ppermute | solution.py:395
  157.5 12.8 %collective-permute-start.35 = (bf16[64,1024]{1,0:T(8,128)(2,1)S(1)}, bf16[64,1024]{1,0:T(8,128)(2,1)S(1)}, u32[]{:S(2)}, u32[]{:S(2)}) collective-permute-start(bf16[64,1024]{1,0:T(8,128)(2,1)S(1)} %get-tuple-element.59), channel_id=1, source_target_pairs={{0,16},{8,24},{16,0},{24,8},{1,17},{9,25},{17,1},{25,9},{2,18},{10... | collective-permute-start | bytes 393224 | tf_op jit(solution)/shard_map/ppermute | solution.py:395
  157.5 12.8 %collective-permute-start.36 = (bf16[64,1024]{1,0:T(8,128)(2,1)S(1)}, bf16[64,1024]{1,0:T(8,128)(2,1)S(1)}, u32[]{:S(2)}, u32[]{:S(2)}) collective-permute-start(bf16[64,1024]{1,0:T(8,128)(2,1)S(1)} %get-tuple-element.60), channel_id=1, source_target_pairs={{0,24},{8,0},{16,8},{24,16},{1,25},{9,1},{17,9},{25,17},{2,26},{10... | collective-permute-start | bytes 393224 | tf_op jit(solution)/shard_map/ppermute | solution.py:395
